TPU v7x, 512 devices: a whole 4x4x16 slice. The times are simulated.
512 devices in a mesh: sp: 64 (over z, y), tp: 8 (over x, core).
Axes of the slice: x: 4, y: 4, z: 16, core: 2. Of those that a mesh axis runs over, the one named last changes fastest.
Arguments:
- residual: bfloat16 [12288, 2048], P(('sp', 'tp')), may hold values from -6 to 6
- queries: bfloat16 [12288, 1024], P('sp', 'tp'), may hold values from -6 to 6
- key_pairs: bfloat16 [12288, 1024], P('sp', 'tp'), may hold values from -6 to 6
- values: bfloat16 [12288, 1024], P('sp', 'tp'), may hold values from -6 to 6
- second_weight: float32 [8], P('tp'), may hold values from 0.3 to 0.8
- head_gain: float32 [1024], P('tp'), may hold values from 0.1 to 1.9
- out_weight: bfloat16 [1024, 2048], P('tp'), may hold values from -0.1875 to 0.1875
- norm_gain: float32 [2048], replicated, may hold values from 0.1 to 1.9
- up_weight: bfloat16 [2048, 5632], P('sp', 'tp'), may hold values from -0.125 to 0.125
- gate_weight: bfloat16 [2048, 5632], P('sp', 'tp'), may hold values from -0.125 to 0.125
- conv_weight: float32 [3, 5632], P(None, 'tp'), may hold values from -3.5 to 3.5
- conv_bias: float32 [5632], P('tp'), may hold values from -3 to 3
- down_weight: bfloat16 [5632, 2048], P('tp', 'sp'), may hold values from -0.078125 to 0.078125
Outputs:
- layer_out: bfloat16 [12288, 2048], P(('sp', 'tp'))
All inputs are finite; a program needn't handle non-finite values.
Results may differ from a plain program's by a relative error of at most 0.017.
Values may be sent and summed in bfloat16 or wider, within the bound.
No kernel may reach another device: no remote copies, remote signals or barrier semaphores. Data moves between devices by JAX's collectives and lax.ppermute only.
A program may use at most 64 MiB of HBM per device.

v0:
```python
import jax
import jax.numpy as jnp
from jax import lax
from jax.sharding import Mesh
from jax.sharding import PartitionSpec as P

HD = 64
VD = 128
SP = ("sp_0", "sp_1")
SP_TP = ("sp_0", "sp_1", "tp")


eps = 1e-05
neg_fill = -1e30


def in_one_piece(arrays, axis, dim, along):
    both = jnp.concatenate(arrays, axis=along)
    out, at, done = (lax.all_gather(both, axis, axis=dim, tiled=True), 0, [])
    for a in arrays:
        done.append(lax.slice_in_dim(out, at, at + a.shape[along], axis=along))
        at += a.shape[along]
    return tuple(done)


def gathered_by_axis(shard, axes, dim):
    for axis in reversed(axes):
        shard = lax.all_gather(shard, axis, axis=dim, tiled=True)
    return shard


def cut_along(shard, dim, count):
    before, after = (shard.shape[:dim], shard.shape[dim + 1 :])
    return jnp.moveaxis(shard.reshape(*before, count, -1, *after), dim, 0)


def sent_and_summed(shard, axis, dim):
    count = lax.axis_size(axis)
    tiles = lax.all_to_all(cut_along(shard, dim, count), axis, 0, 0, tiled=True)
    return jnp.sum(tiles.astype(jnp.float32), axis=0)


def joined_along(tiles, dim):
    tiles = jnp.moveaxis(tiles, 0, dim)
    shape = tiles.shape
    return tiles.reshape(*shape[:dim], shape[dim] * shape[dim + 1], *shape[dim + 2 :])


def from_everyone(shard, axis):
    copies = jnp.broadcast_to(shard, (lax.axis_size(axis), *shard.shape))
    return lax.all_to_all(copies, axis, split_axis=0, concat_axis=0, tiled=True)


def gathered_copies(shard, axis, dim):
    return joined_along(from_everyone(shard, axis), dim)


def from_behind(value, axis, steps):
    count = lax.axis_size(axis)
    leading, last = (max(0, -steps), min(count, count - steps))
    return lax.ppermute(value, axis, [(source, source + steps) for source in range(leading, last)])


def normalize(rows_in, gain):
    values_f = rows_in.astype(jnp.float32)
    scale_inv = lax.rsqrt(jnp.mean(values_f * values_f, axis=-1, keepdims=True) + eps)
    return (values_f * scale_inv * gain).astype(jnp.bfloat16)


def local(
    residual,
    queries,
    key_pairs,
    values,
    second_weight,
    head_gain,
    out_weight,
    norm_gain,
    up_weight,
    gate_weight,
    conv_weight,
    conv_bias,
    down_weight,
):
    tok_rows = queries.shape[0]
    head_count = second_weight.shape[0]
    ff_local = up_weight.shape[1]
    sp_index = lax.axis_index(SP)
    up_all, gate_all = in_one_piece((up_weight, gate_weight), SP, 0, 1)
    down_all = gathered_by_axis(down_weight, SP, 1)
    query = queries.reshape(tok_rows, head_count, 2, HD)
    query_pos = sp_index * tok_rows + jnp.arange(tok_rows)
    last_query = (sp_index + 1) * tok_rows
    initial = (
        jnp.full((head_count, 2, tok_rows), neg_fill, jnp.float32),
        jnp.zeros((head_count, 2, tok_rows), jnp.float32),
        jnp.zeros((head_count, 2, tok_rows, VD), jnp.float32),
    )
    key_piece, value_piece = in_one_piece((key_pairs, values), SP, 0, 1)
    piece_len = key_piece.shape[0]

    def compute(state_in):
        maxima, totals, weighted = state_in
        key_rows = key_piece.reshape(piece_len, head_count, 2, HD)
        value_rows = value_piece.reshape(piece_len, head_count, VD)
        scores = jnp.einsum(
            "qhmd,khmd->hmqk", query, key_rows, preferred_element_type=jnp.float32
        ) * HD ** (-0.5)
        visible = jnp.arange(piece_len)[None, :] <= query_pos[:, None]
        scores = jnp.where(visible, scores, neg_fill)
        new_max = jnp.maximum(maxima, jnp.max(scores, axis=-1))
        exp_scores = jnp.where(visible, jnp.exp(scores - new_max[..., None]), jnp.float32(0.0))
        totals = jnp.sum(exp_scores, axis=-1)
        weighted = jnp.einsum(
            "hmqk,khe->hmqe",
            exp_scores.astype(jnp.bfloat16),
            value_rows,
            preferred_element_type=jnp.float32,
        )
        return (new_max, totals, weighted)

    def keep_state(state_in):
        return state_in

    maxima, totals, weighted = lax.cond(jnp.int32(0) < last_query, compute, keep_state, initial)
    diff = (
        weighted[:, 0] / totals[:, 0, :, None]
        - second_weight[:, None, None] * weighted[:, 1] / totals[:, 1, :, None]
    )
    diff = jnp.transpose(diff, (1, 0, 2))
    scale_inv = lax.rsqrt(jnp.mean(diff * diff, axis=-1, keepdims=True) + eps)
    attended = (
        (diff * scale_inv * head_gain.reshape(head_count, VD) * 0.8)
        .reshape(tok_rows, head_count * VD)
        .astype(jnp.bfloat16)
    )
    proj = sent_and_summed(
        jnp.dot(attended, out_weight, preferred_element_type=jnp.float32).astype(jnp.bfloat16),
        "tp",
        0,
    ).astype(jnp.bfloat16)
    mid = (residual.astype(jnp.float32) + proj.astype(jnp.float32)).astype(jnp.bfloat16)
    normed_all = gathered_copies(normalize(mid, norm_gain), "tp", 0)
    up_proj = jnp.dot(normed_all, up_all, preferred_element_type=jnp.float32).astype(jnp.bfloat16)
    gate_proj = jnp.dot(normed_all, gate_all, preferred_element_type=jnp.float32).astype(
        jnp.bfloat16
    )
    taps = conv_weight.shape[0]
    rim_rows = from_behind(up_proj[tok_rows - (taps - 1) :], SP, 1)
    extended = jnp.concatenate((rim_rows, up_proj), axis=0)
    conv_out = jnp.zeros((tok_rows, ff_local), jnp.float32) + conv_bias[None, :]
    for tap in range(taps):
        conv_out = conv_out + conv_weight[tap][None, :] * extended[tap : tap + tok_rows].astype(
            jnp.float32
        )
    hidden = (jax.nn.silu(conv_out) * gate_proj.astype(jnp.float32)).astype(jnp.bfloat16)
    ffn_out = sent_and_summed(
        jnp.dot(hidden, down_all, preferred_element_type=jnp.float32).astype(jnp.bfloat16), "tp", 0
    ).astype(jnp.bfloat16)
    return (mid.astype(jnp.float32) + ffn_out.astype(jnp.float32)).astype(jnp.bfloat16)


def solution(mesh):
    finer = Mesh(mesh.devices.reshape(16, 4, mesh.shape["tp"]), ("sp_0", "sp_1", "tp"))
    in_specs = (
        P(SP_TP, None),
        P(SP, "tp"),
        P(SP, "tp"),
        P(SP, "tp"),
        P("tp"),
        P("tp"),
        P("tp", None),
        P(),
        P(SP, "tp"),
        P(SP, "tp"),
        P(None, "tp"),
        P("tp"),
        P("tp", SP),
    )
    out_specs = P(SP_TP, None)
    return jax.shard_map(local, mesh=finer, in_specs=in_specs, out_specs=out_specs, check_vma=False)
```

profile of v0, /device:TPU:1, one launch (start us, length us, event | category | flops | bytes accessed | tf_op | source)
XLA Modules:
  0.0 416.4 jit_solution(16489077189879358978)
XLA Ops:
  6.5 0.0 copy-start
  6.5 0.0 all-gather.4.cloned.1.call-start
  6.5 1.5 pad_maximum_fusion.2
  8.1 0.0 all-gather.4.cloned.1.call-update
  8.1 0.0 all-gather.6.cloned.1.call-start
  8.1 1.5 pad_maximum_fusion.3
  9.7 0.0 all-gather.6.cloned.1.call-update
  9.7 0.0 all-gather.8.cloned.1.call-start
  9.8 12.5 %all_gather.14 = bf16[704,128]{0,1:T(8,128)(2,1)} all-gather(bf16[704,32]{0,1:T(8,128)(2,1)} %param.27), channel_id=1, replica_groups=mesh['sp_0'=16,'sp_1'=4,'tp'=8] {'sp_1'}, dimensions={1}, use_global_device_ids=true | all-gather | bytes 225280 | tf_op jit(solution)/shard_map/all_gather | solution.py:28
  22.3 0.0 all-gather.8.cloned.1.call-update
  22.9 135.3 %all-gather.4.cloned.1.call-done = bf16[12288,256]{1,0:T(8,128)(2,1)} async-done(((bf16[192,256]{1,0:T(8,128)(2,1)}), bf16[12288,256]{1,0:T(8,128)(2,1)}) %all-gather.4.cloned.1.call-update) | async-done | bytes 6291472 | tf_op jit(solution)/shard_map/all_gather | solution.py:19
  158.3 0.0 copy-start.5
  158.3 0.0 copy-start.1
  158.3 0.0 copy-start.3
  158.3 40.7 %conditional.1 = (f32[192]{0:T(256)S(1)}, f32[192]{0:T(256)S(1)}, f32[1,1,192,128]{3,2,1,0:T(8,128)S(1)}, f32[1,1,192,128]{3,2,1,0:T(8,128)S(1)}) conditional(s32[]{:T(128)} %convert_element_type.65, () %tuple.19, (s32[]{:T(128)}, s32[192]{0:T(256)S(1)}, bf16[192,128]{1,0:T(8,128)(2,1)}, bf16[12288,256]{1,0:T(8,128)(2,1)}) %tuple.20), branch_computations={%region_0.0_spmd.clone, %region_1.4_spmd.clone} | conditional | flops 1856765696 | bytes 85883216 | solution.py:125
  158.3 1.5 iota_compare_fusion
  159.8 0.0 copy-start.2
  159.8 3.2 slice.68
  163.0 4.7 %copy.17 = bf16[12288,128]{0,1:T(8,128)(2,1)} copy(bf16[12288,128]{1,0:T(8,128)(2,1)} %slice.68) | data formatting | bytes 6291456 | tf_op jit(solution)/shard_map/slice | solution.py:21
  167.6 0.0 copy-done.2
  167.6 0.1 copy.18
  167.8 12.6 %fusion.82 = (f32[2,192]{1,0:T(2,128)S(1)}, f32[2,192,12288]{2,1,0:T(8,128)}) fusion(bf16[192,2,64]{0,2,1:T(8,128)(2,1)S(1)} %bitcast.70, bf16[12288,2,64]{0,2,1:T(8,128)(2,1)} %bitcast.65, pred[192,12288]{1,0:T(8,128)(4,1)S(1)} %iota_compare_fusion), kind=kOutput, calls=%fused_computation.88 | convolution fusion | flops 618135168 | bytes 24430080 | tf_op jit(solution)/shard_map/cond/branch_1_fun/qhmd,khmd->hmqk/dot_general | solution.py:106
  180.4 9.6 %fusion.9 = f32[1,2,192,128]{3,2,1,0:T(8,128)S(1)} fusion(bf16[12288,256]{1,0:T(8,128)(2,1)} %get-tuple-element.62, f32[2,192,12288]{2,1,0:T(8,128)} %get-tuple-element.75, f32[2,192]{1,0:T(2,128)S(1)} %broadcast_maximum_fusion, pred[192,12288]{1,0:T(8,128)(4,1)S(1)} %iota_compare_fusion), kind=kOutput, calls=%fused_computation.11 | convolution fusion | flops 1222115328 | bytes 24577536 | tf_op jit(solution)/shard_map/cond/branch_1_fun/hmqk,khe->hmqe/dot_general | solution.py:114
  190.0 8.9 %fusion = f32[2,192]{1,0:T(2,128)S(1)} fusion(f32[2,192,12288]{2,1,0:T(8,128)} %get-tuple-element.75, f32[2,192]{1,0:T(2,128)S(1)} %broadcast_maximum_fusion, pred[192,12288]{1,0:T(8,128)(4,1)S(1)} %iota_compare_fusion), kind=kLoop, calls=%fused_computation.2 | loop fusion | flops 14155392 | bytes 21236736 | tf_op jit(solution)/shard_map/cond/branch_1_fun/reduce_sum | solution.py:113
  199.0 0.2 fusion.69
  199.2 0.0 copy-done
  199.2 0.0 copy-done.5
  199.2 0.5 convolution_convert_fusion.1
  199.7 0.0 copy-start.4
  199.7 0.0 copy-start.6
  199.7 24.8 %all_to_all.15 = bf16[8,24,2048]{2,1,0:T(8,128)(2,1)S(1)} all-to-all(bf16[8,24,2048]{2,1,0:T(8,128)(2,1)S(1)} %bitcast.66), channel_id=1, replica_groups=mesh['sp_0'=16,'sp_1'=4,'tp'=8] {'tp'}, dimensions={0} | all-to-all | bytes 1572864 | tf_op jit(solution)/shard_map/all_to_all | solution.py:39
  224.6 0.1 reduce_sum.54
  224.7 0.0 copy-done.1
  224.7 0.1 fusion.58
  224.9 0.0 copy-done.3
  224.9 0.1 fusion.60
  225.0 1.0 broadcast_in_dim.34
  225.9 4.5 %all-to-all-start.1 = ((bf16[8,24,2048]{2,1,0:T(8,128)(2,1)}), bf16[8,24,2048]{2,1,0:T(8,128)(2,1)S(1)}, u32[]{:S(2)}, u32[]{:S(2)}) async-start(bf16[8,24,2048]{2,1,0:T(8,128)(2,1)} %broadcast_in_dim.34), calls=%async_computation.1 | async-start | bytes 1572864 | tf_op jit(solution)/shard_map/all_to_all | solution.py:51
  230.4 75.8 %all-gather.6.cloned.1.call-done = bf16[2048,1408]{1,0:T(8,128)(2,1)} async-done(((bf16[32,1408]{1,0:T(8,128)(2,1)}), bf16[2048,1408]{1,0:T(8,128)(2,1)}) %all-gather.6.cloned.1.call-update) | async-done | bytes 5767184 | tf_op jit(solution)/shard_map/all_gather | solution.py:19
  306.2 0.0 all-to-all-done.1
  306.2 2.7 fusion.19
  308.9 1.5 collective-permute-start
  310.4 0.0 copy-done.4
  310.4 67.6 %all-gather.8.cloned.1.call-done = bf16[704,2048]{0,1:T(8,128)(2,1)} async-done(((bf16[704,128]{0,1:T(8,128)(2,1)}), bf16[704,2048]{0,1:T(8,128)(2,1)}) %all-gather.8.cloned.1.call-update) | async-done | bytes 2883600 | tf_op jit(solution)/shard_map/all_gather | solution.py:28
  378.1 0.0 collective-permute-done
  378.1 0.0 copy-done.6
  378.1 5.2 %convolution_convert_fusion = bf16[192,2048]{1,0:T(8,128)(2,1)S(1)} fusion(bf16[704,2048]{0,1:T(8,128)(2,1)} %all-gather.8.cloned.1.call-done, bf16[192,2048]{1,0:T(8,128)(2,1)S(1)} %bitcast.68, bf16[2048,1408]{1,0:T(8,128)(2,1)} %all-gather.6.cloned.1.call-done, bf16[192,704]{1,0:T(8,128)(2,1)S(1)} %fusion.19, ...), kind=kOutput, calls=%fused_computation.19 | convolution fusion | flops 1110798336 | bytes 8148736 | tf_op jit(solution)/shard_map/dot_general | solution.py:158
  383.3 25.7 %all_to_all.16 = bf16[8,24,2048]{2,1,0:T(8,128)(2,1)S(1)} all-to-all(bf16[8,24,2048]{2,1,0:T(8,128)(2,1)S(1)} %bitcast.69), channel_id=1, replica_groups=mesh['sp_0'=16,'sp_1'=4,'tp'=8] {'tp'}, dimensions={0} | all-to-all | bytes 1572864 | tf_op jit(solution)/shard_map/all_to_all | solution.py:39
  409.0 0.1 reduce_sum.56
  409.2 0.7 fusion.61
  (9 shorter events, 0.1 us)
Async XLA Ops:
  6.5 192.7 %copy-start = (bf16[128,2048]{1,0:T(8,128)(2,1)S(1)}, bf16[128,2048]{1,0:T(8,128)(2,1)}, u32[]{:S(2)}) copy-start(bf16[128,2048]{1,0:T(8,128)(2,1)} %param.21) | copy-start | bytes 1572868
  6.5 151.8 %all-gather.4.cloned.1.call-start = ((), (), s32[]{:S(2)}) async-start(), calls=%async_computation.3 | async-start | bytes 6389760 | tf_op jit(solution)/shard_map/all_gather | solution.py:19
  8.1 298.1 %all-gather.6.cloned.1.call-start = ((), (), s32[]{:S(2)}) async-start(), calls=%async_computation.4 | async-start | bytes 5857280 | tf_op jit(solution)/shard_map/all_gather | solution.py:19
  9.7 368.4 %all-gather.8.cloned.1.call-start = ((), (), s32[]{:S(2)}) async-start(), calls=%async_computation.5 | async-start | bytes 3342336 | tf_op jit(solution)/shard_map/all_gather | solution.py:28
  158.3 40.9 %copy-start.5 = (f32[128]{0:T(128)S(1)}, f32[128]{0:T(128)}, u32[]{:S(2)}) copy-start(f32[128]{0:T(128)} %param.20) | copy-start | bytes 1540
  158.3 66.4 %copy-start.1 = (bf16[24,2048]{1,0:T(8,128)(2,1)S(1)}, bf16[24,2048]{1,0:T(8,128)(2,1)}, u32[]{:S(2)}) copy-start(bf16[24,2048]{1,0:T(8,128)(2,1)} %param.15) | copy-start | bytes 294916
  158.3 66.6 %copy-start.3 = (f32[2048]{0:T(1024)S(1)}, f32[2048]{0:T(1024)}, u32[]{:S(2)}) copy-start(f32[2048]{0:T(1024)} %param.22) | copy-start | bytes 24580
  159.8 7.9 %copy-start.2 = (bf16[192,128]{1,0:T(8,128)(2,1)S(1)}, bf16[192,128]{1,0:T(8,128)(2,1)}, u32[]{:S(2)}) copy-start(bf16[192,128]{1,0:T(8,128)(2,1)} %get-tuple-element.61) | copy-start | bytes 147460 | tf_op jit(solution)/shard_map/cond
  199.7 110.7 %copy-start.4 = (f32[3,704]{1,0:T(4,128)S(1)}, f32[3,704]{1,0:T(4,128)}, u32[]{:S(2)}) copy-start(f32[3,704]{1,0:T(4,128)} %param.25) | copy-start | bytes 25348
  199.7 178.4 %copy-start.6 = (f32[704]{0:T(1024)S(1)}, f32[704]{0:T(1024)}, u32[]{:S(2)}) copy-start(f32[704]{0:T(1024)} %param.26) | copy-start | bytes 8452
  225.9 80.3 %all-to-all-start.1 = ((bf16[8,24,2048]{2,1,0:T(8,128)(2,1)}), bf16[8,24,2048]{2,1,0:T(8,128)(2,1)S(1)}, u32[]{:S(2)}, u32[]{:S(2)}) async-start(bf16[8,24,2048]{2,1,0:T(8,128)(2,1)} %broadcast_in_dim.34), calls=%async_computation.1 | async-start | bytes 1572864 | tf_op jit(solution)/shard_map/all_to_all | solution.py:51
  308.9 69.2 %collective-permute-start = (bf16[2,704]{1,0:T(2,128)(2,1)S(1)}, bf16[2,704]{1,0:T(2,128)(2,1)S(1)}, u32[]{:S(2)}, u32[]{:S(2)}) collective-permute-start(bf16[2,704]{1,0:T(2,128)(2,1)S(1)} %slice.79), channel_id=1, source_target_pairs={{0,8},{8,16},{16,24},{24,32},{32,40},{40,48},{48,56},{56,64},{64,7... | collective-permute-start | bytes 8456 | tf_op jit(solution)/shard_map/ppermute | solution.py:61
Sparse Core Ops, SparseCore 0:
  10.3 147.9 all-gather.3
  161.2 144.9 all-gather.5
  308.3 69.7 all-gather.7
where the time goes:
time: 417 us; the launch traced here: 416 us
  waiting for transfers between devices  279 us (67%)
  blocking collectives  63.1 us (15%)
  matrix products  30.6 us (7%)
  other arithmetic  14.9 us (4%)
  between operations  13.9 us (3%)
  local copies, waits for them, and re-layouts  9 us (2%)
  starting transfers between devices  6.04 us (1%)
    all_gather x2, waiting for transfers between devices, in_one_piece(): out, at, done = (lax.all_gather(both, axis, axis=dim, tiled=True), 0, [])  211 us
    all_gather x1, waiting for transfers between devices, gathered_by_axis(): shard = lax.all_gather(shard, axis, axis=dim, tiled=True)  67.6 us
    all_to_all x2, blocking collectives, sent_and_summed(): tiles = lax.all_to_all(cut_along(shard, dim, count), axis, 0, 0, tiled=True)  50.6 us
    dot_general x1, matrix products, compute(): jnp.einsum('qhmd,khmd->hmqk', query, key_rows, preferred_element_type=jnp...  12.6 us
    all_gather x1, blocking collectives, gathered_by_axis(): shard = lax.all_gather(shard, axis, axis=dim, tiled=True)  12.5 us
    dot_general x1, matrix products, compute(): jnp.einsum('hmqk,khe->hmqe', exp_scores.astype(jnp.bfloat16), value_rows,...  9.63 us
    reduce_sum x1, other arithmetic, compute(): totals = jnp.sum(exp_scores, axis=-1)  8.94 us
  transfers between devices with their start and end apart: 5, of which 3 were waited for; matrix products, arithmetic and copies ran while one was open for 11% of the time, Pallas kernels for 0%

commit v1 on v0

v1 whole, which is shorter than its diff:
```python
import jax
import jax.numpy as jnp
from jax import lax
from jax.experimental import pallas as pl
from jax.experimental.pallas import tpu as pltpu
from jax.sharding import Mesh
from jax.sharding import PartitionSpec as P

HD = 64
VD = 128
SP = ("z", "y")
SP_TP = ("z", "y", "tp")
NZ = 16
NY = 4
eps = 1e-05
neg_fill = -1e30
TILE = 128
FAR = (4, 8, 12)
NEAR = ((1, 5, 9, 13), (2, 6, 10, 14), (3, 7, 11, 15))

VMEM = pl.BlockSpec(memory_space=pltpu.VMEM)
SMEM = pl.BlockSpec(memory_space=pltpu.SMEM)


def shifted(value, axis, steps):
    count = lax.axis_size(axis)
    return lax.ppermute(value, axis, [(i, (i + steps) % count) for i in range(count)])


def dot_nt(a, b):
    return lax.dot_general(a, b, (((1,), (1,)), ((), ())), preferred_element_type=jnp.float32)


def attend_kernel(where_ref, q_ref, own_ref, far_ref, n1_ref, n2_ref, n3_ref, out_ref):
    z = where_ref[0]
    y = where_ref[1]
    rows = own_ref.shape[0]

    def row_bias(offsets):
        lane = lax.broadcasted_iota(jnp.int32, (1, rows * len(offsets)), 1)
        bias = jnp.zeros(lane.shape, jnp.float32)
        for i, off in enumerate(offsets):
            inside = jnp.logical_and(lane >= i * rows, lane < (i + 1) * rows)
            bias = jnp.where(jnp.logical_and(inside, off > z), neg_fill, bias)
        return bias

    pieces = ((far_ref, FAR), (n1_ref, NEAR[0]), (n2_ref, NEAR[1]), (n3_ref, NEAR[2]))
    biases = [row_bias(offsets) for _, offsets in pieces]
    lane_q = lax.broadcasted_iota(jnp.int32, (TILE, 2 * HD), 1)
    lane_s = lax.broadcasted_iota(jnp.int32, (TILE, VD), 1)

    @pl.loop(0, NY * rows // TILE)
    def _(t):
        at = pl.multiple_of(t * TILE, TILE)
        q = q_ref[pl.ds(at, TILE), :] * jnp.bfloat16(HD**-0.5)
        zero = jnp.zeros_like(q)
        q2 = jnp.concatenate(
            (jnp.where(lane_q < HD, q, zero), jnp.where(lane_q < HD, zero, q)), axis=0
        )
        s_own = dot_nt(q2, own_ref[:, : 2 * HD])
        r = lax.broadcasted_iota(jnp.int32, s_own.shape, 0)
        r = jnp.where(r >= TILE, r - TILE, r) + at
        k = lax.broadcasted_iota(jnp.int32, s_own.shape, 1) + y * rows
        s_own = jnp.where(k <= r, s_own, neg_fill)
        scores = [s_own] + [
            dot_nt(q2, ref[:, : 2 * HD]) + bias for (ref, _), bias in zip(pieces, biases)
        ]
        top = jnp.max(scores[0], axis=1, keepdims=True)
        for s in scores[1:]:
            top = jnp.maximum(top, jnp.max(s, axis=1, keepdims=True))
        total = jnp.zeros((2 * TILE, 1), jnp.float32)
        acc = jnp.zeros((2 * TILE, VD), jnp.float32)
        for s, ref in zip(scores, (own_ref, far_ref, n1_ref, n2_ref, n3_ref)):
            e = jnp.exp(s - top)
            total = total + jnp.sum(e, axis=1, keepdims=True)
            acc = acc + jnp.dot(
                e.astype(jnp.bfloat16), ref[:, 2 * HD :], preferred_element_type=jnp.float32
            )
        mean = acc / total
        lse = top + jnp.log(total)
        hi = lse.astype(jnp.bfloat16).astype(jnp.float32)
        mid = (lse - hi).astype(jnp.bfloat16).astype(jnp.float32)
        low = lse - hi - mid
        stat = jnp.zeros((TILE, VD), jnp.float32)
        for m in range(2):
            for i, v in enumerate((hi, mid, low)):
                stat = jnp.where(lane_s == 3 * m + i, v[m * TILE : (m + 1) * TILE], stat)
        out_ref[pl.ds(at, TILE), 0:VD] = mean[:TILE].astype(jnp.bfloat16)
        out_ref[pl.ds(at, TILE), VD : 2 * VD] = mean[TILE:].astype(jnp.bfloat16)
        out_ref[pl.ds(at, TILE), 2 * VD : 3 * VD] = stat.astype(jnp.bfloat16)


def project_kernel(weight2_ref, got_ref, gain_ref, out_w_ref, out_ref):
    means = []
    for m in range(2):
        lses = []
        for y in range(NY):
            part = got_ref[y, :, 2 * VD + 3 * m : 2 * VD + 3 * m + 3].astype(jnp.float32)
            lses.append(part[:, 0:1] + part[:, 1:2] + part[:, 2:3])
        top = lses[0]
        for v in lses[1:]:
            top = jnp.maximum(top, v)
        total = jnp.zeros_like(top)
        acc = jnp.zeros((top.shape[0], VD), jnp.float32)
        for y in range(NY):
            share = jnp.exp(lses[y] - top)
            total = total + share
            acc = acc + share * got_ref[y, :, m * VD : (m + 1) * VD].astype(jnp.float32)
        means.append(acc / total)
    diff = means[0] - weight2_ref[0] * means[1]
    scale_inv = lax.rsqrt(jnp.mean(diff * diff, axis=-1, keepdims=True) + eps)
    attended = (diff * scale_inv * gain_ref[...] * 0.8).astype(jnp.bfloat16)
    out_ref[...] = jnp.dot(attended, out_w_ref[...], preferred_element_type=jnp.float32).astype(
        jnp.bfloat16
    )


def mid_kernel(parts_ref, residual_ref, gain_ref, mid_ref, normed_ref):
    proj = parts_ref[0].astype(jnp.float32)
    for i in range(1, parts_ref.shape[0]):
        proj = proj + parts_ref[i].astype(jnp.float32)
    proj = proj.astype(jnp.bfloat16).astype(jnp.float32)
    mid = (residual_ref[...].astype(jnp.float32) + proj).astype(jnp.bfloat16)
    mid_ref[...] = mid
    mid_f = mid.astype(jnp.float32)
    scale_inv = lax.rsqrt(jnp.mean(mid_f * mid_f, axis=-1, keepdims=True) + eps)
    normed_ref[...] = (mid_f * scale_inv * gain_ref[...]).astype(jnp.bfloat16)


def last_kernel(parts_ref, mid_ref, out_ref):
    ffn = parts_ref[0].astype(jnp.float32)
    for i in range(1, parts_ref.shape[0]):
        ffn = ffn + parts_ref[i].astype(jnp.float32)
    ffn = ffn.astype(jnp.bfloat16).astype(jnp.float32)
    out_ref[...] = (mid_ref[...].astype(jnp.float32) + ffn).astype(jnp.bfloat16)


def local(
    residual,
    queries,
    key_pairs,
    values,
    second_weight,
    head_gain,
    out_weight,
    norm_gain,
    up_weight,
    gate_weight,
    conv_weight,
    conv_bias,
    down_weight,
):
    rows = queries.shape[0]
    ff = up_weight.shape[1]
    d = residual.shape[1]
    tp = lax.axis_size("tp")
    where = jnp.stack((lax.axis_index("z"), lax.axis_index("y"))).astype(jnp.int32)
    own_w = jnp.concatenate((up_weight, gate_weight, down_weight.T), axis=1)
    row_w = lax.all_gather(own_w, "y", axis=0, tiled=True)
    all_w = lax.all_gather(row_w, "z", axis=0, tiled=True)

    kv = jnp.concatenate((key_pairs, values), axis=1)
    q_all = lax.all_gather(queries, "y", axis=0, tiled=True)
    f4, f8, f12 = (shifted(kv, "z", s) for s in (4, 8, -4))
    held = jnp.concatenate((kv, f4, f8, f12), axis=0)
    n1 = shifted(held, "z", 1)
    n2a = shifted(held[: 2 * rows], "z", 2)
    back = jnp.concatenate((f12, kv), axis=0)
    n2b = shifted(back, "z", -2)
    n2 = jnp.concatenate((n2a, n2b), axis=0)
    n3 = shifted(jnp.concatenate((f4, f8, f12, kv), axis=0), "z", -1)
    far = held[rows:]
    parts = pl.pallas_call(
        attend_kernel,
        out_shape=jax.ShapeDtypeStruct((NY * rows, 3 * VD), jnp.bfloat16),
        in_specs=[SMEM] + [VMEM] * 6,
        out_specs=VMEM,
        name="attend",
    )(where, q_all, kv, far, n1, n2, n3)
    got = lax.all_to_all(parts.reshape(NY, rows, 3 * VD), "y", 0, 0, tiled=True)
    proj = pl.pallas_call(
        project_kernel,
        out_shape=jax.ShapeDtypeStruct((rows, d), jnp.bfloat16),
        in_specs=[SMEM] + [VMEM] * 3,
        out_specs=VMEM,
        name="project",
    )(second_weight, got, head_gain.reshape(1, VD), out_weight)
    proj_parts = lax.all_to_all(proj.reshape(tp, rows // tp, d), "tp", 0, 0, tiled=True)
    mid, normed = pl.pallas_call(
        mid_kernel,
        out_shape=[jax.ShapeDtypeStruct((rows // tp, d), jnp.bfloat16)] * 2,
        in_specs=[VMEM] * 3,
        out_specs=[VMEM] * 2,
        name="mid",
    )(proj_parts, residual, norm_gain.reshape(1, d))
    normed_all = lax.all_gather(normed, "tp", axis=0, tiled=True)
    both = jnp.dot(normed_all, all_w[:, : 2 * ff], preferred_element_type=jnp.float32).astype(
        jnp.bfloat16
    )
    up_proj, gate_proj = both[:, :ff], both[:, ff:]
    taps = conv_weight.shape[0]
    count = lax.axis_size("z") * lax.axis_size("y")
    rim_rows = lax.ppermute(
        up_proj[rows - (taps - 1) :], SP, [(i, i + 1) for i in range(count - 1)]
    )
    extended = jnp.concatenate((rim_rows, up_proj), axis=0)
    conv_out = jnp.zeros((rows, ff), jnp.float32) + conv_bias[None, :]
    for tap in range(taps):
        conv_out = conv_out + conv_weight[tap][None, :] * extended[tap : tap + rows].astype(
            jnp.float32
        )
    hidden = (jax.nn.silu(conv_out) * gate_proj.astype(jnp.float32)).astype(jnp.bfloat16)
    ffn = dot_nt(hidden, all_w[:, 2 * ff :]).astype(jnp.bfloat16)
    ffn_parts = lax.all_to_all(ffn.reshape(tp, rows // tp, d), "tp", 0, 0, tiled=True)
    return pl.pallas_call(
        last_kernel,
        out_shape=jax.ShapeDtypeStruct((rows // tp, d), jnp.bfloat16),
        in_specs=[VMEM] * 2,
        out_specs=VMEM,
        name="last",
    )(ffn_parts, mid)


def solution(mesh):
    finer = Mesh(mesh.devices.reshape(NZ, NY, mesh.shape["tp"]), ("z", "y", "tp"))
    in_specs = (
        P(SP_TP, None),
        P(SP, "tp"),
        P(SP, "tp"),
        P(SP, "tp"),
        P("tp"),
        P("tp"),
        P("tp", None),
        P(),
        P(SP, "tp"),
        P(SP, "tp"),
        P(None, "tp"),
        P("tp"),
        P("tp", SP),
    )
    out_specs = P(SP_TP, None)
    return jax.shard_map(local, mesh=finer, in_specs=in_specs, out_specs=out_specs, check_vma=False)
```

time: 417 us -> 204 us (0.49)
  waiting for transfers between devices: 279 us -> 27.1 us
  starting transfers between devices: 6.04 us -> 49.7 us
  matrix products: 30.6 us -> 7.27 us
  Pallas kernels: 0 us -> 19.3 us
  blocking collectives: 63.1 us -> 76 us
  other arithmetic: 14.9 us -> 2.24 us
  local copies, waits for them, and re-layouts: 9 us -> 4.2 us
    all_gather x3 -> x1, waiting for transfers between devices: 279 us -> 9.56 us  [local(): all_w = lax.all_gather(row_w, 'z', axis=0, tiled=True)]
    ppermute x1 -> x8, starting transfers between devices: 1.47 us -> 46.2 us  [the longest x7 44 us: shifted(): lax.ppermute(value, axis, [(i, (i + steps) % count) for i in range(count)])]
    all_gather x1 -> x3, blocking collectives: 12.5 us -> 38.3 us  [the longest x1 14.6 us: local(): normed_all = lax.all_gather(normed, 'tp', axis=0, tiled=True)]
    dot_general x5 -> x2, matrix products: 30.6 us -> 7.27 us  [the longest x1 4.06 us: local(): jnp.dot(normed_all, all_w[:, :2 * ff], preferred_element_type=jnp.float32)]
    pallas_call x0 -> x4, Pallas kernels: none -> 19.3 us  [the longest x1 12 us: local(): pl.pallas_call(attend_kernel, out_shape=jax.ShapeDtypeStruct((NY * rows,...]
    all_to_all x2, blocking collectives: 50.6 us -> 37.7 us  [the longest x1 19.9 us: local(): lax.all_to_all(proj.reshape(tp, rows // tp, d), 'tp', 0, 0, tiled=True)]
    ppermute x1 -> x8, waiting for transfers between devices: 0.01 us -> 10.5 us  [the longest x7 9.85 us: shifted(): lax.ppermute(value, axis, [(i, (i + steps) % count) for i in range(count)])]
    reduce_sum x5 -> x0, other arithmetic: 9.54 us -> none  [the longest x1 8.94 us: compute(): totals = jnp.sum(exp_scores, axis=-1)]
  transfers between devices with their start and end apart: 5 -> 10, of which waited for: 3 -> 6; matrix products, arithmetic and copies ran while one was open for 11% -> 2% of each run, Pallas kernels for 0% -> 9%
where the time goes in v1:
time: 204 us; the launch traced here: 200 us
  blocking collectives  76 us (37%)
  starting transfers between devices  49.7 us (24%)
  waiting for transfers between devices  27.1 us (13%)
  Pallas kernels  19.3 us (9%)
  between operations  14.2 us (7%)
  matrix products  7.27 us (4%)
  local copies, waits for them, and re-layouts  4.2 us (2%)
  other arithmetic  2.24 us (1%)
    ppermute x7, starting transfers between devices, shifted(): lax.ppermute(value, axis, [(i, (i + steps) % count) for i in range(count)])  44 us
    all_to_all x1, blocking collectives, local(): lax.all_to_all(proj.reshape(tp, rows // tp, d), 'tp', 0, 0, tiled=True)  19.9 us
    all_to_all x1, blocking collectives, local(): lax.all_to_all(ffn.reshape(tp, rows // tp, d), 'tp', 0, 0, tiled=True)  17.8 us
    all_gather x1, blocking collectives, local(): normed_all = lax.all_gather(normed, 'tp', axis=0, tiled=True)  14.6 us
    all_gather x1, blocking collectives, local(): row_w = lax.all_gather(own_w, 'y', axis=0, tiled=True)  12.7 us
    pallas_call x1, Pallas kernels, local(): pl.pallas_call(attend_kernel, out_shape=jax.ShapeDtypeStruct((NY * rows,...  12 us
    all_gather x1, blocking collectives, local(): q_all = lax.all_gather(queries, 'y', axis=0, tiled=True)  11.1 us
    ppermute x7, waiting for transfers between devices, shifted(): lax.ppermute(value, axis, [(i, (i + steps) % count) for i in range(count)])  9.85 us
  transfers between devices with their start and end apart: 10, of which 6 were waited for; matrix products, arithmetic and copies ran while one was open for 2% of the time, Pallas kernels for 9%

profile of v1, /device:TPU:1, one launch (start us, length us, event | category | flops | bytes accessed | tf_op | source)
XLA Modules:
  0.0 200.0 jit_solution(17571154578842836478)
XLA Ops:
  6.5 0.0 all-gather.2.cloned.1.call-start
  6.5 0.9 concatenate.34
  7.5 12.7 %all_gather.14 = bf16[128,2112]{1,0:T(8,128)(2,1)} all-gather(bf16[32,2112]{1,0:T(8,128)(2,1)S(1)} %concatenate.34), channel_id=1, replica_groups=mesh['z'=16,'y'=4,'tp'=8] {'y'}, dimensions={0}, use_global_device_ids=true | all-gather | bytes 675840 | tf_op jit(solution)/shard_map/all_gather | solution.py:159
  20.2 0.0 all-gather.2.cloned.1.call-update
  20.2 0.8 constant_dynamic-update-slice_fusion.1
  21.0 0.8 constant_dynamic-update-slice_fusion.own_ref
  21.8 0.0 copy-start.1
  21.8 9.3 %collective-permute-start = (bf16[192,256]{1,0:T(8,128)(2,1)S(1)}, bf16[192,256]{1,0:T(8,128)(2,1)S(1)}, u32[]{:S(2)}, u32[]{:S(2)}) collective-permute-start(bf16[192,256]{1,0:T(8,128)(2,1)S(1)} %constant_dynamic-update-slice_fusion.own_ref), channel_id=1, source_target_pairs={{0,128},{32,160},{64,192},{96,224},{128,256},{160,288},{192,320},{... | collective-permute-start | bytes 294920 | tf_op jit(solution)/shard_map/ppermute | solution.py:27
  31.1 5.6 %collective-permute-start.2 = (bf16[192,256]{1,0:T(8,128)(2,1)S(1)}, bf16[192,256]{1,0:T(8,128)(2,1)S(1)}, u32[]{:S(2)}, u32[]{:S(2)}) collective-permute-start(bf16[192,256]{1,0:T(8,128)(2,1)S(1)} %constant_dynamic-update-slice_fusion.own_ref), channel_id=1, source_target_pairs={{0,384},{32,416},{64,448},{96,480},{128,0},{160,32},{192,64},{224,... | collective-permute-start | bytes 294920 | tf_op jit(solution)/shard_map/ppermute | solution.py:27
  36.7 10.3 %collective-permute-start.1 = (bf16[192,256]{1,0:T(8,128)(2,1)S(1)}, bf16[192,256]{1,0:T(8,128)(2,1)S(1)}, u32[]{:S(2)}, u32[]{:S(2)}) collective-permute-start(bf16[192,256]{1,0:T(8,128)(2,1)S(1)} %constant_dynamic-update-slice_fusion.own_ref), channel_id=1, source_target_pairs={{0,256},{32,288},{64,320},{96,352},{128,384},{160,416},{192,448},{... | collective-permute-start | bytes 294920 | tf_op jit(solution)/shard_map/ppermute | solution.py:27
  47.0 0.0 collective-permute-done
  47.0 1.6 collective-permute-done.2
  48.6 1.9 collective-permute-start.4
  50.5 5.5 %collective-permute-start.5 = (bf16[384,256]{1,0:T(8,128)(2,1)S(1)}, bf16[384,256]{1,0:T(8,128)(2,1)S(1)}, u32[]{:S(2)}, u32[]{:S(2)}) collective-permute-start(bf16[384,256]{1,0:T(8,128)(2,1)S(1)} %get-tuple-element.15), channel_id=1, source_target_pairs={{0,448},{32,480},{64,0},{96,32},{128,64},{160,96},{192,128},{224,1... | collective-permute-start | bytes 589832 | tf_op jit(solution)/shard_map/ppermute | solution.py:27
  56.0 0.0 collective-permute-done.1
  56.0 0.1 pad_maximum_fusion.2
  56.1 4.0 %collective-permute-start.3 = (bf16[768,256]{1,0:T(8,128)(2,1)S(1)}, bf16[768,256]{1,0:T(8,128)(2,1)S(1)}, u32[]{:S(2)}, u32[]{:S(2)}) collective-permute-start(bf16[768,256]{1,0:T(8,128)(2,1)S(1)} %get-tuple-element.13), channel_id=1, source_target_pairs={{0,32},{32,64},{64,96},{96,128},{128,160},{160,192},{192,224},{224... | collective-permute-start | bytes 1179656 | tf_op jit(solution)/shard_map/ppermute | solution.py:27
  60.1 7.5 %collective-permute-start.6 = (bf16[768,256]{1,0:T(8,128)(2,1)S(1)}, bf16[768,256]{1,0:T(8,128)(2,1)S(1)}, u32[]{:S(2)}, u32[]{:S(2)}) collective-permute-start(bf16[768,256]{1,0:T(8,128)(2,1)S(1)} %get-tuple-element.12), channel_id=1, source_target_pairs={{0,480},{32,0},{64,32},{96,64},{128,96},{160,128},{192,160},{224,1... | collective-permute-start | bytes 1179656 | tf_op jit(solution)/shard_map/ppermute | solution.py:27
  67.6 0.7 pad_add_fusion.where_ref
  68.3 11.1 %all_gather.12.q_ref = bf16[768,128]{1,0:T(8,128)(2,1)} all-gather(bf16[192,128]{1,0:T(8,128)(2,1)} %param.14), channel_id=1, replica_groups=mesh['z'=16,'y'=4,'tp'=8] {'y'}, dimensions={0}, use_global_device_ids=true | all-gather | bytes 245760 | tf_op jit(solution)/shard_map/all_gather | solution.py:163
  79.3 0.7 pad_maximum_fusion.5.far_ref
  80.1 0.0 collective-permute-done.4
  80.1 0.0 collective-permute-done.5
  80.1 0.8 pad_maximum_fusion.1.n2_ref
  80.8 5.5 %collective-permute-done.3.n1_ref = bf16[768,256]{1,0:T(8,128)(2,1)S(1)} collective-permute-done((bf16[768,256]{1,0:T(8,128)(2,1)S(1)}, bf16[768,256]{1,0:T(8,128)(2,1)S(1)}, u32[]{:S(2)}, u32[]{:S(2)}) %collective-permute-start.3) | collective-permute-done | bytes 393248 | tf_op jit(solution)/shard_map/ppermute | solution.py:27
  86.4 0.0 copy-start.2
  86.4 2.7 %collective-permute-done.6.n3_ref = bf16[768,256]{1,0:T(8,128)(2,1)S(1)} collective-permute-done((bf16[768,256]{1,0:T(8,128)(2,1)S(1)}, bf16[768,256]{1,0:T(8,128)(2,1)S(1)}, u32[]{:S(2)}, u32[]{:S(2)}) %collective-permute-start.6) | collective-permute-done | bytes 393248 | tf_op jit(solution)/shard_map/ppermute | solution.py:27
  89.1 0.0 copy-done.1
  89.1 0.0 copy-done.2
  89.1 0.0 copy-start.3
  89.1 0.8 copy-done.3
  89.8 12.0 %attend.1 = bf16[768,384]{1,0:T(8,128)(2,1)} custom-call(s32[2]{0:T(128)} %pad_add_fusion.where_ref, bf16[768,128]{1,0:T(8,128)(2,1)} %all_gather.12.q_ref, bf16[192,256]{1,0:T(8,128)(2,1)} %copy-done.1, bf16[576,256]{1,0:T(8,128)(2,1)} %pad_maximum_fusion.5.far_ref, bf16[768,256]{1,0:T(8,128)(2,1)} %copy-done.2, bf16[768,256]{1,0:T(8,128)(2,1)} %pad_maximum_fusion.1.n2_ref, ...), custom_call_target="tpu_custom_call" | custom-call | tf_op jit(solution)/shard_map/attend/pallas_call | solution.py:173
  101.9 3.5 %all-to-all-start = ((bf16[4,192,384]{2,1,0:T(8,128)(2,1)}), bf16[4,192,384]{2,1,0:T(8,128)(2,1)S(1)}, u32[]{:S(2)}, u32[]{:S(2)}) async-start(bf16[4,192,384]{2,1,0:T(8,128)(2,1)} %bitcast.10), calls=%async_computation | async-start | bytes 1179648 | tf_op jit(solution)/shard_map/all_to_all | solution.py:180
  106.0 7.1 %all-to-all-done.got_ref = bf16[4,192,384]{2,1,0:T(8,128)(2,1)S(1)} async-done(((bf16[4,192,384]{2,1,0:T(8,128)(2,1)}), bf16[4,192,384]{2,1,0:T(8,128)(2,1)S(1)}, u32[]{:S(2)}, u32[]{:S(2)}) %all-to-all-start) | async-done | bytes 589856 | tf_op jit(solution)/shard_map/all_to_all | solution.py:180
  113.1 0.0 copy-start
  113.1 0.8 copy-done
  113.9 3.3 %project.1 = bf16[192,2048]{1,0:T(8,128)(2,1)} custom-call(f32[1]{0:T(128)S(6)} %copy.15.weight2_ref, bf16[4,192,384]{2,1,0:T(8,128)(2,1)} %copy-done, f32[1,128]{1,0:T(1,128)} %bitcast.14, bf16[128,2048]{1,0:T(8,128)(2,1)} %out_w_ref.1), custom_call_target="tpu_custom_call" | custom-call | tf_op jit(solution)/shard_map/project/pallas_call | solution.py:181
  117.1 19.9 %all_to_all.15.parts_ref = bf16[8,24,2048]{2,1,0:T(8,128)(2,1)} all-to-all(bf16[8,24,2048]{2,1,0:T(8,128)(2,1)} %bitcast.9), channel_id=1, replica_groups=mesh['z'=16,'y'=4,'tp'=8] {'tp'}, dimensions={0} | all-to-all | bytes 1572864 | tf_op jit(solution)/shard_map/all_to_all | solution.py:188
  137.1 0.0 copy-start.4
  137.1 2.1 %mid.1 = (bf16[24,2048]{1,0:T(8,128)(2,1)}, bf16[24,2048]{1,0:T(8,128)(2,1)}) custom-call(bf16[8,24,2048]{2,1,0:T(8,128)(2,1)} %all_to_all.15.parts_ref, bf16[24,2048]{1,0:T(8,128)(2,1)} %residual_ref.1, f32[1,2048]{1,0:T(1,128)} %bitcast.13), custom_call_target="tpu_custom_call" | custom-call | tf_op jit(solution)/shard_map/mid/pallas_call | solution.py:189
  139.1 0.0 copy-start.5
  139.1 14.6 %all_gather.13 = bf16[192,2048]{1,0:T(8,128)(2,1)S(1)} all-gather(bf16[24,2048]{1,0:T(8,128)(2,1)} %get-tuple-element.7), channel_id=1, replica_groups=mesh['z'=16,'y'=4,'tp'=8] {'tp'}, dimensions={0}, use_global_device_ids=true | all-gather | bytes 884736 | tf_op jit(solution)/shard_map/all_gather | solution.py:196
  153.7 9.6 %all-gather.2.cloned.1.call-done = bf16[2048,2112]{1,0:T(8,128)(2,1)} async-done(((bf16[128,2112]{1,0:T(8,128)(2,1)}), bf16[2048,2112]{1,0:T(8,128)(2,1)}) %all-gather.2.cloned.1.call-update) | async-done | bytes 8650768 | tf_op jit(solution)/shard_map/all_gather | solution.py:160
  163.3 4.1 %fusion.7 = bf16[192,1408]{1,0:T(8,128)(2,1)S(1)} fusion(bf16[192,2048]{1,0:T(8,128)(2,1)S(1)} %all_gather.13, bf16[2048,2112]{1,0:T(8,128)(2,1)} %all-gather.2.cloned.1.call-done), kind=kOutput, calls=%fused_computation.5 | convolution fusion | flops 1107566592 | bytes 7094272 | tf_op jit(solution)/shard_map/dot_general | solution.py:197
  167.4 2.2 %collective-permute-start.7 = (bf16[2,704]{1,0:T(2,128)(2,1)S(1)}, bf16[2,704]{1,0:T(2,128)(2,1)S(1)}, u32[]{:S(2)}, u32[]{:S(2)}) collective-permute-start(bf16[2,704]{1,0:T(2,128)(2,1)S(1)} %slice.46), channel_id=1, source_target_pairs={{0,8},{8,16},{16,24},{24,32},{32,40},{40,48},{48,56},{56,64},{64,7... | collective-permute-start | bytes 8456 | tf_op jit(solution)/shard_map/ppermute | solution.py:203
  169.6 0.0 copy-done.4
  169.6 0.6 collective-permute-done.7
  170.3 0.0 copy-done.5
  170.3 3.2 %fusion.4 = bf16[192,2048]{1,0:T(8,128)(2,1)S(1)} fusion(bf16[2048,2112]{1,0:T(8,128)(2,1)} %all-gather.2.cloned.1.call-done, bf16[192,704]{1,0:T(8,128)(2,1)S(1)} %slice.47, bf16[2,704]{1,0:T(2,128)(2,1)S(1)} %collective-permute-done.7, bf16[192,1408]{1,0:T(8,128)(2,1)S(1)} %fusion.7, f32[704]{0:T(1024)S(1)} %get-tuple-element.10, ...), kind=kOutput, calls=%fused_computation.4 | convolution fusion | flops 557015040 | bytes 4541440 | tf_op jit(solution)/shard_map/dot_general | solution.py:31
  173.5 17.8 %all_to_all.16.parts_ref = bf16[8,24,2048]{2,1,0:T(8,128)(2,1)} all-to-all(bf16[8,24,2048]{2,1,0:T(8,128)(2,1)S(1)} %bitcast.11), channel_id=1, replica_groups=mesh['z'=16,'y'=4,'tp'=8] {'tp'}, dimensions={0} | all-to-all | bytes 1572864 | tf_op jit(solution)/shard_map/all_to_all | solution.py:214
  191.2 1.9 last.1
  (4 shorter events, 0.1 us)
Async XLA Ops:
  6.5 156.8 %all-gather.2.cloned.1.call-start = ((), (), s32[]{:S(2)}) async-start(), calls=%async_computation.3 | async-start | bytes 9469952 | tf_op jit(solution)/shard_map/all_gather | solution.py:160
  21.8 67.2 %copy-start.1 = (bf16[192,256]{1,0:T(8,128)(2,1)}, bf16[192,256]{1,0:T(8,128)(2,1)S(1)}, u32[]{:S(2)}) copy-start(bf16[192,256]{1,0:T(8,128)(2,1)S(1)} %constant_dynamic-update-slice_fusion.own_ref) | copy-start | bytes 294916
  21.8 25.1 %collective-permute-start = (bf16[192,256]{1,0:T(8,128)(2,1)S(1)}, bf16[192,256]{1,0:T(8,128)(2,1)S(1)}, u32[]{:S(2)}, u32[]{:S(2)}) collective-permute-start(bf16[192,256]{1,0:T(8,128)(2,1)S(1)} %constant_dynamic-update-slice_fusion.own_ref), channel_id=1, source_target_pairs={{0,128},{32,160},{64,192},{96,224},{128,256},{160,288},{192,320},{... | collective-permute-start | bytes 294920 | tf_op jit(solution)/shard_map/ppermute | solution.py:27
  31.1 17.4 %collective-permute-start.2 = (bf16[192,256]{1,0:T(8,128)(2,1)S(1)}, bf16[192,256]{1,0:T(8,128)(2,1)S(1)}, u32[]{:S(2)}, u32[]{:S(2)}) collective-permute-start(bf16[192,256]{1,0:T(8,128)(2,1)S(1)} %constant_dynamic-update-slice_fusion.own_ref), channel_id=1, source_target_pairs={{0,384},{32,416},{64,448},{96,480},{128,0},{160,32},{192,64},{224,... | collective-permute-start | bytes 294920 | tf_op jit(solution)/shard_map/ppermute | solution.py:27
  36.7 19.3 %collective-permute-start.1 = (bf16[192,256]{1,0:T(8,128)(2,1)S(1)}, bf16[192,256]{1,0:T(8,128)(2,1)S(1)}, u32[]{:S(2)}, u32[]{:S(2)}) collective-permute-start(bf16[192,256]{1,0:T(8,128)(2,1)S(1)} %constant_dynamic-update-slice_fusion.own_ref), channel_id=1, source_target_pairs={{0,256},{32,288},{64,320},{96,352},{128,384},{160,416},{192,448},{... | collective-permute-start | bytes 294920 | tf_op jit(solution)/shard_map/ppermute | solution.py:27
  48.6 31.5 %collective-permute-start.4 = (bf16[384,256]{1,0:T(8,128)(2,1)S(1)}, bf16[384,256]{1,0:T(8,128)(2,1)S(1)}, u32[]{:S(2)}, u32[]{:S(2)}) collective-permute-start(bf16[384,256]{1,0:T(8,128)(2,1)S(1)} %get-tuple-element.14), channel_id=1, source_target_pairs={{0,64},{32,96},{64,128},{96,160},{128,192},{160,224},{192,256},{22... | collective-permute-start | bytes 589832 | tf_op jit(solution)/shard_map/ppermute | solution.py:27
  50.5 29.5 %collective-permute-start.5 = (bf16[384,256]{1,0:T(8,128)(2,1)S(1)}, bf16[384,256]{1,0:T(8,128)(2,1)S(1)}, u32[]{:S(2)}, u32[]{:S(2)}) collective-permute-start(bf16[384,256]{1,0:T(8,128)(2,1)S(1)} %get-tuple-element.15), channel_id=1, source_target_pairs={{0,448},{32,480},{64,0},{96,32},{128,64},{160,96},{192,128},{224,1... | collective-permute-start | bytes 589832 | tf_op jit(solution)/shard_map/ppermute | solution.py:27
  56.1 30.3 %collective-permute-start.3 = (bf16[768,256]{1,0:T(8,128)(2,1)S(1)}, bf16[768,256]{1,0:T(8,128)(2,1)S(1)}, u32[]{:S(2)}, u32[]{:S(2)}) collective-permute-start(bf16[768,256]{1,0:T(8,128)(2,1)S(1)} %get-tuple-element.13), channel_id=1, source_target_pairs={{0,32},{32,64},{64,96},{96,128},{128,160},{160,192},{192,224},{224... | collective-permute-start | bytes 1179656 | tf_op jit(solution)/shard_map/ppermute | solution.py:27
  60.1 29.0 %collective-permute-start.6 = (bf16[768,256]{1,0:T(8,128)(2,1)S(1)}, bf16[768,256]{1,0:T(8,128)(2,1)S(1)}, u32[]{:S(2)}, u32[]{:S(2)}) collective-permute-start(bf16[768,256]{1,0:T(8,128)(2,1)S(1)} %get-tuple-element.12), channel_id=1, source_target_pairs={{0,480},{32,0},{64,32},{96,64},{128,96},{160,128},{192,160},{224,1... | collective-permute-start | bytes 1179656 | tf_op jit(solution)/shard_map/ppermute | solution.py:27
  86.4 2.7 %copy-start.2 = (bf16[768,256]{1,0:T(8,128)(2,1)}, bf16[768,256]{1,0:T(8,128)(2,1)S(1)}, u32[]{:S(2)}) copy-start(bf16[768,256]{1,0:T(8,128)(2,1)S(1)} %collective-permute-done.3.n1_ref) | copy-start | bytes 1179652
  89.1 0.8 copy-start.3
  101.9 11.2 %all-to-all-start = ((bf16[4,192,384]{2,1,0:T(8,128)(2,1)}), bf16[4,192,384]{2,1,0:T(8,128)(2,1)S(1)}, u32[]{:S(2)}, u32[]{:S(2)}) async-start(bf16[4,192,384]{2,1,0:T(8,128)(2,1)} %bitcast.10), calls=%async_computation | async-start | bytes 1179648 | tf_op jit(solution)/shard_map/all_to_all | solution.py:180
  113.1 0.8 copy-start
  137.1 32.5 %copy-start.4 = (f32[3,704]{1,0:T(4,128)S(1)}, f32[3,704]{1,0:T(4,128)}, u32[]{:S(2)}) copy-start(f32[3,704]{1,0:T(4,128)} %param.23) | copy-start | bytes 25348
  139.1 31.1 %copy-start.5 = (f32[704]{0:T(1024)S(1)}, f32[704]{0:T(1024)}, u32[]{:S(2)}) copy-start(f32[704]{0:T(1024)} %param.24) | copy-start | bytes 8452
  167.4 2.9 %collective-permute-start.7 = (bf16[2,704]{1,0:T(2,128)(2,1)S(1)}, bf16[2,704]{1,0:T(2,128)(2,1)S(1)}, u32[]{:S(2)}, u32[]{:S(2)}) collective-permute-start(bf16[2,704]{1,0:T(2,128)(2,1)S(1)} %slice.46), channel_id=1, source_target_pairs={{0,8},{8,16},{16,24},{24,32},{32,40},{40,48},{48,56},{56,64},{64,7... | collective-permute-start | bytes 8456 | tf_op jit(solution)/shard_map/ppermute | solution.py:203
Sparse Core Ops, SparseCore 0:
  20.3 142.9 all-gather.1

commit v2 on v1

--- a/solution.py
+++ b/solution.py
@@ -90,49 +90,29 @@
         out_ref[pl.ds(at, TILE), 2 * VD : 3 * VD] = stat.astype(jnp.bfloat16)
 
 
-def project_kernel(weight2_ref, got_ref, gain_ref, out_w_ref, out_ref):
+def merged(got):
+    got = got.astype(jnp.float32)
     means = []
     for m in range(2):
-        lses = []
-        for y in range(NY):
-            part = got_ref[y, :, 2 * VD + 3 * m : 2 * VD + 3 * m + 3].astype(jnp.float32)
-            lses.append(part[:, 0:1] + part[:, 1:2] + part[:, 2:3])
-        top = lses[0]
-        for v in lses[1:]:
-            top = jnp.maximum(top, v)
-        total = jnp.zeros_like(top)
-        acc = jnp.zeros((top.shape[0], VD), jnp.float32)
-        for y in range(NY):
-            share = jnp.exp(lses[y] - top)
-            total = total + share
-            acc = acc + share * got_ref[y, :, m * VD : (m + 1) * VD].astype(jnp.float32)
-        means.append(acc / total)
-    diff = means[0] - weight2_ref[0] * means[1]
-    scale_inv = lax.rsqrt(jnp.mean(diff * diff, axis=-1, keepdims=True) + eps)
-    attended = (diff * scale_inv * gain_ref[...] * 0.8).astype(jnp.bfloat16)
-    out_ref[...] = jnp.dot(attended, out_w_ref[...], preferred_element_type=jnp.float32).astype(
-        jnp.bfloat16
-    )
-
-
-def mid_kernel(parts_ref, residual_ref, gain_ref, mid_ref, normed_ref):
-    proj = parts_ref[0].astype(jnp.float32)
-    for i in range(1, parts_ref.shape[0]):
-        proj = proj + parts_ref[i].astype(jnp.float32)
-    proj = proj.astype(jnp.bfloat16).astype(jnp.float32)
-    mid = (residual_ref[...].astype(jnp.float32) + proj).astype(jnp.bfloat16)
-    mid_ref[...] = mid
-    mid_f = mid.astype(jnp.float32)
-    scale_inv = lax.rsqrt(jnp.mean(mid_f * mid_f, axis=-1, keepdims=True) + eps)
-    normed_ref[...] = (mid_f * scale_inv * gain_ref[...]).astype(jnp.bfloat16)
-
-
-def last_kernel(parts_ref, mid_ref, out_ref):
-    ffn = parts_ref[0].astype(jnp.float32)
-    for i in range(1, parts_ref.shape[0]):
-        ffn = ffn + parts_ref[i].astype(jnp.float32)
-    ffn = ffn.astype(jnp.bfloat16).astype(jnp.float32)
-    out_ref[...] = (mid_ref[...].astype(jnp.float32) + ffn).astype(jnp.bfloat16)
+        stat = got[:, :, 2 * VD + 3 * m : 2 * VD + 3 * m + 3]
+        lse = stat[..., 0:1] + stat[..., 1:2] + stat[..., 2:3]
+        share = jnp.exp(lse - jnp.max(lse, axis=0, keepdims=True))
+        acc = jnp.sum(share * got[:, :, m * VD : (m + 1) * VD], axis=0)
+        means.append(acc / jnp.sum(share, axis=0))
+    return means
+
+
+def normalize(rows_in, gain):
+    values_f = rows_in.astype(jnp.float32)
+    scale_inv = lax.rsqrt(jnp.mean(values_f * values_f, axis=-1, keepdims=True) + eps)
+    return (values_f * scale_inv * gain).astype(jnp.bfloat16)
+
+
+def summed_over_tp(shard):
+    count = lax.axis_size("tp")
+    cut = shard.reshape(count, shard.shape[0] // count, shard.shape[1])
+    tiles = lax.all_to_all(cut, "tp", 0, 0, tiled=True)
+    return jnp.sum(tiles.astype(jnp.float32), axis=0).astype(jnp.bfloat16)
 
 
 def local(
@@ -152,8 +132,6 @@
 ):
     rows = queries.shape[0]
     ff = up_weight.shape[1]
-    d = residual.shape[1]
-    tp = lax.axis_size("tp")
     where = jnp.stack((lax.axis_index("z"), lax.axis_index("y"))).astype(jnp.int32)
     own_w = jnp.concatenate((up_weight, gate_weight, down_weight.T), axis=1)
     row_w = lax.all_gather(own_w, "y", axis=0, tiled=True)
@@ -162,6 +140,7 @@
     kv = jnp.concatenate((key_pairs, values), axis=1)
     q_all = lax.all_gather(queries, "y", axis=0, tiled=True)
     f4, f8, f12 = (shifted(kv, "z", s) for s in (4, 8, -4))
+    f4, f8, f12, q_all = lax.optimization_barrier((f4, f8, f12, q_all))
     held = jnp.concatenate((kv, f4, f8, f12), axis=0)
     n1 = shifted(held, "z", 1)
     n2a = shifted(held[: 2 * rows], "z", 2)
@@ -178,32 +157,25 @@
         name="attend",
     )(where, q_all, kv, far, n1, n2, n3)
     got = lax.all_to_all(parts.reshape(NY, rows, 3 * VD), "y", 0, 0, tiled=True)
-    proj = pl.pallas_call(
-        project_kernel,
-        out_shape=jax.ShapeDtypeStruct((rows, d), jnp.bfloat16),
-        in_specs=[SMEM] + [VMEM] * 3,
-        out_specs=VMEM,
-        name="project",
-    )(second_weight, got, head_gain.reshape(1, VD), out_weight)
-    proj_parts = lax.all_to_all(proj.reshape(tp, rows // tp, d), "tp", 0, 0, tiled=True)
-    mid, normed = pl.pallas_call(
-        mid_kernel,
-        out_shape=[jax.ShapeDtypeStruct((rows // tp, d), jnp.bfloat16)] * 2,
-        in_specs=[VMEM] * 3,
-        out_specs=[VMEM] * 2,
-        name="mid",
-    )(proj_parts, residual, norm_gain.reshape(1, d))
-    normed_all = lax.all_gather(normed, "tp", axis=0, tiled=True)
-    both = jnp.dot(normed_all, all_w[:, : 2 * ff], preferred_element_type=jnp.float32).astype(
-        jnp.bfloat16
+    means = merged(got)
+    diff = means[0] - second_weight[0] * means[1]
+    scale_inv = lax.rsqrt(jnp.mean(diff * diff, axis=-1, keepdims=True) + eps)
+    attended = (diff * scale_inv * head_gain * 0.8).astype(jnp.bfloat16)
+    proj = summed_over_tp(
+        jnp.dot(attended, out_weight, preferred_element_type=jnp.float32).astype(jnp.bfloat16)
     )
-    up_proj, gate_proj = both[:, :ff], both[:, ff:]
+    mid = (residual.astype(jnp.float32) + proj.astype(jnp.float32)).astype(jnp.bfloat16)
+    normed_all = lax.all_gather(normalize(mid, norm_gain), "tp", axis=0, tiled=True)
+    count = lax.axis_size("z") * lax.axis_size("y")
+    rim_rows = lax.ppermute(normed_all[rows - 8 :], SP, [(i, i + 1) for i in range(count - 1)])
+    both = jnp.dot(
+        jnp.concatenate((normed_all, rim_rows), axis=0),
+        all_w[:, : 2 * ff],
+        preferred_element_type=jnp.float32,
+    ).astype(jnp.bfloat16)
+    up_proj, gate_proj = both[:rows, :ff], both[:rows, ff:]
     taps = conv_weight.shape[0]
-    count = lax.axis_size("z") * lax.axis_size("y")
-    rim_rows = lax.ppermute(
-        up_proj[rows - (taps - 1) :], SP, [(i, i + 1) for i in range(count - 1)]
-    )
-    extended = jnp.concatenate((rim_rows, up_proj), axis=0)
+    extended = jnp.concatenate((both[rows + 8 - (taps - 1) :, :ff], up_proj), axis=0)
     conv_out = jnp.zeros((rows, ff), jnp.float32) + conv_bias[None, :]
     for tap in range(taps):
         conv_out = conv_out + conv_weight[tap][None, :] * extended[tap : tap + rows].astype(
@@ -211,14 +183,8 @@
         )
     hidden = (jax.nn.silu(conv_out) * gate_proj.astype(jnp.float32)).astype(jnp.bfloat16)
     ffn = dot_nt(hidden, all_w[:, 2 * ff :]).astype(jnp.bfloat16)
-    ffn_parts = lax.all_to_all(ffn.reshape(tp, rows // tp, d), "tp", 0, 0, tiled=True)
-    return pl.pallas_call(
-        last_kernel,
-        out_shape=jax.ShapeDtypeStruct((rows // tp, d), jnp.bfloat16),
-        in_specs=[VMEM] * 2,
-        out_specs=VMEM,
-        name="last",
-    )(ffn_parts, mid)
+    ffn_out = summed_over_tp(ffn)
+    return (mid.astype(jnp.float32) + ffn_out.astype(jnp.float32)).astype(jnp.bfloat16)
 
 
 def solution(mesh):

time: 204 us -> 200 us (0.980); the launches traced: 200 us -> 199 us
  Pallas kernels: 19.3 us -> 12.1 us
  waiting for transfers between devices: 27.1 us -> 32.8 us
  other arithmetic: 2.24 us -> 5.11 us
    ppermute x7, waiting for transfers between devices: 9.85 us -> 22.3 us  [shifted(): lax.ppermute(value, axis, [(i, (i + steps) % count) for i in range(count)])]
    pallas_call x3 -> x0, Pallas kernels: 7.27 us -> none  [the longest x1 3.29 us: local(): pl.pallas_call(project_kernel, out_shape=jax.ShapeDtypeStruct((rows, d),...]
    all_gather x1, waiting for transfers between devices: 9.56 us -> 2.91 us  [local(): all_w = lax.all_gather(row_w, 'z', axis=0, tiled=True)]
    dot_general x1 -> x2, matrix products: 4.06 us -> 4.56 us  [the longest x1 4.1 us: local(): jnp.dot(jnp.concatenate((normed_all, rim_rows), axis=0), all_w[:, :2 * ff...]
  transfers between devices with their start and end apart: 10 -> 10, of which waited for: 6 -> 6; matrix products, arithmetic and copies ran while one was open for 2% -> 3% of each run, Pallas kernels for 9% -> 6%
where the time goes in v2:
time: 200 us; the launch traced here: 199 us
  blocking collectives  74.9 us (37%)
  starting transfers between devices  47.9 us (24%)
  waiting for transfers between devices  32.8 us (16%)
  between operations  14.3 us (7%)
  Pallas kernels  12.1 us (6%)
  matrix products  7.76 us (4%)
  other arithmetic  5.11 us (3%)
  local copies, waits for them, and re-layouts  4.39 us (2%)
    ppermute x7, starting transfers between devices, shifted(): lax.ppermute(value, axis, [(i, (i + steps) % count) for i in range(count)])  42.2 us
    all_to_all x2, blocking collectives, summed_over_tp(): tiles = lax.all_to_all(cut, 'tp', 0, 0, tiled=True)  36.9 us
    ppermute x7, waiting for transfers between devices, shifted(): lax.ppermute(value, axis, [(i, (i + steps) % count) for i in range(count)])  22.3 us
    all_gather x1, blocking collectives, local(): lax.all_gather(normalize(mid, norm_gain), 'tp', axis=0, tiled=True)  14.2 us
    all_gather x1, blocking collectives, local(): row_w = lax.all_gather(own_w, 'y', axis=0, tiled=True)  12.7 us
    pallas_call x1, Pallas kernels, local(): pl.pallas_call(attend_kernel, out_shape=jax.ShapeDtypeStruct((NY * rows,...  12.1 us
    all_gather x1, blocking collectives, local(): q_all = lax.all_gather(queries, 'y', axis=0, tiled=True)  11.1 us
    all_to_all x1, waiting for transfers between devices, local(): got = lax.all_to_all(parts.reshape(NY, rows, 3 * VD), 'y', 0, 0, tiled=True)  6.66 us
  transfers between devices with their start and end apart: 10, of which 6 were waited for; matrix products, arithmetic and copies ran while one was open for 3% of the time, Pallas kernels for 6%

profile of v2, /device:TPU:1, one launch (start us, length us, event | category | flops | bytes accessed | tf_op | source)
XLA Modules:
  0.0 199.3 jit_solution(5485476055614543409)
XLA Ops:
  6.5 0.0 copy-start
  6.5 0.0 all-gather.2.cloned.1.call-start
  6.5 1.0 concatenate.38
  7.5 12.7 %all_gather.14 = bf16[128,2112]{1,0:T(8,128)(2,1)} all-gather(bf16[32,2112]{1,0:T(8,128)(2,1)S(1)} %concatenate.38), channel_id=1, replica_groups=mesh['z'=16,'y'=4,'tp'=8] {'y'}, dimensions={0}, use_global_device_ids=true | all-gather | bytes 675840 | tf_op jit(solution)/shard_map/all_gather | solution.py:137
  20.2 0.0 all-gather.2.cloned.1.call-update
  20.3 0.8 constant_dynamic-update-slice_fusion.1
  21.1 0.8 constant_dynamic-update-slice_fusion.own_ref
  21.9 0.0 copy-start.1
  21.9 9.3 %collective-permute-start = (bf16[192,256]{1,0:T(8,128)(2,1)S(1)}, bf16[192,256]{1,0:T(8,128)(2,1)S(1)}, u32[]{:S(2)}, u32[]{:S(2)}) collective-permute-start(bf16[192,256]{1,0:T(8,128)(2,1)S(1)} %constant_dynamic-update-slice_fusion.own_ref), channel_id=1, source_target_pairs={{0,128},{32,160},{64,192},{96,224},{128,256},{160,288},{192,320},{... | collective-permute-start | bytes 294920 | tf_op jit(solution)/shard_map/ppermute | solution.py:27
  31.2 10.6 %collective-permute-start.1 = (bf16[192,256]{1,0:T(8,128)(2,1)S(1)}, bf16[192,256]{1,0:T(8,128)(2,1)S(1)}, u32[]{:S(2)}, u32[]{:S(2)}) collective-permute-start(bf16[192,256]{1,0:T(8,128)(2,1)S(1)} %constant_dynamic-update-slice_fusion.own_ref), channel_id=1, source_target_pairs={{0,256},{32,288},{64,320},{96,352},{128,384},{160,416},{192,448},{... | collective-permute-start | bytes 294920 | tf_op jit(solution)/shard_map/ppermute | solution.py:27
  41.8 5.2 %collective-permute-start.2 = (bf16[192,256]{1,0:T(8,128)(2,1)S(1)}, bf16[192,256]{1,0:T(8,128)(2,1)S(1)}, u32[]{:S(2)}, u32[]{:S(2)}) collective-permute-start(bf16[192,256]{1,0:T(8,128)(2,1)S(1)} %constant_dynamic-update-slice_fusion.own_ref), channel_id=1, source_target_pairs={{0,384},{32,416},{64,448},{96,480},{128,0},{160,32},{192,64},{224,... | collective-permute-start | bytes 294920 | tf_op jit(solution)/shard_map/ppermute | solution.py:27
  47.0 11.1 %all_gather.12.q_ref = bf16[768,128]{1,0:T(8,128)(2,1)} all-gather(bf16[192,128]{1,0:T(8,128)(2,1)} %param.14), channel_id=1, replica_groups=mesh['z'=16,'y'=4,'tp'=8] {'y'}, dimensions={0}, use_global_device_ids=true | all-gather | bytes 245760 | tf_op jit(solution)/shard_map/all_gather | solution.py:141
  58.1 0.0 collective-permute-done
  58.1 0.0 collective-permute-done.1
  58.1 2.4 %collective-permute-done.2 = bf16[192,256]{1,0:T(8,128)(2,1)S(1)} collective-permute-done((bf16[192,256]{1,0:T(8,128)(2,1)S(1)}, bf16[192,256]{1,0:T(8,128)(2,1)S(1)}, u32[]{:S(2)}, u32[]{:S(2)}) %collective-permute-start.2) | collective-permute-done | bytes 98336 | tf_op jit(solution)/shard_map/ppermute | solution.py:27
  60.5 0.1 pad_maximum_fusion.2
  60.5 2.9 %collective-permute-start.3 = (bf16[768,256]{1,0:T(8,128)(2,1)S(1)}, bf16[768,256]{1,0:T(8,128)(2,1)S(1)}, u32[]{:S(2)}, u32[]{:S(2)}) collective-permute-start(bf16[768,256]{1,0:T(8,128)(2,1)S(1)} %get-tuple-element.31), channel_id=1, source_target_pairs={{0,32},{32,64},{64,96},{96,128},{128,160},{160,192},{192,224},{224... | collective-permute-start | bytes 1179656 | tf_op jit(solution)/shard_map/ppermute | solution.py:27
  63.4 6.8 %collective-permute-start.6 = (bf16[768,256]{1,0:T(8,128)(2,1)S(1)}, bf16[768,256]{1,0:T(8,128)(2,1)S(1)}, u32[]{:S(2)}, u32[]{:S(2)}) collective-permute-start(bf16[768,256]{1,0:T(8,128)(2,1)S(1)} %get-tuple-element.30), channel_id=1, source_target_pairs={{0,480},{32,0},{64,32},{96,64},{128,96},{160,128},{192,160},{224,1... | collective-permute-start | bytes 1179656 | tf_op jit(solution)/shard_map/ppermute | solution.py:27
  70.3 1.9 collective-permute-start.4
  72.2 5.5 %collective-permute-start.5 = (bf16[384,256]{1,0:T(8,128)(2,1)S(1)}, bf16[384,256]{1,0:T(8,128)(2,1)S(1)}, u32[]{:S(2)}, u32[]{:S(2)}) collective-permute-start(bf16[384,256]{1,0:T(8,128)(2,1)S(1)} %get-tuple-element.33), channel_id=1, source_target_pairs={{0,448},{32,480},{64,0},{96,32},{128,64},{160,96},{192,128},{224,1... | collective-permute-start | bytes 589832 | tf_op jit(solution)/shard_map/ppermute | solution.py:27
  77.7 0.7 pad_add_fusion.where_ref
  78.4 0.7 pad_maximum_fusion.5.far_ref
  79.1 19.8 %collective-permute-done.4 = bf16[384,256]{1,0:T(8,128)(2,1)S(1)} collective-permute-done((bf16[384,256]{1,0:T(8,128)(2,1)S(1)}, bf16[384,256]{1,0:T(8,128)(2,1)S(1)}, u32[]{:S(2)}, u32[]{:S(2)}) %collective-permute-start.4) | collective-permute-done | bytes 196640 | tf_op jit(solution)/shard_map/ppermute | solution.py:27
  98.9 0.1 collective-permute-done.5
  99.0 0.8 pad_maximum_fusion.1.n2_ref
  99.8 0.0 collective-permute-done.3.n1_ref
  99.8 0.0 copy-start.3
  99.8 0.0 collective-permute-done.6.n3_ref
  99.8 0.0 copy-done.1
  99.9 0.7 copy-done.3
  100.6 0.7 copy-done.4
  101.3 12.1 %attend.1 = bf16[768,384]{1,0:T(8,128)(2,1)} custom-call(s32[2]{0:T(128)} %pad_add_fusion.where_ref, bf16[768,128]{1,0:T(8,128)(2,1)} %all_gather.12.q_ref, bf16[192,256]{1,0:T(8,128)(2,1)} %copy-done.1, bf16[576,256]{1,0:T(8,128)(2,1)} %pad_maximum_fusion.5.far_ref, bf16[768,256]{1,0:T(8,128)(2,1)} %copy-done.3, bf16[768,256]{1,0:T(8,128)(2,1)} %pad_maximum_fusion.1.n2_ref, ...), custom_call_target="tpu_custom_call" | custom-call | tf_op jit(solution)/shard_map/attend/pallas_call | solution.py:152
  113.4 3.5 %all-to-all-start = ((bf16[4,192,384]{2,1,0:T(8,128)(2,1)}), bf16[4,192,384]{2,1,0:T(8,128)(2,1)S(1)}, u32[]{:S(2)}, u32[]{:S(2)}) async-start(bf16[4,192,384]{2,1,0:T(8,128)(2,1)} %bitcast.10), calls=%async_computation | async-start | bytes 1179648 | tf_op jit(solution)/shard_map/all_to_all | solution.py:159
  117.5 6.7 %all-to-all-done = bf16[4,192,384]{2,1,0:T(8,128)(2,1)S(1)} async-done(((bf16[4,192,384]{2,1,0:T(8,128)(2,1)}), bf16[4,192,384]{2,1,0:T(8,128)(2,1)S(1)}, u32[]{:S(2)}, u32[]{:S(2)}) %all-to-all-start) | async-done | bytes 589856 | tf_op jit(solution)/shard_map/all_to_all | solution.py:159
  124.2 0.1 convert_element_type.57
  124.3 0.0 copy-start.7
  124.3 0.7 fusion.38
  125.0 0.6 fusion.15
  125.6 0.3 fusion.14
  125.8 0.0 copy-start.6
  125.9 0.1 copy.17
  126.0 0.1 copy.18
  126.1 0.1 multiply_reduce_fusion
  126.1 0.0 copy-done
  126.1 0.0 copy-done.7
  126.2 0.5 convolution_convert_fusion
  126.6 20.2 %all_to_all.15 = bf16[8,24,2048]{2,1,0:T(8,128)(2,1)S(1)} all-to-all(bf16[8,24,2048]{2,1,0:T(8,128)(2,1)S(1)} %bitcast.9), channel_id=1, replica_groups=mesh['z'=16,'y'=4,'tp'=8] {'tp'}, dimensions={0} | all-to-all | bytes 1572864 | tf_op jit(solution)/shard_map/all_to_all | solution.py:114
  146.8 0.1 reduce_sum.83
  146.9 0.0 copy-done.2
  146.9 0.1 fusion.27
  147.1 0.0 copy-done.5
  147.1 0.1 fusion.29
  147.2 14.2 %all_gather.13 = bf16[192,2048]{1,0:T(8,128)(2,1)S(1)} all-gather(bf16[24,2048]{1,0:T(8,128)(2,1)S(1)} %fusion.29), channel_id=1, replica_groups=mesh['z'=16,'y'=4,'tp'=8] {'tp'}, dimensions={0}, use_global_device_ids=true | all-gather | bytes 884736 | tf_op jit(solution)/shard_map/all_gather | solution.py:168
  161.4 2.2 %collective-permute-start.7 = (bf16[8,2048]{1,0:T(8,128)(2,1)S(1)}, bf16[8,2048]{1,0:T(8,128)(2,1)S(1)}, u32[]{:S(2)}, u32[]{:S(2)}) collective-permute-start(bf16[8,2048]{1,0:T(8,128)(2,1)S(1)} %slice.96), channel_id=1, source_target_pairs={{0,8},{8,16},{16,24},{24,32},{32,40},{40,48},{48,56},{56,64},{64,7... | collective-permute-start | bytes 98312 | tf_op jit(solution)/shard_map/ppermute | solution.py:170
  163.6 0.0 copy-done.6
  163.7 0.0 copy-start.8
  163.7 0.9 collective-permute-done.7
  164.6 2.9 %all-gather.2.cloned.1.call-done = bf16[2048,2112]{1,0:T(8,128)(2,1)} async-done(((bf16[128,2112]{1,0:T(8,128)(2,1)}), bf16[2048,2112]{1,0:T(8,128)(2,1)}) %all-gather.2.cloned.1.call-update) | async-done | bytes 8650768 | tf_op jit(solution)/shard_map/all_gather | solution.py:138
  167.5 4.1 %fusion.4 = bf16[200,1408]{1,0:T(8,128)(2,1)S(1)} fusion(bf16[2048,2112]{1,0:T(8,128)(2,1)} %all-gather.2.cloned.1.call-done, bf16[8,2048]{1,0:T(8,128)(2,1)S(1)} %collective-permute-done.7, bf16[192,2048]{1,0:T(8,128)(2,1)S(1)} %all_gather.13), kind=kOutput, calls=%fused_computation.4 | convolution fusion | flops 1155353600 | bytes 7149568 | tf_op jit(solution)/shard_map/dot_general | solution.py:171
  171.7 0.0 copy-done.8
  171.7 3.2 %fusion.7 = bf16[192,2048]{1,0:T(8,128)(2,1)S(1)} fusion(bf16[2048,2112]{1,0:T(8,128)(2,1)} %all-gather.2.cloned.1.call-done, bf16[192,704]{1,0:T(8,128)(2,1)S(1)} %slice.99, bf16[2,704]{1,0:T(2,128)(2,1)S(1)} %slice.98, bf16[200,1408]{1,0:T(8,128)(2,1)S(1)} %fusion.4, f32[704]{0:T(1024)S(1)} %get-tuple-element.20, f32[704]{0:T(1024)S(1)} %get-tuple-element.21, ...), kind=kOutput, calls=%fused_computation.5 | convolution fusion | flops 557015040 | bytes 4541440 | tf_op jit(solution)/shard_map/dot_general | solution.py:31
  174.9 16.7 %all_to_all.16 = bf16[8,24,2048]{2,1,0:T(8,128)(2,1)S(1)} all-to-all(bf16[8,24,2048]{2,1,0:T(8,128)(2,1)S(1)} %bitcast.11), channel_id=1, replica_groups=mesh['z'=16,'y'=4,'tp'=8] {'tp'}, dimensions={0} | all-to-all | bytes 1572864 | tf_op jit(solution)/shard_map/all_to_all | solution.py:114
  191.6 0.1 reduce_sum.85
  191.7 0.7 fusion.30
  (10 shorter events, 0.1 us)
Async XLA Ops:
  6.5 119.6 %copy-start = (bf16[128,2048]{1,0:T(8,128)(2,1)S(1)}, bf16[128,2048]{1,0:T(8,128)(2,1)}, u32[]{:S(2)}) copy-start(bf16[128,2048]{1,0:T(8,128)(2,1)} %param.19) | copy-start | bytes 1572868
  6.5 161.0 %all-gather.2.cloned.1.call-start = ((), (), s32[]{:S(2)}) async-start(), calls=%async_computation.3 | async-start | bytes 9469952 | tf_op jit(solution)/shard_map/all_gather | solution.py:138
  21.9 78.0 %copy-start.1 = (bf16[192,256]{1,0:T(8,128)(2,1)}, bf16[192,256]{1,0:T(8,128)(2,1)S(1)}, u32[]{:S(2)}) copy-start(bf16[192,256]{1,0:T(8,128)(2,1)S(1)} %constant_dynamic-update-slice_fusion.own_ref) | copy-start | bytes 294916
  21.9 36.2 %collective-permute-start = (bf16[192,256]{1,0:T(8,128)(2,1)S(1)}, bf16[192,256]{1,0:T(8,128)(2,1)S(1)}, u32[]{:S(2)}, u32[]{:S(2)}) collective-permute-start(bf16[192,256]{1,0:T(8,128)(2,1)S(1)} %constant_dynamic-update-slice_fusion.own_ref), channel_id=1, source_target_pairs={{0,128},{32,160},{64,192},{96,224},{128,256},{160,288},{192,320},{... | collective-permute-start | bytes 294920 | tf_op jit(solution)/shard_map/ppermute | solution.py:27
  31.2 26.9 %collective-permute-start.1 = (bf16[192,256]{1,0:T(8,128)(2,1)S(1)}, bf16[192,256]{1,0:T(8,128)(2,1)S(1)}, u32[]{:S(2)}, u32[]{:S(2)}) collective-permute-start(bf16[192,256]{1,0:T(8,128)(2,1)S(1)} %constant_dynamic-update-slice_fusion.own_ref), channel_id=1, source_target_pairs={{0,256},{32,288},{64,320},{96,352},{128,384},{160,416},{192,448},{... | collective-permute-start | bytes 294920 | tf_op jit(solution)/shard_map/ppermute | solution.py:27
  41.8 18.6 %collective-permute-start.2 = (bf16[192,256]{1,0:T(8,128)(2,1)S(1)}, bf16[192,256]{1,0:T(8,128)(2,1)S(1)}, u32[]{:S(2)}, u32[]{:S(2)}) collective-permute-start(bf16[192,256]{1,0:T(8,128)(2,1)S(1)} %constant_dynamic-update-slice_fusion.own_ref), channel_id=1, source_target_pairs={{0,384},{32,416},{64,448},{96,480},{128,0},{160,32},{192,64},{224,... | collective-permute-start | bytes 294920 | tf_op jit(solution)/shard_map/ppermute | solution.py:27
  60.5 39.3 %collective-permute-start.3 = (bf16[768,256]{1,0:T(8,128)(2,1)S(1)}, bf16[768,256]{1,0:T(8,128)(2,1)S(1)}, u32[]{:S(2)}, u32[]{:S(2)}) collective-permute-start(bf16[768,256]{1,0:T(8,128)(2,1)S(1)} %get-tuple-element.31), channel_id=1, source_target_pairs={{0,32},{32,64},{64,96},{96,128},{128,160},{160,192},{192,224},{224... | collective-permute-start | bytes 1179656 | tf_op jit(solution)/shard_map/ppermute | solution.py:27
  63.4 36.4 %collective-permute-start.6 = (bf16[768,256]{1,0:T(8,128)(2,1)S(1)}, bf16[768,256]{1,0:T(8,128)(2,1)S(1)}, u32[]{:S(2)}, u32[]{:S(2)}) collective-permute-start(bf16[768,256]{1,0:T(8,128)(2,1)S(1)} %get-tuple-element.30), channel_id=1, source_target_pairs={{0,480},{32,0},{64,32},{96,64},{128,96},{160,128},{192,160},{224,1... | collective-permute-start | bytes 1179656 | tf_op jit(solution)/shard_map/ppermute | solution.py:27
  70.3 28.6 %collective-permute-start.4 = (bf16[384,256]{1,0:T(8,128)(2,1)S(1)}, bf16[384,256]{1,0:T(8,128)(2,1)S(1)}, u32[]{:S(2)}, u32[]{:S(2)}) collective-permute-start(bf16[384,256]{1,0:T(8,128)(2,1)S(1)} %get-tuple-element.32), channel_id=1, source_target_pairs={{0,64},{32,96},{64,128},{96,160},{128,192},{160,224},{192,256},{22... | collective-permute-start | bytes 589832 | tf_op jit(solution)/shard_map/ppermute | solution.py:27
  72.2 26.8 %collective-permute-start.5 = (bf16[384,256]{1,0:T(8,128)(2,1)S(1)}, bf16[384,256]{1,0:T(8,128)(2,1)S(1)}, u32[]{:S(2)}, u32[]{:S(2)}) collective-permute-start(bf16[384,256]{1,0:T(8,128)(2,1)S(1)} %get-tuple-element.33), channel_id=1, source_target_pairs={{0,448},{32,480},{64,0},{96,32},{128,64},{160,96},{192,128},{224,1... | collective-permute-start | bytes 589832 | tf_op jit(solution)/shard_map/ppermute | solution.py:27
  99.8 0.7 copy-start.3
  100.6 0.7 copy-start.4
  113.4 10.8 %all-to-all-start = ((bf16[4,192,384]{2,1,0:T(8,128)(2,1)}), bf16[4,192,384]{2,1,0:T(8,128)(2,1)S(1)}, u32[]{:S(2)}, u32[]{:S(2)}) async-start(bf16[4,192,384]{2,1,0:T(8,128)(2,1)} %bitcast.10), calls=%async_computation | async-start | bytes 1179648 | tf_op jit(solution)/shard_map/all_to_all | solution.py:159
  124.3 1.9 copy-start.7
  125.0 21.9 %copy-start.2 = (bf16[24,2048]{1,0:T(8,128)(2,1)S(1)}, bf16[24,2048]{1,0:T(8,128)(2,1)}, u32[]{:S(2)}) copy-start(bf16[24,2048]{1,0:T(8,128)(2,1)} %param.13) | copy-start | bytes 294916
  125.6 21.5 %copy-start.5 = (f32[2048]{0:T(1024)S(1)}, f32[2048]{0:T(1024)}, u32[]{:S(2)}) copy-start(f32[2048]{0:T(1024)} %param.20) | copy-start | bytes 24580
  125.8 37.8 %copy-start.6 = (f32[3,704]{1,0:T(4,128)S(1)}, f32[3,704]{1,0:T(4,128)}, u32[]{:S(2)}) copy-start(f32[3,704]{1,0:T(4,128)} %param.23) | copy-start | bytes 25348
  161.4 3.2 %collective-permute-start.7 = (bf16[8,2048]{1,0:T(8,128)(2,1)S(1)}, bf16[8,2048]{1,0:T(8,128)(2,1)S(1)}, u32[]{:S(2)}, u32[]{:S(2)}) collective-permute-start(bf16[8,2048]{1,0:T(8,128)(2,1)S(1)} %slice.96), channel_id=1, source_target_pairs={{0,8},{8,16},{16,24},{24,32},{32,40},{40,48},{48,56},{56,64},{64,7... | collective-permute-start | bytes 98312 | tf_op jit(solution)/shard_map/ppermute | solution.py:170
  163.7 8.0 %copy-start.8 = (f32[704]{0:T(1024)S(1)}, f32[704]{0:T(1024)}, u32[]{:S(2)}) copy-start(f32[704]{0:T(1024)} %param.24) | copy-start | bytes 8452
Sparse Core Ops, SparseCore 0:
  20.4 147.0 all-gather.1

commit v3 on v2

--- a/solution.py
+++ b/solution.py
@@ -8,10 +8,12 @@
 
 HD = 64
 VD = 128
-SP = ("z", "y")
-SP_TP = ("z", "y", "tp")
-NZ = 16
+SP = ("z", "yh", "yl")
+TP = ("x", "c")
+Y = ("yh", "yl")
+SHARDS = ("x", "yl")
 NY = 4
+LANES = 128
 eps = 1e-05
 neg_fill = -1e30
 TILE = 128
@@ -25,6 +27,10 @@
 def shifted(value, axis, steps):
     count = lax.axis_size(axis)
     return lax.ppermute(value, axis, [(i, (i + steps) % count) for i in range(count)])
+
+
+def swapped(value):
+    return lax.ppermute(value, ("yl", "c"), [(0, 0), (1, 2), (2, 1), (3, 3)])
 
 
 def dot_nt(a, b):
@@ -108,10 +114,10 @@
     return (values_f * scale_inv * gain).astype(jnp.bfloat16)
 
 
-def summed_over_tp(shard):
-    count = lax.axis_size("tp")
+def summed_over_shards(shard):
+    count = lax.axis_size(SHARDS)
     cut = shard.reshape(count, shard.shape[0] // count, shard.shape[1])
-    tiles = lax.all_to_all(cut, "tp", 0, 0, tiled=True)
+    tiles = lax.all_to_all(cut, SHARDS, 0, 0, tiled=True)
     return jnp.sum(tiles.astype(jnp.float32), axis=0).astype(jnp.bfloat16)
 
 
@@ -132,16 +138,37 @@
 ):
     rows = queries.shape[0]
     ff = up_weight.shape[1]
-    where = jnp.stack((lax.axis_index("z"), lax.axis_index("y"))).astype(jnp.int32)
-    own_w = jnp.concatenate((up_weight, gate_weight, down_weight.T), axis=1)
-    row_w = lax.all_gather(own_w, "y", axis=0, tiled=True)
-    all_w = lax.all_gather(row_w, "z", axis=0, tiled=True)
+    half = ff // 2
+    core = lax.axis_index("c")
+    pair = lax.axis_index("yl")
+    y_index = lax.axis_index("yh") * 2 + pair
+    where = jnp.stack((lax.axis_index("z"), y_index)).astype(jnp.int32)
+
+    down_t = down_weight.T
+    gap = -2 * half % LANES
+    width = 2 * half + gap + half
+    tail = -width % LANES
+    cuts = []
+    for h in range(2):
+        units = slice(h * half, (h + 1) * half)
+        cuts += [up_weight[:, units], gate_weight[:, units]]
+        cuts += [jnp.zeros((up_weight.shape[0], gap), jnp.bfloat16), down_t[:, units]]
+        cuts += [jnp.zeros((up_weight.shape[0], tail), jnp.bfloat16)]
+    row_w = lax.all_gather(jnp.concatenate(cuts, axis=1), Y, axis=0, tiled=True)
+    low, high = row_w[:, : width + tail], row_w[:, width + tail :]
+    for_peer = lax.ppermute(jnp.where(core == 0, high, low), ("yl", "c"), [(0, 1), (3, 2)])
+    kept = jnp.where(core == pair, jnp.where(core == 0, low, high), for_peer)
+    mine = lax.all_gather(kept, "z", axis=0, tiled=True)
 
     kv = jnp.concatenate((key_pairs, values), axis=1)
-    q_all = lax.all_gather(queries, "y", axis=0, tiled=True)
+    q_all = lax.all_gather(queries, Y, axis=0, tiled=True)
     f4, f8, f12 = (shifted(kv, "z", s) for s in (4, 8, -4))
-    f4, f8, f12, q_all = lax.optimization_barrier((f4, f8, f12, q_all))
     held = jnp.concatenate((kv, f4, f8, f12), axis=0)
+    conv = jnp.concatenate((conv_weight, conv_bias[None, :]), axis=0)
+    held, out_weight, residual, conv = lax.optimization_barrier(
+        (held, out_weight, residual, conv)
+    )
+    out_weight, residual, conv = swapped(out_weight), swapped(residual), swapped(conv)
     n1 = shifted(held, "z", 1)
     n2a = shifted(held[: 2 * rows], "z", 2)
     back = jnp.concatenate((f12, kv), axis=0)
@@ -156,53 +183,64 @@
         out_specs=VMEM,
         name="attend",
     )(where, q_all, kv, far, n1, n2, n3)
-    got = lax.all_to_all(parts.reshape(NY, rows, 3 * VD), "y", 0, 0, tiled=True)
+    got = lax.all_to_all(parts.reshape(NY, rows, 3 * VD), Y, 0, 0, tiled=True)
     means = merged(got)
     diff = means[0] - second_weight[0] * means[1]
     scale_inv = lax.rsqrt(jnp.mean(diff * diff, axis=-1, keepdims=True) + eps)
-    attended = (diff * scale_inv * head_gain * 0.8).astype(jnp.bfloat16)
-    proj = summed_over_tp(
+    attended = swapped((diff * scale_inv * head_gain * 0.8).astype(jnp.bfloat16))
+    proj = summed_over_shards(
         jnp.dot(attended, out_weight, preferred_element_type=jnp.float32).astype(jnp.bfloat16)
     )
     mid = (residual.astype(jnp.float32) + proj.astype(jnp.float32)).astype(jnp.bfloat16)
-    normed_all = lax.all_gather(normalize(mid, norm_gain), "tp", axis=0, tiled=True)
-    count = lax.axis_size("z") * lax.axis_size("y")
-    rim_rows = lax.ppermute(normed_all[rows - 8 :], SP, [(i, i + 1) for i in range(count - 1)])
-    both = jnp.dot(
-        jnp.concatenate((normed_all, rim_rows), axis=0),
-        all_w[:, : 2 * ff],
-        preferred_element_type=jnp.float32,
-    ).astype(jnp.bfloat16)
-    up_proj, gate_proj = both[:rows, :ff], both[:rows, ff:]
+    normed = normalize(mid, norm_gain)
+    mine, _ = lax.optimization_barrier((mine, normed))
+    other = lax.ppermute(mine, "c", [(0, 1), (1, 0)])
+    normed_all = lax.all_gather(normed, SHARDS, axis=0, tiled=True)
+    tokens = ("z", "yh", "c")
+    count = lax.axis_size(tokens)
+    rim_rows = lax.ppermute(normed_all[rows - 8 :], tokens, [(i, i + 1) for i in range(count - 1)])
+    normed_ext = jnp.concatenate((normed_all, rim_rows), axis=0)
     taps = conv_weight.shape[0]
-    extended = jnp.concatenate((both[rows + 8 - (taps - 1) :, :ff], up_proj), axis=0)
-    conv_out = jnp.zeros((rows, ff), jnp.float32) + conv_bias[None, :]
-    for tap in range(taps):
-        conv_out = conv_out + conv_weight[tap][None, :] * extended[tap : tap + rows].astype(
-            jnp.float32
-        )
-    hidden = (jax.nn.silu(conv_out) * gate_proj.astype(jnp.float32)).astype(jnp.bfloat16)
-    ffn = dot_nt(hidden, all_w[:, 2 * ff :]).astype(jnp.bfloat16)
-    ffn_out = summed_over_tp(ffn)
-    return (mid.astype(jnp.float32) + ffn_out.astype(jnp.float32)).astype(jnp.bfloat16)
+    first, second = conv[:, :half], conv[:, half:]
+    ffn = jnp.zeros((), jnp.float32)
+    for w, units in (
+        (mine, jnp.where(core == 0, first, second)),
+        (other, jnp.where(core == 0, second, first)),
+    ):
+        both = jnp.dot(
+            normed_ext, w[:, : 2 * half + gap], preferred_element_type=jnp.float32
+        ).astype(jnp.bfloat16)
+        up_proj, gate_proj = both[:rows, :half], both[:rows, half : 2 * half]
+        extended = jnp.concatenate((both[rows + 8 - (taps - 1) :, :half], up_proj), axis=0)
+        conv_out = jnp.zeros((rows, half), jnp.float32) + units[taps][None, :]
+        for tap in range(taps):
+            conv_out = conv_out + units[tap][None, :] * extended[tap : tap + rows].astype(
+                jnp.float32
+            )
+        hidden = (jax.nn.silu(conv_out) * gate_proj.astype(jnp.float32)).astype(jnp.bfloat16)
+        ffn = ffn + dot_nt(hidden, w[:, 2 * half + gap : width])
+    ffn_out = summed_over_shards(ffn.astype(jnp.bfloat16))
+    return swapped((mid.astype(jnp.float32) + ffn_out.astype(jnp.float32)).astype(jnp.bfloat16))
 
 
 def solution(mesh):
-    finer = Mesh(mesh.devices.reshape(NZ, NY, mesh.shape["tp"]), ("z", "y", "tp"))
+    z = mesh.shape["sp"] // NY
+    shape = (z, 2, 2, mesh.shape["tp"] // 2, 2)
+    finer = Mesh(mesh.devices.reshape(shape), ("z", "yh", "yl", "x", "c"))
     in_specs = (
-        P(SP_TP, None),
-        P(SP, "tp"),
-        P(SP, "tp"),
-        P(SP, "tp"),
-        P("tp"),
-        P("tp"),
-        P("tp", None),
+        P(SP + TP, None),
+        P(SP, TP),
+        P(SP, TP),
+        P(SP, TP),
+        P(TP),
+        P(TP),
+        P(TP, None),
         P(),
-        P(SP, "tp"),
-        P(SP, "tp"),
-        P(None, "tp"),
-        P("tp"),
-        P("tp", SP),
+        P(SP, TP),
+        P(SP, TP),
+        P(None, TP),
+        P(TP),
+        P(TP, SP),
     )
-    out_specs = P(SP_TP, None)
+    out_specs = P(SP + TP, None)
     return jax.shard_map(local, mesh=finer, in_specs=in_specs, out_specs=out_specs, check_vma=False)

time: 200 us -> 236 us (1.18)
  starting transfers between devices: 47.9 us -> 81.4 us
  waiting for transfers between devices: 32.8 us -> 45.5 us
  blocking collectives: 74.9 us -> 63 us
    ppermute x1 -> x8, starting transfers between devices: 2.18 us -> 35.5 us  [the longest x5 24.9 us: swapped(): return lax.ppermute(value, ('yl', 'c'), [(0, 0), (1, 2), (2, 1), (3, 3)])]
    all_to_all x2 -> x1, blocking collectives: 36.9 us -> 14.9 us  [summed_over_shards(): tiles = lax.all_to_all(cut, SHARDS, 0, 0, tiled=True)]
    ppermute x1 -> x8, waiting for transfers between devices: 0.94 us -> 20.6 us  [the longest x5 10.2 us: swapped(): return lax.ppermute(value, ('yl', 'c'), [(0, 0), (1, 2), (2, 1), (3, 3)])]
    all_gather x3, blocking collectives: 38 us -> 48.1 us  [the longest x1 25.1 us: local(): normed_all = lax.all_gather(normed, SHARDS, axis=0, tiled=True)]
    all_to_all x1 -> x2, starting transfers between devices: 3.48 us -> 8.39 us  [the longest x1 4.42 us: local(): got = lax.all_to_all(parts.reshape(NY, rows, 3 * VD), Y, 0, 0, tiled=True)]
    ppermute x7, starting transfers between devices: 42.2 us -> 37.5 us  [shifted(): lax.ppermute(value, axis, [(i, (i + steps) % count) for i in range(count)])]
    all_gather x1, waiting for transfers between devices: 2.91 us -> 0.02 us  [local(): mine = lax.all_gather(kept, 'z', axis=0, tiled=True)]
    ppermute x7, waiting for transfers between devices: 22.3 us -> 19.7 us  [shifted(): lax.ppermute(value, axis, [(i, (i + steps) % count) for i in range(count)])]
  transfers between devices with their start and end apart: 10 -> 18, of which waited for: 6 -> 11; matrix products, arithmetic and copies ran while one was open for 3% -> 5% of each run, Pallas kernels for 6% -> 5%
where the time goes in v3:
time: 236 us; the launch traced here: 234 us
  starting transfers between devices  81.4 us (34%)
  blocking collectives  63 us (27%)
  waiting for transfers between devices  45.5 us (19%)
  between operations  14.6 us (6%)
  Pallas kernels  12 us (5%)
  matrix products  7.81 us (3%)
  local copies, waits for them, and re-layouts  5.27 us (2%)
  other arithmetic  4.65 us (2%)
    ppermute x7, starting transfers between devices, shifted(): lax.ppermute(value, axis, [(i, (i + steps) % count) for i in range(count)])  37.5 us
    all_gather x1, blocking collectives, local(): normed_all = lax.all_gather(normed, SHARDS, axis=0, tiled=True)  25.1 us
    ppermute x5, starting transfers between devices, swapped(): return lax.ppermute(value, ('yl', 'c'), [(0, 0), (1, 2), (2, 1), (3, 3)])  24.9 us
    ppermute x7, waiting for transfers between devices, shifted(): lax.ppermute(value, axis, [(i, (i + steps) % count) for i in range(count)])  19.7 us
    all_to_all x1, blocking collectives, summed_over_shards(): tiles = lax.all_to_all(cut, SHARDS, 0, 0, tiled=True)  14.9 us
    pallas_call x1, Pallas kernels, local(): pl.pallas_call(attend_kernel, out_shape=jax.ShapeDtypeStruct((NY * rows,...  12 us
    all_gather x1, blocking collectives, local(): q_all = lax.all_gather(queries, Y, axis=0, tiled=True)  11.6 us
    all_gather x1, blocking collectives, local(): row_w = lax.all_gather(jnp.concatenate(cuts, axis=1), Y, axis=0, tiled=True)  11.4 us
  transfers between devices with their start and end apart: 18, of which 11 were waited for; matrix products, arithmetic and copies ran while one was open for 5% of the time, Pallas kernels for 5%

profile of v3, /device:TPU:1, one launch (start us, length us, event | category | flops | bytes accessed | tf_op | source)
XLA Modules:
  0.0 234.3 jit_solution(12577169003687458776)
XLA Ops:
  6.5 0.0 all-gather.2.cloned.1.call-start
  6.6 0.9 fusion.48
  7.5 0.9 fusion.46
  8.4 0.1 concatenate.37
  8.6 11.4 %all_gather.14 = bf16[128,2304]{1,0:T(8,128)(2,1)S(1)} all-gather(bf16[32,2304]{1,0:T(8,128)(2,1)S(1)} %concatenate.37), channel_id=1, replica_groups=mesh['z'=16,'yh'=2,'yl'=2,'x'=4,'c'=2] {'yh','yl'}, dimensions={0}, use_global_device_ids=true | all-gather | bytes 737280 | tf_op jit(solution)/shard_map/all_gather | solution.py:157
  20.0 1.3 collective-permute-start.12
  21.3 9.4 %collective-permute-done.12 = bf16[128,1152]{1,0:T(8,128)(2,1)S(1)} collective-permute-done((bf16[128,1152]{1,0:T(8,128)(2,1)S(1)}, bf16[128,1152]{1,0:T(8,128)(2,1)S(1)}, u32[]{:S(2)}, u32[]{:S(2)}) %collective-permute-start.12) | collective-permute-done | bytes 294944 | tf_op jit(solution)/shard_map/ppermute | solution.py:159
  30.7 0.8 select_select_fusion
  31.6 7.6 %collective-permute-start.2 = (bf16[192,256]{1,0:T(8,128)(2,1)S(1)}, bf16[192,256]{1,0:T(8,128)(2,1)S(1)}, u32[]{:S(2)}, u32[]{:S(2)}) collective-permute-start(bf16[192,256]{1,0:T(8,128)(2,1)S(1)} %constant_dynamic-update-slice_fusion.own_ref), channel_id=1, source_target_pairs={{0,384},{32,416},{64,448},{96,480},{128,0},{160,32},{192,64},{224,... | collective-permute-start | bytes 294920 | tf_op jit(solution)/shard_map/ppermute | solution.py:29
  39.2 4.9 %collective-permute-start.1 = (bf16[192,256]{1,0:T(8,128)(2,1)S(1)}, bf16[192,256]{1,0:T(8,128)(2,1)S(1)}, u32[]{:S(2)}, u32[]{:S(2)}) collective-permute-start(bf16[192,256]{1,0:T(8,128)(2,1)S(1)} %constant_dynamic-update-slice_fusion.own_ref), channel_id=1, source_target_pairs={{0,256},{32,288},{64,320},{96,352},{128,384},{160,416},{192,448},{... | collective-permute-start | bytes 294920 | tf_op jit(solution)/shard_map/ppermute | solution.py:29
  44.1 7.3 %collective-permute-start = (bf16[192,256]{1,0:T(8,128)(2,1)S(1)}, bf16[192,256]{1,0:T(8,128)(2,1)S(1)}, u32[]{:S(2)}, u32[]{:S(2)}) collective-permute-start(bf16[192,256]{1,0:T(8,128)(2,1)S(1)} %constant_dynamic-update-slice_fusion.own_ref), channel_id=1, source_target_pairs={{0,128},{32,160},{64,192},{96,224},{128,256},{160,288},{192,320},{... | collective-permute-start | bytes 294920 | tf_op jit(solution)/shard_map/ppermute | solution.py:29
  51.5 2.5 %collective-permute-done.1 = bf16[192,256]{1,0:T(8,128)(2,1)S(1)} collective-permute-done((bf16[192,256]{1,0:T(8,128)(2,1)S(1)}, bf16[192,256]{1,0:T(8,128)(2,1)S(1)}, u32[]{:S(2)}, u32[]{:S(2)}) %collective-permute-start.1) | collective-permute-done | bytes 98336 | tf_op jit(solution)/shard_map/ppermute | solution.py:29
  54.0 8.5 %collective-permute-done = bf16[192,256]{1,0:T(8,128)(2,1)S(1)} collective-permute-done((bf16[192,256]{1,0:T(8,128)(2,1)S(1)}, bf16[192,256]{1,0:T(8,128)(2,1)S(1)}, u32[]{:S(2)}, u32[]{:S(2)}) %collective-permute-start) | collective-permute-done | bytes 98336 | tf_op jit(solution)/shard_map/ppermute | solution.py:29
  62.4 0.1 pad_maximum_fusion.2
  62.5 6.0 %collective-permute-start.4 = (bf16[768,256]{1,0:T(8,128)(2,1)S(1)}, bf16[768,256]{1,0:T(8,128)(2,1)S(1)}, u32[]{:S(2)}, u32[]{:S(2)}) collective-permute-start(bf16[768,256]{1,0:T(8,128)(2,1)S(1)} %get-tuple-element.11), channel_id=1, source_target_pairs={{0,32},{32,64},{64,96},{96,128},{128,160},{160,192},{192,224},{224... | collective-permute-start | bytes 1179656 | tf_op jit(solution)/shard_map/ppermute | solution.py:29
  68.6 5.5 %collective-permute-start.7 = (bf16[768,256]{1,0:T(8,128)(2,1)S(1)}, bf16[768,256]{1,0:T(8,128)(2,1)S(1)}, u32[]{:S(2)}, u32[]{:S(2)}) collective-permute-start(bf16[768,256]{1,0:T(8,128)(2,1)S(1)} %get-tuple-element.37), channel_id=1, source_target_pairs={{0,480},{32,0},{64,32},{96,64},{128,96},{160,128},{192,160},{224,1... | collective-permute-start | bytes 1179656 | tf_op jit(solution)/shard_map/ppermute | solution.py:29
  74.0 3.1 %collective-permute-start.6 = (bf16[384,256]{1,0:T(8,128)(2,1)S(1)}, bf16[384,256]{1,0:T(8,128)(2,1)S(1)}, u32[]{:S(2)}, u32[]{:S(2)}) collective-permute-start(bf16[384,256]{1,0:T(8,128)(2,1)S(1)} %pad_maximum_fusion.3), channel_id=1, source_target_pairs={{0,448},{32,480},{64,0},{96,32},{128,64},{160,96},{192,128},{224,1... | collective-permute-start | bytes 589832 | tf_op jit(solution)/shard_map/ppermute | solution.py:29
  77.1 3.1 %collective-permute-start.5 = (bf16[384,256]{1,0:T(8,128)(2,1)S(1)}, bf16[384,256]{1,0:T(8,128)(2,1)S(1)}, u32[]{:S(2)}, u32[]{:S(2)}) collective-permute-start(bf16[384,256]{1,0:T(8,128)(2,1)S(1)} %slice.138), channel_id=1, source_target_pairs={{0,64},{32,96},{64,128},{96,160},{128,192},{160,224},{192,256},{22... | collective-permute-start | bytes 589832 | tf_op jit(solution)/shard_map/ppermute | solution.py:29
  80.3 11.6 %all_gather.12.q_ref = bf16[768,128]{1,0:T(8,128)(2,1)} all-gather(bf16[192,128]{1,0:T(8,128)(2,1)S(1)} %copy-done.5), channel_id=1, replica_groups=mesh['z'=16,'yh'=2,'yl'=2,'x'=4,'c'=2] {'yh','yl'}, dimensions={0}, use_global_device_ids=true | all-gather | bytes 245760 | tf_op jit(solution)/shard_map/all_gather | solution.py:164
  91.9 0.6 pad_add_fusion.where_ref
  92.5 0.7 slice.137.far_ref
  93.3 8.4 %collective-permute-done.6 = bf16[384,256]{1,0:T(8,128)(2,1)S(1)} collective-permute-done((bf16[384,256]{1,0:T(8,128)(2,1)S(1)}, bf16[384,256]{1,0:T(8,128)(2,1)S(1)}, u32[]{:S(2)}, u32[]{:S(2)}) %collective-permute-start.6) | collective-permute-done | bytes 196640 | tf_op jit(solution)/shard_map/ppermute | solution.py:29
  101.7 0.2 collective-permute-done.5
  102.0 0.8 pad_maximum_fusion.1.n2_ref
  102.8 0.7 copy-done.1
  103.5 0.7 copy-done.2
  104.3 12.0 %attend.1 = bf16[768,384]{1,0:T(8,128)(2,1)} custom-call(s32[2]{0:T(128)} %pad_add_fusion.where_ref, bf16[768,128]{1,0:T(8,128)(2,1)} %all_gather.12.q_ref, bf16[192,256]{1,0:T(8,128)(2,1)} %copy-done, bf16[576,256]{1,0:T(8,128)(2,1)} %slice.137.far_ref, bf16[768,256]{1,0:T(8,128)(2,1)} %copy-done.1, bf16[768,256]{1,0:T(8,128)(2,1)} %pad_maximum_fusion.1.n2_ref, ...), custom_call_target="tpu_custom_call" | custom-call | tf_op jit(solution)/shard_map/attend/pallas_call | solution.py:179
  116.3 4.4 %all-to-all-start = ((bf16[4,192,384]{2,1,0:T(8,128)(2,1)}), bf16[4,192,384]{2,1,0:T(8,128)(2,1)S(1)}, u32[]{:S(2)}, u32[]{:S(2)}) async-start(bf16[4,192,384]{2,1,0:T(8,128)(2,1)} %bitcast.12), calls=%async_computation | async-start | bytes 1179648 | tf_op jit(solution)/shard_map/all_to_all | solution.py:186
  121.4 8.0 %collective-permute-start.9 = (bf16[128,2048]{1,0:T(8,128)(2,1)S(1)}, bf16[128,2048]{1,0:T(8,128)(2,1)S(1)}, u32[]{:S(2)}, u32[]{:S(2)}) collective-permute-start(bf16[128,2048]{1,0:T(8,128)(2,1)S(1)} %copy-done.10), channel_id=1, source_target_pairs={{0,0},{1,8},{8,1},{9,9},{2,2},{3,10},{10,3},{11,11},{4,4},{5,12},{... | collective-permute-start | bytes 1572872 | tf_op jit(solution)/shard_map/ppermute | solution.py:33
  129.4 0.1 convert_element_type.75
  129.5 0.7 fusion.44
  130.2 0.6 fusion.16
  130.8 0.3 fusion.15
  131.0 0.1 copy.18
  131.1 0.1 copy.17
  131.2 0.1 multiply_reduce_fusion
  131.3 0.1 multiply_convert_fusion.4
  131.4 6.3 %collective-permute-start.8 = (bf16[192,128]{0,1:T(8,128)(2,1)S(1)}, bf16[192,128]{0,1:T(8,128)(2,1)S(1)}, u32[]{:S(2)}, u32[]{:S(2)}) collective-permute-start(bf16[192,128]{0,1:T(8,128)(2,1)S(1)} %multiply_convert_fusion.4), channel_id=1, source_target_pairs={{0,0},{1,8},{8,1},{9,9},{2,2},{3,10},{10,3},{11,11},{4,4},{5,12},{... | collective-permute-start | bytes 147464 | tf_op jit(solution)/shard_map/ppermute | solution.py:33
  137.7 1.9 collective-permute-done.8
  139.6 1.3 convolution_convert_fusion
  140.9 4.0 %all-to-all-start.1 = ((bf16[8,24,2048]{2,1,0:T(8,128)(2,1)}), bf16[8,24,2048]{2,1,0:T(8,128)(2,1)S(1)}, u32[]{:S(2)}, u32[]{:S(2)}) async-start(bf16[8,24,2048]{2,1,0:T(8,128)(2,1)} %bitcast.4), calls=%async_computation.1 | async-start | bytes 1572864 | tf_op jit(solution)/shard_map/all_to_all | solution.py:120
  144.9 5.4 %collective-permute-start.3 = (bf16[24,2048]{1,0:T(8,128)(2,1)S(1)}, bf16[24,2048]{1,0:T(8,128)(2,1)S(1)}, u32[]{:S(2)}, u32[]{:S(2)}) collective-permute-start(bf16[24,2048]{1,0:T(8,128)(2,1)S(1)} %copy-done.11), channel_id=1, source_target_pairs={{0,0},{1,8},{8,1},{9,9},{2,2},{3,10},{10,3},{11,11},{4,4},{5,12},{... | collective-permute-start | bytes 294920 | tf_op jit(solution)/shard_map/ppermute | solution.py:33
  150.3 5.2 %all-to-all-done.1 = bf16[8,24,2048]{2,1,0:T(8,128)(2,1)S(1)} async-done(((bf16[8,24,2048]{2,1,0:T(8,128)(2,1)}), bf16[8,24,2048]{2,1,0:T(8,128)(2,1)S(1)}, u32[]{:S(2)}, u32[]{:S(2)}) %all-to-all-start.1) | async-done | bytes 786464 | tf_op jit(solution)/shard_map/all_to_all | solution.py:120
  155.5 0.1 reduce_sum.83
  155.6 2.6 %collective-permute-done.3 = bf16[24,2048]{1,0:T(8,128)(2,1)S(1)} collective-permute-done((bf16[24,2048]{1,0:T(8,128)(2,1)S(1)}, bf16[24,2048]{1,0:T(8,128)(2,1)S(1)}, u32[]{:S(2)}, u32[]{:S(2)}) %collective-permute-start.3) | collective-permute-done | bytes 98336 | tf_op jit(solution)/shard_map/ppermute | solution.py:33
  158.2 0.1 fusion.20
  158.4 0.1 fusion.22
  158.5 2.0 collective-permute-start.13
  160.6 2.9 %collective-permute-start.10 = (f32[4,704]{1,0:T(4,128)S(1)}, f32[4,704]{1,0:T(4,128)S(1)}, u32[]{:S(2)}, u32[]{:S(2)}) collective-permute-start(f32[4,704]{1,0:T(4,128)S(1)} %pad_maximum_fusion.8), channel_id=1, source_target_pairs={{0,0},{1,8},{8,1},{9,9},{2,2},{3,10},{10,3},{11,11},{4,4},{5,12},{... | collective-permute-start | bytes 33800 | tf_op jit(solution)/shard_map/ppermute | solution.py:33
  163.5 2.1 collective-permute-done.10
  165.6 0.1 slice_select_fusion
  165.7 25.1 %all_gather.13 = bf16[192,2048]{1,0:T(8,128)(2,1)S(1)} all-gather(bf16[24,2048]{1,0:T(8,128)(2,1)S(1)} %fusion.22), channel_id=1, replica_groups=mesh['z'=16,'yh'=2,'yl'=2,'x'=4,'c'=2] {'x','yl'}, dimensions={0}, use_global_device_ids=true | all-gather | bytes 884736 | tf_op jit(solution)/shard_map/all_gather | solution.py:198
  190.8 7.3 %collective-permute-start.11 = (bf16[8,2048]{1,0:T(8,128)(2,1)S(1)}, bf16[8,2048]{1,0:T(8,128)(2,1)S(1)}, u32[]{:S(2)}, u32[]{:S(2)}) collective-permute-start(bf16[8,2048]{1,0:T(8,128)(2,1)S(1)} %slice.192), channel_id=1, source_target_pairs={{0,1},{1,16},{16,17},{17,32},{32,33},{33,48},{48,49},{49,64},{64,6... | collective-permute-start | bytes 98312 | tf_op jit(solution)/shard_map/ppermute | solution.py:201
  198.1 0.1 constant_dynamic-update-slice_fusion.3
  198.2 0.9 collective-permute-done.11
  199.1 2.7 %fusion.8 = bf16[200,768]{1,0:T(8,128)(2,1)S(1)} fusion(bf16[200,2048]{1,0:T(8,128)(2,1)S(1)} %constant_dynamic-update-slice_fusion.2, bf16[2048,1152]{1,0:T(8,128)(2,1)} %all-gather.2.cloned.1.call-done), kind=kOutput, calls=%fused_computation.10 | convolution fusion | flops 629299200 | bytes 4272128 | tf_op jit(solution)/shard_map/dot_general | solution.py:210
  201.9 2.2 fusion.6
  204.1 0.9 fusion.11
  205.0 0.8 fusion.4
  205.8 14.9 %all_to_all.15 = bf16[8,24,2048]{2,1,0:T(8,128)(2,1)S(1)} all-to-all(bf16[8,24,2048]{2,1,0:T(8,128)(2,1)S(1)} %bitcast.13), channel_id=1, replica_groups=mesh['z'=16,'yh'=2,'yl'=2,'x'=4,'c'=2] {'x','yl'}, dimensions={0} | all-to-all | bytes 1572864 | tf_op jit(solution)/shard_map/all_to_all | solution.py:120
  220.7 0.1 reduce_sum.85
  220.8 2.3 collective-permute-start.14
  223.1 3.6 %collective-permute-done.14 = bf16[24,2048]{1,0:T(8,128)(2,1)S(1)} collective-permute-done((bf16[24,2048]{1,0:T(8,128)(2,1)S(1)}, bf16[24,2048]{1,0:T(8,128)(2,1)S(1)}, u32[]{:S(2)}, u32[]{:S(2)}) %collective-permute-start.14) | collective-permute-done | bytes 98336 | tf_op jit(solution)/shard_map/ppermute | solution.py:33
  226.8 0.6 copy.23
  (50 shorter events, 0.4 us)
Async XLA Ops:
  6.5 25.0 %copy-start.3 = (bf16[192,128]{1,0:T(8,128)(2,1)S(1)}, bf16[192,128]{1,0:T(8,128)(2,1)}, u32[]{:S(2)}) copy-start(bf16[192,128]{1,0:T(8,128)(2,1)} %param.15) | copy-start | bytes 147460
  6.5 25.0 %copy-start.4 = (bf16[192,128]{1,0:T(8,128)(2,1)S(1)}, bf16[192,128]{1,0:T(8,128)(2,1)}, u32[]{:S(2)}) copy-start(bf16[192,128]{1,0:T(8,128)(2,1)} %param.16) | copy-start | bytes 147460
  6.5 44.9 %copy-start.8 = (f32[704]{0:T(1024)S(1)}, f32[704]{0:T(1024)}, u32[]{:S(2)}) copy-start(f32[704]{0:T(1024)} %param.24) | copy-start | bytes 8452
  6.5 44.9 %copy-start.6 = (f32[3,704]{1,0:T(4,128)S(1)}, f32[3,704]{1,0:T(4,128)}, u32[]{:S(2)}) copy-start(f32[3,704]{1,0:T(4,128)} %param.23) | copy-start | bytes 25348
  6.5 73.7 %copy-start.5 = (bf16[192,128]{1,0:T(8,128)(2,1)S(1)}, bf16[192,128]{1,0:T(8,128)(2,1)}, u32[]{:S(2)}) copy-start(bf16[192,128]{1,0:T(8,128)(2,1)} %param.14) | copy-start | bytes 147460
  6.5 152.0 %all-gather.2.cloned.1.call-start = ((), (), s32[]{:S(2)}) async-start(), calls=%async_computation.3 | async-start | bytes 5013504 | tf_op jit(solution)/shard_map/all_gather | solution.py:161
  20.0 10.7 %collective-permute-start.12 = (bf16[128,1152]{1,0:T(8,128)(2,1)S(1)}, bf16[128,1152]{1,0:T(8,128)(2,1)S(1)}, u32[]{:S(2)}, u32[]{:S(2)}) collective-permute-start(bf16[128,1152]{1,0:T(8,128)(2,1)S(1)} %broadcast_select_fusion), channel_id=1, source_target_pairs={{0,1},{9,8},{2,3},{11,10},{4,5},{13,12},{6,7},{15,14},{16,17},{25,... | collective-permute-start | bytes 884744 | tf_op jit(solution)/shard_map/ppermute | solution.py:159
  31.6 71.2 %copy-start = (bf16[192,256]{1,0:T(8,128)(2,1)}, bf16[192,256]{1,0:T(8,128)(2,1)S(1)}, u32[]{:S(2)}) copy-start(bf16[192,256]{1,0:T(8,128)(2,1)S(1)} %constant_dynamic-update-slice_fusion.own_ref) | copy-start | bytes 294916
  31.6 19.9 %collective-permute-start.2 = (bf16[192,256]{1,0:T(8,128)(2,1)S(1)}, bf16[192,256]{1,0:T(8,128)(2,1)S(1)}, u32[]{:S(2)}, u32[]{:S(2)}) collective-permute-start(bf16[192,256]{1,0:T(8,128)(2,1)S(1)} %constant_dynamic-update-slice_fusion.own_ref), channel_id=1, source_target_pairs={{0,384},{32,416},{64,448},{96,480},{128,0},{160,32},{192,64},{224,... | collective-permute-start | bytes 294920 | tf_op jit(solution)/shard_map/ppermute | solution.py:29
  39.2 14.7 %collective-permute-start.1 = (bf16[192,256]{1,0:T(8,128)(2,1)S(1)}, bf16[192,256]{1,0:T(8,128)(2,1)S(1)}, u32[]{:S(2)}, u32[]{:S(2)}) collective-permute-start(bf16[192,256]{1,0:T(8,128)(2,1)S(1)} %constant_dynamic-update-slice_fusion.own_ref), channel_id=1, source_target_pairs={{0,256},{32,288},{64,320},{96,352},{128,384},{160,416},{192,448},{... | collective-permute-start | bytes 294920 | tf_op jit(solution)/shard_map/ppermute | solution.py:29
  44.1 18.3 %collective-permute-start = (bf16[192,256]{1,0:T(8,128)(2,1)S(1)}, bf16[192,256]{1,0:T(8,128)(2,1)S(1)}, u32[]{:S(2)}, u32[]{:S(2)}) collective-permute-start(bf16[192,256]{1,0:T(8,128)(2,1)S(1)} %constant_dynamic-update-slice_fusion.own_ref), channel_id=1, source_target_pairs={{0,128},{32,160},{64,192},{96,224},{128,256},{160,288},{192,320},{... | collective-permute-start | bytes 294920 | tf_op jit(solution)/shard_map/ppermute | solution.py:29
  62.5 58.8 %copy-start.10 = (bf16[128,2048]{1,0:T(8,128)(2,1)S(1)}, bf16[128,2048]{1,0:T(8,128)(2,1)}, u32[]{:S(2)}) copy-start(bf16[128,2048]{1,0:T(8,128)(2,1)} %param.19) | copy-start | bytes 1572868
  62.5 40.2 %collective-permute-start.4 = (bf16[768,256]{1,0:T(8,128)(2,1)S(1)}, bf16[768,256]{1,0:T(8,128)(2,1)S(1)}, u32[]{:S(2)}, u32[]{:S(2)}) collective-permute-start(bf16[768,256]{1,0:T(8,128)(2,1)S(1)} %get-tuple-element.11), channel_id=1, source_target_pairs={{0,32},{32,64},{64,96},{96,128},{128,160},{160,192},{192,224},{224... | collective-permute-start | bytes 1179656 | tf_op jit(solution)/shard_map/ppermute | solution.py:29
  68.6 34.2 %collective-permute-start.7 = (bf16[768,256]{1,0:T(8,128)(2,1)S(1)}, bf16[768,256]{1,0:T(8,128)(2,1)S(1)}, u32[]{:S(2)}, u32[]{:S(2)}) collective-permute-start(bf16[768,256]{1,0:T(8,128)(2,1)S(1)} %get-tuple-element.37), channel_id=1, source_target_pairs={{0,480},{32,0},{64,32},{96,64},{128,96},{160,128},{192,160},{224,1... | collective-permute-start | bytes 1179656 | tf_op jit(solution)/shard_map/ppermute | solution.py:29
  74.0 27.7 %collective-permute-start.6 = (bf16[384,256]{1,0:T(8,128)(2,1)S(1)}, bf16[384,256]{1,0:T(8,128)(2,1)S(1)}, u32[]{:S(2)}, u32[]{:S(2)}) collective-permute-start(bf16[384,256]{1,0:T(8,128)(2,1)S(1)} %pad_maximum_fusion.3), channel_id=1, source_target_pairs={{0,448},{32,480},{64,0},{96,32},{128,64},{160,96},{192,128},{224,1... | collective-permute-start | bytes 589832 | tf_op jit(solution)/shard_map/ppermute | solution.py:29
  77.1 24.8 %collective-permute-start.5 = (bf16[384,256]{1,0:T(8,128)(2,1)S(1)}, bf16[384,256]{1,0:T(8,128)(2,1)S(1)}, u32[]{:S(2)}, u32[]{:S(2)}) collective-permute-start(bf16[384,256]{1,0:T(8,128)(2,1)S(1)} %slice.138), channel_id=1, source_target_pairs={{0,64},{32,96},{64,128},{96,160},{128,192},{160,224},{192,256},{22... | collective-permute-start | bytes 589832 | tf_op jit(solution)/shard_map/ppermute | solution.py:29
  102.8 0.8 copy-start.1
  103.5 0.7 copy-start.2
  116.3 13.1 %all-to-all-start = ((bf16[4,192,384]{2,1,0:T(8,128)(2,1)}), bf16[4,192,384]{2,1,0:T(8,128)(2,1)S(1)}, u32[]{:S(2)}, u32[]{:S(2)}) async-start(bf16[4,192,384]{2,1,0:T(8,128)(2,1)} %bitcast.12), calls=%async_computation | async-start | bytes 1179648 | tf_op jit(solution)/shard_map/all_to_all | solution.py:186
  121.4 16.3 %collective-permute-start.9 = (bf16[128,2048]{1,0:T(8,128)(2,1)S(1)}, bf16[128,2048]{1,0:T(8,128)(2,1)S(1)}, u32[]{:S(2)}, u32[]{:S(2)}) collective-permute-start(bf16[128,2048]{1,0:T(8,128)(2,1)S(1)} %copy-done.10), channel_id=1, source_target_pairs={{0,0},{1,8},{8,1},{9,9},{2,2},{3,10},{10,3},{11,11},{4,4},{5,12},{... | collective-permute-start | bytes 1572872 | tf_op jit(solution)/shard_map/ppermute | solution.py:33
  129.5 1.8 copy-start.9
  130.2 14.7 %copy-start.11 = (bf16[24,2048]{1,0:T(8,128)(2,1)S(1)}, bf16[24,2048]{1,0:T(8,128)(2,1)}, u32[]{:S(2)}) copy-start(bf16[24,2048]{1,0:T(8,128)(2,1)} %param.13) | copy-start | bytes 294916
  130.7 27.6 %copy-start.7 = (f32[2048]{0:T(1024)S(1)}, f32[2048]{0:T(1024)}, u32[]{:S(2)}) copy-start(f32[2048]{0:T(1024)} %param.20) | copy-start | bytes 24580
  131.4 8.2 %collective-permute-start.8 = (bf16[192,128]{0,1:T(8,128)(2,1)S(1)}, bf16[192,128]{0,1:T(8,128)(2,1)S(1)}, u32[]{:S(2)}, u32[]{:S(2)}) collective-permute-start(bf16[192,128]{0,1:T(8,128)(2,1)S(1)} %multiply_convert_fusion.4), channel_id=1, source_target_pairs={{0,0},{1,8},{8,1},{9,9},{2,2},{3,10},{10,3},{11,11},{4,4},{5,12},{... | collective-permute-start | bytes 147464 | tf_op jit(solution)/shard_map/ppermute | solution.py:33
  140.9 14.6 %all-to-all-start.1 = ((bf16[8,24,2048]{2,1,0:T(8,128)(2,1)}), bf16[8,24,2048]{2,1,0:T(8,128)(2,1)S(1)}, u32[]{:S(2)}, u32[]{:S(2)}) async-start(bf16[8,24,2048]{2,1,0:T(8,128)(2,1)} %bitcast.4), calls=%async_computation.1 | async-start | bytes 1572864 | tf_op jit(solution)/shard_map/all_to_all | solution.py:120
  144.9 13.3 %collective-permute-start.3 = (bf16[24,2048]{1,0:T(8,128)(2,1)S(1)}, bf16[24,2048]{1,0:T(8,128)(2,1)S(1)}, u32[]{:S(2)}, u32[]{:S(2)}) collective-permute-start(bf16[24,2048]{1,0:T(8,128)(2,1)S(1)} %copy-done.11), channel_id=1, source_target_pairs={{0,0},{1,8},{8,1},{9,9},{2,2},{3,10},{10,3},{11,11},{4,4},{5,12},{... | collective-permute-start | bytes 294920 | tf_op jit(solution)/shard_map/ppermute | solution.py:33
  158.5 45.6 %collective-permute-start.13 = (bf16[2048,1152]{1,0:T(8,128)(2,1)}, bf16[2048,1152]{1,0:T(8,128)(2,1)S(1)}, u32[]{:S(2)}, u32[]{:S(2)}) collective-permute-start(bf16[2048,1152]{1,0:T(8,128)(2,1)} %all-gather.2.cloned.1.call-done), channel_id=1, source_target_pairs={{0,1},{1,0},{2,3},{3,2},{4,5},{5,4},{6,7},{7,6},{8,9},{9,8},{10,11... | collective-permute-start | bytes 14155784 | tf_op jit(solution)/shard_map/ppermute | solution.py:197
  160.6 5.0 %collective-permute-start.10 = (f32[4,704]{1,0:T(4,128)S(1)}, f32[4,704]{1,0:T(4,128)S(1)}, u32[]{:S(2)}, u32[]{:S(2)}) collective-permute-start(f32[4,704]{1,0:T(4,128)S(1)} %pad_maximum_fusion.8), channel_id=1, source_target_pairs={{0,0},{1,8},{8,1},{9,9},{2,2},{3,10},{10,3},{11,11},{4,4},{5,12},{... | collective-permute-start | bytes 33800 | tf_op jit(solution)/shard_map/ppermute | solution.py:33
  190.8 8.3 %collective-permute-start.11 = (bf16[8,2048]{1,0:T(8,128)(2,1)S(1)}, bf16[8,2048]{1,0:T(8,128)(2,1)S(1)}, u32[]{:S(2)}, u32[]{:S(2)}) collective-permute-start(bf16[8,2048]{1,0:T(8,128)(2,1)S(1)} %slice.192), channel_id=1, source_target_pairs={{0,1},{1,16},{16,17},{17,32},{32,33},{33,48},{48,49},{49,64},{64,6... | collective-permute-start | bytes 98312 | tf_op jit(solution)/shard_map/ppermute | solution.py:201
  220.8 5.9 %collective-permute-start.14 = (bf16[24,2048]{1,0:T(8,128)(2,1)S(1)}, bf16[24,2048]{1,0:T(8,128)(2,1)S(1)}, u32[]{:S(2)}, u32[]{:S(2)}) collective-permute-start(bf16[24,2048]{1,0:T(8,128)(2,1)S(1)} %fusion.23), channel_id=1, source_target_pairs={{0,0},{1,8},{8,1},{9,9},{2,2},{3,10},{10,3},{11,11},{4,4},{5,12},{... | collective-permute-start | bytes 294920 | tf_op jit(solution)/shard_map/ppermute | solution.py:33
Sparse Core Ops, SparseCore 0:
  31.6 99.3 all-gather.1

commit v4 on v3

--- a/solution.py
+++ b/solution.py
@@ -37,10 +37,16 @@
     return lax.dot_general(a, b, (((1,), (1,)), ((), ())), preferred_element_type=jnp.float32)
 
 
-def attend_kernel(where_ref, q_ref, own_ref, far_ref, n1_ref, n2_ref, n3_ref, out_ref):
+def attend_kernel(where_ref, rows_ref, own_ref, far_ref, n1_ref, n2_ref, n3_ref, out_ref, q_ref):
     z = where_ref[0]
     y = where_ref[1]
     rows = own_ref.shape[0]
+    w_rows = rows_ref.shape[0] // NY
+    for i in range(NY * rows // w_rows):
+        y_at, lane_at = divmod(i, rows // w_rows)
+        q_ref[i * w_rows : (i + 1) * w_rows, :] = rows_ref[
+            y_at * w_rows : (y_at + 1) * w_rows, lane_at * 2 * HD : (lane_at + 1) * 2 * HD
+        ]
 
     def row_bias(offsets):
         lane = lax.broadcasted_iota(jnp.int32, (1, rows * len(offsets)), 1)
@@ -154,14 +160,17 @@
         cuts += [up_weight[:, units], gate_weight[:, units]]
         cuts += [jnp.zeros((up_weight.shape[0], gap), jnp.bfloat16), down_t[:, units]]
         cuts += [jnp.zeros((up_weight.shape[0], tail), jnp.bfloat16)]
+    w_rows = up_weight.shape[0]
+    cuts += [queries[i : i + w_rows] for i in range(0, rows, w_rows)]
     row_w = lax.all_gather(jnp.concatenate(cuts, axis=1), Y, axis=0, tiled=True)
-    low, high = row_w[:, : width + tail], row_w[:, width + tail :]
+    span = width + tail
+    low, high = row_w[:, :span], row_w[:, span : 2 * span]
+    q_rows = row_w[:, 2 * span :]
     for_peer = lax.ppermute(jnp.where(core == 0, high, low), ("yl", "c"), [(0, 1), (3, 2)])
     kept = jnp.where(core == pair, jnp.where(core == 0, low, high), for_peer)
     mine = lax.all_gather(kept, "z", axis=0, tiled=True)
 
     kv = jnp.concatenate((key_pairs, values), axis=1)
-    q_all = lax.all_gather(queries, Y, axis=0, tiled=True)
     f4, f8, f12 = (shifted(kv, "z", s) for s in (4, 8, -4))
     held = jnp.concatenate((kv, f4, f8, f12), axis=0)
     conv = jnp.concatenate((conv_weight, conv_bias[None, :]), axis=0)
@@ -181,8 +190,9 @@
         out_shape=jax.ShapeDtypeStruct((NY * rows, 3 * VD), jnp.bfloat16),
         in_specs=[SMEM] + [VMEM] * 6,
         out_specs=VMEM,
+        scratch_shapes=[pltpu.VMEM((NY * rows, 2 * HD), jnp.bfloat16)],
         name="attend",
-    )(where, q_all, kv, far, n1, n2, n3)
+    )(where, q_rows, kv, far, n1, n2, n3)
     got = lax.all_to_all(parts.reshape(NY, rows, 3 * VD), Y, 0, 0, tiled=True)
     means = merged(got)
     diff = means[0] - second_weight[0] * means[1]
@@ -195,7 +205,11 @@
     normed = normalize(mid, norm_gain)
     mine, _ = lax.optimization_barrier((mine, normed))
     other = lax.ppermute(mine, "c", [(0, 1), (1, 0)])
-    normed_all = lax.all_gather(normed, SHARDS, axis=0, tiled=True)
+    peer = lax.ppermute(normed, "yl", [(0, 1), (1, 0)])
+    both_rows = jnp.concatenate(
+        (jnp.where(pair == 0, normed, peer), jnp.where(pair == 0, peer, normed)), axis=0
+    )
+    normed_all = lax.all_gather(both_rows, "x", axis=0, tiled=True)
     tokens = ("z", "yh", "c")
     count = lax.axis_size(tokens)
     rim_rows = lax.ppermute(normed_all[rows - 8 :], tokens, [(i, i + 1) for i in range(count - 1)])

time: 236 us -> 232 us (0.983)
  blocking collectives: 63 us -> 37 us
  waiting for transfers between devices: 45.5 us -> 60.6 us
  matrix products: 7.81 us -> 11.1 us
    all_gather x2 -> x1, blocking collectives: 36.8 us -> 10.9 us  [local(): normed_all = lax.all_gather(both_rows, 'x', axis=0, tiled=True)]
    ppermute x7, waiting for transfers between devices: 19.7 us -> 30.4 us  [shifted(): lax.ppermute(value, axis, [(i, (i + steps) % count) for i in range(count)])]
    ppermute x0 -> x1, waiting for transfers between devices: none -> 4.51 us  [local(): peer = lax.ppermute(normed, 'yl', [(0, 1), (1, 0)])]
  transfers between devices with their start and end apart: 18 -> 19, of which waited for: 11 -> 12; matrix products, arithmetic and copies ran while one was open for 5% -> 5% of each run, Pallas kernels for 5% -> 5%
where the time goes in v4:
time: 232 us; the launch traced here: 230 us
  starting transfers between devices  83.1 us (36%)
  waiting for transfers between devices  60.6 us (26%)
  blocking collectives  37 us (16%)
  between operations  14.6 us (6%)
  Pallas kernels  12 us (5%)
  matrix products  11.1 us (5%)
  local copies, waits for them, and re-layouts  6.75 us (3%)
  other arithmetic  4.86 us (2%)
    ppermute x7, starting transfers between devices, shifted(): lax.ppermute(value, axis, [(i, (i + steps) % count) for i in range(count)])  37.3 us
    ppermute x7, waiting for transfers between devices, shifted(): lax.ppermute(value, axis, [(i, (i + steps) % count) for i in range(count)])  30.4 us
    ppermute x5, starting transfers between devices, swapped(): return lax.ppermute(value, ('yl', 'c'), [(0, 0), (1, 2), (2, 1), (3, 3)])  24.9 us
    all_to_all x1, blocking collectives, summed_over_shards(): tiles = lax.all_to_all(cut, SHARDS, 0, 0, tiled=True)  13.9 us
    all_gather x1, blocking collectives, local(): row_w = lax.all_gather(jnp.concatenate(cuts, axis=1), Y, axis=0, tiled=True)  12.2 us
    pallas_call x1, Pallas kernels, local(): pl.pallas_call(attend_kernel, out_shape=jax.ShapeDtypeStruct((NY * rows,...  12 us
    all_gather x1, blocking collectives, local(): normed_all = lax.all_gather(both_rows, 'x', axis=0, tiled=True)  10.9 us
    ppermute x5, waiting for transfers between devices, swapped(): return lax.ppermute(value, ('yl', 'c'), [(0, 0), (1, 2), (2, 1), (3, 3)])  10.3 us
  transfers between devices with their start and end apart: 19, of which 12 were waited for; matrix products, arithmetic and copies ran while one was open for 5% of the time, Pallas kernels for 5%

profile of v4, /device:TPU:1, one launch (start us, length us, event | category | flops | bytes accessed | tf_op | source)
XLA Modules:
  0.0 230.0 jit_solution(15364485245735190339)
XLA Ops:
  6.6 0.9 fusion.49
  7.5 0.8 fusion.46
  8.3 0.9 fusion.47
  9.2 0.1 concatenate.36
  9.3 12.2 %all_gather.9 = bf16[128,3072]{1,0:T(8,128)(2,1)S(1)} all-gather(bf16[32,3072]{1,0:T(8,128)(2,1)S(1)} %concatenate.36), channel_id=1, replica_groups=mesh['z'=16,'yh'=2,'yl'=2,'x'=4,'c'=2] {'yh','yl'}, dimensions={0}, use_global_device_ids=true | all-gather | bytes 983040 | tf_op jit(solution)/shard_map/all_gather | solution.py:165
  21.6 1.3 collective-permute-start.13
  22.9 9.1 %collective-permute-done.13 = bf16[128,1152]{1,0:T(8,128)(2,1)S(1)} collective-permute-done((bf16[128,1152]{1,0:T(8,128)(2,1)S(1)}, bf16[128,1152]{1,0:T(8,128)(2,1)S(1)}, u32[]{:S(2)}, u32[]{:S(2)}) %collective-permute-start.13) | collective-permute-done | bytes 294944 | tf_op jit(solution)/shard_map/ppermute | solution.py:169
  32.1 0.8 select_select_fusion
  32.9 7.4 %collective-permute-start.2 = (bf16[192,256]{1,0:T(8,128)(2,1)S(1)}, bf16[192,256]{1,0:T(8,128)(2,1)S(1)}, u32[]{:S(2)}, u32[]{:S(2)}) collective-permute-start(bf16[192,256]{1,0:T(8,128)(2,1)S(1)} %constant_dynamic-update-slice_fusion.own_ref), channel_id=1, source_target_pairs={{0,384},{32,416},{64,448},{96,480},{128,0},{160,32},{192,64},{224,... | collective-permute-start | bytes 294920 | tf_op jit(solution)/shard_map/ppermute | solution.py:29
  40.4 4.9 %collective-permute-start.1 = (bf16[192,256]{1,0:T(8,128)(2,1)S(1)}, bf16[192,256]{1,0:T(8,128)(2,1)S(1)}, u32[]{:S(2)}, u32[]{:S(2)}) collective-permute-start(bf16[192,256]{1,0:T(8,128)(2,1)S(1)} %constant_dynamic-update-slice_fusion.own_ref), channel_id=1, source_target_pairs={{0,256},{32,288},{64,320},{96,352},{128,384},{160,416},{192,448},{... | collective-permute-start | bytes 294920 | tf_op jit(solution)/shard_map/ppermute | solution.py:29
  45.3 7.3 %collective-permute-start = (bf16[192,256]{1,0:T(8,128)(2,1)S(1)}, bf16[192,256]{1,0:T(8,128)(2,1)S(1)}, u32[]{:S(2)}, u32[]{:S(2)}) collective-permute-start(bf16[192,256]{1,0:T(8,128)(2,1)S(1)} %constant_dynamic-update-slice_fusion.own_ref), channel_id=1, source_target_pairs={{0,128},{32,160},{64,192},{96,224},{128,256},{160,288},{192,320},{... | collective-permute-start | bytes 294920 | tf_op jit(solution)/shard_map/ppermute | solution.py:29
  52.6 2.5 %collective-permute-done.1 = bf16[192,256]{1,0:T(8,128)(2,1)S(1)} collective-permute-done((bf16[192,256]{1,0:T(8,128)(2,1)S(1)}, bf16[192,256]{1,0:T(8,128)(2,1)S(1)}, u32[]{:S(2)}, u32[]{:S(2)}) %collective-permute-start.1) | collective-permute-done | bytes 98336 | tf_op jit(solution)/shard_map/ppermute | solution.py:29
  55.1 8.3 %collective-permute-done = bf16[192,256]{1,0:T(8,128)(2,1)S(1)} collective-permute-done((bf16[192,256]{1,0:T(8,128)(2,1)S(1)}, bf16[192,256]{1,0:T(8,128)(2,1)S(1)}, u32[]{:S(2)}, u32[]{:S(2)}) %collective-permute-start) | collective-permute-done | bytes 98336 | tf_op jit(solution)/shard_map/ppermute | solution.py:29
  63.5 6.0 %collective-permute-start.4 = (bf16[768,256]{1,0:T(8,128)(2,1)S(1)}, bf16[768,256]{1,0:T(8,128)(2,1)S(1)}, u32[]{:S(2)}, u32[]{:S(2)}) collective-permute-start(bf16[768,256]{1,0:T(8,128)(2,1)S(1)} %get-tuple-element.11), channel_id=1, source_target_pairs={{0,32},{32,64},{64,96},{96,128},{128,160},{160,192},{192,224},{224... | collective-permute-start | bytes 1179656 | tf_op jit(solution)/shard_map/ppermute | solution.py:29
  69.5 5.6 %collective-permute-start.7 = (bf16[768,256]{1,0:T(8,128)(2,1)S(1)}, bf16[768,256]{1,0:T(8,128)(2,1)S(1)}, u32[]{:S(2)}, u32[]{:S(2)}) collective-permute-start(bf16[768,256]{1,0:T(8,128)(2,1)S(1)} %get-tuple-element.37), channel_id=1, source_target_pairs={{0,480},{32,0},{64,32},{96,64},{128,96},{160,128},{192,160},{224,1... | collective-permute-start | bytes 1179656 | tf_op jit(solution)/shard_map/ppermute | solution.py:29
  75.1 3.1 %collective-permute-start.6 = (bf16[384,256]{1,0:T(8,128)(2,1)S(1)}, bf16[384,256]{1,0:T(8,128)(2,1)S(1)}, u32[]{:S(2)}, u32[]{:S(2)}) collective-permute-start(bf16[384,256]{1,0:T(8,128)(2,1)S(1)} %pad_maximum_fusion.3), channel_id=1, source_target_pairs={{0,448},{32,480},{64,0},{96,32},{128,64},{160,96},{192,128},{224,1... | collective-permute-start | bytes 589832 | tf_op jit(solution)/shard_map/ppermute | solution.py:29
  78.2 3.1 %collective-permute-start.5 = (bf16[384,256]{1,0:T(8,128)(2,1)S(1)}, bf16[384,256]{1,0:T(8,128)(2,1)S(1)}, u32[]{:S(2)}, u32[]{:S(2)}) collective-permute-start(bf16[384,256]{1,0:T(8,128)(2,1)S(1)} %slice.172), channel_id=1, source_target_pairs={{0,64},{32,96},{64,128},{96,160},{128,192},{160,224},{192,256},{22... | collective-permute-start | bytes 589832 | tf_op jit(solution)/shard_map/ppermute | solution.py:29
  81.3 0.7 slice.210.rows_ref
  82.0 0.6 pad_add_fusion.where_ref
  82.6 0.7 slice.171.far_ref
  83.4 19.5 %collective-permute-done.6 = bf16[384,256]{1,0:T(8,128)(2,1)S(1)} collective-permute-done((bf16[384,256]{1,0:T(8,128)(2,1)S(1)}, bf16[384,256]{1,0:T(8,128)(2,1)S(1)}, u32[]{:S(2)}, u32[]{:S(2)}) %collective-permute-start.6) | collective-permute-done | bytes 196640 | tf_op jit(solution)/shard_map/ppermute | solution.py:29
  102.9 0.1 collective-permute-done.5
  103.0 0.8 pad_maximum_fusion.1.n2_ref
  103.8 0.7 copy-done.1
  104.5 0.7 copy-done.2
  105.3 12.0 %attend.1 = bf16[768,384]{1,0:T(8,128)(2,1)} custom-call(s32[2]{0:T(128)} %pad_add_fusion.where_ref, bf16[128,768]{1,0:T(8,128)(2,1)} %slice.210.rows_ref, bf16[192,256]{1,0:T(8,128)(2,1)} %copy-done, bf16[576,256]{1,0:T(8,128)(2,1)} %slice.171.far_ref, bf16[768,256]{1,0:T(8,128)(2,1)} %copy-done.1, bf16[768,256]{1,0:T(8,128)(2,1)} %pad_maximum_fusion.1.n2_ref, ...), custom_call_target="tpu_custom_call" | custom-call | tf_op jit(solution)/shard_map/attend/pallas_call | solution.py:188
  117.3 4.4 %all-to-all-start = ((bf16[4,192,384]{2,1,0:T(8,128)(2,1)}), bf16[4,192,384]{2,1,0:T(8,128)(2,1)S(1)}, u32[]{:S(2)}, u32[]{:S(2)}) async-start(bf16[4,192,384]{2,1,0:T(8,128)(2,1)} %bitcast.12), calls=%async_computation | async-start | bytes 1179648 | tf_op jit(solution)/shard_map/all_to_all | solution.py:196
  122.4 8.1 %collective-permute-start.9 = (bf16[128,2048]{1,0:T(8,128)(2,1)}, bf16[128,2048]{1,0:T(8,128)(2,1)S(1)}, u32[]{:S(2)}, u32[]{:S(2)}) collective-permute-start(bf16[128,2048]{1,0:T(8,128)(2,1)} %param.19), channel_id=1, source_target_pairs={{0,0},{1,8},{8,1},{9,9},{2,2},{3,10},{10,3},{11,11},{4,4},{5,12},{... | collective-permute-start | bytes 1572872 | tf_op jit(solution)/shard_map/ppermute | solution.py:33
  130.5 0.1 convert_element_type.75
  130.6 0.7 fusion.44
  131.3 0.4 fusion.16
  131.7 0.4 fusion.18
  132.1 0.3 fusion.15
  132.3 0.1 copy.18
  132.4 0.1 copy.17
  132.6 0.1 multiply_convert_fusion.4
  132.7 6.3 %collective-permute-start.8 = (bf16[192,128]{0,1:T(8,128)(2,1)S(1)}, bf16[192,128]{0,1:T(8,128)(2,1)S(1)}, u32[]{:S(2)}, u32[]{:S(2)}) collective-permute-start(bf16[192,128]{0,1:T(8,128)(2,1)S(1)} %multiply_convert_fusion.4), channel_id=1, source_target_pairs={{0,0},{1,8},{8,1},{9,9},{2,2},{3,10},{10,3},{11,11},{4,4},{5,12},{... | collective-permute-start | bytes 147464 | tf_op jit(solution)/shard_map/ppermute | solution.py:33
  139.0 1.9 collective-permute-done.8
  140.9 1.3 convolution_convert_fusion
  142.2 3.9 %all-to-all-start.1 = ((bf16[8,24,2048]{2,1,0:T(8,128)(2,1)}), bf16[8,24,2048]{2,1,0:T(8,128)(2,1)S(1)}, u32[]{:S(2)}, u32[]{:S(2)}) async-start(bf16[8,24,2048]{2,1,0:T(8,128)(2,1)} %bitcast.5), calls=%async_computation.1 | async-start | bytes 1572864 | tf_op jit(solution)/shard_map/all_to_all | solution.py:126
  146.2 5.4 %collective-permute-start.3 = (bf16[24,2048]{1,0:T(8,128)(2,1)S(1)}, bf16[24,2048]{1,0:T(8,128)(2,1)S(1)}, u32[]{:S(2)}, u32[]{:S(2)}) collective-permute-start(bf16[24,2048]{1,0:T(8,128)(2,1)S(1)} %copy-done.9), channel_id=1, source_target_pairs={{0,0},{1,8},{8,1},{9,9},{2,2},{3,10},{10,3},{11,11},{4,4},{5,12},{... | collective-permute-start | bytes 294920 | tf_op jit(solution)/shard_map/ppermute | solution.py:33
  151.5 5.2 %all-to-all-done.1 = bf16[8,24,2048]{2,1,0:T(8,128)(2,1)S(1)} async-done(((bf16[8,24,2048]{2,1,0:T(8,128)(2,1)}), bf16[8,24,2048]{2,1,0:T(8,128)(2,1)S(1)}, u32[]{:S(2)}, u32[]{:S(2)}) %all-to-all-start.1) | async-done | bytes 786464 | tf_op jit(solution)/shard_map/all_to_all | solution.py:126
  156.8 0.1 reduce_sum.83
  156.9 2.6 %collective-permute-done.3 = bf16[24,2048]{1,0:T(8,128)(2,1)S(1)} collective-permute-done((bf16[24,2048]{1,0:T(8,128)(2,1)S(1)}, bf16[24,2048]{1,0:T(8,128)(2,1)S(1)}, u32[]{:S(2)}, u32[]{:S(2)}) %collective-permute-start.3) | collective-permute-done | bytes 98336 | tf_op jit(solution)/shard_map/ppermute | solution.py:33
  159.5 0.1 fusion.20
  159.7 0.1 fusion.22
  159.8 2.0 collective-permute-start.14
  161.8 2.9 %collective-permute-start.10 = (f32[4,704]{1,0:T(4,128)S(1)}, f32[4,704]{1,0:T(4,128)S(1)}, u32[]{:S(2)}, u32[]{:S(2)}) collective-permute-start(f32[4,704]{1,0:T(4,128)S(1)} %pad_maximum_fusion.9), channel_id=1, source_target_pairs={{0,0},{1,8},{8,1},{9,9},{2,2},{3,10},{10,3},{11,11},{4,4},{5,12},{... | collective-permute-start | bytes 33800 | tf_op jit(solution)/shard_map/ppermute | solution.py:33
  164.8 2.1 collective-permute-done.10
  166.8 0.1 slice_select_fusion
  166.9 1.9 collective-permute-start.11
  168.9 4.5 %collective-permute-done.11 = bf16[24,2048]{1,0:T(8,128)(2,1)S(1)} collective-permute-done((bf16[24,2048]{1,0:T(8,128)(2,1)S(1)}, bf16[24,2048]{1,0:T(8,128)(2,1)S(1)}, u32[]{:S(2)}, u32[]{:S(2)}) %collective-permute-start.11) | collective-permute-done | bytes 98336 | tf_op jit(solution)/shard_map/ppermute | solution.py:208
  173.5 10.9 %all_gather.10 = bf16[192,2048]{1,0:T(8,128)(2,1)S(1)} all-gather(bf16[48,2048]{1,0:T(8,128)(2,1)S(1)} %pad_maximum_fusion.4), channel_id=1, replica_groups=mesh['z'=16,'yh'=2,'yl'=2,'x'=4,'c'=2] {'x'}, dimensions={0}, use_global_device_ids=true | all-gather | bytes 983040 | tf_op jit(solution)/shard_map/all_gather | solution.py:212
  184.4 7.2 %collective-permute-start.12 = (bf16[8,2048]{1,0:T(8,128)(2,1)S(1)}, bf16[8,2048]{1,0:T(8,128)(2,1)S(1)}, u32[]{:S(2)}, u32[]{:S(2)}) collective-permute-start(bf16[8,2048]{1,0:T(8,128)(2,1)S(1)} %slice.223), channel_id=1, source_target_pairs={{0,1},{1,16},{16,17},{17,32},{32,33},{33,48},{48,49},{49,64},{64,6... | collective-permute-start | bytes 98312 | tf_op jit(solution)/shard_map/ppermute | solution.py:215
  191.7 0.9 collective-permute-done.12
  192.6 2.7 %fusion.8 = bf16[200,768]{1,0:T(8,128)(2,1)S(1)} fusion(bf16[200,2048]{1,0:T(8,128)(2,1)S(1)} %constant_dynamic-update-slice_fusion.2, bf16[2048,1152]{1,0:T(8,128)(2,1)} %all-gather.2.cloned.1.call-done), kind=kOutput, calls=%fused_computation.10 | convolution fusion | flops 629299200 | bytes 4272128 | tf_op jit(solution)/shard_map/dot_general | solution.py:224
  195.4 2.2 fusion.6
  197.6 2.7 %fusion.11 = bf16[200,768]{1,0:T(8,128)(2,1)S(1)} fusion(bf16[200,2048]{1,0:T(8,128)(2,1)S(1)} %constant_dynamic-update-slice_fusion.2, bf16[2048,1152]{1,0:T(8,128)(2,1)} %collective-permute-done.14), kind=kOutput, calls=%fused_computation.11 | convolution fusion | flops 629299200 | bytes 4272128 | tf_op jit(solution)/shard_map/dot_general | solution.py:224
  200.3 2.2 fusion.4
  202.5 13.9 %all_to_all.15 = bf16[8,24,2048]{2,1,0:T(8,128)(2,1)S(1)} all-to-all(bf16[8,24,2048]{2,1,0:T(8,128)(2,1)S(1)} %bitcast.13), channel_id=1, replica_groups=mesh['z'=16,'yh'=2,'yl'=2,'x'=4,'c'=2] {'x','yl'}, dimensions={0} | all-to-all | bytes 1572864 | tf_op jit(solution)/shard_map/all_to_all | solution.py:126
  216.4 0.1 reduce_sum.85
  216.6 2.2 collective-permute-start.15
  218.8 3.7 %collective-permute-done.15 = bf16[24,2048]{1,0:T(8,128)(2,1)S(1)} collective-permute-done((bf16[24,2048]{1,0:T(8,128)(2,1)S(1)}, bf16[24,2048]{1,0:T(8,128)(2,1)S(1)}, u32[]{:S(2)}, u32[]{:S(2)}) %collective-permute-start.15) | collective-permute-done | bytes 98336 | tf_op jit(solution)/shard_map/ppermute | solution.py:33
  222.5 0.6 copy.23
  (52 shorter events, 0.6 us)
Async XLA Ops:
  6.5 26.3 %copy-start.3 = (bf16[192,128]{1,0:T(8,128)(2,1)S(1)}, bf16[192,128]{1,0:T(8,128)(2,1)}, u32[]{:S(2)}) copy-start(bf16[192,128]{1,0:T(8,128)(2,1)} %param.15) | copy-start | bytes 147460
  6.5 26.4 %copy-start.4 = (bf16[192,128]{1,0:T(8,128)(2,1)S(1)}, bf16[192,128]{1,0:T(8,128)(2,1)}, u32[]{:S(2)}) copy-start(bf16[192,128]{1,0:T(8,128)(2,1)} %param.16) | copy-start | bytes 147460
  6.5 46.0 %copy-start.7 = (f32[704]{0:T(1024)S(1)}, f32[704]{0:T(1024)}, u32[]{:S(2)}) copy-start(f32[704]{0:T(1024)} %param.24) | copy-start | bytes 8452
  6.5 46.1 %copy-start.5 = (f32[3,704]{1,0:T(4,128)S(1)}, f32[3,704]{1,0:T(4,128)}, u32[]{:S(2)}) copy-start(f32[3,704]{1,0:T(4,128)} %param.23) | copy-start | bytes 25348
  6.5 153.3 %all-gather.2.cloned.1.call-start = ((), (), s32[]{:S(2)}) async-start(), calls=%async_computation.3 | async-start | bytes 5013504 | tf_op jit(solution)/shard_map/all_gather | solution.py:171
  21.6 10.5 %collective-permute-start.13 = (bf16[128,1152]{1,0:T(8,128)(2,1)S(1)}, bf16[128,1152]{1,0:T(8,128)(2,1)S(1)}, u32[]{:S(2)}, u32[]{:S(2)}) collective-permute-start(bf16[128,1152]{1,0:T(8,128)(2,1)S(1)} %broadcast_select_fusion), channel_id=1, source_target_pairs={{0,1},{9,8},{2,3},{11,10},{4,5},{13,12},{6,7},{15,14},{16,17},{25,... | collective-permute-start | bytes 884744 | tf_op jit(solution)/shard_map/ppermute | solution.py:169
  32.9 70.9 %copy-start = (bf16[192,256]{1,0:T(8,128)(2,1)}, bf16[192,256]{1,0:T(8,128)(2,1)S(1)}, u32[]{:S(2)}) copy-start(bf16[192,256]{1,0:T(8,128)(2,1)S(1)} %constant_dynamic-update-slice_fusion.own_ref) | copy-start | bytes 294916
  32.9 19.7 %collective-permute-start.2 = (bf16[192,256]{1,0:T(8,128)(2,1)S(1)}, bf16[192,256]{1,0:T(8,128)(2,1)S(1)}, u32[]{:S(2)}, u32[]{:S(2)}) collective-permute-start(bf16[192,256]{1,0:T(8,128)(2,1)S(1)} %constant_dynamic-update-slice_fusion.own_ref), channel_id=1, source_target_pairs={{0,384},{32,416},{64,448},{96,480},{128,0},{160,32},{192,64},{224,... | collective-permute-start | bytes 294920 | tf_op jit(solution)/shard_map/ppermute | solution.py:29
  40.4 14.7 %collective-permute-start.1 = (bf16[192,256]{1,0:T(8,128)(2,1)S(1)}, bf16[192,256]{1,0:T(8,128)(2,1)S(1)}, u32[]{:S(2)}, u32[]{:S(2)}) collective-permute-start(bf16[192,256]{1,0:T(8,128)(2,1)S(1)} %constant_dynamic-update-slice_fusion.own_ref), channel_id=1, source_target_pairs={{0,256},{32,288},{64,320},{96,352},{128,384},{160,416},{192,448},{... | collective-permute-start | bytes 294920 | tf_op jit(solution)/shard_map/ppermute | solution.py:29
  45.3 18.1 %collective-permute-start = (bf16[192,256]{1,0:T(8,128)(2,1)S(1)}, bf16[192,256]{1,0:T(8,128)(2,1)S(1)}, u32[]{:S(2)}, u32[]{:S(2)}) collective-permute-start(bf16[192,256]{1,0:T(8,128)(2,1)S(1)} %constant_dynamic-update-slice_fusion.own_ref), channel_id=1, source_target_pairs={{0,128},{32,160},{64,192},{96,224},{128,256},{160,288},{192,320},{... | collective-permute-start | bytes 294920 | tf_op jit(solution)/shard_map/ppermute | solution.py:29
  63.5 40.3 %collective-permute-start.4 = (bf16[768,256]{1,0:T(8,128)(2,1)S(1)}, bf16[768,256]{1,0:T(8,128)(2,1)S(1)}, u32[]{:S(2)}, u32[]{:S(2)}) collective-permute-start(bf16[768,256]{1,0:T(8,128)(2,1)S(1)} %get-tuple-element.11), channel_id=1, source_target_pairs={{0,32},{32,64},{64,96},{96,128},{128,160},{160,192},{192,224},{224... | collective-permute-start | bytes 1179656 | tf_op jit(solution)/shard_map/ppermute | solution.py:29
  69.5 34.3 %collective-permute-start.7 = (bf16[768,256]{1,0:T(8,128)(2,1)S(1)}, bf16[768,256]{1,0:T(8,128)(2,1)S(1)}, u32[]{:S(2)}, u32[]{:S(2)}) collective-permute-start(bf16[768,256]{1,0:T(8,128)(2,1)S(1)} %get-tuple-element.37), channel_id=1, source_target_pairs={{0,480},{32,0},{64,32},{96,64},{128,96},{160,128},{192,160},{224,1... | collective-permute-start | bytes 1179656 | tf_op jit(solution)/shard_map/ppermute | solution.py:29
  75.1 27.8 %collective-permute-start.6 = (bf16[384,256]{1,0:T(8,128)(2,1)S(1)}, bf16[384,256]{1,0:T(8,128)(2,1)S(1)}, u32[]{:S(2)}, u32[]{:S(2)}) collective-permute-start(bf16[384,256]{1,0:T(8,128)(2,1)S(1)} %pad_maximum_fusion.3), channel_id=1, source_target_pairs={{0,448},{32,480},{64,0},{96,32},{128,64},{160,96},{192,128},{224,1... | collective-permute-start | bytes 589832 | tf_op jit(solution)/shard_map/ppermute | solution.py:29
  78.2 24.8 %collective-permute-start.5 = (bf16[384,256]{1,0:T(8,128)(2,1)S(1)}, bf16[384,256]{1,0:T(8,128)(2,1)S(1)}, u32[]{:S(2)}, u32[]{:S(2)}) collective-permute-start(bf16[384,256]{1,0:T(8,128)(2,1)S(1)} %slice.172), channel_id=1, source_target_pairs={{0,64},{32,96},{64,128},{96,160},{128,192},{160,224},{192,256},{22... | collective-permute-start | bytes 589832 | tf_op jit(solution)/shard_map/ppermute | solution.py:29
  103.8 0.8 copy-start.1
  104.5 0.7 copy-start.2
  117.3 13.2 %all-to-all-start = ((bf16[4,192,384]{2,1,0:T(8,128)(2,1)}), bf16[4,192,384]{2,1,0:T(8,128)(2,1)S(1)}, u32[]{:S(2)}, u32[]{:S(2)}) async-start(bf16[4,192,384]{2,1,0:T(8,128)(2,1)} %bitcast.12), calls=%async_computation | async-start | bytes 1179648 | tf_op jit(solution)/shard_map/all_to_all | solution.py:196
  122.4 16.6 %collective-permute-start.9 = (bf16[128,2048]{1,0:T(8,128)(2,1)}, bf16[128,2048]{1,0:T(8,128)(2,1)S(1)}, u32[]{:S(2)}, u32[]{:S(2)}) collective-permute-start(bf16[128,2048]{1,0:T(8,128)(2,1)} %param.19), channel_id=1, source_target_pairs={{0,0},{1,8},{8,1},{9,9},{2,2},{3,10},{10,3},{11,11},{4,4},{5,12},{... | collective-permute-start | bytes 1572872 | tf_op jit(solution)/shard_map/ppermute | solution.py:33
  130.6 2.0 copy-start.8
  131.3 14.9 %copy-start.9 = (bf16[24,2048]{1,0:T(8,128)(2,1)S(1)}, bf16[24,2048]{1,0:T(8,128)(2,1)}, u32[]{:S(2)}) copy-start(bf16[24,2048]{1,0:T(8,128)(2,1)} %param.13) | copy-start | bytes 294916
  132.0 27.6 %copy-start.6 = (f32[2048]{0:T(1024)S(1)}, f32[2048]{0:T(1024)}, u32[]{:S(2)}) copy-start(f32[2048]{0:T(1024)} %param.20) | copy-start | bytes 24580
  132.7 8.2 %collective-permute-start.8 = (bf16[192,128]{0,1:T(8,128)(2,1)S(1)}, bf16[192,128]{0,1:T(8,128)(2,1)S(1)}, u32[]{:S(2)}, u32[]{:S(2)}) collective-permute-start(bf16[192,128]{0,1:T(8,128)(2,1)S(1)} %multiply_convert_fusion.4), channel_id=1, source_target_pairs={{0,0},{1,8},{8,1},{9,9},{2,2},{3,10},{10,3},{11,11},{4,4},{5,12},{... | collective-permute-start | bytes 147464 | tf_op jit(solution)/shard_map/ppermute | solution.py:33
  142.2 14.5 %all-to-all-start.1 = ((bf16[8,24,2048]{2,1,0:T(8,128)(2,1)}), bf16[8,24,2048]{2,1,0:T(8,128)(2,1)S(1)}, u32[]{:S(2)}, u32[]{:S(2)}) async-start(bf16[8,24,2048]{2,1,0:T(8,128)(2,1)} %bitcast.5), calls=%async_computation.1 | async-start | bytes 1572864 | tf_op jit(solution)/shard_map/all_to_all | solution.py:126
  146.2 13.4 %collective-permute-start.3 = (bf16[24,2048]{1,0:T(8,128)(2,1)S(1)}, bf16[24,2048]{1,0:T(8,128)(2,1)S(1)}, u32[]{:S(2)}, u32[]{:S(2)}) collective-permute-start(bf16[24,2048]{1,0:T(8,128)(2,1)S(1)} %copy-done.9), channel_id=1, source_target_pairs={{0,0},{1,8},{8,1},{9,9},{2,2},{3,10},{10,3},{11,11},{4,4},{5,12},{... | collective-permute-start | bytes 294920 | tf_op jit(solution)/shard_map/ppermute | solution.py:33
  159.8 37.8 %collective-permute-start.14 = (bf16[2048,1152]{1,0:T(8,128)(2,1)}, bf16[2048,1152]{1,0:T(8,128)(2,1)}, u32[]{:S(2)}, u32[]{:S(2)}) collective-permute-start(bf16[2048,1152]{1,0:T(8,128)(2,1)} %all-gather.2.cloned.1.call-done), channel_id=1, source_target_pairs={{0,1},{1,0},{2,3},{3,2},{4,5},{5,4},{6,7},{7,6},{8,9},{9,8},{10,11... | collective-permute-start | bytes 14155784 | tf_op jit(solution)/shard_map/ppermute | solution.py:207
  161.8 5.0 %collective-permute-start.10 = (f32[4,704]{1,0:T(4,128)S(1)}, f32[4,704]{1,0:T(4,128)S(1)}, u32[]{:S(2)}, u32[]{:S(2)}) collective-permute-start(f32[4,704]{1,0:T(4,128)S(1)} %pad_maximum_fusion.9), channel_id=1, source_target_pairs={{0,0},{1,8},{8,1},{9,9},{2,2},{3,10},{10,3},{11,11},{4,4},{5,12},{... | collective-permute-start | bytes 33800 | tf_op jit(solution)/shard_map/ppermute | solution.py:33
  166.9 6.5 %collective-permute-start.11 = (bf16[24,2048]{1,0:T(8,128)(2,1)S(1)}, bf16[24,2048]{1,0:T(8,128)(2,1)S(1)}, u32[]{:S(2)}, u32[]{:S(2)}) collective-permute-start(bf16[24,2048]{1,0:T(8,128)(2,1)S(1)} %fusion.22), channel_id=1, source_target_pairs={{0,8},{8,0},{1,9},{9,1},{2,10},{10,2},{3,11},{11,3},{4,12},{12,4},... | collective-permute-start | bytes 294920 | tf_op jit(solution)/shard_map/ppermute | solution.py:208
  184.4 8.2 %collective-permute-start.12 = (bf16[8,2048]{1,0:T(8,128)(2,1)S(1)}, bf16[8,2048]{1,0:T(8,128)(2,1)S(1)}, u32[]{:S(2)}, u32[]{:S(2)}) collective-permute-start(bf16[8,2048]{1,0:T(8,128)(2,1)S(1)} %slice.223), channel_id=1, source_target_pairs={{0,1},{1,16},{16,17},{17,32},{32,33},{33,48},{48,49},{49,64},{64,6... | collective-permute-start | bytes 98312 | tf_op jit(solution)/shard_map/ppermute | solution.py:215
  216.6 5.9 %collective-permute-start.15 = (bf16[24,2048]{1,0:T(8,128)(2,1)S(1)}, bf16[24,2048]{1,0:T(8,128)(2,1)S(1)}, u32[]{:S(2)}, u32[]{:S(2)}) collective-permute-start(bf16[24,2048]{1,0:T(8,128)(2,1)S(1)} %fusion.23), channel_id=1, source_target_pairs={{0,0},{1,8},{8,1},{9,9},{2,2},{3,10},{10,3},{11,11},{4,4},{5,12},{... | collective-permute-start | bytes 294920 | tf_op jit(solution)/shard_map/ppermute | solution.py:33
Sparse Core Ops, SparseCore 0:
  33.0 98.7 all-gather.1

commit v5 on v2

v5 whole, which is shorter than its diff:
```python
import jax
import jax.numpy as jnp
from jax import lax
from jax.experimental import pallas as pl
from jax.experimental.pallas import tpu as pltpu
from jax.sharding import Mesh
from jax.sharding import PartitionSpec as P

HD = 64
VD = 128
SP = ("z", "y")
SP_TP = ("z", "y", "tp")
NZ = 16
NY = 4
eps = 1e-05
neg_fill = -1e30
TILE = 128
LANES = 128
EARLY = ((5, 11), (1, 6, 12), (15, 4, 10))
LATE = ((8,), (2, 7, 13), (14, 3, 9))

VMEM = pl.BlockSpec(memory_space=pltpu.VMEM)
SMEM = pl.BlockSpec(memory_space=pltpu.SMEM)


def shifted(value, axis, steps):
    count = lax.axis_size(axis)
    return lax.ppermute(value, axis, [(i, (i + steps) % count) for i in range(count)])


def dot_nt(a, b):
    return lax.dot_general(a, b, (((1,), (1,)), ((), ())), preferred_element_type=jnp.float32)


def row_bias(offsets, rows, z):
    lane = lax.broadcasted_iota(jnp.int32, (1, rows * len(offsets)), 1)
    bias = jnp.zeros(lane.shape, jnp.float32)
    for i, off in enumerate(offsets):
        inside = jnp.logical_and(lane >= i * rows, lane < (i + 1) * rows)
        bias = jnp.where(jnp.logical_and(inside, off > z), neg_fill, bias)
    return bias


def both_maps(q):
    lane = lax.broadcasted_iota(jnp.int32, q.shape, 1)
    q = q * jnp.bfloat16(HD**-0.5)
    zero = jnp.zeros_like(q)
    return jnp.concatenate((jnp.where(lane < HD, q, zero), jnp.where(lane < HD, zero, q)), axis=0)


def softmax_step(scores, refs, top, total, acc):
    new_top = top
    for s in scores:
        new_top = jnp.maximum(new_top, jnp.max(s, axis=1, keepdims=True))
    keep = jnp.exp(top - new_top)
    total = total * keep
    acc = acc * keep
    for s, ref in zip(scores, refs):
        e = jnp.exp(s - new_top)
        total = total + jnp.sum(e, axis=1, keepdims=True)
        acc = acc + jnp.dot(
            e.astype(jnp.bfloat16), ref[:, 2 * HD :], preferred_element_type=jnp.float32
        )
    return new_top, total, acc


def packed(columns):
    lane = lax.broadcasted_iota(jnp.int32, (TILE, VD), 1)
    block = jnp.zeros((TILE, VD), jnp.float32)
    for m in range(2):
        for i, v in enumerate(columns):
            column = v[m * TILE : (m + 1) * TILE]
            block = jnp.where(lane == m * len(columns) + i, column, block)
    return block


def early_kernel(where_ref, rows_ref, held_ref, n1_ref, m1_ref, state_ref, q_ref):
    z = where_ref[0]
    y = where_ref[1]
    rows = held_ref.shape[0] // 3
    own_ref, far_ref = held_ref.at[0:rows], held_ref.at[rows:]
    w_rows = rows_ref.shape[0] // NY
    for i in range(NY * rows // w_rows):
        y_at, lane_at = divmod(i, rows // w_rows)
        q_ref[i * w_rows : (i + 1) * w_rows, :] = rows_ref[
            y_at * w_rows : (y_at + 1) * w_rows, lane_at * 2 * HD : (lane_at + 1) * 2 * HD
        ]
    refs = (far_ref, n1_ref, m1_ref)
    biases = [row_bias(offsets, rows, z) for offsets in EARLY]

    @pl.loop(0, NY * rows // TILE)
    def _(t):
        at = pl.multiple_of(t * TILE, TILE)
        q2 = both_maps(q_ref[pl.ds(at, TILE), :])
        s_own = dot_nt(q2, own_ref[:, : 2 * HD])
        r = lax.broadcasted_iota(jnp.int32, s_own.shape, 0)
        r = jnp.where(r >= TILE, r - TILE, r) + at
        k = lax.broadcasted_iota(jnp.int32, s_own.shape, 1) + y * rows
        s_own = jnp.where(k <= r, s_own, neg_fill)
        scores = [s_own] + [dot_nt(q2, ref[:, : 2 * HD]) + b for ref, b in zip(refs, biases)]
        top = jnp.full((2 * TILE, 1), neg_fill, jnp.float32)
        zero = jnp.zeros((2 * TILE, 1), jnp.float32)
        acc = jnp.zeros((2 * TILE, VD), jnp.float32)
        top, total, acc = softmax_step(scores, (own_ref, *refs), top, zero, acc)
        state_ref[pl.ds(at, TILE), 0:VD] = acc[:TILE]
        state_ref[pl.ds(at, TILE), VD : 2 * VD] = acc[TILE:]
        state_ref[pl.ds(at, TILE), 2 * VD : 3 * VD] = packed((top, total))


def late_kernel(where_ref, q_ref, state_ref, e8_ref, n2_ref, m2_ref, out_ref):
    z = where_ref[0]
    refs = (e8_ref, n2_ref, m2_ref)
    rows = e8_ref.shape[0]
    biases = [row_bias(offsets, rows, z) for offsets in LATE]

    @pl.loop(0, NY * rows // TILE)
    def _(t):
        at = pl.multiple_of(t * TILE, TILE)
        q2 = both_maps(q_ref[pl.ds(at, TILE), :])
        scores = [dot_nt(q2, ref[:, : 2 * HD]) + b for ref, b in zip(refs, biases)]
        stat = state_ref[pl.ds(at, TILE), 2 * VD : 3 * VD]
        top = jnp.concatenate((stat[:, 0:1], stat[:, 2:3]), axis=0)
        total = jnp.concatenate((stat[:, 1:2], stat[:, 3:4]), axis=0)
        acc = jnp.concatenate(
            (state_ref[pl.ds(at, TILE), 0:VD], state_ref[pl.ds(at, TILE), VD : 2 * VD]), axis=0
        )
        top, total, acc = softmax_step(scores, refs, top, total, acc)
        mean = acc / total
        lse = top + jnp.log(total)
        hi = lse.astype(jnp.bfloat16).astype(jnp.float32)
        mid = (lse - hi).astype(jnp.bfloat16).astype(jnp.float32)
        out_ref[pl.ds(at, TILE), 0:VD] = mean[:TILE].astype(jnp.bfloat16)
        out_ref[pl.ds(at, TILE), VD : 2 * VD] = mean[TILE:].astype(jnp.bfloat16)
        out_ref[pl.ds(at, TILE), 2 * VD : 3 * VD] = packed((hi, mid, lse - hi - mid)).astype(
            jnp.bfloat16
        )


def merged(got):
    got = got.astype(jnp.float32)
    means = []
    for m in range(2):
        stat = got[:, :, 2 * VD + 3 * m : 2 * VD + 3 * m + 3]
        lse = stat[..., 0:1] + stat[..., 1:2] + stat[..., 2:3]
        share = jnp.exp(lse - jnp.max(lse, axis=0, keepdims=True))
        acc = jnp.sum(share * got[:, :, m * VD : (m + 1) * VD], axis=0)
        means.append(acc / jnp.sum(share, axis=0))
    return means


def normalize(rows_in, gain):
    values_f = rows_in.astype(jnp.float32)
    scale_inv = lax.rsqrt(jnp.mean(values_f * values_f, axis=-1, keepdims=True) + eps)
    return (values_f * scale_inv * gain).astype(jnp.bfloat16)


def summed_over_tp(shard):
    count = lax.axis_size("tp")
    cut = shard.reshape(count, shard.shape[0] // count, shard.shape[1])
    tiles = lax.all_to_all(cut, "tp", 0, 0, tiled=True)
    return jnp.sum(tiles.astype(jnp.float32), axis=0).astype(jnp.bfloat16)


def local(
    residual,
    queries,
    key_pairs,
    values,
    second_weight,
    head_gain,
    out_weight,
    norm_gain,
    up_weight,
    gate_weight,
    conv_weight,
    conv_bias,
    down_weight,
):
    rows = queries.shape[0]
    ff = up_weight.shape[1]
    where = jnp.stack((lax.axis_index("z"), lax.axis_index("y"))).astype(jnp.int32)
    w_rows = up_weight.shape[0]
    width = 2 * ff + ff
    tail = -width % LANES
    cuts = [up_weight, gate_weight, down_weight.T, jnp.zeros((w_rows, tail), jnp.bfloat16)]
    cuts += [queries[i : i + w_rows] for i in range(0, rows, w_rows)]
    row_w = lax.all_gather(jnp.concatenate(cuts, axis=1), "y", axis=0, tiled=True)
    all_w = lax.all_gather(row_w[:, :width], "z", axis=0, tiled=True)
    q_rows = row_w[:, width + tail :]

    kv = jnp.concatenate((key_pairs, values), axis=1)
    f5, f11 = shifted(kv, "z", 5), shifted(kv, "z", -5)
    held = jnp.concatenate((kv, f5, f11), axis=0)
    n1 = shifted(held, "z", 1)
    m1 = shifted(held, "z", -1)
    e8 = shifted(f5, "z", 3)
    n2 = shifted(n1, "z", 1)
    m2 = shifted(m1, "z", -1)
    state, q_all = pl.pallas_call(
        early_kernel,
        out_shape=[
            jax.ShapeDtypeStruct((NY * rows, 3 * VD), jnp.float32),
            jax.ShapeDtypeStruct((NY * rows, 2 * HD), jnp.bfloat16),
        ],
        in_specs=[SMEM] + [VMEM] * 4,
        out_specs=[VMEM] * 2,
        name="early",
    )(where, q_rows, held, n1, m1)
    parts = pl.pallas_call(
        late_kernel,
        out_shape=jax.ShapeDtypeStruct((NY * rows, 3 * VD), jnp.bfloat16),
        in_specs=[SMEM] + [VMEM] * 5,
        out_specs=VMEM,
        name="late",
    )(where, q_all, state, e8, n2, m2)
    got = lax.all_to_all(parts.reshape(NY, rows, 3 * VD), "y", 0, 0, tiled=True)
    means = merged(got)
    diff = means[0] - second_weight[0] * means[1]
    scale_inv = lax.rsqrt(jnp.mean(diff * diff, axis=-1, keepdims=True) + eps)
    attended = (diff * scale_inv * head_gain * 0.8).astype(jnp.bfloat16)
    proj = summed_over_tp(
        jnp.dot(attended, out_weight, preferred_element_type=jnp.float32).astype(jnp.bfloat16)
    )
    mid = (residual.astype(jnp.float32) + proj.astype(jnp.float32)).astype(jnp.bfloat16)
    normed_all = lax.all_gather(normalize(mid, norm_gain), "tp", axis=0, tiled=True)
    count = lax.axis_size("z") * lax.axis_size("y")
    rim_rows = lax.ppermute(normed_all[rows - 8 :], SP, [(i, i + 1) for i in range(count - 1)])
    both = jnp.dot(
        jnp.concatenate((normed_all, rim_rows), axis=0),
        all_w[:, : 2 * ff],
        preferred_element_type=jnp.float32,
    ).astype(jnp.bfloat16)
    up_proj, gate_proj = both[:rows, :ff], both[:rows, ff:]
    taps = conv_weight.shape[0]
    extended = jnp.concatenate((both[rows + 8 - (taps - 1) :, :ff], up_proj), axis=0)
    conv_out = jnp.zeros((rows, ff), jnp.float32) + conv_bias[None, :]
    for tap in range(taps):
        conv_out = conv_out + conv_weight[tap][None, :] * extended[tap : tap + rows].astype(
            jnp.float32
        )
    hidden = (jax.nn.silu(conv_out) * gate_proj.astype(jnp.float32)).astype(jnp.bfloat16)
    ffn = dot_nt(hidden, all_w[:, 2 * ff : width]).astype(jnp.bfloat16)
    ffn_out = summed_over_tp(ffn)
    return (mid.astype(jnp.float32) + ffn_out.astype(jnp.float32)).astype(jnp.bfloat16)


def solution(mesh):
    finer = Mesh(mesh.devices.reshape(NZ, NY, mesh.shape["tp"]), ("z", "y", "tp"))
    in_specs = (
        P(SP_TP, None),
        P(SP, "tp"),
        P(SP, "tp"),
        P(SP, "tp"),
        P("tp"),
        P("tp"),
        P("tp", None),
        P(),
        P(SP, "tp"),
        P(SP, "tp"),
        P(None, "tp"),
        P("tp"),
        P("tp", SP),
    )
    out_specs = P(SP_TP, None)
    return jax.shard_map(local, mesh=finer, in_specs=in_specs, out_specs=out_specs, check_vma=False)
```

time: 200 us -> 191 us (0.955)
  blocking collectives: 74.9 us -> 66.7 us
  Pallas kernels: 12.1 us -> 17.8 us
  waiting for transfers between devices: 32.8 us -> 28.9 us
    all_gather x2 -> x1, blocking collectives: 23.8 us -> 12.1 us  [local(): lax.all_gather(jnp.concatenate(cuts, axis=1), 'y', axis=0, tiled=True)]
    pallas_call x1 -> x2, Pallas kernels: 12.1 us -> 17.8 us  [the longest x1 8.98 us: local(): pl.pallas_call(early_kernel, out_shape=[jax.ShapeDtypeStruct((NY * rows,...]
    all_to_all x2, blocking collectives: 36.9 us -> 40.4 us  [summed_over_tp(): tiles = lax.all_to_all(cut, 'tp', 0, 0, tiled=True)]
    slice x0 -> x3, local copies, waits for them, and re-layouts: none -> 2.39 us  [the longest x1 0.86 us: local(): all_w = lax.all_gather(row_w[:, :width], 'z', axis=0, tiled=True)]
  transfers between devices with their start and end apart: 10 -> 10, of which waited for: 6 -> 7; matrix products, arithmetic and copies ran while one was open for 3% -> 2% of each run, Pallas kernels for 6% -> 9%
where the time goes in v5:
time: 191 us
  blocking collectives  66.7 us (35%)
  starting transfers between devices  46.9 us (25%)
  waiting for transfers between devices  28.9 us (15%)
  Pallas kernels  17.8 us (9%)
  between operations  14.4 us (8%)
  matrix products  7.76 us (4%)
  local copies, waits for them, and re-layouts  4.5 us (2%)
  other arithmetic  3.52 us (2%)
    ppermute x7, starting transfers between devices, shifted(): lax.ppermute(value, axis, [(i, (i + steps) % count) for i in range(count)])  41.3 us
    all_to_all x2, blocking collectives, summed_over_tp(): tiles = lax.all_to_all(cut, 'tp', 0, 0, tiled=True)  40.4 us
    ppermute x7, waiting for transfers between devices, shifted(): lax.ppermute(value, axis, [(i, (i + steps) % count) for i in range(count)])  20.3 us
    all_gather x1, blocking collectives, local(): lax.all_gather(normalize(mid, norm_gain), 'tp', axis=0, tiled=True)  14.2 us
    all_gather x1, blocking collectives, local(): lax.all_gather(jnp.concatenate(cuts, axis=1), 'y', axis=0, tiled=True)  12.1 us
    pallas_call x1, Pallas kernels, local(): pl.pallas_call(early_kernel, out_shape=[jax.ShapeDtypeStruct((NY * rows,...  8.98 us
    pallas_call x1, Pallas kernels, local(): pl.pallas_call(late_kernel, out_shape=jax.ShapeDtypeStruct((NY * rows, 3...  8.79 us
    all_to_all x1, waiting for transfers between devices, local(): got = lax.all_to_all(parts.reshape(NY, rows, 3 * VD), 'y', 0, 0, tiled=True)  6.66 us
  transfers between devices with their start and end apart: 10, of which 7 were waited for; matrix products, arithmetic and copies ran while one was open for 2% of the time, Pallas kernels for 9%

profile of v5, /device:TPU:1, one launch (start us, length us, event | category | flops | bytes accessed | tf_op | source)
XLA Modules:
  0.0 190.5 jit_solution(4572254861392517258)
XLA Ops:
  6.5 0.0 copy-start
  6.5 0.0 all-gather.2.cloned.1.call-start
  6.5 0.8 fusion.40
  7.4 1.0 concatenate.15
  8.4 12.1 %all_gather.9 = bf16[128,2944]{1,0:T(8,128)(2,1)S(1)} all-gather(bf16[32,2944]{1,0:T(8,128)(2,1)S(1)} %concatenate.15), channel_id=1, replica_groups=mesh['z'=16,'y'=4,'tp'=8] {'y'}, dimensions={0}, use_global_device_ids=true | all-gather | bytes 942080 | tf_op jit(solution)/shard_map/all_gather | solution.py:187
  20.5 0.9 slice.126
  21.3 0.0 all-gather.2.cloned.1.call-update
  21.4 0.0 copy-done.8
  21.4 0.0 copy-done.9
  21.4 11.2 %collective-permute-start = (bf16[192,256]{1,0:T(8,128)(2,1)S(1)}, bf16[192,256]{1,0:T(8,128)(2,1)S(1)}, u32[]{:S(2)}, u32[]{:S(2)}) collective-permute-start(bf16[192,256]{1,0:T(8,128)(2,1)S(1)} %constant_dynamic-update-slice_fusion), channel_id=1, source_target_pairs={{0,160},{32,192},{64,224},{96,256},{128,288},{160,320},{192,352},{... | collective-permute-start | bytes 294920 | tf_op jit(solution)/shard_map/ppermute | solution.py:28
  32.6 5.9 %collective-permute-start.1 = (bf16[192,256]{1,0:T(8,128)(2,1)S(1)}, bf16[192,256]{1,0:T(8,128)(2,1)S(1)}, u32[]{:S(2)}, u32[]{:S(2)}) collective-permute-start(bf16[192,256]{1,0:T(8,128)(2,1)S(1)} %constant_dynamic-update-slice_fusion), channel_id=1, source_target_pairs={{0,352},{32,384},{64,416},{96,448},{128,480},{160,0},{192,32},{224... | collective-permute-start | bytes 294920 | tf_op jit(solution)/shard_map/ppermute | solution.py:28
  38.5 0.3 collective-permute-done
  38.7 6.6 %collective-permute-done.1 = bf16[192,256]{1,0:T(8,128)(2,1)S(1)} collective-permute-done((bf16[192,256]{1,0:T(8,128)(2,1)S(1)}, bf16[192,256]{1,0:T(8,128)(2,1)S(1)}, u32[]{:S(2)}, u32[]{:S(2)}) %collective-permute-start.1) | collective-permute-done | bytes 98336 | tf_op jit(solution)/shard_map/ppermute | solution.py:28
  45.3 0.0 copy-start.1
  45.3 1.9 %collective-permute-start.2 = (bf16[576,256]{1,0:T(8,128)(2,1)S(1)}, bf16[576,256]{1,0:T(8,128)(2,1)S(1)}, u32[]{:S(2)}, u32[]{:S(2)}) collective-permute-start(bf16[576,256]{1,0:T(8,128)(2,1)S(1)} %pad_maximum_fusion.2.held_ref), channel_id=1, source_target_pairs={{0,32},{32,64},{64,96},{96,128},{128,160},{160,192},{192,224},{224... | collective-permute-start | bytes 884744 | tf_op jit(solution)/shard_map/ppermute | solution.py:28
  47.3 8.0 %collective-permute-start.3 = (bf16[576,256]{1,0:T(8,128)(2,1)S(1)}, bf16[576,256]{1,0:T(8,128)(2,1)S(1)}, u32[]{:S(2)}, u32[]{:S(2)}) collective-permute-start(bf16[576,256]{1,0:T(8,128)(2,1)S(1)} %pad_maximum_fusion.2.held_ref), channel_id=1, source_target_pairs={{0,480},{32,0},{64,32},{96,64},{128,96},{160,128},{192,160},{224,1... | collective-permute-start | bytes 884744 | tf_op jit(solution)/shard_map/ppermute | solution.py:28
  55.3 11.8 %collective-permute-done.2.n1_ref = bf16[576,256]{1,0:T(8,128)(2,1)S(1)} collective-permute-done((bf16[576,256]{1,0:T(8,128)(2,1)S(1)}, bf16[576,256]{1,0:T(8,128)(2,1)S(1)}, u32[]{:S(2)}, u32[]{:S(2)}) %collective-permute-start.2) | collective-permute-done | bytes 294944 | tf_op jit(solution)/shard_map/ppermute | solution.py:28
  67.0 1.9 %collective-permute-start.5 = (bf16[576,256]{1,0:T(8,128)(2,1)S(1)}, bf16[576,256]{1,0:T(8,128)(2,1)S(1)}, u32[]{:S(2)}, u32[]{:S(2)}) collective-permute-start(bf16[576,256]{1,0:T(8,128)(2,1)S(1)} %collective-permute-done.2.n1_ref), channel_id=1, source_target_pairs={{0,32},{32,64},{64,96},{96,128},{128,160},{160,192},{192,224},{224... | collective-permute-start | bytes 884744 | tf_op jit(solution)/shard_map/ppermute | solution.py:28
  69.0 0.0 collective-permute-done.3.m1_ref
  69.0 0.0 copy-start.4
  69.0 5.2 %collective-permute-start.6 = (bf16[576,256]{1,0:T(8,128)(2,1)S(1)}, bf16[576,256]{1,0:T(8,128)(2,1)S(1)}, u32[]{:S(2)}, u32[]{:S(2)}) collective-permute-start(bf16[576,256]{1,0:T(8,128)(2,1)S(1)} %collective-permute-done.3.m1_ref), channel_id=1, source_target_pairs={{0,480},{32,0},{64,32},{96,64},{128,96},{160,128},{192,160},{224,1... | collective-permute-start | bytes 884744 | tf_op jit(solution)/shard_map/ppermute | solution.py:28
  74.2 0.7 slice.116.rows_ref
  74.9 7.1 %collective-permute-start.4 = (bf16[192,256]{1,0:T(8,128)(2,1)S(1)}, bf16[192,256]{1,0:T(8,128)(2,1)S(1)}, u32[]{:S(2)}, u32[]{:S(2)}) collective-permute-start(bf16[192,256]{1,0:T(8,128)(2,1)S(1)} %collective-permute-done), channel_id=1, source_target_pairs={{0,96},{32,128},{64,160},{96,192},{128,224},{160,256},{192,288},{2... | collective-permute-start | bytes 294920 | tf_op jit(solution)/shard_map/ppermute | solution.py:28
  82.1 0.7 pad_add_fusion.where_ref
  82.7 0.0 copy-done.1
  82.7 0.0 copy-done.3
  82.7 0.0 copy-done.4
  82.7 9.0 %early.1 = (f32[768,384]{1,0:T(8,128)}, bf16[768,128]{1,0:T(8,128)(2,1)}) custom-call(s32[2]{0:T(128)} %pad_add_fusion.where_ref, bf16[128,768]{1,0:T(8,128)(2,1)} %slice.116.rows_ref, bf16[576,256]{1,0:T(8,128)(2,1)} %copy-done.1, bf16[576,256]{1,0:T(8,128)(2,1)} %copy-done.3, bf16[576,256]{1,0:T(8,128)(2,1)} %copy-done.4), custom_call_target="tpu_custom_call" | custom-call | tf_op jit(solution)/shard_map/early/pallas_call | solution.py:199
  91.7 1.7 collective-permute-done.4.e8_ref
  93.5 0.0 collective-permute-done.5.n2_ref
  93.5 0.0 collective-permute-done.6.m2_ref
  93.5 0.0 copy-start.6
  93.5 0.6 copy-done.7
  94.1 0.1 copy-done.5
  94.2 0.1 copy-done.6
  94.3 8.8 %late.1 = bf16[768,384]{1,0:T(8,128)(2,1)} custom-call(s32[2]{0:T(128)} %pad_add_fusion.where_ref, bf16[768,128]{1,0:T(8,128)(2,1)} %get-tuple-element.7.q_ref, f32[768,384]{1,0:T(8,128)} %get-tuple-element.8.state_ref, bf16[192,256]{1,0:T(8,128)(2,1)} %copy-done.7, bf16[576,256]{1,0:T(8,128)(2,1)} %copy-done.5, bf16[576,256]{1,0:T(8,128)(2,1)} %copy-done.6), custom_call_target="tpu_custom_call" | custom-call | tf_op jit(solution)/shard_map/late/pallas_call | solution.py:209
  103.1 3.5 %all-to-all-start = ((bf16[4,192,384]{2,1,0:T(8,128)(2,1)}), bf16[4,192,384]{2,1,0:T(8,128)(2,1)S(1)}, u32[]{:S(2)}, u32[]{:S(2)}) async-start(bf16[4,192,384]{2,1,0:T(8,128)(2,1)} %bitcast.10), calls=%async_computation | async-start | bytes 1179648 | tf_op jit(solution)/shard_map/all_to_all | solution.py:216
  107.2 6.7 %all-to-all-done = bf16[4,192,384]{2,1,0:T(8,128)(2,1)S(1)} async-done(((bf16[4,192,384]{2,1,0:T(8,128)(2,1)}), bf16[4,192,384]{2,1,0:T(8,128)(2,1)S(1)}, u32[]{:S(2)}, u32[]{:S(2)}) %all-to-all-start) | async-done | bytes 589856 | tf_op jit(solution)/shard_map/all_to_all | solution.py:216
  113.9 0.1 convert_element_type.57
  114.0 0.7 fusion.38
  114.7 0.6 fusion.15
  115.2 0.3 fusion.14
  115.5 0.1 copy.17
  115.6 0.1 copy.18
  115.7 0.1 multiply_reduce_fusion
  115.8 0.0 copy-done
  115.8 0.0 copy-start.2
  115.8 0.5 convolution_convert_fusion
  116.3 0.0 copy-start.10
  116.3 0.0 copy-start.11
  116.3 23.4 %all_to_all.15 = bf16[8,24,2048]{2,1,0:T(8,128)(2,1)S(1)} all-to-all(bf16[8,24,2048]{2,1,0:T(8,128)(2,1)S(1)} %bitcast.9), channel_id=1, replica_groups=mesh['z'=16,'y'=4,'tp'=8] {'tp'}, dimensions={0} | all-to-all | bytes 1572864 | tf_op jit(solution)/shard_map/all_to_all | solution.py:160
  139.7 0.1 reduce_sum.83
  139.8 0.1 fusion.27
  140.0 0.1 fusion.29
  140.1 14.2 %all_gather.10 = bf16[192,2048]{1,0:T(8,128)(2,1)S(1)} all-gather(bf16[24,2048]{1,0:T(8,128)(2,1)S(1)} %fusion.29), channel_id=1, replica_groups=mesh['z'=16,'y'=4,'tp'=8] {'tp'}, dimensions={0}, use_global_device_ids=true | all-gather | bytes 884736 | tf_op jit(solution)/shard_map/all_gather | solution.py:225
  154.3 2.2 %collective-permute-start.7 = (bf16[8,2048]{1,0:T(8,128)(2,1)S(1)}, bf16[8,2048]{1,0:T(8,128)(2,1)S(1)}, u32[]{:S(2)}, u32[]{:S(2)}) collective-permute-start(bf16[8,2048]{1,0:T(8,128)(2,1)S(1)} %slice.125), channel_id=1, source_target_pairs={{0,8},{8,16},{16,24},{24,32},{32,40},{40,48},{48,56},{56,64},{64,7... | collective-permute-start | bytes 98312 | tf_op jit(solution)/shard_map/ppermute | solution.py:227
  156.5 0.0 copy-start.13
  156.6 0.9 collective-permute-done.7
  157.5 1.0 all-gather.2.cloned.1.call-done
  158.5 4.1 %fusion.4 = bf16[200,1408]{1,0:T(8,128)(2,1)S(1)} fusion(bf16[2048,2112]{1,0:T(8,128)(2,1)} %all-gather.2.cloned.1.call-done, bf16[8,2048]{1,0:T(8,128)(2,1)S(1)} %collective-permute-done.7, bf16[192,2048]{1,0:T(8,128)(2,1)S(1)} %all_gather.10), kind=kOutput, calls=%fused_computation.4 | convolution fusion | flops 1155353600 | bytes 7149568 | tf_op jit(solution)/shard_map/dot_general | solution.py:228
  162.6 3.2 %fusion.7 = bf16[192,2048]{1,0:T(8,128)(2,1)S(1)} fusion(bf16[2048,2112]{1,0:T(8,128)(2,1)} %all-gather.2.cloned.1.call-done, bf16[192,704]{1,0:T(8,128)(2,1)S(1)} %slice.129, bf16[2,704]{1,0:T(2,128)(2,1)S(1)} %slice.128, bf16[200,1408]{1,0:T(8,128)(2,1)S(1)} %fusion.4, f32[704]{0:T(1024)S(1)} %get-tuple-element.16, f32[704]{0:T(1024)S(1)} %get-tuple-element.17, ...), kind=kOutput, calls=%fused_computation.5 | convolution fusion | flops 557015040 | bytes 4541440 | tf_op jit(solution)/shard_map/dot_general | solution.py:32
  165.9 17.0 %all_to_all.16 = bf16[8,24,2048]{2,1,0:T(8,128)(2,1)S(1)} all-to-all(bf16[8,24,2048]{2,1,0:T(8,128)(2,1)S(1)} %bitcast.11), channel_id=1, replica_groups=mesh['z'=16,'y'=4,'tp'=8] {'tp'}, dimensions={0} | all-to-all | bytes 1572864 | tf_op jit(solution)/shard_map/all_to_all | solution.py:160
  182.9 0.1 reduce_sum.85
  183.0 0.7 fusion.30
  (21 shorter events, 0.2 us)
Async XLA Ops:
  6.5 109.3 %copy-start = (bf16[128,2048]{1,0:T(8,128)(2,1)S(1)}, bf16[128,2048]{1,0:T(8,128)(2,1)}, u32[]{:S(2)}) copy-start(bf16[128,2048]{1,0:T(8,128)(2,1)} %param.19) | copy-start | bytes 1572868
  6.5 14.8 %copy-start.8 = (bf16[192,128]{1,0:T(8,128)(2,1)S(1)}, bf16[192,128]{1,0:T(8,128)(2,1)}, u32[]{:S(2)}) copy-start(bf16[192,128]{1,0:T(8,128)(2,1)} %param.15) | copy-start | bytes 147460
  6.5 14.8 %copy-start.9 = (bf16[192,128]{1,0:T(8,128)(2,1)S(1)}, bf16[192,128]{1,0:T(8,128)(2,1)}, u32[]{:S(2)}) copy-start(bf16[192,128]{1,0:T(8,128)(2,1)} %param.16) | copy-start | bytes 147460
  6.5 152.0 %all-gather.2.cloned.1.call-start = ((), (), s32[]{:S(2)}) async-start(), calls=%async_computation.3 | async-start | bytes 9469952 | tf_op jit(solution)/shard_map/all_gather | solution.py:188
  21.4 17.3 %collective-permute-start = (bf16[192,256]{1,0:T(8,128)(2,1)S(1)}, bf16[192,256]{1,0:T(8,128)(2,1)S(1)}, u32[]{:S(2)}, u32[]{:S(2)}) collective-permute-start(bf16[192,256]{1,0:T(8,128)(2,1)S(1)} %constant_dynamic-update-slice_fusion), channel_id=1, source_target_pairs={{0,160},{32,192},{64,224},{96,256},{128,288},{160,320},{192,352},{... | collective-permute-start | bytes 294920 | tf_op jit(solution)/shard_map/ppermute | solution.py:28
  32.6 12.7 %collective-permute-start.1 = (bf16[192,256]{1,0:T(8,128)(2,1)S(1)}, bf16[192,256]{1,0:T(8,128)(2,1)S(1)}, u32[]{:S(2)}, u32[]{:S(2)}) collective-permute-start(bf16[192,256]{1,0:T(8,128)(2,1)S(1)} %constant_dynamic-update-slice_fusion), channel_id=1, source_target_pairs={{0,352},{32,384},{64,416},{96,448},{128,480},{160,0},{192,32},{224... | collective-permute-start | bytes 294920 | tf_op jit(solution)/shard_map/ppermute | solution.py:28
  45.3 37.4 %copy-start.1 = (bf16[576,256]{1,0:T(8,128)(2,1)}, bf16[576,256]{1,0:T(8,128)(2,1)S(1)}, u32[]{:S(2)}) copy-start(bf16[576,256]{1,0:T(8,128)(2,1)S(1)} %pad_maximum_fusion.2.held_ref) | copy-start | bytes 884740
  45.3 21.7 %collective-permute-start.2 = (bf16[576,256]{1,0:T(8,128)(2,1)S(1)}, bf16[576,256]{1,0:T(8,128)(2,1)S(1)}, u32[]{:S(2)}, u32[]{:S(2)}) collective-permute-start(bf16[576,256]{1,0:T(8,128)(2,1)S(1)} %pad_maximum_fusion.2.held_ref), channel_id=1, source_target_pairs={{0,32},{32,64},{64,96},{96,128},{128,160},{160,192},{192,224},{224... | collective-permute-start | bytes 884744 | tf_op jit(solution)/shard_map/ppermute | solution.py:28
  47.3 21.7 %collective-permute-start.3 = (bf16[576,256]{1,0:T(8,128)(2,1)S(1)}, bf16[576,256]{1,0:T(8,128)(2,1)S(1)}, u32[]{:S(2)}, u32[]{:S(2)}) collective-permute-start(bf16[576,256]{1,0:T(8,128)(2,1)S(1)} %pad_maximum_fusion.2.held_ref), channel_id=1, source_target_pairs={{0,480},{32,0},{64,32},{96,64},{128,96},{160,128},{192,160},{224,1... | collective-permute-start | bytes 884744 | tf_op jit(solution)/shard_map/ppermute | solution.py:28
  67.0 15.7 %copy-start.3 = (bf16[576,256]{1,0:T(8,128)(2,1)}, bf16[576,256]{1,0:T(8,128)(2,1)S(1)}, u32[]{:S(2)}) copy-start(bf16[576,256]{1,0:T(8,128)(2,1)S(1)} %collective-permute-done.2.n1_ref) | copy-start | bytes 884740
  67.0 26.4 %collective-permute-start.5 = (bf16[576,256]{1,0:T(8,128)(2,1)S(1)}, bf16[576,256]{1,0:T(8,128)(2,1)S(1)}, u32[]{:S(2)}, u32[]{:S(2)}) collective-permute-start(bf16[576,256]{1,0:T(8,128)(2,1)S(1)} %collective-permute-done.2.n1_ref), channel_id=1, source_target_pairs={{0,32},{32,64},{64,96},{96,128},{128,160},{160,192},{192,224},{224... | collective-permute-start | bytes 884744 | tf_op jit(solution)/shard_map/ppermute | solution.py:28
  69.0 13.8 %copy-start.4 = (bf16[576,256]{1,0:T(8,128)(2,1)}, bf16[576,256]{1,0:T(8,128)(2,1)S(1)}, u32[]{:S(2)}) copy-start(bf16[576,256]{1,0:T(8,128)(2,1)S(1)} %collective-permute-done.3.m1_ref) | copy-start | bytes 884740
  69.0 24.5 %collective-permute-start.6 = (bf16[576,256]{1,0:T(8,128)(2,1)S(1)}, bf16[576,256]{1,0:T(8,128)(2,1)S(1)}, u32[]{:S(2)}, u32[]{:S(2)}) collective-permute-start(bf16[576,256]{1,0:T(8,128)(2,1)S(1)} %collective-permute-done.3.m1_ref), channel_id=1, source_target_pairs={{0,480},{32,0},{64,32},{96,64},{128,96},{160,128},{192,160},{224,1... | collective-permute-start | bytes 884744 | tf_op jit(solution)/shard_map/ppermute | solution.py:28
  74.9 18.6 %collective-permute-start.4 = (bf16[192,256]{1,0:T(8,128)(2,1)S(1)}, bf16[192,256]{1,0:T(8,128)(2,1)S(1)}, u32[]{:S(2)}, u32[]{:S(2)}) collective-permute-start(bf16[192,256]{1,0:T(8,128)(2,1)S(1)} %collective-permute-done), channel_id=1, source_target_pairs={{0,96},{32,128},{64,160},{96,192},{128,224},{160,256},{192,288},{2... | collective-permute-start | bytes 294920 | tf_op jit(solution)/shard_map/ppermute | solution.py:28
  93.5 0.6 copy-start.7
  93.5 0.7 copy-start.5
  93.5 0.8 copy-start.6
  103.1 10.8 %all-to-all-start = ((bf16[4,192,384]{2,1,0:T(8,128)(2,1)}), bf16[4,192,384]{2,1,0:T(8,128)(2,1)S(1)}, u32[]{:S(2)}, u32[]{:S(2)}) async-start(bf16[4,192,384]{2,1,0:T(8,128)(2,1)} %bitcast.10), calls=%async_computation | async-start | bytes 1179648 | tf_op jit(solution)/shard_map/all_to_all | solution.py:216
  114.7 1.1 copy-start.12
  115.8 24.0 %copy-start.2 = (bf16[24,2048]{1,0:T(8,128)(2,1)S(1)}, bf16[24,2048]{1,0:T(8,128)(2,1)}, u32[]{:S(2)}) copy-start(bf16[24,2048]{1,0:T(8,128)(2,1)} %param.13) | copy-start | bytes 294916
  116.3 23.7 %copy-start.10 = (f32[2048]{0:T(1024)S(1)}, f32[2048]{0:T(1024)}, u32[]{:S(2)}) copy-start(f32[2048]{0:T(1024)} %param.20) | copy-start | bytes 24580
  116.3 40.2 %copy-start.11 = (f32[3,704]{1,0:T(4,128)S(1)}, f32[3,704]{1,0:T(4,128)}, u32[]{:S(2)}) copy-start(f32[3,704]{1,0:T(4,128)} %param.23) | copy-start | bytes 25348
  154.3 3.2 %collective-permute-start.7 = (bf16[8,2048]{1,0:T(8,128)(2,1)S(1)}, bf16[8,2048]{1,0:T(8,128)(2,1)S(1)}, u32[]{:S(2)}, u32[]{:S(2)}) collective-permute-start(bf16[8,2048]{1,0:T(8,128)(2,1)S(1)} %slice.125), channel_id=1, source_target_pairs={{0,8},{8,16},{16,24},{24,32},{32,40},{40,48},{48,56},{56,64},{64,7... | collective-permute-start | bytes 98312 | tf_op jit(solution)/shard_map/ppermute | solution.py:227
  156.5 6.1 %copy-start.13 = (f32[704]{0:T(1024)S(1)}, f32[704]{0:T(1024)}, u32[]{:S(2)}) copy-start(f32[704]{0:T(1024)} %param.24) | copy-start | bytes 8452
Sparse Core Ops, SparseCore 0:
  21.5 136.9 all-gather.1

commit v6 on v5

v6 whole, which is shorter than its diff:
```python
import jax
import jax.numpy as jnp
from jax import lax
from jax.experimental import pallas as pl
from jax.experimental.pallas import tpu as pltpu
from jax.sharding import Mesh
from jax.sharding import PartitionSpec as P

HD = 64
VD = 128
SP = ("z", "y")
SP_TP = ("z", "y", "x", "c")
TP = ("x", "c")
NZ = 16
NY = 4
eps = 1e-05
neg_fill = -1e30
TILE = 128
LANES = 128
OFFSETS = (0, 1, 15, 2, 14, 3, 13, 4, 12, 5, 11, 6, 10, 7, 9, 8)
CHUNK = 4

VMEM = pl.BlockSpec(memory_space=pltpu.VMEM)
SMEM = pl.BlockSpec(memory_space=pltpu.SMEM)


def shifted(value, axis, steps):
    count = lax.axis_size(axis)
    return lax.ppermute(value, axis, [(i, (i + steps) % count) for i in range(count)])


def dot_nt(a, b):
    return lax.dot_general(a, b, (((1,), (1,)), ((), ())), preferred_element_type=jnp.float32)


def row_bias(offsets, rows, z):
    lane = lax.broadcasted_iota(jnp.int32, (1, rows * len(offsets)), 1)
    bias = jnp.zeros(lane.shape, jnp.float32)
    for i, off in enumerate(offsets):
        inside = jnp.logical_and(lane >= i * rows, lane < (i + 1) * rows)
        bias = jnp.where(jnp.logical_and(inside, off > z), neg_fill, bias)
    return bias


def both_maps(q):
    lane = lax.broadcasted_iota(jnp.int32, q.shape, 1)
    q = q * jnp.bfloat16(HD**-0.5)
    zero = jnp.zeros_like(q)
    return jnp.concatenate((jnp.where(lane < HD, q, zero), jnp.where(lane < HD, zero, q)), axis=0)


def packed(columns):
    lane = lax.broadcasted_iota(jnp.int32, (TILE, VD), 1)
    block = jnp.zeros((TILE, VD), jnp.float32)
    for m in range(2):
        for i, v in enumerate(columns):
            column = v[m * TILE : (m + 1) * TILE]
            block = jnp.where(lane == m * len(columns) + i, column, block)
    return block


def attend_kernel(where_ref, rows_ref, *refs):
    blocks, (out_ref, q_ref, kv_ref) = refs[:-3], refs[-3:]
    z = where_ref[0]
    y = where_ref[1]
    rows = blocks[0].shape[0]
    w_rows = rows_ref.shape[0] // NY
    for i in range(NY * rows // w_rows):
        y_at, lane_at = divmod(i, rows // w_rows)
        q_ref[i * w_rows : (i + 1) * w_rows, :] = rows_ref[
            y_at * w_rows : (y_at + 1) * w_rows, lane_at * 2 * HD : (lane_at + 1) * 2 * HD
        ]
    for i, block in enumerate(blocks):
        kv_ref[i * rows : (i + 1) * rows, :] = block[...]
    span = CHUNK * rows
    chunks = [OFFSETS[i : i + CHUNK] for i in range(0, len(OFFSETS), CHUNK)]
    biases = [row_bias(offsets, rows, z) for offsets in chunks]

    @pl.loop(0, NY * rows // TILE)
    def _(t):
        at = pl.multiple_of(t * TILE, TILE)
        q2 = both_maps(q_ref[pl.ds(at, TILE), :])
        scores = []
        for i, bias in enumerate(biases):
            keys = kv_ref[i * span : (i + 1) * span, : 2 * HD]
            scores.append(dot_nt(q2, keys) + bias)
        r = lax.broadcasted_iota(jnp.int32, scores[0].shape, 0)
        r = jnp.where(r >= TILE, r - TILE, r) + at
        k = lax.broadcasted_iota(jnp.int32, scores[0].shape, 1)
        hidden = jnp.logical_and(k < rows, k + y * rows > r)
        scores[0] = jnp.where(hidden, neg_fill, scores[0])
        top = jnp.max(scores[0], axis=1, keepdims=True)
        for s in scores[1:]:
            top = jnp.maximum(top, jnp.max(s, axis=1, keepdims=True))
        total = jnp.zeros((2 * TILE, 1), jnp.float32)
        acc = jnp.zeros((2 * TILE, VD), jnp.float32)
        for i, s in enumerate(scores):
            e = jnp.exp(s - top)
            total = total + jnp.sum(e, axis=1, keepdims=True)
            acc = acc + jnp.dot(
                e.astype(jnp.bfloat16),
                kv_ref[i * span : (i + 1) * span, 2 * HD :],
                preferred_element_type=jnp.float32,
            )
        mean = acc / total
        lse = top + jnp.log(total)
        hi = lse.astype(jnp.bfloat16).astype(jnp.float32)
        mid = (lse - hi).astype(jnp.bfloat16).astype(jnp.float32)
        out_ref[pl.ds(at, TILE), 0:VD] = mean[:TILE].astype(jnp.bfloat16)
        out_ref[pl.ds(at, TILE), VD : 2 * VD] = mean[TILE:].astype(jnp.bfloat16)
        out_ref[pl.ds(at, TILE), 2 * VD : 3 * VD] = packed((hi, mid, lse - hi - mid)).astype(
            jnp.bfloat16
        )


def merged(got):
    got = got.astype(jnp.float32)
    means = []
    for m in range(2):
        stat = got[:, :, 2 * VD + 3 * m : 2 * VD + 3 * m + 3]
        lse = stat[..., 0:1] + stat[..., 1:2] + stat[..., 2:3]
        share = jnp.exp(lse - jnp.max(lse, axis=0, keepdims=True))
        acc = jnp.sum(share * got[:, :, m * VD : (m + 1) * VD], axis=0)
        means.append(acc / jnp.sum(share, axis=0))
    return means


def normalize(rows_in, gain):
    values_f = rows_in.astype(jnp.float32)
    scale_inv = lax.rsqrt(jnp.mean(values_f * values_f, axis=-1, keepdims=True) + eps)
    return (values_f * scale_inv * gain).astype(jnp.bfloat16)


def summed_over_tp(shard):
    core = lax.axis_index("c")
    count = lax.axis_size(TP)
    cut = shard.reshape(count // 2, 2, shard.shape[0] // count, shard.shape[1])
    own = jnp.where(core == 0, cut[:, 0], cut[:, 1])
    for_peer = jnp.where(core == 0, cut[:, 1], cut[:, 0])
    from_peer = lax.ppermute(for_peer, "c", [(0, 1), (1, 0)])
    both = (own.astype(jnp.float32) + from_peer.astype(jnp.float32)).astype(jnp.bfloat16)
    tiles = lax.all_to_all(both, "x", 0, 0, tiled=True)
    return jnp.sum(tiles.astype(jnp.float32), axis=0).astype(jnp.bfloat16)


def local(
    residual,
    queries,
    key_pairs,
    values,
    second_weight,
    head_gain,
    out_weight,
    norm_gain,
    up_weight,
    gate_weight,
    conv_weight,
    conv_bias,
    down_weight,
):
    rows = queries.shape[0]
    ff = up_weight.shape[1]
    where = jnp.stack((lax.axis_index("z"), lax.axis_index("y"))).astype(jnp.int32)
    w_rows = up_weight.shape[0]
    width = 2 * ff + ff
    tail = -width % LANES
    cuts = [up_weight, gate_weight, down_weight.T, jnp.zeros((w_rows, tail), jnp.bfloat16)]
    cuts += [queries[i : i + w_rows] for i in range(0, rows, w_rows)]
    row_w = lax.all_gather(jnp.concatenate(cuts, axis=1), "y", axis=0, tiled=True)
    all_w = lax.all_gather(row_w[:, :width], "z", axis=0, tiled=True)
    q_rows = row_w[:, width + tail :]

    kv = jnp.concatenate((key_pairs, values), axis=1)
    ahead, behind, blocks = kv, kv, [kv]
    for _ in range(lax.axis_size("z") // 2 - 1):
        ahead, behind = shifted(ahead, "z", 1), shifted(behind, "z", -1)
        blocks += [ahead, behind]
    cut = rows // 2
    far = (shifted(ahead[:cut], "z", 1), shifted(behind[cut:], "z", -1))
    blocks.append(jnp.concatenate(far, axis=0))
    blocks = [pltpu.with_memory_space_constraint(b, pltpu.VMEM) for b in blocks]
    parts = pl.pallas_call(
        attend_kernel,
        out_shape=jax.ShapeDtypeStruct((NY * rows, 3 * VD), jnp.bfloat16),
        in_specs=[SMEM] + [VMEM] * (1 + len(blocks)),
        out_specs=VMEM,
        scratch_shapes=[
            pltpu.VMEM((NY * rows, 2 * HD), jnp.bfloat16),
            pltpu.VMEM((len(blocks) * rows, 2 * HD + VD), jnp.bfloat16),
        ],
        name="attend",
    )(where, q_rows, *blocks)
    got = lax.all_to_all(parts.reshape(NY, rows, 3 * VD), "y", 0, 0, tiled=True)
    means = merged(got)
    diff = means[0] - second_weight[0] * means[1]
    scale_inv = lax.rsqrt(jnp.mean(diff * diff, axis=-1, keepdims=True) + eps)
    attended = (diff * scale_inv * head_gain * 0.8).astype(jnp.bfloat16)
    proj = summed_over_tp(
        jnp.dot(attended, out_weight, preferred_element_type=jnp.float32).astype(jnp.bfloat16)
    )
    mid = (residual.astype(jnp.float32) + proj.astype(jnp.float32)).astype(jnp.bfloat16)
    normed_all = lax.all_gather(normalize(mid, norm_gain), TP, axis=0, tiled=True)
    count = lax.axis_size("z") * lax.axis_size("y")
    rim_rows = lax.ppermute(normed_all[rows - 8 :], SP, [(i, i + 1) for i in range(count - 1)])
    both = jnp.dot(
        jnp.concatenate((normed_all, rim_rows), axis=0),
        all_w[:, : 2 * ff],
        preferred_element_type=jnp.float32,
    ).astype(jnp.bfloat16)
    up_proj, gate_proj = both[:rows, :ff], both[:rows, ff:]
    taps = conv_weight.shape[0]
    extended = jnp.concatenate((both[rows + 8 - (taps - 1) :, :ff], up_proj), axis=0)
    conv_out = jnp.zeros((rows, ff), jnp.float32) + conv_bias[None, :]
    for tap in range(taps):
        conv_out = conv_out + conv_weight[tap][None, :] * extended[tap : tap + rows].astype(
            jnp.float32
        )
    hidden = (jax.nn.silu(conv_out) * gate_proj.astype(jnp.float32)).astype(jnp.bfloat16)
    ffn = dot_nt(hidden, all_w[:, 2 * ff : width]).astype(jnp.bfloat16)
    ffn_out = summed_over_tp(ffn)
    return (mid.astype(jnp.float32) + ffn_out.astype(jnp.float32)).astype(jnp.bfloat16)


def solution(mesh):
    finer = Mesh(mesh.devices.reshape(NZ, NY, mesh.shape["tp"] // 2, 2), ("z", "y", "x", "c"))
    in_specs = (
        P(SP_TP, None),
        P(SP, TP),
        P(SP, TP),
        P(SP, TP),
        P(TP),
        P(TP),
        P(TP, None),
        P(),
        P(SP, TP),
        P(SP, TP),
        P(None, TP),
        P(TP),
        P(TP, SP),
    )
    out_specs = P(SP_TP, None)
    return jax.shard_map(local, mesh=finer, in_specs=in_specs, out_specs=out_specs, check_vma=False)
```

time: 191 us -> 200 us (1.047)
  starting transfers between devices: 46.9 us -> 87.8 us
  blocking collectives: 66.7 us -> 48.2 us
  Pallas kernels: 17.8 us -> 11 us
  waiting for transfers between devices: 28.9 us -> 22.3 us
    ppermute x7 -> x16, starting transfers between devices: 41.3 us -> 63.6 us  [shifted(): lax.ppermute(value, axis, [(i, (i + steps) % count) for i in range(count)])]
    all_to_all x2, blocking collectives: 40.4 us -> 21 us  [summed_over_tp(): tiles = lax.all_to_all(both, 'x', 0, 0, tiled=True)]
    ppermute x0 -> x2, starting transfers between devices: none -> 18.6 us  [summed_over_tp(): from_peer = lax.ppermute(for_peer, 'c', [(0, 1), (1, 0)])]
    ppermute x7 -> x16, waiting for transfers between devices: 20.3 us -> 12 us  [shifted(): lax.ppermute(value, axis, [(i, (i + steps) % count) for i in range(count)])]
    pallas_call x2 -> x1, Pallas kernels: 17.8 us -> 11 us  [local(): pl.pallas_call(attend_kernel, out_shape=jax.ShapeDtypeStruct((NY * rows,...]
    ppermute x0 -> x2, waiting for transfers between devices: none -> 2.65 us  [summed_over_tp(): from_peer = lax.ppermute(for_peer, 'c', [(0, 1), (1, 0)])]
  transfers between devices with their start and end apart: 10 -> 21, of which waited for: 7 -> 17; matrix products, arithmetic and copies ran while one was open for 2% -> 2% of each run, Pallas kernels for 9% -> 6%
where the time goes in v6:
time: 200 us; the launch traced here: 199 us
  starting transfers between devices  87.8 us (44%)
  blocking collectives  48.2 us (24%)
  waiting for transfers between devices  22.3 us (11%)
  between operations  14.5 us (7%)
  Pallas kernels  11 us (6%)
  matrix products  7.76 us (4%)
  other arithmetic  3.73 us (2%)
  local copies, waits for them, and re-layouts  3.67 us (2%)
    ppermute x16, starting transfers between devices, shifted(): lax.ppermute(value, axis, [(i, (i + steps) % count) for i in range(count)])  63.6 us
    all_to_all x2, blocking collectives, summed_over_tp(): tiles = lax.all_to_all(both, 'x', 0, 0, tiled=True)  21 us
    ppermute x2, starting transfers between devices, summed_over_tp(): from_peer = lax.ppermute(for_peer, 'c', [(0, 1), (1, 0)])  18.6 us
    all_gather x1, blocking collectives, local(): lax.all_gather(normalize(mid, norm_gain), TP, axis=0, tiled=True)  15 us
    all_gather x1, blocking collectives, local(): lax.all_gather(jnp.concatenate(cuts, axis=1), 'y', axis=0, tiled=True)  12.1 us
    ppermute x16, waiting for transfers between devices, shifted(): lax.ppermute(value, axis, [(i, (i + steps) % count) for i in range(count)])  12 us
    pallas_call x1, Pallas kernels, local(): pl.pallas_call(attend_kernel, out_shape=jax.ShapeDtypeStruct((NY * rows,...  11 us
    all_to_all x1, waiting for transfers between devices, local(): got = lax.all_to_all(parts.reshape(NY, rows, 3 * VD), 'y', 0, 0, tiled=True)  6.65 us
  transfers between devices with their start and end apart: 21, of which 17 were waited for; matrix products, arithmetic and copies ran while one was open for 2% of the time, Pallas kernels for 6%

profile of v6, /device:TPU:1, one launch (start us, length us, event | category | flops | bytes accessed | tf_op | source)
XLA Modules:
  0.0 199.0 jit_solution(12877825821012519917)
XLA Ops:
  6.5 0.8 fusion.44
  7.4 1.0 concatenate.15
  8.4 12.1 %all_gather.9 = bf16[128,2944]{1,0:T(8,128)(2,1)S(1)} all-gather(bf16[32,2944]{1,0:T(8,128)(2,1)S(1)} %concatenate.15), channel_id=1, replica_groups=mesh['z'=16,'y'=4,'x'=4,'c'=2] {'y'}, dimensions={0}, use_global_device_ids=true | all-gather | bytes 942080 | tf_op jit(solution)/shard_map/all_gather | solution.py:169
  20.5 0.8 slice.158
  21.4 4.6 %collective-permute-start = (bf16[192,256]{1,0:T(8,128)(2,1)S(1)}, bf16[192,256]{1,0:T(8,128)(2,1)S(1)}, u32[]{:S(2)}, u32[]{:S(2)}) collective-permute-start(bf16[192,256]{1,0:T(8,128)(2,1)S(1)} %constant_dynamic-update-slice_fusion.refs_0_), channel_id=1, source_target_pairs={{0,32},{32,64},{64,96},{96,128},{128,160},{160,192},{192,224},{224... | collective-permute-start | bytes 294920 | tf_op jit(solution)/shard_map/ppermute | solution.py:29
  26.0 9.5 %collective-permute-start.1 = (bf16[192,256]{1,0:T(8,128)(2,1)S(1)}, bf16[192,256]{1,0:T(8,128)(2,1)S(1)}, u32[]{:S(2)}, u32[]{:S(2)}) collective-permute-start(bf16[192,256]{1,0:T(8,128)(2,1)S(1)} %constant_dynamic-update-slice_fusion.refs_0_), channel_id=1, source_target_pairs={{0,480},{32,0},{64,32},{96,64},{128,96},{160,128},{192,160},{224,1... | collective-permute-start | bytes 294920 | tf_op jit(solution)/shard_map/ppermute | solution.py:29
  35.5 0.1 collective-permute-done.refs_1_
  35.5 1.9 collective-permute-start.2
  37.5 4.6 %collective-permute-start.3 = (bf16[192,256]{1,0:T(8,128)(2,1)S(1)}, bf16[192,256]{1,0:T(8,128)(2,1)S(1)}, u32[]{:S(2)}, u32[]{:S(2)}) collective-permute-start(bf16[192,256]{1,0:T(8,128)(2,1)S(1)} %collective-permute-done.1.refs_2_), channel_id=1, source_target_pairs={{0,480},{32,0},{64,32},{96,64},{128,96},{160,128},{192,160},{224,1... | collective-permute-start | bytes 294920 | tf_op jit(solution)/shard_map/ppermute | solution.py:29
  42.0 0.1 collective-permute-done.2.refs_3_
  42.1 1.9 collective-permute-start.4
  44.0 4.6 %collective-permute-start.5 = (bf16[192,256]{1,0:T(8,128)(2,1)S(1)}, bf16[192,256]{1,0:T(8,128)(2,1)S(1)}, u32[]{:S(2)}, u32[]{:S(2)}) collective-permute-start(bf16[192,256]{1,0:T(8,128)(2,1)S(1)} %collective-permute-done.3.refs_4_), channel_id=1, source_target_pairs={{0,480},{32,0},{64,32},{96,64},{128,96},{160,128},{192,160},{224,1... | collective-permute-start | bytes 294920 | tf_op jit(solution)/shard_map/ppermute | solution.py:29
  48.6 0.1 collective-permute-done.4.refs_5_
  48.6 1.9 collective-permute-start.6
  50.6 1.4 collective-permute-done.5.refs_6_
  52.0 5.4 %collective-permute-start.7 = (bf16[192,256]{1,0:T(8,128)(2,1)S(1)}, bf16[192,256]{1,0:T(8,128)(2,1)S(1)}, u32[]{:S(2)}, u32[]{:S(2)}) collective-permute-start(bf16[192,256]{1,0:T(8,128)(2,1)S(1)} %collective-permute-done.5.refs_6_), channel_id=1, source_target_pairs={{0,480},{32,0},{64,32},{96,64},{128,96},{160,128},{192,160},{224,1... | collective-permute-start | bytes 294920 | tf_op jit(solution)/shard_map/ppermute | solution.py:29
  57.4 0.7 collective-permute-done.6.refs_7_
  58.2 1.9 collective-permute-start.8
  60.1 1.1 collective-permute-done.7.refs_8_
  61.1 5.4 %collective-permute-start.9 = (bf16[192,256]{1,0:T(8,128)(2,1)S(1)}, bf16[192,256]{1,0:T(8,128)(2,1)S(1)}, u32[]{:S(2)}, u32[]{:S(2)}) collective-permute-start(bf16[192,256]{1,0:T(8,128)(2,1)S(1)} %collective-permute-done.7.refs_8_), channel_id=1, source_target_pairs={{0,480},{32,0},{64,32},{96,64},{128,96},{160,128},{192,160},{224,1... | collective-permute-start | bytes 294920 | tf_op jit(solution)/shard_map/ppermute | solution.py:29
  66.6 1.4 collective-permute-done.8.refs_9_
  68.0 1.9 collective-permute-start.10
  69.9 0.8 collective-permute-done.9.refs_10_
  70.7 5.4 %collective-permute-start.11 = (bf16[192,256]{1,0:T(8,128)(2,1)S(1)}, bf16[192,256]{1,0:T(8,128)(2,1)S(1)}, u32[]{:S(2)}, u32[]{:S(2)}) collective-permute-start(bf16[192,256]{1,0:T(8,128)(2,1)S(1)} %collective-permute-done.9.refs_10_), channel_id=1, source_target_pairs={{0,480},{32,0},{64,32},{96,64},{128,96},{160,128},{192,160},{224,1... | collective-permute-start | bytes 294920 | tf_op jit(solution)/shard_map/ppermute | solution.py:29
  76.1 2.0 collective-permute-done.10.refs_11_
  78.1 1.9 collective-permute-start.12
  80.0 0.7 collective-permute-done.11.refs_12_
  80.7 5.4 %collective-permute-start.13 = (bf16[192,256]{1,0:T(8,128)(2,1)S(1)}, bf16[192,256]{1,0:T(8,128)(2,1)S(1)}, u32[]{:S(2)}, u32[]{:S(2)}) collective-permute-start(bf16[192,256]{1,0:T(8,128)(2,1)S(1)} %collective-permute-done.11.refs_12_), channel_id=1, source_target_pairs={{0,480},{32,0},{64,32},{96,64},{128,96},{160,128},{192,160},{224,1... | collective-permute-start | bytes 294920 | tf_op jit(solution)/shard_map/ppermute | solution.py:29
  86.1 2.0 %collective-permute-done.12.refs_13_ = bf16[192,256]{1,0:T(8,128)(2,1)S(1)} collective-permute-done((bf16[192,256]{1,0:T(8,128)(2,1)S(1)}, bf16[192,256]{1,0:T(8,128)(2,1)S(1)}, u32[]{:S(2)}, u32[]{:S(2)}) %collective-permute-start.12) | collective-permute-done | bytes 98336 | tf_op jit(solution)/shard_map/ppermute | solution.py:29
  88.1 1.9 collective-permute-start.14
  90.0 0.7 collective-permute-done.13.refs_14_
  90.7 5.4 %collective-permute-start.15 = (bf16[96,256]{1,0:T(8,128)(2,1)S(1)}, bf16[96,256]{1,0:T(8,128)(2,1)S(1)}, u32[]{:S(2)}, u32[]{:S(2)}) collective-permute-start(bf16[96,256]{1,0:T(8,128)(2,1)S(1)} %slice.146), channel_id=1, source_target_pairs={{0,480},{32,0},{64,32},{96,64},{128,96},{160,128},{192,160},{224,1... | collective-permute-start | bytes 147464 | tf_op jit(solution)/shard_map/ppermute | solution.py:29
  96.1 0.6 pad_add_fusion.where_ref
  96.7 0.7 slice.144.rows_ref
  97.4 1.0 collective-permute-done.15
  98.5 11.0 %attend.1 = bf16[768,384]{1,0:T(8,128)(2,1)} custom-call(s32[2]{0:T(128)} %pad_add_fusion.where_ref, bf16[128,768]{1,0:T(8,128)(2,1)} %slice.144.rows_ref, bf16[192,256]{1,0:T(8,128)(2,1)S(1)} %constant_dynamic-update-slice_fusion.refs_0_, bf16[192,256]{1,0:T(8,128)(2,1)S(1)} %collective-permute-done.refs_1_, ...), custom_call_target="tpu_custom_call" | custom-call | tf_op jit(solution)/shard_map/attend/pallas_call | solution.py:182
  109.5 3.5 %all-to-all-start = ((bf16[4,192,384]{2,1,0:T(8,128)(2,1)}), bf16[4,192,384]{2,1,0:T(8,128)(2,1)S(1)}, u32[]{:S(2)}, u32[]{:S(2)}) async-start(bf16[4,192,384]{2,1,0:T(8,128)(2,1)} %bitcast.51), calls=%async_computation | async-start | bytes 1179648 | tf_op jit(solution)/shard_map/all_to_all | solution.py:193
  113.6 6.7 %all-to-all-done = bf16[4,192,384]{2,1,0:T(8,128)(2,1)S(1)} async-done(((bf16[4,192,384]{2,1,0:T(8,128)(2,1)}), bf16[4,192,384]{2,1,0:T(8,128)(2,1)S(1)}, u32[]{:S(2)}, u32[]{:S(2)}) %all-to-all-start) | async-done | bytes 589856 | tf_op jit(solution)/shard_map/all_to_all | solution.py:193
  120.3 0.1 convert_element_type.81
  120.4 0.7 fusion.42
  121.1 0.6 fusion.19
  121.7 0.3 fusion.17
  121.9 0.1 copy.35
  122.1 0.1 copy.36
  122.2 0.1 multiply_reduce_fusion
  122.3 0.5 convolution_convert_fusion
  122.8 15.7 %collective-permute-start.16 = (bf16[4,24,2048]{2,1,0:T(8,128)(2,1)S(1)}, bf16[4,24,2048]{2,1,0:T(8,128)(2,1)S(1)}, u32[]{:S(2)}, u32[]{:S(2)}) collective-permute-start(bf16[4,24,2048]{2,1,0:T(8,128)(2,1)S(1)} %fusion.15), channel_id=1, source_target_pairs={{0,1},{1,0},{2,3},{3,2},{4,5},{5,4},{6,7},{7,6},{8,9},{9,8},{10,11... | collective-permute-start | bytes 1179656 | tf_op jit(solution)/shard_map/ppermute | solution.py:140
  138.5 1.3 collective-permute-done.16
  139.8 0.1 fusion.14
  140.0 11.0 %all_to_all.15 = bf16[4,24,2048]{2,1,0:T(8,128)(2,1)S(1)} all-to-all(bf16[4,24,2048]{2,1,0:T(8,128)(2,1)S(1)} %fusion.14), channel_id=1, replica_groups=mesh['z'=16,'y'=4,'x'=4,'c'=2] {'x'}, dimensions={0} | all-to-all | bytes 786432 | tf_op jit(solution)/shard_map/all_to_all | solution.py:142
  150.9 0.1 reduce_sum.83
  151.0 0.1 fusion.31
  151.2 0.1 fusion.33
  151.3 15.0 %all_gather.10 = bf16[192,2048]{1,0:T(8,128)(2,1)S(1)} all-gather(bf16[24,2048]{1,0:T(8,128)(2,1)S(1)} %fusion.33), channel_id=1, replica_groups=mesh['z'=16,'y'=4,'x'=4,'c'=2] {'x','c'}, dimensions={0}, use_global_device_ids=true | all-gather | bytes 884736 | tf_op jit(solution)/shard_map/all_gather | solution.py:202
  166.3 2.2 %collective-permute-start.17 = (bf16[8,2048]{1,0:T(8,128)(2,1)S(1)}, bf16[8,2048]{1,0:T(8,128)(2,1)S(1)}, u32[]{:S(2)}, u32[]{:S(2)}) collective-permute-start(bf16[8,2048]{1,0:T(8,128)(2,1)S(1)} %slice.157), channel_id=1, source_target_pairs={{0,8},{8,16},{16,24},{24,32},{32,40},{40,48},{48,56},{56,64},{64,7... | collective-permute-start | bytes 98312 | tf_op jit(solution)/shard_map/ppermute | solution.py:204
  168.5 0.9 collective-permute-done.17
  169.5 4.1 %fusion.4 = bf16[200,1408]{1,0:T(8,128)(2,1)S(1)} fusion(bf16[2048,2112]{1,0:T(8,128)(2,1)} %all-gather.2.cloned.1.call-done, bf16[8,2048]{1,0:T(8,128)(2,1)S(1)} %collective-permute-done.17, bf16[192,2048]{1,0:T(8,128)(2,1)S(1)} %all_gather.10), kind=kOutput, calls=%fused_computation.4 | convolution fusion | flops 1155353600 | bytes 7149568 | tf_op jit(solution)/shard_map/dot_general | solution.py:205
  173.6 3.2 %fusion.7 = bf16[192,2048]{1,0:T(8,128)(2,1)S(1)} fusion(bf16[2048,2112]{1,0:T(8,128)(2,1)} %all-gather.2.cloned.1.call-done, bf16[192,704]{1,0:T(8,128)(2,1)S(1)} %slice.161, bf16[2,704]{1,0:T(2,128)(2,1)S(1)} %slice.160, bf16[200,1408]{1,0:T(8,128)(2,1)S(1)} %fusion.4, f32[704]{0:T(1024)S(1)} %get-tuple-element.12, f32[704]{0:T(1024)S(1)} %get-tuple-element.13, ...), kind=kOutput, calls=%fused_computation.5 | convolution fusion | flops 557015040 | bytes 4541440 | tf_op jit(solution)/shard_map/dot_general | solution.py:33
  176.9 2.9 %collective-permute-start.18 = (bf16[4,24,2048]{2,1,0:T(8,128)(2,1)S(1)}, bf16[4,24,2048]{2,1,0:T(8,128)(2,1)S(1)}, u32[]{:S(2)}, u32[]{:S(2)}) collective-permute-start(bf16[4,24,2048]{2,1,0:T(8,128)(2,1)S(1)} %select_bitcast_fusion), channel_id=1, source_target_pairs={{0,1},{1,0},{2,3},{3,2},{4,5},{5,4},{6,7},{7,6},{8,9},{9,8},{10,11... | collective-permute-start | bytes 1179656 | tf_op jit(solution)/shard_map/ppermute | solution.py:140
  179.8 1.3 collective-permute-done.18
  181.2 0.1 fusion.13
  181.3 10.0 %all_to_all.16 = bf16[4,24,2048]{2,1,0:T(8,128)(2,1)S(1)} all-to-all(bf16[4,24,2048]{2,1,0:T(8,128)(2,1)S(1)} %fusion.13), channel_id=1, replica_groups=mesh['z'=16,'y'=4,'x'=4,'c'=2] {'x'}, dimensions={0} | all-to-all | bytes 786432 | tf_op jit(solution)/shard_map/all_to_all | solution.py:142
  191.4 0.1 reduce_sum.85
  191.4 0.7 fusion.34
  (36 shorter events, 0.3 us)
Async XLA Ops:
  6.5 115.7 %copy-start = (bf16[128,2048]{1,0:T(8,128)(2,1)S(1)}, bf16[128,2048]{1,0:T(8,128)(2,1)}, u32[]{:S(2)}) copy-start(bf16[128,2048]{1,0:T(8,128)(2,1)} %param.19) | copy-start | bytes 1572868
  6.5 14.8 %copy-start.2 = (bf16[192,128]{1,0:T(8,128)(2,1)S(1)}, bf16[192,128]{1,0:T(8,128)(2,1)}, u32[]{:S(2)}) copy-start(bf16[192,128]{1,0:T(8,128)(2,1)} %param.15) | copy-start | bytes 147460
  6.5 14.8 %copy-start.3 = (bf16[192,128]{1,0:T(8,128)(2,1)S(1)}, bf16[192,128]{1,0:T(8,128)(2,1)}, u32[]{:S(2)}) copy-start(bf16[192,128]{1,0:T(8,128)(2,1)} %param.16) | copy-start | bytes 147460
  6.5 162.9 %all-gather.2.cloned.1.call-start = ((), (), s32[]{:S(2)}) async-start(), calls=%async_computation.3 | async-start | bytes 9469952 | tf_op jit(solution)/shard_map/all_gather | solution.py:170
  21.4 14.1 %collective-permute-start = (bf16[192,256]{1,0:T(8,128)(2,1)S(1)}, bf16[192,256]{1,0:T(8,128)(2,1)S(1)}, u32[]{:S(2)}, u32[]{:S(2)}) collective-permute-start(bf16[192,256]{1,0:T(8,128)(2,1)S(1)} %constant_dynamic-update-slice_fusion.refs_0_), channel_id=1, source_target_pairs={{0,32},{32,64},{64,96},{96,128},{128,160},{160,192},{192,224},{224... | collective-permute-start | bytes 294920 | tf_op jit(solution)/shard_map/ppermute | solution.py:29
  26.0 11.5 %collective-permute-start.1 = (bf16[192,256]{1,0:T(8,128)(2,1)S(1)}, bf16[192,256]{1,0:T(8,128)(2,1)S(1)}, u32[]{:S(2)}, u32[]{:S(2)}) collective-permute-start(bf16[192,256]{1,0:T(8,128)(2,1)S(1)} %constant_dynamic-update-slice_fusion.refs_0_), channel_id=1, source_target_pairs={{0,480},{32,0},{64,32},{96,64},{128,96},{160,128},{192,160},{224,1... | collective-permute-start | bytes 294920 | tf_op jit(solution)/shard_map/ppermute | solution.py:29
  35.5 6.6 %collective-permute-start.2 = (bf16[192,256]{1,0:T(8,128)(2,1)S(1)}, bf16[192,256]{1,0:T(8,128)(2,1)S(1)}, u32[]{:S(2)}, u32[]{:S(2)}) collective-permute-start(bf16[192,256]{1,0:T(8,128)(2,1)S(1)} %collective-permute-done.refs_1_), channel_id=1, source_target_pairs={{0,32},{32,64},{64,96},{96,128},{128,160},{160,192},{192,224},{224... | collective-permute-start | bytes 294920 | tf_op jit(solution)/shard_map/ppermute | solution.py:29
  37.5 6.6 %collective-permute-start.3 = (bf16[192,256]{1,0:T(8,128)(2,1)S(1)}, bf16[192,256]{1,0:T(8,128)(2,1)S(1)}, u32[]{:S(2)}, u32[]{:S(2)}) collective-permute-start(bf16[192,256]{1,0:T(8,128)(2,1)S(1)} %collective-permute-done.1.refs_2_), channel_id=1, source_target_pairs={{0,480},{32,0},{64,32},{96,64},{128,96},{160,128},{192,160},{224,1... | collective-permute-start | bytes 294920 | tf_op jit(solution)/shard_map/ppermute | solution.py:29
  42.1 6.6 %collective-permute-start.4 = (bf16[192,256]{1,0:T(8,128)(2,1)S(1)}, bf16[192,256]{1,0:T(8,128)(2,1)S(1)}, u32[]{:S(2)}, u32[]{:S(2)}) collective-permute-start(bf16[192,256]{1,0:T(8,128)(2,1)S(1)} %collective-permute-done.2.refs_3_), channel_id=1, source_target_pairs={{0,32},{32,64},{64,96},{96,128},{128,160},{160,192},{192,224},{224... | collective-permute-start | bytes 294920 | tf_op jit(solution)/shard_map/ppermute | solution.py:29
  44.0 8.0 %collective-permute-start.5 = (bf16[192,256]{1,0:T(8,128)(2,1)S(1)}, bf16[192,256]{1,0:T(8,128)(2,1)S(1)}, u32[]{:S(2)}, u32[]{:S(2)}) collective-permute-start(bf16[192,256]{1,0:T(8,128)(2,1)S(1)} %collective-permute-done.3.refs_4_), channel_id=1, source_target_pairs={{0,480},{32,0},{64,32},{96,64},{128,96},{160,128},{192,160},{224,1... | collective-permute-start | bytes 294920 | tf_op jit(solution)/shard_map/ppermute | solution.py:29
  48.6 9.5 %collective-permute-start.6 = (bf16[192,256]{1,0:T(8,128)(2,1)S(1)}, bf16[192,256]{1,0:T(8,128)(2,1)S(1)}, u32[]{:S(2)}, u32[]{:S(2)}) collective-permute-start(bf16[192,256]{1,0:T(8,128)(2,1)S(1)} %collective-permute-done.4.refs_5_), channel_id=1, source_target_pairs={{0,32},{32,64},{64,96},{96,128},{128,160},{160,192},{192,224},{224... | collective-permute-start | bytes 294920 | tf_op jit(solution)/shard_map/ppermute | solution.py:29
  52.0 9.2 %collective-permute-start.7 = (bf16[192,256]{1,0:T(8,128)(2,1)S(1)}, bf16[192,256]{1,0:T(8,128)(2,1)S(1)}, u32[]{:S(2)}, u32[]{:S(2)}) collective-permute-start(bf16[192,256]{1,0:T(8,128)(2,1)S(1)} %collective-permute-done.5.refs_6_), channel_id=1, source_target_pairs={{0,480},{32,0},{64,32},{96,64},{128,96},{160,128},{192,160},{224,1... | collective-permute-start | bytes 294920 | tf_op jit(solution)/shard_map/ppermute | solution.py:29
  58.2 9.8 %collective-permute-start.8 = (bf16[192,256]{1,0:T(8,128)(2,1)S(1)}, bf16[192,256]{1,0:T(8,128)(2,1)S(1)}, u32[]{:S(2)}, u32[]{:S(2)}) collective-permute-start(bf16[192,256]{1,0:T(8,128)(2,1)S(1)} %collective-permute-done.6.refs_7_), channel_id=1, source_target_pairs={{0,32},{32,64},{64,96},{96,128},{128,160},{160,192},{192,224},{224... | collective-permute-start | bytes 294920 | tf_op jit(solution)/shard_map/ppermute | solution.py:29
  61.1 9.5 %collective-permute-start.9 = (bf16[192,256]{1,0:T(8,128)(2,1)S(1)}, bf16[192,256]{1,0:T(8,128)(2,1)S(1)}, u32[]{:S(2)}, u32[]{:S(2)}) collective-permute-start(bf16[192,256]{1,0:T(8,128)(2,1)S(1)} %collective-permute-done.7.refs_8_), channel_id=1, source_target_pairs={{0,480},{32,0},{64,32},{96,64},{128,96},{160,128},{192,160},{224,1... | collective-permute-start | bytes 294920 | tf_op jit(solution)/shard_map/ppermute | solution.py:29
  68.0 10.1 %collective-permute-start.10 = (bf16[192,256]{1,0:T(8,128)(2,1)S(1)}, bf16[192,256]{1,0:T(8,128)(2,1)S(1)}, u32[]{:S(2)}, u32[]{:S(2)}) collective-permute-start(bf16[192,256]{1,0:T(8,128)(2,1)S(1)} %collective-permute-done.8.refs_9_), channel_id=1, source_target_pairs={{0,32},{32,64},{64,96},{96,128},{128,160},{160,192},{192,224},{224... | collective-permute-start | bytes 294920 | tf_op jit(solution)/shard_map/ppermute | solution.py:29
  70.7 10.0 %collective-permute-start.11 = (bf16[192,256]{1,0:T(8,128)(2,1)S(1)}, bf16[192,256]{1,0:T(8,128)(2,1)S(1)}, u32[]{:S(2)}, u32[]{:S(2)}) collective-permute-start(bf16[192,256]{1,0:T(8,128)(2,1)S(1)} %collective-permute-done.9.refs_10_), channel_id=1, source_target_pairs={{0,480},{32,0},{64,32},{96,64},{128,96},{160,128},{192,160},{224,1... | collective-permute-start | bytes 294920 | tf_op jit(solution)/shard_map/ppermute | solution.py:29
  78.1 10.1 %collective-permute-start.12 = (bf16[192,256]{1,0:T(8,128)(2,1)S(1)}, bf16[192,256]{1,0:T(8,128)(2,1)S(1)}, u32[]{:S(2)}, u32[]{:S(2)}) collective-permute-start(bf16[192,256]{1,0:T(8,128)(2,1)S(1)} %collective-permute-done.10.refs_11_), channel_id=1, source_target_pairs={{0,32},{32,64},{64,96},{96,128},{128,160},{160,192},{192,224},{224... | collective-permute-start | bytes 294920 | tf_op jit(solution)/shard_map/ppermute | solution.py:29
  80.7 10.0 %collective-permute-start.13 = (bf16[192,256]{1,0:T(8,128)(2,1)S(1)}, bf16[192,256]{1,0:T(8,128)(2,1)S(1)}, u32[]{:S(2)}, u32[]{:S(2)}) collective-permute-start(bf16[192,256]{1,0:T(8,128)(2,1)S(1)} %collective-permute-done.11.refs_12_), channel_id=1, source_target_pairs={{0,480},{32,0},{64,32},{96,64},{128,96},{160,128},{192,160},{224,1... | collective-permute-start | bytes 294920 | tf_op jit(solution)/shard_map/ppermute | solution.py:29
  88.1 9.3 %collective-permute-start.14 = (bf16[96,256]{1,0:T(8,128)(2,1)S(1)}, bf16[96,256]{1,0:T(8,128)(2,1)S(1)}, u32[]{:S(2)}, u32[]{:S(2)}) collective-permute-start(bf16[96,256]{1,0:T(8,128)(2,1)S(1)} %slice.145), channel_id=1, source_target_pairs={{0,32},{32,64},{64,96},{96,128},{128,160},{160,192},{192,224},{224... | collective-permute-start | bytes 147464 | tf_op jit(solution)/shard_map/ppermute | solution.py:29
  90.7 7.8 %collective-permute-start.15 = (bf16[96,256]{1,0:T(8,128)(2,1)S(1)}, bf16[96,256]{1,0:T(8,128)(2,1)S(1)}, u32[]{:S(2)}, u32[]{:S(2)}) collective-permute-start(bf16[96,256]{1,0:T(8,128)(2,1)S(1)} %slice.146), channel_id=1, source_target_pairs={{0,480},{32,0},{64,32},{96,64},{128,96},{160,128},{192,160},{224,1... | collective-permute-start | bytes 147464 | tf_op jit(solution)/shard_map/ppermute | solution.py:29
  109.5 10.8 %all-to-all-start = ((bf16[4,192,384]{2,1,0:T(8,128)(2,1)}), bf16[4,192,384]{2,1,0:T(8,128)(2,1)S(1)}, u32[]{:S(2)}, u32[]{:S(2)}) async-start(bf16[4,192,384]{2,1,0:T(8,128)(2,1)} %bitcast.51), calls=%async_computation | async-start | bytes 1179648 | tf_op jit(solution)/shard_map/all_to_all | solution.py:193
  120.4 1.9 copy-start.6
  121.9 29.1 %copy-start.1 = (bf16[24,2048]{1,0:T(8,128)(2,1)S(1)}, bf16[24,2048]{1,0:T(8,128)(2,1)}, u32[]{:S(2)}) copy-start(bf16[24,2048]{1,0:T(8,128)(2,1)} %param.13) | copy-start | bytes 294916
  122.1 29.1 %copy-start.4 = (f32[2048]{0:T(1024)S(1)}, f32[2048]{0:T(1024)}, u32[]{:S(2)}) copy-start(f32[2048]{0:T(1024)} %param.20) | copy-start | bytes 24580
  122.3 46.2 %copy-start.5 = (f32[3,704]{1,0:T(4,128)S(1)}, f32[3,704]{1,0:T(4,128)}, u32[]{:S(2)}) copy-start(f32[3,704]{1,0:T(4,128)} %param.23) | copy-start | bytes 25348
  122.8 17.0 %collective-permute-start.16 = (bf16[4,24,2048]{2,1,0:T(8,128)(2,1)S(1)}, bf16[4,24,2048]{2,1,0:T(8,128)(2,1)S(1)}, u32[]{:S(2)}, u32[]{:S(2)}) collective-permute-start(bf16[4,24,2048]{2,1,0:T(8,128)(2,1)S(1)} %fusion.15), channel_id=1, source_target_pairs={{0,1},{1,0},{2,3},{3,2},{4,5},{5,4},{6,7},{7,6},{8,9},{9,8},{10,11... | collective-permute-start | bytes 1179656 | tf_op jit(solution)/shard_map/ppermute | solution.py:140
  166.3 3.2 %collective-permute-start.17 = (bf16[8,2048]{1,0:T(8,128)(2,1)S(1)}, bf16[8,2048]{1,0:T(8,128)(2,1)S(1)}, u32[]{:S(2)}, u32[]{:S(2)}) collective-permute-start(bf16[8,2048]{1,0:T(8,128)(2,1)S(1)} %slice.157), channel_id=1, source_target_pairs={{0,8},{8,16},{16,24},{24,32},{32,40},{40,48},{48,56},{56,64},{64,7... | collective-permute-start | bytes 98312 | tf_op jit(solution)/shard_map/ppermute | solution.py:204
  168.5 5.1 %copy-start.7 = (f32[704]{0:T(1024)S(1)}, f32[704]{0:T(1024)}, u32[]{:S(2)}) copy-start(f32[704]{0:T(1024)} %param.24) | copy-start | bytes 8452
  176.9 4.3 %collective-permute-start.18 = (bf16[4,24,2048]{2,1,0:T(8,128)(2,1)S(1)}, bf16[4,24,2048]{2,1,0:T(8,128)(2,1)S(1)}, u32[]{:S(2)}, u32[]{:S(2)}) collective-permute-start(bf16[4,24,2048]{2,1,0:T(8,128)(2,1)S(1)} %select_bitcast_fusion), channel_id=1, source_target_pairs={{0,1},{1,0},{2,3},{3,2},{4,5},{5,4},{6,7},{7,6},{8,9},{9,8},{10,11... | collective-permute-start | bytes 1179656 | tf_op jit(solution)/shard_map/ppermute | solution.py:140
Sparse Core Ops, SparseCore 0:
  21.4 128.5 all-gather.1

commit v7 on v6

--- a/solution.py
+++ b/solution.py
@@ -17,16 +17,16 @@
 neg_fill = -1e30
 TILE = 128
 LANES = 128
-OFFSETS = (0, 1, 15, 2, 14, 3, 13, 4, 12, 5, 11, 6, 10, 7, 9, 8)
+OFFSETS = (0, 5, 11, 1, 6, 12, 15, 4, 10, 2, 7, 13, 14, 3, 9, 8)
 CHUNK = 4
 
 VMEM = pl.BlockSpec(memory_space=pltpu.VMEM)
 SMEM = pl.BlockSpec(memory_space=pltpu.SMEM)
 
 
-def shifted(value, axis, steps):
-    count = lax.axis_size(axis)
-    return lax.ppermute(value, axis, [(i, (i + steps) % count) for i in range(count)])
+def shifted(value, steps, targets):
+    count = lax.axis_size("z")
+    return lax.ppermute(value, "z", [((i - steps) % count, i) for i in targets])
 
 
 def dot_nt(a, b):
@@ -63,15 +63,17 @@
     blocks, (out_ref, q_ref, kv_ref) = refs[:-3], refs[-3:]
     z = where_ref[0]
     y = where_ref[1]
-    rows = blocks[0].shape[0]
+    rows = kv_ref.shape[0] // len(OFFSETS)
     w_rows = rows_ref.shape[0] // NY
     for i in range(NY * rows // w_rows):
         y_at, lane_at = divmod(i, rows // w_rows)
         q_ref[i * w_rows : (i + 1) * w_rows, :] = rows_ref[
             y_at * w_rows : (y_at + 1) * w_rows, lane_at * 2 * HD : (lane_at + 1) * 2 * HD
         ]
-    for i, block in enumerate(blocks):
-        kv_ref[i * rows : (i + 1) * rows, :] = block[...]
+    filled = 0
+    for block in blocks:
+        kv_ref[filled : filled + block.shape[0], :] = block[...]
+        filled += block.shape[0]
     span = CHUNK * rows
     chunks = [OFFSETS[i : i + CHUNK] for i in range(0, len(OFFSETS), CHUNK)]
     biases = [row_bias(offsets, rows, z) for offsets in chunks]
@@ -171,13 +173,16 @@
     q_rows = row_w[:, width + tail :]
 
     kv = jnp.concatenate((key_pairs, values), axis=1)
-    ahead, behind, blocks = kv, kv, [kv]
-    for _ in range(lax.axis_size("z") // 2 - 1):
-        ahead, behind = shifted(ahead, "z", 1), shifted(behind, "z", -1)
-        blocks += [ahead, behind]
-    cut = rows // 2
-    far = (shifted(ahead[:cut], "z", 1), shifted(behind[cut:], "z", -1))
-    blocks.append(jnp.concatenate(far, axis=0))
+    last = lax.axis_size("z")
+    f5 = shifted(kv, 5, [0, 1, *range(5, last)])
+    f11 = shifted(kv, -5, [0, 1, *range(11, last)])
+    held = jnp.concatenate((kv, f5, f11), axis=0)
+    n1 = shifted(held, 1, range(1, last))
+    m1 = shifted(held, -1, [0, *range(4, last)])
+    n2 = shifted(n1, 1, range(2, last))
+    m2 = shifted(m1, -1, range(3, last))
+    e8 = shifted(n2[rows : 2 * rows], 1, range(8, last))
+    blocks = [held, n1, m1, n2, m2, e8]
     blocks = [pltpu.with_memory_space_constraint(b, pltpu.VMEM) for b in blocks]
     parts = pl.pallas_call(
         attend_kernel,
@@ -186,7 +191,7 @@
         out_specs=VMEM,
         scratch_shapes=[
             pltpu.VMEM((NY * rows, 2 * HD), jnp.bfloat16),
-            pltpu.VMEM((len(blocks) * rows, 2 * HD + VD), jnp.bfloat16),
+            pltpu.VMEM((len(OFFSETS) * rows, 2 * HD + VD), jnp.bfloat16),
         ],
         name="attend",
     )(where, q_rows, *blocks)

time: 200 us -> 184 us (0.920)
  starting transfers between devices: 87.8 us -> 47.2 us
  waiting for transfers between devices: 22.3 us -> 45.9 us
    ppermute x16 -> x7, starting transfers between devices: 63.6 us -> 32.8 us  [shifted(): return lax.ppermute(value, 'z', [((i - steps) % count, i) for i in targets])]
    ppermute x16 -> x7, waiting for transfers between devices: 12 us -> 28 us  [shifted(): return lax.ppermute(value, 'z', [((i - steps) % count, i) for i in targets])]
    ppermute x2, starting transfers between devices: 18.6 us -> 8.71 us  [summed_over_tp(): from_peer = lax.ppermute(for_peer, 'c', [(0, 1), (1, 0)])]
    all_gather x1, waiting for transfers between devices: 0.01 us -> 7.54 us  [local(): all_w = lax.all_gather(row_w[:, :width], 'z', axis=0, tiled=True)]
  transfers between devices with their start and end apart: 21 -> 12, of which waited for: 17 -> 10; matrix products, arithmetic and copies ran while one was open for 2% -> 2% of each run, Pallas kernels for 6% -> 6%
where the time goes in v7:
time: 184 us; the launch traced here: 183 us
  blocking collectives  49.1 us (27%)
  starting transfers between devices  47.2 us (26%)
  waiting for transfers between devices  45.9 us (25%)
  between operations  14.4 us (8%)
  Pallas kernels  11 us (6%)
  matrix products  7.76 us (4%)
  other arithmetic  3.74 us (2%)
  local copies, waits for them, and re-layouts  3.67 us (2%)
    ppermute x7, starting transfers between devices, shifted(): return lax.ppermute(value, 'z', [((i - steps) % count, i) for i in targets])  32.8 us
    ppermute x7, waiting for transfers between devices, shifted(): return lax.ppermute(value, 'z', [((i - steps) % count, i) for i in targets])  28 us
    all_to_all x2, blocking collectives, summed_over_tp(): tiles = lax.all_to_all(both, 'x', 0, 0, tiled=True)  22 us
    all_gather x1, blocking collectives, local(): lax.all_gather(normalize(mid, norm_gain), TP, axis=0, tiled=True)  15 us
    all_gather x1, blocking collectives, local(): lax.all_gather(jnp.concatenate(cuts, axis=1), 'y', axis=0, tiled=True)  12.1 us
    pallas_call x1, Pallas kernels, local(): pl.pallas_call(attend_kernel, out_shape=jax.ShapeDtypeStruct((NY * rows,...  11 us
    ppermute x2, starting transfers between devices, summed_over_tp(): from_peer = lax.ppermute(for_peer, 'c', [(0, 1), (1, 0)])  8.71 us
    all_gather x1, waiting for transfers between devices, local(): all_w = lax.all_gather(row_w[:, :width], 'z', axis=0, tiled=True)  7.54 us
  transfers between devices with their start and end apart: 12, of which 10 were waited for; matrix products, arithmetic and copies ran while one was open for 2% of the time, Pallas kernels for 6%

profile of v7, /device:TPU:1, one launch (start us, length us, event | category | flops | bytes accessed | tf_op | source)
XLA Modules:
  0.0 182.8 jit_solution(253553574733151675)
XLA Ops:
  6.5 0.0 copy-start
  6.5 0.0 all-gather.2.cloned.1.call-start
  6.5 0.8 fusion.44
  7.4 1.0 concatenate.15
  8.4 12.1 %all_gather.9 = bf16[128,2944]{1,0:T(8,128)(2,1)S(1)} all-gather(bf16[32,2944]{1,0:T(8,128)(2,1)S(1)} %concatenate.15), channel_id=1, replica_groups=mesh['z'=16,'y'=4,'x'=4,'c'=2] {'y'}, dimensions={0}, use_global_device_ids=true | all-gather | bytes 942080 | tf_op jit(solution)/shard_map/all_gather | solution.py:171
  20.5 0.8 slice.153
  21.3 0.0 all-gather.2.cloned.1.call-update
  21.3 0.0 copy-done.2
  21.4 0.0 copy-done.3
  21.4 11.2 %collective-permute-start = (bf16[192,256]{1,0:T(8,128)(2,1)S(1)}, bf16[192,256]{1,0:T(8,128)(2,1)S(1)}, u32[]{:S(2)}, u32[]{:S(2)}) collective-permute-start(bf16[192,256]{1,0:T(8,128)(2,1)S(1)} %constant_dynamic-update-slice_fusion), channel_id=1, source_target_pairs={{352,0},{384,32},{0,160},{32,192},{64,224},{96,256},{128,288},{160... | collective-permute-start | bytes 294920 | tf_op jit(solution)/shard_map/ppermute | solution.py:29
  32.6 5.9 %collective-permute-start.1 = (bf16[192,256]{1,0:T(8,128)(2,1)S(1)}, bf16[192,256]{1,0:T(8,128)(2,1)S(1)}, u32[]{:S(2)}, u32[]{:S(2)}) collective-permute-start(bf16[192,256]{1,0:T(8,128)(2,1)S(1)} %constant_dynamic-update-slice_fusion), channel_id=1, source_target_pairs={{160,0},{192,32},{0,352},{32,384},{64,416},{96,448},{128,480},{161... | collective-permute-start | bytes 294920 | tf_op jit(solution)/shard_map/ppermute | solution.py:29
  38.5 0.1 collective-permute-done
  38.6 5.8 %collective-permute-done.1 = bf16[192,256]{1,0:T(8,128)(2,1)S(1)} collective-permute-done((bf16[192,256]{1,0:T(8,128)(2,1)S(1)}, bf16[192,256]{1,0:T(8,128)(2,1)S(1)}, u32[]{:S(2)}, u32[]{:S(2)}) %collective-permute-start.1) | collective-permute-done | bytes 98336 | tf_op jit(solution)/shard_map/ppermute | solution.py:29
  44.4 2.1 %collective-permute-start.2 = (bf16[576,256]{1,0:T(8,128)(2,1)S(1)}, bf16[576,256]{1,0:T(8,128)(2,1)S(1)}, u32[]{:S(2)}, u32[]{:S(2)}) collective-permute-start(bf16[576,256]{1,0:T(8,128)(2,1)S(1)} %pad_maximum_fusion.2.refs_0_), channel_id=1, source_target_pairs={{0,32},{32,64},{64,96},{96,128},{128,160},{160,192},{192,224},{224... | collective-permute-start | bytes 884744 | tf_op jit(solution)/shard_map/ppermute | solution.py:29
  46.5 4.5 %collective-permute-start.3 = (bf16[576,256]{1,0:T(8,128)(2,1)S(1)}, bf16[576,256]{1,0:T(8,128)(2,1)S(1)}, u32[]{:S(2)}, u32[]{:S(2)}) collective-permute-start(bf16[576,256]{1,0:T(8,128)(2,1)S(1)} %pad_maximum_fusion.2.refs_0_), channel_id=1, source_target_pairs={{32,0},{160,128},{192,160},{224,192},{256,224},{288,256},{320,288}... | collective-permute-start | bytes 884744 | tf_op jit(solution)/shard_map/ppermute | solution.py:29
  51.1 6.3 %collective-permute-done.2.refs_1_ = bf16[576,256]{1,0:T(8,128)(2,1)S(1)} collective-permute-done((bf16[576,256]{1,0:T(8,128)(2,1)S(1)}, bf16[576,256]{1,0:T(8,128)(2,1)S(1)}, u32[]{:S(2)}, u32[]{:S(2)}) %collective-permute-start.2) | collective-permute-done | bytes 294944 | tf_op jit(solution)/shard_map/ppermute | solution.py:29
  57.4 0.7 collective-permute-start.4
  58.1 5.2 %collective-permute-done.3.refs_2_ = bf16[576,256]{1,0:T(8,128)(2,1)S(1)} collective-permute-done((bf16[576,256]{1,0:T(8,128)(2,1)S(1)}, bf16[576,256]{1,0:T(8,128)(2,1)S(1)}, u32[]{:S(2)}, u32[]{:S(2)}) %collective-permute-start.3) | collective-permute-done | bytes 294944 | tf_op jit(solution)/shard_map/ppermute | solution.py:29
  63.3 7.7 %collective-permute-start.5 = (bf16[576,256]{1,0:T(8,128)(2,1)S(1)}, bf16[576,256]{1,0:T(8,128)(2,1)S(1)}, u32[]{:S(2)}, u32[]{:S(2)}) collective-permute-start(bf16[576,256]{1,0:T(8,128)(2,1)S(1)} %collective-permute-done.3.refs_2_), channel_id=1, source_target_pairs={{128,96},{160,128},{192,160},{224,192},{256,224},{288,256},{320,28... | collective-permute-start | bytes 884744 | tf_op jit(solution)/shard_map/ppermute | solution.py:29
  71.0 0.7 slice.140.rows_ref
  71.7 0.0 collective-permute-done.4.refs_3_
  71.8 0.7 collective-permute-start.6
  72.4 0.6 pad_add_fusion.where_ref
  73.0 10.5 %collective-permute-done.5.refs_4_ = bf16[576,256]{1,0:T(8,128)(2,1)S(1)} collective-permute-done((bf16[576,256]{1,0:T(8,128)(2,1)S(1)}, bf16[576,256]{1,0:T(8,128)(2,1)S(1)}, u32[]{:S(2)}, u32[]{:S(2)}) %collective-permute-start.5) | collective-permute-done | bytes 294944 | tf_op jit(solution)/shard_map/ppermute | solution.py:29
  83.6 0.0 collective-permute-done.6.refs_5_
  83.6 11.0 %attend.1 = bf16[768,384]{1,0:T(8,128)(2,1)} custom-call(s32[2]{0:T(128)} %pad_add_fusion.where_ref, bf16[128,768]{1,0:T(8,128)(2,1)} %slice.140.rows_ref, bf16[576,256]{1,0:T(8,128)(2,1)S(1)} %pad_maximum_fusion.2.refs_0_, bf16[576,256]{1,0:T(8,128)(2,1)S(1)} %collective-permute-done.2.refs_1_, bf16[576,256]{1,0:T(8,128)(2,1)S(1)} %collective-permute-done.3.refs_2_, ...), custom_call_target="tpu_custom_call" | custom-call | tf_op jit(solution)/shard_map/attend/pallas_call | solution.py:187
  94.6 3.5 %all-to-all-start = ((bf16[4,192,384]{2,1,0:T(8,128)(2,1)}), bf16[4,192,384]{2,1,0:T(8,128)(2,1)S(1)}, u32[]{:S(2)}, u32[]{:S(2)}) async-start(bf16[4,192,384]{2,1,0:T(8,128)(2,1)} %bitcast.51), calls=%async_computation | async-start | bytes 1179648 | tf_op jit(solution)/shard_map/all_to_all | solution.py:198
  98.7 6.8 %all-to-all-done = bf16[4,192,384]{2,1,0:T(8,128)(2,1)S(1)} async-done(((bf16[4,192,384]{2,1,0:T(8,128)(2,1)}), bf16[4,192,384]{2,1,0:T(8,128)(2,1)S(1)}, u32[]{:S(2)}, u32[]{:S(2)}) %all-to-all-start) | async-done | bytes 589856 | tf_op jit(solution)/shard_map/all_to_all | solution.py:198
  105.5 0.1 convert_element_type.81
  105.6 0.0 copy-start.6
  105.6 0.7 fusion.42
  106.3 0.6 fusion.19
  106.9 0.3 fusion.17
  107.2 0.0 copy-start.1
  107.2 0.1 copy.35
  107.3 0.0 copy-start.4
  107.3 0.1 copy.36
  107.4 0.1 multiply_reduce_fusion
  107.5 0.0 copy-done
  107.5 0.0 copy-done.6
  107.5 0.0 copy-start.5
  107.5 0.5 convolution_convert_fusion
  108.0 5.5 %collective-permute-start.7 = (bf16[4,24,2048]{2,1,0:T(8,128)(2,1)S(1)}, bf16[4,24,2048]{2,1,0:T(8,128)(2,1)S(1)}, u32[]{:S(2)}, u32[]{:S(2)}) collective-permute-start(bf16[4,24,2048]{2,1,0:T(8,128)(2,1)S(1)} %fusion.15), channel_id=1, source_target_pairs={{0,1},{1,0},{2,3},{3,2},{4,5},{5,4},{6,7},{7,6},{8,9},{9,8},{10,11... | collective-permute-start | bytes 1179656 | tf_op jit(solution)/shard_map/ppermute | solution.py:142
  113.6 1.3 collective-permute-done.7
  114.9 0.1 fusion.14
  115.0 11.0 %all_to_all.15 = bf16[4,24,2048]{2,1,0:T(8,128)(2,1)S(1)} all-to-all(bf16[4,24,2048]{2,1,0:T(8,128)(2,1)S(1)} %fusion.14), channel_id=1, replica_groups=mesh['z'=16,'y'=4,'x'=4,'c'=2] {'x'}, dimensions={0} | all-to-all | bytes 786432 | tf_op jit(solution)/shard_map/all_to_all | solution.py:144
  126.1 0.1 reduce_sum.83
  126.1 0.0 copy-done.1
  126.1 0.1 fusion.31
  126.3 0.0 copy-done.4
  126.3 0.1 fusion.33
  126.4 15.0 %all_gather.10 = bf16[192,2048]{1,0:T(8,128)(2,1)S(1)} all-gather(bf16[24,2048]{1,0:T(8,128)(2,1)S(1)} %fusion.33), channel_id=1, replica_groups=mesh['z'=16,'y'=4,'x'=4,'c'=2] {'x','c'}, dimensions={0}, use_global_device_ids=true | all-gather | bytes 884736 | tf_op jit(solution)/shard_map/all_gather | solution.py:207
  141.4 2.2 %collective-permute-start.8 = (bf16[8,2048]{1,0:T(8,128)(2,1)S(1)}, bf16[8,2048]{1,0:T(8,128)(2,1)S(1)}, u32[]{:S(2)}, u32[]{:S(2)}) collective-permute-start(bf16[8,2048]{1,0:T(8,128)(2,1)S(1)} %slice.152), channel_id=1, source_target_pairs={{0,8},{8,16},{16,24},{24,32},{32,40},{40,48},{48,56},{56,64},{64,7... | collective-permute-start | bytes 98312 | tf_op jit(solution)/shard_map/ppermute | solution.py:209
  143.6 0.0 copy-start.7
  143.7 0.9 collective-permute-done.8
  144.6 7.5 %all-gather.2.cloned.1.call-done = bf16[2048,2112]{1,0:T(8,128)(2,1)} async-done(((bf16[128,2112]{1,0:T(8,128)(2,1)}), bf16[2048,2112]{1,0:T(8,128)(2,1)}) %all-gather.2.cloned.1.call-update) | async-done | bytes 8650768 | tf_op jit(solution)/shard_map/all_gather | solution.py:172
  152.1 4.1 %fusion.4 = bf16[200,1408]{1,0:T(8,128)(2,1)S(1)} fusion(bf16[2048,2112]{1,0:T(8,128)(2,1)} %all-gather.2.cloned.1.call-done, bf16[8,2048]{1,0:T(8,128)(2,1)S(1)} %collective-permute-done.8, bf16[192,2048]{1,0:T(8,128)(2,1)S(1)} %all_gather.10), kind=kOutput, calls=%fused_computation.4 | convolution fusion | flops 1155353600 | bytes 7149568 | tf_op jit(solution)/shard_map/dot_general | solution.py:210
  156.3 3.2 %fusion.7 = bf16[192,2048]{1,0:T(8,128)(2,1)S(1)} fusion(bf16[2048,2112]{1,0:T(8,128)(2,1)} %all-gather.2.cloned.1.call-done, bf16[192,704]{1,0:T(8,128)(2,1)S(1)} %slice.156, bf16[2,704]{1,0:T(2,128)(2,1)S(1)} %slice.155, bf16[200,1408]{1,0:T(8,128)(2,1)S(1)} %fusion.4, f32[704]{0:T(1024)S(1)} %get-tuple-element.12, f32[704]{0:T(1024)S(1)} %get-tuple-element.13, ...), kind=kOutput, calls=%fused_computation.5 | convolution fusion | flops 557015040 | bytes 4541440 | tf_op jit(solution)/shard_map/dot_general | solution.py:33
  159.6 3.2 %collective-permute-start.9 = (bf16[4,24,2048]{2,1,0:T(8,128)(2,1)S(1)}, bf16[4,24,2048]{2,1,0:T(8,128)(2,1)S(1)}, u32[]{:S(2)}, u32[]{:S(2)}) collective-permute-start(bf16[4,24,2048]{2,1,0:T(8,128)(2,1)S(1)} %select_bitcast_fusion), channel_id=1, source_target_pairs={{0,1},{1,0},{2,3},{3,2},{4,5},{5,4},{6,7},{7,6},{8,9},{9,8},{10,11... | collective-permute-start | bytes 1179656 | tf_op jit(solution)/shard_map/ppermute | solution.py:142
  162.7 1.3 collective-permute-done.9
  164.1 0.1 fusion.13
  164.2 11.0 %all_to_all.16 = bf16[4,24,2048]{2,1,0:T(8,128)(2,1)S(1)} all-to-all(bf16[4,24,2048]{2,1,0:T(8,128)(2,1)S(1)} %fusion.13), channel_id=1, replica_groups=mesh['z'=16,'y'=4,'x'=4,'c'=2] {'x'}, dimensions={0} | all-to-all | bytes 786432 | tf_op jit(solution)/shard_map/all_to_all | solution.py:144
  175.2 0.1 reduce_sum.85
  175.3 0.7 fusion.34
  (17 shorter events, 0.2 us)
Async XLA Ops:
  6.5 101.0 %copy-start = (bf16[128,2048]{1,0:T(8,128)(2,1)S(1)}, bf16[128,2048]{1,0:T(8,128)(2,1)}, u32[]{:S(2)}) copy-start(bf16[128,2048]{1,0:T(8,128)(2,1)} %param.19) | copy-start | bytes 1572868
  6.5 14.8 %copy-start.2 = (bf16[192,128]{1,0:T(8,128)(2,1)S(1)}, bf16[192,128]{1,0:T(8,128)(2,1)}, u32[]{:S(2)}) copy-start(bf16[192,128]{1,0:T(8,128)(2,1)} %param.15) | copy-start | bytes 147460
  6.5 14.8 %copy-start.3 = (bf16[192,128]{1,0:T(8,128)(2,1)S(1)}, bf16[192,128]{1,0:T(8,128)(2,1)}, u32[]{:S(2)}) copy-start(bf16[192,128]{1,0:T(8,128)(2,1)} %param.16) | copy-start | bytes 147460
  6.5 145.6 %all-gather.2.cloned.1.call-start = ((), (), s32[]{:S(2)}) async-start(), calls=%async_computation.3 | async-start | bytes 9469952 | tf_op jit(solution)/shard_map/all_gather | solution.py:172
  21.4 17.2 %collective-permute-start = (bf16[192,256]{1,0:T(8,128)(2,1)S(1)}, bf16[192,256]{1,0:T(8,128)(2,1)S(1)}, u32[]{:S(2)}, u32[]{:S(2)}) collective-permute-start(bf16[192,256]{1,0:T(8,128)(2,1)S(1)} %constant_dynamic-update-slice_fusion), channel_id=1, source_target_pairs={{352,0},{384,32},{0,160},{32,192},{64,224},{96,256},{128,288},{160... | collective-permute-start | bytes 294920 | tf_op jit(solution)/shard_map/ppermute | solution.py:29
  32.6 11.8 %collective-permute-start.1 = (bf16[192,256]{1,0:T(8,128)(2,1)S(1)}, bf16[192,256]{1,0:T(8,128)(2,1)S(1)}, u32[]{:S(2)}, u32[]{:S(2)}) collective-permute-start(bf16[192,256]{1,0:T(8,128)(2,1)S(1)} %constant_dynamic-update-slice_fusion), channel_id=1, source_target_pairs={{160,0},{192,32},{0,352},{32,384},{64,416},{96,448},{128,480},{161... | collective-permute-start | bytes 294920 | tf_op jit(solution)/shard_map/ppermute | solution.py:29
  44.4 13.1 %collective-permute-start.2 = (bf16[576,256]{1,0:T(8,128)(2,1)S(1)}, bf16[576,256]{1,0:T(8,128)(2,1)S(1)}, u32[]{:S(2)}, u32[]{:S(2)}) collective-permute-start(bf16[576,256]{1,0:T(8,128)(2,1)S(1)} %pad_maximum_fusion.2.refs_0_), channel_id=1, source_target_pairs={{0,32},{32,64},{64,96},{96,128},{128,160},{160,192},{192,224},{224... | collective-permute-start | bytes 884744 | tf_op jit(solution)/shard_map/ppermute | solution.py:29
  46.5 16.8 %collective-permute-start.3 = (bf16[576,256]{1,0:T(8,128)(2,1)S(1)}, bf16[576,256]{1,0:T(8,128)(2,1)S(1)}, u32[]{:S(2)}, u32[]{:S(2)}) collective-permute-start(bf16[576,256]{1,0:T(8,128)(2,1)S(1)} %pad_maximum_fusion.2.refs_0_), channel_id=1, source_target_pairs={{32,0},{160,128},{192,160},{224,192},{256,224},{288,256},{320,288}... | collective-permute-start | bytes 884744 | tf_op jit(solution)/shard_map/ppermute | solution.py:29
  57.4 14.3 %collective-permute-start.4 = (bf16[576,256]{1,0:T(8,128)(2,1)S(1)}, bf16[576,256]{1,0:T(8,128)(2,1)S(1)}, u32[]{:S(2)}, u32[]{:S(2)}) collective-permute-start(bf16[576,256]{1,0:T(8,128)(2,1)S(1)} %collective-permute-done.2.refs_1_), channel_id=1, source_target_pairs={{32,64},{64,96},{96,128},{128,160},{160,192},{192,224},{224,256},{... | collective-permute-start | bytes 884744 | tf_op jit(solution)/shard_map/ppermute | solution.py:29
  63.3 20.3 %collective-permute-start.5 = (bf16[576,256]{1,0:T(8,128)(2,1)S(1)}, bf16[576,256]{1,0:T(8,128)(2,1)S(1)}, u32[]{:S(2)}, u32[]{:S(2)}) collective-permute-start(bf16[576,256]{1,0:T(8,128)(2,1)S(1)} %collective-permute-done.3.refs_2_), channel_id=1, source_target_pairs={{128,96},{160,128},{192,160},{224,192},{256,224},{288,256},{320,28... | collective-permute-start | bytes 884744 | tf_op jit(solution)/shard_map/ppermute | solution.py:29
  71.8 11.8 %collective-permute-start.6 = (bf16[192,256]{1,0:T(8,128)(2,1)S(1)}, bf16[192,256]{1,0:T(8,128)(2,1)S(1)}, u32[]{:S(2)}, u32[]{:S(2)}) collective-permute-start(bf16[192,256]{1,0:T(8,128)(2,1)S(1)} %slice.141), channel_id=1, source_target_pairs={{224,256},{256,288},{288,320},{320,352},{352,384},{384,416},{416,4... | collective-permute-start | bytes 294920 | tf_op jit(solution)/shard_map/ppermute | solution.py:29
  94.6 11.0 %all-to-all-start = ((bf16[4,192,384]{2,1,0:T(8,128)(2,1)}), bf16[4,192,384]{2,1,0:T(8,128)(2,1)S(1)}, u32[]{:S(2)}, u32[]{:S(2)}) async-start(bf16[4,192,384]{2,1,0:T(8,128)(2,1)} %bitcast.51), calls=%async_computation | async-start | bytes 1179648 | tf_op jit(solution)/shard_map/all_to_all | solution.py:198
  105.6 1.9 %copy-start.6 = (f32[128]{0:T(128)S(1)}, f32[128]{0:T(128)}, u32[]{:S(2)}) copy-start(f32[128]{0:T(128)} %param.18) | copy-start | bytes 1540
  107.2 18.9 %copy-start.1 = (bf16[24,2048]{1,0:T(8,128)(2,1)S(1)}, bf16[24,2048]{1,0:T(8,128)(2,1)}, u32[]{:S(2)}) copy-start(bf16[24,2048]{1,0:T(8,128)(2,1)} %param.13) | copy-start | bytes 294916
  107.3 19.0 %copy-start.4 = (f32[2048]{0:T(1024)S(1)}, f32[2048]{0:T(1024)}, u32[]{:S(2)}) copy-start(f32[2048]{0:T(1024)} %param.20) | copy-start | bytes 24580
  107.5 36.1 %copy-start.5 = (f32[3,704]{1,0:T(4,128)S(1)}, f32[3,704]{1,0:T(4,128)}, u32[]{:S(2)}) copy-start(f32[3,704]{1,0:T(4,128)} %param.23) | copy-start | bytes 25348
  108.0 6.9 %collective-permute-start.7 = (bf16[4,24,2048]{2,1,0:T(8,128)(2,1)S(1)}, bf16[4,24,2048]{2,1,0:T(8,128)(2,1)S(1)}, u32[]{:S(2)}, u32[]{:S(2)}) collective-permute-start(bf16[4,24,2048]{2,1,0:T(8,128)(2,1)S(1)} %fusion.15), channel_id=1, source_target_pairs={{0,1},{1,0},{2,3},{3,2},{4,5},{5,4},{6,7},{7,6},{8,9},{9,8},{10,11... | collective-permute-start | bytes 1179656 | tf_op jit(solution)/shard_map/ppermute | solution.py:142
  141.4 3.2 %collective-permute-start.8 = (bf16[8,2048]{1,0:T(8,128)(2,1)S(1)}, bf16[8,2048]{1,0:T(8,128)(2,1)S(1)}, u32[]{:S(2)}, u32[]{:S(2)}) collective-permute-start(bf16[8,2048]{1,0:T(8,128)(2,1)S(1)} %slice.152), channel_id=1, source_target_pairs={{0,8},{8,16},{16,24},{24,32},{32,40},{40,48},{48,56},{56,64},{64,7... | collective-permute-start | bytes 98312 | tf_op jit(solution)/shard_map/ppermute | solution.py:209
  143.6 12.6 %copy-start.7 = (f32[704]{0:T(1024)S(1)}, f32[704]{0:T(1024)}, u32[]{:S(2)}) copy-start(f32[704]{0:T(1024)} %param.24) | copy-start | bytes 8452
  159.6 4.5 %collective-permute-start.9 = (bf16[4,24,2048]{2,1,0:T(8,128)(2,1)S(1)}, bf16[4,24,2048]{2,1,0:T(8,128)(2,1)S(1)}, u32[]{:S(2)}, u32[]{:S(2)}) collective-permute-start(bf16[4,24,2048]{2,1,0:T(8,128)(2,1)S(1)} %select_bitcast_fusion), channel_id=1, source_target_pairs={{0,1},{1,0},{2,3},{3,2},{4,5},{5,4},{6,7},{7,6},{8,9},{9,8},{10,11... | collective-permute-start | bytes 1179656 | tf_op jit(solution)/shard_map/ppermute | solution.py:142
Sparse Core Ops, SparseCore 0:
  21.4 130.6 all-gather.1

commit v8 on v7

--- a/solution.py
+++ b/solution.py
@@ -115,6 +115,41 @@
         )
 
 
+def ffn_kernel(rows_ref, rim_ref, w_ref, taps_ref, bias_ref, out_ref, x_ref, acc_ref, held_ref, sems):
+    rows, d = rows_ref.shape
+    rim = rim_ref.shape[0]
+    ff = bias_ref.shape[1]
+    pieces = sems.shape[0]
+    deep = d // pieces
+    copies = []
+    for i in range(pieces):
+        part = pl.ds(i * deep, deep)
+        copies.append(pltpu.make_async_copy(w_ref.at[part, :], held_ref.at[part, :], sems.at[i]))
+        copies[-1].start()
+    x_ref[:rows, :] = rows_ref[...]
+    x_ref[rows:, :] = rim_ref[...]
+    for i in range(pieces):
+        copies[i].wait()
+        part = jnp.dot(
+            x_ref[:, i * deep : (i + 1) * deep],
+            held_ref[i * deep : (i + 1) * deep, : 2 * ff],
+            preferred_element_type=jnp.float32,
+        )
+        acc_ref[...] = part if i == 0 else acc_ref[...] + part
+    up = acc_ref[:, :ff].astype(jnp.bfloat16).astype(jnp.float32)
+    gate = acc_ref[:rows, ff : 2 * ff].astype(jnp.bfloat16).astype(jnp.float32)
+    before = up[rows:]
+    up = up[:rows]
+    at = lax.broadcasted_iota(jnp.int32, up.shape, 0)
+    one = jnp.where(at == 0, before[rim - 1 : rim], pltpu.roll(up, 1, 0))
+    two = pltpu.roll(up, 2, 0)
+    two = jnp.where(at == 0, before[rim - 2 : rim - 1], two)
+    two = jnp.where(at == 1, before[rim - 1 : rim], two)
+    conv = bias_ref[...] + taps_ref[0:1] * two + taps_ref[1:2] * one + taps_ref[2:3] * up
+    hidden = (conv / (1.0 + jnp.exp(-conv)) * gate).astype(jnp.bfloat16)
+    out_ref[...] = dot_nt(hidden, held_ref[:, 2 * ff :]).astype(jnp.bfloat16)
+
+
 def merged(got):
     got = got.astype(jnp.float32)
     means = []
@@ -207,21 +242,23 @@
     normed_all = lax.all_gather(normalize(mid, norm_gain), TP, axis=0, tiled=True)
     count = lax.axis_size("z") * lax.axis_size("y")
     rim_rows = lax.ppermute(normed_all[rows - 8 :], SP, [(i, i + 1) for i in range(count - 1)])
-    both = jnp.dot(
-        jnp.concatenate((normed_all, rim_rows), axis=0),
-        all_w[:, : 2 * ff],
-        preferred_element_type=jnp.float32,
-    ).astype(jnp.bfloat16)
-    up_proj, gate_proj = both[:rows, :ff], both[:rows, ff:]
-    taps = conv_weight.shape[0]
-    extended = jnp.concatenate((both[rows + 8 - (taps - 1) :, :ff], up_proj), axis=0)
-    conv_out = jnp.zeros((rows, ff), jnp.float32) + conv_bias[None, :]
-    for tap in range(taps):
-        conv_out = conv_out + conv_weight[tap][None, :] * extended[tap : tap + rows].astype(
-            jnp.float32
-        )
-    hidden = (jax.nn.silu(conv_out) * gate_proj.astype(jnp.float32)).astype(jnp.bfloat16)
-    ffn = dot_nt(hidden, all_w[:, 2 * ff : width]).astype(jnp.bfloat16)
+    d = normed_all.shape[1]
+    in_vmem = [
+        pltpu.with_memory_space_constraint(v, pltpu.VMEM) for v in (normed_all, rim_rows)
+    ]
+    ffn = pl.pallas_call(
+        ffn_kernel,
+        out_shape=pltpu.VMEM((rows, d), jnp.bfloat16),
+        in_specs=[VMEM, VMEM, pl.BlockSpec(memory_space=pl.ANY), VMEM, VMEM],
+        out_specs=VMEM,
+        scratch_shapes=[
+            pltpu.VMEM((rows + rim_rows.shape[0], d), jnp.bfloat16),
+            pltpu.VMEM((rows + rim_rows.shape[0], 2 * ff), jnp.float32),
+            pltpu.VMEM((d, width), jnp.bfloat16),
+            pltpu.SemaphoreType.DMA((8,)),
+        ],
+        name="ffn",
+    )(*in_vmem, all_w, conv_weight, conv_bias.reshape(1, ff))
     ffn_out = summed_over_tp(ffn)
     return (mid.astype(jnp.float32) + ffn_out.astype(jnp.float32)).astype(jnp.bfloat16)
 

time: 184 us -> 182 us (0.989)
  matrix products: 7.76 us -> 0.46 us
  Pallas kernels: 11 us -> 17.1 us
    dot_general x2 -> x0, matrix products: 7.3 us -> none  [the longest x1 4.1 us: local(): jnp.dot(jnp.concatenate((normed_all, rim_rows), axis=0), all_w[:, :2 * ff...]
    pallas_call x0 -> x1, Pallas kernels: none -> 6.04 us  [local(): pl.pallas_call(ffn_kernel, out_shape=pltpu.VMEM((rows, d), jnp.bfloat16),...]
  transfers between devices with their start and end apart: 12 -> 12, of which waited for: 10 -> 10; matrix products, arithmetic and copies ran while one was open for 2% -> 3% of each run, Pallas kernels for 6% -> 6%
where the time goes in v8:
time: 182 us
  blocking collectives  49.2 us (27%)
  starting transfers between devices  47.3 us (26%)
  waiting for transfers between devices  45.3 us (25%)
  Pallas kernels  17.1 us (9%)
  between operations  14.3 us (8%)
  local copies, waits for them, and re-layouts  4.18 us (2%)
  other arithmetic  3.73 us (2%)
    ppermute x7, starting transfers between devices, shifted(): return lax.ppermute(value, 'z', [((i - steps) % count, i) for i in targets])  32.8 us
    ppermute x7, waiting for transfers between devices, shifted(): return lax.ppermute(value, 'z', [((i - steps) % count, i) for i in targets])  28 us
    all_to_all x2, blocking collectives, summed_over_tp(): tiles = lax.all_to_all(both, 'x', 0, 0, tiled=True)  22 us
    all_gather x1, blocking collectives, local(): lax.all_gather(normalize(mid, norm_gain), TP, axis=0, tiled=True)  15 us
    all_gather x1, blocking collectives, local(): lax.all_gather(jnp.concatenate(cuts, axis=1), 'y', axis=0, tiled=True)  12.2 us
    pallas_call x1, Pallas kernels, local(): pl.pallas_call(attend_kernel, out_shape=jax.ShapeDtypeStruct((NY * rows,...  11 us
    ppermute x2, starting transfers between devices, summed_over_tp(): from_peer = lax.ppermute(for_peer, 'c', [(0, 1), (1, 0)])  8.85 us
    all_gather x1, waiting for transfers between devices, local(): all_w = lax.all_gather(row_w[:, :width], 'z', axis=0, tiled=True)  7.4 us
  transfers between devices with their start and end apart: 12, of which 10 were waited for; matrix products, arithmetic and copies ran while one was open for 3% of the time, Pallas kernels for 6%

profile of v8, /device:TPU:1, one launch (start us, length us, event | category | flops | bytes accessed | tf_op | source)
XLA Modules:
  0.0 181.6 jit_solution(11142344108221010879)
XLA Ops:
  6.5 0.0 copy-start
  6.5 0.0 all-gather.2.cloned.1.call-start
  6.5 0.8 fusion.20
  7.4 1.0 concatenate.9
  8.3 0.0 copy-start.2
  8.4 0.0 copy-start.3
  8.4 12.2 %all_gather.9 = bf16[128,2944]{1,0:T(8,128)(2,1)S(1)} all-gather(bf16[32,2944]{1,0:T(8,128)(2,1)S(1)} %concatenate.9), channel_id=1, replica_groups=mesh['z'=16,'y'=4,'x'=4,'c'=2] {'y'}, dimensions={0}, use_global_device_ids=true | all-gather | bytes 942080 | tf_op jit(solution)/shard_map/all_gather | solution.py:206
  20.6 0.8 slice.113
  21.4 0.0 all-gather.2.cloned.1.call-update
  21.5 0.0 copy-done.2
  21.5 0.0 copy-done.3
  21.5 11.2 %collective-permute-start = (bf16[192,256]{1,0:T(8,128)(2,1)S(1)}, bf16[192,256]{1,0:T(8,128)(2,1)S(1)}, u32[]{:S(2)}, u32[]{:S(2)}) collective-permute-start(bf16[192,256]{1,0:T(8,128)(2,1)S(1)} %constant_dynamic-update-slice_fusion), channel_id=1, source_target_pairs={{352,0},{384,32},{0,160},{32,192},{64,224},{96,256},{128,288},{160... | collective-permute-start | bytes 294920 | tf_op jit(solution)/shard_map/ppermute | solution.py:29
  32.7 5.9 %collective-permute-start.1 = (bf16[192,256]{1,0:T(8,128)(2,1)S(1)}, bf16[192,256]{1,0:T(8,128)(2,1)S(1)}, u32[]{:S(2)}, u32[]{:S(2)}) collective-permute-start(bf16[192,256]{1,0:T(8,128)(2,1)S(1)} %constant_dynamic-update-slice_fusion), channel_id=1, source_target_pairs={{160,0},{192,32},{0,352},{32,384},{64,416},{96,448},{128,480},{161... | collective-permute-start | bytes 294920 | tf_op jit(solution)/shard_map/ppermute | solution.py:29
  38.6 0.1 collective-permute-done
  38.7 5.8 %collective-permute-done.1 = bf16[192,256]{1,0:T(8,128)(2,1)S(1)} collective-permute-done((bf16[192,256]{1,0:T(8,128)(2,1)S(1)}, bf16[192,256]{1,0:T(8,128)(2,1)S(1)}, u32[]{:S(2)}, u32[]{:S(2)}) %collective-permute-start.1) | collective-permute-done | bytes 98336 | tf_op jit(solution)/shard_map/ppermute | solution.py:29
  44.5 2.1 %collective-permute-start.2 = (bf16[576,256]{1,0:T(8,128)(2,1)S(1)}, bf16[576,256]{1,0:T(8,128)(2,1)S(1)}, u32[]{:S(2)}, u32[]{:S(2)}) collective-permute-start(bf16[576,256]{1,0:T(8,128)(2,1)S(1)} %pad_maximum_fusion.refs_0_), channel_id=1, source_target_pairs={{0,32},{32,64},{64,96},{96,128},{128,160},{160,192},{192,224},{224... | collective-permute-start | bytes 884744 | tf_op jit(solution)/shard_map/ppermute | solution.py:29
  46.7 4.5 %collective-permute-start.3 = (bf16[576,256]{1,0:T(8,128)(2,1)S(1)}, bf16[576,256]{1,0:T(8,128)(2,1)S(1)}, u32[]{:S(2)}, u32[]{:S(2)}) collective-permute-start(bf16[576,256]{1,0:T(8,128)(2,1)S(1)} %pad_maximum_fusion.refs_0_), channel_id=1, source_target_pairs={{32,0},{160,128},{192,160},{224,192},{256,224},{288,256},{320,288}... | collective-permute-start | bytes 884744 | tf_op jit(solution)/shard_map/ppermute | solution.py:29
  51.2 6.3 %collective-permute-done.2.refs_1_ = bf16[576,256]{1,0:T(8,128)(2,1)S(1)} collective-permute-done((bf16[576,256]{1,0:T(8,128)(2,1)S(1)}, bf16[576,256]{1,0:T(8,128)(2,1)S(1)}, u32[]{:S(2)}, u32[]{:S(2)}) %collective-permute-start.2) | collective-permute-done | bytes 294944 | tf_op jit(solution)/shard_map/ppermute | solution.py:29
  57.6 0.7 collective-permute-start.4
  58.3 5.2 %collective-permute-done.3.refs_2_ = bf16[576,256]{1,0:T(8,128)(2,1)S(1)} collective-permute-done((bf16[576,256]{1,0:T(8,128)(2,1)S(1)}, bf16[576,256]{1,0:T(8,128)(2,1)S(1)}, u32[]{:S(2)}, u32[]{:S(2)}) %collective-permute-start.3) | collective-permute-done | bytes 294944 | tf_op jit(solution)/shard_map/ppermute | solution.py:29
  63.4 7.7 %collective-permute-start.5 = (bf16[576,256]{1,0:T(8,128)(2,1)S(1)}, bf16[576,256]{1,0:T(8,128)(2,1)S(1)}, u32[]{:S(2)}, u32[]{:S(2)}) collective-permute-start(bf16[576,256]{1,0:T(8,128)(2,1)S(1)} %collective-permute-done.3.refs_2_), channel_id=1, source_target_pairs={{128,96},{160,128},{192,160},{224,192},{256,224},{288,256},{320,28... | collective-permute-start | bytes 884744 | tf_op jit(solution)/shard_map/ppermute | solution.py:29
  71.2 0.7 slice.100.rows_ref
  71.9 0.0 collective-permute-done.4.refs_3_
  71.9 0.7 collective-permute-start.6
  72.6 0.6 pad_add_fusion.where_ref
  73.2 10.5 %collective-permute-done.5.refs_4_ = bf16[576,256]{1,0:T(8,128)(2,1)S(1)} collective-permute-done((bf16[576,256]{1,0:T(8,128)(2,1)S(1)}, bf16[576,256]{1,0:T(8,128)(2,1)S(1)}, u32[]{:S(2)}, u32[]{:S(2)}) %collective-permute-start.5) | collective-permute-done | bytes 294944 | tf_op jit(solution)/shard_map/ppermute | solution.py:29
  83.7 0.0 collective-permute-done.6.refs_5_
  83.7 11.0 %attend.1 = bf16[768,384]{1,0:T(8,128)(2,1)} custom-call(s32[2]{0:T(128)} %pad_add_fusion.where_ref, bf16[128,768]{1,0:T(8,128)(2,1)} %slice.100.rows_ref, bf16[576,256]{1,0:T(8,128)(2,1)S(1)} %pad_maximum_fusion.refs_0_, bf16[576,256]{1,0:T(8,128)(2,1)S(1)} %collective-permute-done.2.refs_1_, bf16[576,256]{1,0:T(8,128)(2,1)S(1)} %collective-permute-done.3.refs_2_, ...), custom_call_target="tpu_custom_call" | custom-call | tf_op jit(solution)/shard_map/attend/pallas_call | solution.py:222
  94.7 3.5 %all-to-all-start = ((bf16[4,192,384]{2,1,0:T(8,128)(2,1)}), bf16[4,192,384]{2,1,0:T(8,128)(2,1)S(1)}, u32[]{:S(2)}, u32[]{:S(2)}) async-start(bf16[4,192,384]{2,1,0:T(8,128)(2,1)} %bitcast.51), calls=%async_computation | async-start | bytes 1179648 | tf_op jit(solution)/shard_map/all_to_all | solution.py:233
  98.9 6.8 %all-to-all-done = bf16[4,192,384]{2,1,0:T(8,128)(2,1)S(1)} async-done(((bf16[4,192,384]{2,1,0:T(8,128)(2,1)}), bf16[4,192,384]{2,1,0:T(8,128)(2,1)S(1)}, u32[]{:S(2)}, u32[]{:S(2)}) %all-to-all-start) | async-done | bytes 589856 | tf_op jit(solution)/shard_map/all_to_all | solution.py:233
  105.7 0.1 convert_element_type.60
  105.8 0.7 fusion.18
  106.5 0.6 fusion.6
  107.0 0.3 fusion.4
  107.3 0.1 copy.35
  107.4 0.1 copy.36
  107.5 0.1 multiply_reduce_fusion
  107.6 0.0 copy-done
  107.6 0.0 copy-done.6
  107.6 0.5 convolution_convert_fusion
  108.1 0.0 copy-start.1
  108.1 0.0 copy-start.4
  108.2 5.7 %collective-permute-start.7 = (bf16[4,24,2048]{2,1,0:T(8,128)(2,1)S(1)}, bf16[4,24,2048]{2,1,0:T(8,128)(2,1)S(1)}, u32[]{:S(2)}, u32[]{:S(2)}) collective-permute-start(bf16[4,24,2048]{2,1,0:T(8,128)(2,1)S(1)} %select_bitcast_fusion), channel_id=1, source_target_pairs={{0,1},{1,0},{2,3},{3,2},{4,5},{5,4},{6,7},{7,6},{8,9},{9,8},{10,11... | collective-permute-start | bytes 1179656 | tf_op jit(solution)/shard_map/ppermute | solution.py:177
  113.8 1.3 collective-permute-done.7
  115.2 0.1 fusion.1
  115.3 0.0 copy-start.5
  115.3 11.0 %all_to_all.15 = bf16[4,24,2048]{2,1,0:T(8,128)(2,1)S(1)} all-to-all(bf16[4,24,2048]{2,1,0:T(8,128)(2,1)S(1)} %fusion.1), channel_id=1, replica_groups=mesh['z'=16,'y'=4,'x'=4,'c'=2] {'x'}, dimensions={0} | all-to-all | bytes 786432 | tf_op jit(solution)/shard_map/all_to_all | solution.py:179
  126.4 0.1 reduce_sum.83
  126.4 0.0 copy-done.1
  126.4 0.1 fusion.10
  126.6 0.1 fusion.12
  126.7 15.0 %all_gather.10.rows_ref = bf16[192,2048]{1,0:T(8,128)(2,1)S(1)} all-gather(bf16[24,2048]{1,0:T(8,128)(2,1)S(1)} %fusion.12), channel_id=1, replica_groups=mesh['z'=16,'y'=4,'x'=4,'c'=2] {'x','c'}, dimensions={0}, use_global_device_ids=true | all-gather | bytes 884736 | tf_op jit(solution)/shard_map/all_gather | solution.py:242
  141.7 2.2 %collective-permute-start.8 = (bf16[8,2048]{1,0:T(8,128)(2,1)S(1)}, bf16[8,2048]{1,0:T(8,128)(2,1)S(1)}, u32[]{:S(2)}, u32[]{:S(2)}) collective-permute-start(bf16[8,2048]{1,0:T(8,128)(2,1)S(1)} %slice.112), channel_id=1, source_target_pairs={{0,8},{8,16},{16,24},{24,32},{32,40},{40,48},{48,56},{56,64},{64,7... | collective-permute-start | bytes 98312 | tf_op jit(solution)/shard_map/ppermute | solution.py:244
  143.9 0.0 copy-done.5
  143.9 0.6 reshape.58.bias_ref
  144.5 0.4 collective-permute-done.8.rim_ref
  144.9 7.4 %all-gather.2.cloned.1.call-done.w_ref = bf16[2048,2112]{1,0:T(8,128)(2,1)} async-done(((bf16[128,2112]{1,0:T(8,128)(2,1)}), bf16[2048,2112]{1,0:T(8,128)(2,1)}) %all-gather.2.cloned.1.call-update) | async-done | bytes 8650768 | tf_op jit(solution)/shard_map/all_gather | solution.py:207
  152.3 6.0 %ffn.1 = bf16[192,2048]{1,0:T(8,128)(2,1)S(1)} custom-call(bf16[192,2048]{1,0:T(8,128)(2,1)S(1)} %all_gather.10.rows_ref, bf16[8,2048]{1,0:T(8,128)(2,1)S(1)} %collective-permute-done.8.rim_ref, bf16[2048,2112]{1,0:T(8,128)(2,1)} %all-gather.2.cloned.1.call-done.w_ref, f32[3,704]{1,0:T(4,128)} %taps_ref.1, f32[1,704]{1,0:T(1,128)} %reshape.58.bias_ref), custom_call_target="tpu_custom_call" | custom-call | tf_op jit(solution)/shard_map/ffn/pallas_call | solution.py:249
  158.4 3.2 %collective-permute-start.9 = (bf16[4,24,2048]{2,1,0:T(8,128)(2,1)S(1)}, bf16[4,24,2048]{2,1,0:T(8,128)(2,1)S(1)}, u32[]{:S(2)}, u32[]{:S(2)}) collective-permute-start(bf16[4,24,2048]{2,1,0:T(8,128)(2,1)S(1)} %fusion.2), channel_id=1, source_target_pairs={{0,1},{1,0},{2,3},{3,2},{4,5},{5,4},{6,7},{7,6},{8,9},{9,8},{10,11... | collective-permute-start | bytes 1179656 | tf_op jit(solution)/shard_map/ppermute | solution.py:177
  161.6 1.3 collective-permute-done.9
  162.9 0.1 fusion
  163.0 11.0 %all_to_all.16 = bf16[4,24,2048]{2,1,0:T(8,128)(2,1)S(1)} all-to-all(bf16[4,24,2048]{2,1,0:T(8,128)(2,1)S(1)} %fusion), channel_id=1, replica_groups=mesh['z'=16,'y'=4,'x'=4,'c'=2] {'x'}, dimensions={0} | all-to-all | bytes 786432 | tf_op jit(solution)/shard_map/all_to_all | solution.py:179
  174.0 0.1 reduce_sum.85
  174.1 0.7 fusion.13
  (12 shorter events, 0.2 us)
Async XLA Ops:
  6.5 101.1 %copy-start = (bf16[128,2048]{1,0:T(8,128)(2,1)S(1)}, bf16[128,2048]{1,0:T(8,128)(2,1)}, u32[]{:S(2)}) copy-start(bf16[128,2048]{1,0:T(8,128)(2,1)} %param.19) | copy-start | bytes 1572868
  6.5 145.7 %all-gather.2.cloned.1.call-start = ((), (), s32[]{:S(2)}) async-start(), calls=%async_computation.3 | async-start | bytes 9469952 | tf_op jit(solution)/shard_map/all_gather | solution.py:207
  8.3 13.1 %copy-start.2 = (bf16[192,128]{1,0:T(8,128)(2,1)S(1)}, bf16[192,128]{1,0:T(8,128)(2,1)}, u32[]{:S(2)}) copy-start(bf16[192,128]{1,0:T(8,128)(2,1)} %param.15) | copy-start | bytes 147460
  8.4 13.1 %copy-start.3 = (bf16[192,128]{1,0:T(8,128)(2,1)S(1)}, bf16[192,128]{1,0:T(8,128)(2,1)}, u32[]{:S(2)}) copy-start(bf16[192,128]{1,0:T(8,128)(2,1)} %param.16) | copy-start | bytes 147460
  21.5 17.2 %collective-permute-start = (bf16[192,256]{1,0:T(8,128)(2,1)S(1)}, bf16[192,256]{1,0:T(8,128)(2,1)S(1)}, u32[]{:S(2)}, u32[]{:S(2)}) collective-permute-start(bf16[192,256]{1,0:T(8,128)(2,1)S(1)} %constant_dynamic-update-slice_fusion), channel_id=1, source_target_pairs={{352,0},{384,32},{0,160},{32,192},{64,224},{96,256},{128,288},{160... | collective-permute-start | bytes 294920 | tf_op jit(solution)/shard_map/ppermute | solution.py:29
  32.7 11.8 %collective-permute-start.1 = (bf16[192,256]{1,0:T(8,128)(2,1)S(1)}, bf16[192,256]{1,0:T(8,128)(2,1)S(1)}, u32[]{:S(2)}, u32[]{:S(2)}) collective-permute-start(bf16[192,256]{1,0:T(8,128)(2,1)S(1)} %constant_dynamic-update-slice_fusion), channel_id=1, source_target_pairs={{160,0},{192,32},{0,352},{32,384},{64,416},{96,448},{128,480},{161... | collective-permute-start | bytes 294920 | tf_op jit(solution)/shard_map/ppermute | solution.py:29
  44.5 13.1 %collective-permute-start.2 = (bf16[576,256]{1,0:T(8,128)(2,1)S(1)}, bf16[576,256]{1,0:T(8,128)(2,1)S(1)}, u32[]{:S(2)}, u32[]{:S(2)}) collective-permute-start(bf16[576,256]{1,0:T(8,128)(2,1)S(1)} %pad_maximum_fusion.refs_0_), channel_id=1, source_target_pairs={{0,32},{32,64},{64,96},{96,128},{128,160},{160,192},{192,224},{224... | collective-permute-start | bytes 884744 | tf_op jit(solution)/shard_map/ppermute | solution.py:29
  46.7 16.8 %collective-permute-start.3 = (bf16[576,256]{1,0:T(8,128)(2,1)S(1)}, bf16[576,256]{1,0:T(8,128)(2,1)S(1)}, u32[]{:S(2)}, u32[]{:S(2)}) collective-permute-start(bf16[576,256]{1,0:T(8,128)(2,1)S(1)} %pad_maximum_fusion.refs_0_), channel_id=1, source_target_pairs={{32,0},{160,128},{192,160},{224,192},{256,224},{288,256},{320,288}... | collective-permute-start | bytes 884744 | tf_op jit(solution)/shard_map/ppermute | solution.py:29
  57.6 14.3 %collective-permute-start.4 = (bf16[576,256]{1,0:T(8,128)(2,1)S(1)}, bf16[576,256]{1,0:T(8,128)(2,1)S(1)}, u32[]{:S(2)}, u32[]{:S(2)}) collective-permute-start(bf16[576,256]{1,0:T(8,128)(2,1)S(1)} %collective-permute-done.2.refs_1_), channel_id=1, source_target_pairs={{32,64},{64,96},{96,128},{128,160},{160,192},{192,224},{224,256},{... | collective-permute-start | bytes 884744 | tf_op jit(solution)/shard_map/ppermute | solution.py:29
  63.4 20.3 %collective-permute-start.5 = (bf16[576,256]{1,0:T(8,128)(2,1)S(1)}, bf16[576,256]{1,0:T(8,128)(2,1)S(1)}, u32[]{:S(2)}, u32[]{:S(2)}) collective-permute-start(bf16[576,256]{1,0:T(8,128)(2,1)S(1)} %collective-permute-done.3.refs_2_), channel_id=1, source_target_pairs={{128,96},{160,128},{192,160},{224,192},{256,224},{288,256},{320,28... | collective-permute-start | bytes 884744 | tf_op jit(solution)/shard_map/ppermute | solution.py:29
  71.9 11.8 %collective-permute-start.6 = (bf16[192,256]{1,0:T(8,128)(2,1)S(1)}, bf16[192,256]{1,0:T(8,128)(2,1)S(1)}, u32[]{:S(2)}, u32[]{:S(2)}) collective-permute-start(bf16[192,256]{1,0:T(8,128)(2,1)S(1)} %slice.101), channel_id=1, source_target_pairs={{224,256},{256,288},{288,320},{320,352},{352,384},{384,416},{416,4... | collective-permute-start | bytes 294920 | tf_op jit(solution)/shard_map/ppermute | solution.py:29
  94.7 11.0 %all-to-all-start = ((bf16[4,192,384]{2,1,0:T(8,128)(2,1)}), bf16[4,192,384]{2,1,0:T(8,128)(2,1)S(1)}, u32[]{:S(2)}, u32[]{:S(2)}) async-start(bf16[4,192,384]{2,1,0:T(8,128)(2,1)} %bitcast.51), calls=%async_computation | async-start | bytes 1179648 | tf_op jit(solution)/shard_map/all_to_all | solution.py:233
  106.5 1.1 copy-start.6
  108.1 18.3 %copy-start.1 = (bf16[24,2048]{1,0:T(8,128)(2,1)S(1)}, bf16[24,2048]{1,0:T(8,128)(2,1)}, u32[]{:S(2)}) copy-start(bf16[24,2048]{1,0:T(8,128)(2,1)} %param.13) | copy-start | bytes 294916
  108.1 18.4 %copy-start.4 = (f32[2048]{0:T(1024)S(1)}, f32[2048]{0:T(1024)}, u32[]{:S(2)}) copy-start(f32[2048]{0:T(1024)} %param.20) | copy-start | bytes 24580
  108.2 7.0 %collective-permute-start.7 = (bf16[4,24,2048]{2,1,0:T(8,128)(2,1)S(1)}, bf16[4,24,2048]{2,1,0:T(8,128)(2,1)S(1)}, u32[]{:S(2)}, u32[]{:S(2)}) collective-permute-start(bf16[4,24,2048]{2,1,0:T(8,128)(2,1)S(1)} %select_bitcast_fusion), channel_id=1, source_target_pairs={{0,1},{1,0},{2,3},{3,2},{4,5},{5,4},{6,7},{7,6},{8,9},{9,8},{10,11... | collective-permute-start | bytes 1179656 | tf_op jit(solution)/shard_map/ppermute | solution.py:177
  115.3 28.6 %copy-start.5 = (f32[704]{0:T(1024)S(1)}, f32[704]{0:T(1024)}, u32[]{:S(2)}) copy-start(f32[704]{0:T(1024)} %param.24) | copy-start | bytes 8452
  141.7 3.2 %collective-permute-start.8 = (bf16[8,2048]{1,0:T(8,128)(2,1)S(1)}, bf16[8,2048]{1,0:T(8,128)(2,1)S(1)}, u32[]{:S(2)}, u32[]{:S(2)}) collective-permute-start(bf16[8,2048]{1,0:T(8,128)(2,1)S(1)} %slice.112), channel_id=1, source_target_pairs={{0,8},{8,16},{16,24},{24,32},{32,40},{40,48},{48,56},{56,64},{64,7... | collective-permute-start | bytes 98312 | tf_op jit(solution)/shard_map/ppermute | solution.py:244
  158.4 4.5 %collective-permute-start.9 = (bf16[4,24,2048]{2,1,0:T(8,128)(2,1)S(1)}, bf16[4,24,2048]{2,1,0:T(8,128)(2,1)S(1)}, u32[]{:S(2)}, u32[]{:S(2)}) collective-permute-start(bf16[4,24,2048]{2,1,0:T(8,128)(2,1)S(1)} %fusion.2), channel_id=1, source_target_pairs={{0,1},{1,0},{2,3},{3,2},{4,5},{5,4},{6,7},{7,6},{8,9},{9,8},{10,11... | collective-permute-start | bytes 1179656 | tf_op jit(solution)/shard_map/ppermute | solution.py:177
Sparse Core Ops, SparseCore 0:
  21.6 130.6 all-gather.1

commit v9 on v8

--- a/solution.py
+++ b/solution.py
@@ -116,28 +116,24 @@
 
 
 def ffn_kernel(rows_ref, rim_ref, w_ref, taps_ref, bias_ref, out_ref, x_ref, acc_ref, held_ref, sems):
-    rows, d = rows_ref.shape
+    rows = rows_ref.shape[0]
     rim = rim_ref.shape[0]
     ff = bias_ref.shape[1]
-    pieces = sems.shape[0]
-    deep = d // pieces
+    edges = [*range(0, 2 * ff - 2 * LANES, 4 * LANES), 2 * ff, 3 * ff]
     copies = []
-    for i in range(pieces):
-        part = pl.ds(i * deep, deep)
-        copies.append(pltpu.make_async_copy(w_ref.at[part, :], held_ref.at[part, :], sems.at[i]))
+    for i, (start, end) in enumerate(zip(edges, edges[1:])):
+        part = pl.ds(start, end - start)
+        copies.append(pltpu.make_async_copy(w_ref.at[:, part], held_ref.at[:, part], sems.at[i]))
         copies[-1].start()
     x_ref[:rows, :] = rows_ref[...]
     x_ref[rows:, :] = rim_ref[...]
-    for i in range(pieces):
+    for i, (start, end) in enumerate(zip(edges[:-1], edges[1:-1])):
         copies[i].wait()
-        part = jnp.dot(
-            x_ref[:, i * deep : (i + 1) * deep],
-            held_ref[i * deep : (i + 1) * deep, : 2 * ff],
-            preferred_element_type=jnp.float32,
-        )
-        acc_ref[...] = part if i == 0 else acc_ref[...] + part
-    up = acc_ref[:, :ff].astype(jnp.bfloat16).astype(jnp.float32)
-    gate = acc_ref[:rows, ff : 2 * ff].astype(jnp.bfloat16).astype(jnp.float32)
+        acc_ref[:, start:end] = jnp.dot(
+            x_ref[...], held_ref[:, start:end], preferred_element_type=jnp.float32
+        ).astype(jnp.bfloat16)
+    up = acc_ref[:, :ff].astype(jnp.float32)
+    gate = acc_ref[:rows, ff : 2 * ff].astype(jnp.float32)
     before = up[rows:]
     up = up[:rows]
     at = lax.broadcasted_iota(jnp.int32, up.shape, 0)
@@ -147,6 +143,7 @@
     two = jnp.where(at == 1, before[rim - 1 : rim], two)
     conv = bias_ref[...] + taps_ref[0:1] * two + taps_ref[1:2] * one + taps_ref[2:3] * up
     hidden = (conv / (1.0 + jnp.exp(-conv)) * gate).astype(jnp.bfloat16)
+    copies[-1].wait()
     out_ref[...] = dot_nt(hidden, held_ref[:, 2 * ff :]).astype(jnp.bfloat16)
 
 
@@ -221,7 +218,7 @@
     blocks = [pltpu.with_memory_space_constraint(b, pltpu.VMEM) for b in blocks]
     parts = pl.pallas_call(
         attend_kernel,
-        out_shape=jax.ShapeDtypeStruct((NY * rows, 3 * VD), jnp.bfloat16),
+        out_shape=pltpu.VMEM((NY * rows, 3 * VD), jnp.bfloat16),
         in_specs=[SMEM] + [VMEM] * (1 + len(blocks)),
         out_specs=VMEM,
         scratch_shapes=[
@@ -253,9 +250,9 @@
         out_specs=VMEM,
         scratch_shapes=[
             pltpu.VMEM((rows + rim_rows.shape[0], d), jnp.bfloat16),
-            pltpu.VMEM((rows + rim_rows.shape[0], 2 * ff), jnp.float32),
+            pltpu.VMEM((rows + rim_rows.shape[0], 2 * ff), jnp.bfloat16),
             pltpu.VMEM((d, width), jnp.bfloat16),
-            pltpu.SemaphoreType.DMA((8,)),
+            pltpu.SemaphoreType.DMA((4,)),
         ],
         name="ffn",
     )(*in_vmem, all_w, conv_weight, conv_bias.reshape(1, ff))

time: 182 us -> 182 us (level)
  no operation moved by 1% of the time
where the time goes in v9:
time: 182 us; the launch traced here: 181 us
  blocking collectives  49.2 us (27%)
  starting transfers between devices  47.4 us (26%)
  waiting for transfers between devices  45.3 us (25%)
  Pallas kernels  16.8 us (9%)
  between operations  14.3 us (8%)
  local copies, waits for them, and re-layouts  4.18 us (2%)
  other arithmetic  3.73 us (2%)
    ppermute x7, starting transfers between devices, shifted(): return lax.ppermute(value, 'z', [((i - steps) % count, i) for i in targets])  32.8 us
    ppermute x7, waiting for transfers between devices, shifted(): return lax.ppermute(value, 'z', [((i - steps) % count, i) for i in targets])  28 us
    all_to_all x2, blocking collectives, summed_over_tp(): tiles = lax.all_to_all(both, 'x', 0, 0, tiled=True)  22 us
    all_gather x1, blocking collectives, local(): lax.all_gather(normalize(mid, norm_gain), TP, axis=0, tiled=True)  15 us
    all_gather x1, blocking collectives, local(): lax.all_gather(jnp.concatenate(cuts, axis=1), 'y', axis=0, tiled=True)  12.2 us
    pallas_call x1, Pallas kernels, local(): pl.pallas_call(attend_kernel, out_shape=pltpu.VMEM((NY * rows, 3 * VD), j...  11 us
    ppermute x2, starting transfers between devices, summed_over_tp(): from_peer = lax.ppermute(for_peer, 'c', [(0, 1), (1, 0)])  8.86 us
    all_gather x1, waiting for transfers between devices, local(): all_w = lax.all_gather(row_w[:, :width], 'z', axis=0, tiled=True)  7.4 us
  transfers between devices with their start and end apart: 12, of which 10 were waited for; matrix products, arithmetic and copies ran while one was open for 3% of the time, Pallas kernels for 6%

profile of v9, /device:TPU:1, one launch (start us, length us, event | category | flops | bytes accessed | tf_op | source)
XLA Modules:
  0.0 181.4 jit_solution(4540968019468914026)
XLA Ops:
  6.5 0.0 copy-start
  6.5 0.0 all-gather.2.cloned.1.call-start
  6.5 0.8 fusion.20
  7.4 1.0 concatenate.9
  8.3 0.0 copy-start.2
  8.4 0.0 copy-start.3
  8.4 12.2 %all_gather.9 = bf16[128,2944]{1,0:T(8,128)(2,1)S(1)} all-gather(bf16[32,2944]{1,0:T(8,128)(2,1)S(1)} %concatenate.9), channel_id=1, replica_groups=mesh['z'=16,'y'=4,'x'=4,'c'=2] {'y'}, dimensions={0}, use_global_device_ids=true | all-gather | bytes 942080 | tf_op jit(solution)/shard_map/all_gather | solution.py:203
  20.6 0.8 slice.113
  21.4 0.0 all-gather.2.cloned.1.call-update
  21.5 0.0 copy-done.2
  21.5 0.0 copy-done.3
  21.5 11.2 %collective-permute-start = (bf16[192,256]{1,0:T(8,128)(2,1)S(1)}, bf16[192,256]{1,0:T(8,128)(2,1)S(1)}, u32[]{:S(2)}, u32[]{:S(2)}) collective-permute-start(bf16[192,256]{1,0:T(8,128)(2,1)S(1)} %constant_dynamic-update-slice_fusion), channel_id=1, source_target_pairs={{352,0},{384,32},{0,160},{32,192},{64,224},{96,256},{128,288},{160... | collective-permute-start | bytes 294920 | tf_op jit(solution)/shard_map/ppermute | solution.py:29
  32.7 5.9 %collective-permute-start.1 = (bf16[192,256]{1,0:T(8,128)(2,1)S(1)}, bf16[192,256]{1,0:T(8,128)(2,1)S(1)}, u32[]{:S(2)}, u32[]{:S(2)}) collective-permute-start(bf16[192,256]{1,0:T(8,128)(2,1)S(1)} %constant_dynamic-update-slice_fusion), channel_id=1, source_target_pairs={{160,0},{192,32},{0,352},{32,384},{64,416},{96,448},{128,480},{161... | collective-permute-start | bytes 294920 | tf_op jit(solution)/shard_map/ppermute | solution.py:29
  38.6 0.1 collective-permute-done
  38.7 5.8 %collective-permute-done.1 = bf16[192,256]{1,0:T(8,128)(2,1)S(1)} collective-permute-done((bf16[192,256]{1,0:T(8,128)(2,1)S(1)}, bf16[192,256]{1,0:T(8,128)(2,1)S(1)}, u32[]{:S(2)}, u32[]{:S(2)}) %collective-permute-start.1) | collective-permute-done | bytes 98336 | tf_op jit(solution)/shard_map/ppermute | solution.py:29
  44.5 2.1 %collective-permute-start.2 = (bf16[576,256]{1,0:T(8,128)(2,1)S(1)}, bf16[576,256]{1,0:T(8,128)(2,1)S(1)}, u32[]{:S(2)}, u32[]{:S(2)}) collective-permute-start(bf16[576,256]{1,0:T(8,128)(2,1)S(1)} %pad_maximum_fusion.refs_0_), channel_id=1, source_target_pairs={{0,32},{32,64},{64,96},{96,128},{128,160},{160,192},{192,224},{224... | collective-permute-start | bytes 884744 | tf_op jit(solution)/shard_map/ppermute | solution.py:29
  46.7 4.5 %collective-permute-start.3 = (bf16[576,256]{1,0:T(8,128)(2,1)S(1)}, bf16[576,256]{1,0:T(8,128)(2,1)S(1)}, u32[]{:S(2)}, u32[]{:S(2)}) collective-permute-start(bf16[576,256]{1,0:T(8,128)(2,1)S(1)} %pad_maximum_fusion.refs_0_), channel_id=1, source_target_pairs={{32,0},{160,128},{192,160},{224,192},{256,224},{288,256},{320,288}... | collective-permute-start | bytes 884744 | tf_op jit(solution)/shard_map/ppermute | solution.py:29
  51.2 6.3 %collective-permute-done.2.refs_1_ = bf16[576,256]{1,0:T(8,128)(2,1)S(1)} collective-permute-done((bf16[576,256]{1,0:T(8,128)(2,1)S(1)}, bf16[576,256]{1,0:T(8,128)(2,1)S(1)}, u32[]{:S(2)}, u32[]{:S(2)}) %collective-permute-start.2) | collective-permute-done | bytes 294944 | tf_op jit(solution)/shard_map/ppermute | solution.py:29
  57.6 0.7 collective-permute-start.4
  58.3 5.2 %collective-permute-done.3.refs_2_ = bf16[576,256]{1,0:T(8,128)(2,1)S(1)} collective-permute-done((bf16[576,256]{1,0:T(8,128)(2,1)S(1)}, bf16[576,256]{1,0:T(8,128)(2,1)S(1)}, u32[]{:S(2)}, u32[]{:S(2)}) %collective-permute-start.3) | collective-permute-done | bytes 294944 | tf_op jit(solution)/shard_map/ppermute | solution.py:29
  63.4 7.7 %collective-permute-start.5 = (bf16[576,256]{1,0:T(8,128)(2,1)S(1)}, bf16[576,256]{1,0:T(8,128)(2,1)S(1)}, u32[]{:S(2)}, u32[]{:S(2)}) collective-permute-start(bf16[576,256]{1,0:T(8,128)(2,1)S(1)} %collective-permute-done.3.refs_2_), channel_id=1, source_target_pairs={{128,96},{160,128},{192,160},{224,192},{256,224},{288,256},{320,28... | collective-permute-start | bytes 884744 | tf_op jit(solution)/shard_map/ppermute | solution.py:29
  71.2 0.7 slice.100.rows_ref
  71.9 0.0 collective-permute-done.4.refs_3_
  71.9 0.7 collective-permute-start.6
  72.6 0.6 pad_add_fusion.where_ref
  73.2 10.5 %collective-permute-done.5.refs_4_ = bf16[576,256]{1,0:T(8,128)(2,1)S(1)} collective-permute-done((bf16[576,256]{1,0:T(8,128)(2,1)S(1)}, bf16[576,256]{1,0:T(8,128)(2,1)S(1)}, u32[]{:S(2)}, u32[]{:S(2)}) %collective-permute-start.5) | collective-permute-done | bytes 294944 | tf_op jit(solution)/shard_map/ppermute | solution.py:29
  83.7 0.0 collective-permute-done.6.refs_5_
  83.7 11.0 %attend.1 = bf16[768,384]{1,0:T(8,128)(2,1)} custom-call(s32[2]{0:T(128)} %pad_add_fusion.where_ref, bf16[128,768]{1,0:T(8,128)(2,1)} %slice.100.rows_ref, bf16[576,256]{1,0:T(8,128)(2,1)S(1)} %pad_maximum_fusion.refs_0_, bf16[576,256]{1,0:T(8,128)(2,1)S(1)} %collective-permute-done.2.refs_1_, bf16[576,256]{1,0:T(8,128)(2,1)S(1)} %collective-permute-done.3.refs_2_, ...), custom_call_target="tpu_custom_call" | custom-call | tf_op jit(solution)/shard_map/attend/pallas_call | solution.py:219
  94.7 3.5 %all-to-all-start = ((bf16[4,192,384]{2,1,0:T(8,128)(2,1)}), bf16[4,192,384]{2,1,0:T(8,128)(2,1)S(1)}, u32[]{:S(2)}, u32[]{:S(2)}) async-start(bf16[4,192,384]{2,1,0:T(8,128)(2,1)} %bitcast.3), calls=%async_computation | async-start | bytes 1179648 | tf_op jit(solution)/shard_map/all_to_all | solution.py:230
  98.9 6.8 %all-to-all-done = bf16[4,192,384]{2,1,0:T(8,128)(2,1)S(1)} async-done(((bf16[4,192,384]{2,1,0:T(8,128)(2,1)}), bf16[4,192,384]{2,1,0:T(8,128)(2,1)S(1)}, u32[]{:S(2)}, u32[]{:S(2)}) %all-to-all-start) | async-done | bytes 589856 | tf_op jit(solution)/shard_map/all_to_all | solution.py:230
  105.7 0.1 convert_element_type.60
  105.8 0.7 fusion.18
  106.5 0.6 fusion.6
  107.0 0.3 fusion.4
  107.3 0.1 copy.35
  107.4 0.1 copy.36
  107.5 0.1 multiply_reduce_fusion
  107.6 0.0 copy-done
  107.6 0.0 copy-done.6
  107.6 0.5 convolution_convert_fusion
  108.1 0.0 copy-start.1
  108.1 0.0 copy-start.4
  108.1 5.7 %collective-permute-start.7 = (bf16[4,24,2048]{2,1,0:T(8,128)(2,1)S(1)}, bf16[4,24,2048]{2,1,0:T(8,128)(2,1)S(1)}, u32[]{:S(2)}, u32[]{:S(2)}) collective-permute-start(bf16[4,24,2048]{2,1,0:T(8,128)(2,1)S(1)} %select_bitcast_fusion), channel_id=1, source_target_pairs={{0,1},{1,0},{2,3},{3,2},{4,5},{5,4},{6,7},{7,6},{8,9},{9,8},{10,11... | collective-permute-start | bytes 1179656 | tf_op jit(solution)/shard_map/ppermute | solution.py:174
  113.8 1.3 collective-permute-done.7
  115.2 0.1 fusion.1
  115.3 0.0 copy-start.5
  115.3 11.0 %all_to_all.15 = bf16[4,24,2048]{2,1,0:T(8,128)(2,1)S(1)} all-to-all(bf16[4,24,2048]{2,1,0:T(8,128)(2,1)S(1)} %fusion.1), channel_id=1, replica_groups=mesh['z'=16,'y'=4,'x'=4,'c'=2] {'x'}, dimensions={0} | all-to-all | bytes 786432 | tf_op jit(solution)/shard_map/all_to_all | solution.py:176
  126.4 0.1 reduce_sum.83
  126.4 0.0 copy-done.1
  126.4 0.1 fusion.10
  126.6 0.0 copy-done.4
  126.6 0.1 fusion.12
  126.7 15.0 %all_gather.10.rows_ref = bf16[192,2048]{1,0:T(8,128)(2,1)S(1)} all-gather(bf16[24,2048]{1,0:T(8,128)(2,1)S(1)} %fusion.12), channel_id=1, replica_groups=mesh['z'=16,'y'=4,'x'=4,'c'=2] {'x','c'}, dimensions={0}, use_global_device_ids=true | all-gather | bytes 884736 | tf_op jit(solution)/shard_map/all_gather | solution.py:239
  141.7 2.2 %collective-permute-start.8 = (bf16[8,2048]{1,0:T(8,128)(2,1)S(1)}, bf16[8,2048]{1,0:T(8,128)(2,1)S(1)}, u32[]{:S(2)}, u32[]{:S(2)}) collective-permute-start(bf16[8,2048]{1,0:T(8,128)(2,1)S(1)} %slice.112), channel_id=1, source_target_pairs={{0,8},{8,16},{16,24},{24,32},{32,40},{40,48},{48,56},{56,64},{64,7... | collective-permute-start | bytes 98312 | tf_op jit(solution)/shard_map/ppermute | solution.py:241
  143.9 0.6 reshape.58.bias_ref
  144.5 0.4 collective-permute-done.8.rim_ref
  144.9 7.4 %all-gather.2.cloned.1.call-done.w_ref = bf16[2048,2112]{1,0:T(8,128)(2,1)} async-done(((bf16[128,2112]{1,0:T(8,128)(2,1)}), bf16[2048,2112]{1,0:T(8,128)(2,1)}) %all-gather.2.cloned.1.call-update) | async-done | bytes 8650768 | tf_op jit(solution)/shard_map/all_gather | solution.py:204
  152.3 5.8 %ffn.1 = bf16[192,2048]{1,0:T(8,128)(2,1)S(1)} custom-call(bf16[192,2048]{1,0:T(8,128)(2,1)S(1)} %all_gather.10.rows_ref, bf16[8,2048]{1,0:T(8,128)(2,1)S(1)} %collective-permute-done.8.rim_ref, bf16[2048,2112]{1,0:T(8,128)(2,1)} %all-gather.2.cloned.1.call-done.w_ref, f32[3,704]{1,0:T(4,128)} %taps_ref.1, f32[1,704]{1,0:T(1,128)} %reshape.58.bias_ref), custom_call_target="tpu_custom_call" | custom-call | tf_op jit(solution)/shard_map/ffn/pallas_call | solution.py:246
  158.1 3.2 %collective-permute-start.9 = (bf16[4,24,2048]{2,1,0:T(8,128)(2,1)S(1)}, bf16[4,24,2048]{2,1,0:T(8,128)(2,1)S(1)}, u32[]{:S(2)}, u32[]{:S(2)}) collective-permute-start(bf16[4,24,2048]{2,1,0:T(8,128)(2,1)S(1)} %fusion.2), channel_id=1, source_target_pairs={{0,1},{1,0},{2,3},{3,2},{4,5},{5,4},{6,7},{7,6},{8,9},{9,8},{10,11... | collective-permute-start | bytes 1179656 | tf_op jit(solution)/shard_map/ppermute | solution.py:174
  161.3 1.3 collective-permute-done.9
  162.6 0.1 fusion
  162.8 11.0 %all_to_all.16 = bf16[4,24,2048]{2,1,0:T(8,128)(2,1)S(1)} all-to-all(bf16[4,24,2048]{2,1,0:T(8,128)(2,1)S(1)} %fusion), channel_id=1, replica_groups=mesh['z'=16,'y'=4,'x'=4,'c'=2] {'x'}, dimensions={0} | all-to-all | bytes 786432 | tf_op jit(solution)/shard_map/all_to_all | solution.py:176
  173.8 0.1 reduce_sum.85
  173.8 0.7 fusion.13
  (12 shorter events, 0.2 us)
Async XLA Ops:
  6.5 101.1 %copy-start = (bf16[128,2048]{1,0:T(8,128)(2,1)S(1)}, bf16[128,2048]{1,0:T(8,128)(2,1)}, u32[]{:S(2)}) copy-start(bf16[128,2048]{1,0:T(8,128)(2,1)} %param.19) | copy-start | bytes 1572868
  6.5 145.7 %all-gather.2.cloned.1.call-start = ((), (), s32[]{:S(2)}) async-start(), calls=%async_computation.3 | async-start | bytes 9469952 | tf_op jit(solution)/shard_map/all_gather | solution.py:204
  8.3 13.1 %copy-start.2 = (bf16[192,128]{1,0:T(8,128)(2,1)S(1)}, bf16[192,128]{1,0:T(8,128)(2,1)}, u32[]{:S(2)}) copy-start(bf16[192,128]{1,0:T(8,128)(2,1)} %param.15) | copy-start | bytes 147460
  8.4 13.1 %copy-start.3 = (bf16[192,128]{1,0:T(8,128)(2,1)S(1)}, bf16[192,128]{1,0:T(8,128)(2,1)}, u32[]{:S(2)}) copy-start(bf16[192,128]{1,0:T(8,128)(2,1)} %param.16) | copy-start | bytes 147460
  21.5 17.2 %collective-permute-start = (bf16[192,256]{1,0:T(8,128)(2,1)S(1)}, bf16[192,256]{1,0:T(8,128)(2,1)S(1)}, u32[]{:S(2)}, u32[]{:S(2)}) collective-permute-start(bf16[192,256]{1,0:T(8,128)(2,1)S(1)} %constant_dynamic-update-slice_fusion), channel_id=1, source_target_pairs={{352,0},{384,32},{0,160},{32,192},{64,224},{96,256},{128,288},{160... | collective-permute-start | bytes 294920 | tf_op jit(solution)/shard_map/ppermute | solution.py:29
  32.7 11.8 %collective-permute-start.1 = (bf16[192,256]{1,0:T(8,128)(2,1)S(1)}, bf16[192,256]{1,0:T(8,128)(2,1)S(1)}, u32[]{:S(2)}, u32[]{:S(2)}) collective-permute-start(bf16[192,256]{1,0:T(8,128)(2,1)S(1)} %constant_dynamic-update-slice_fusion), channel_id=1, source_target_pairs={{160,0},{192,32},{0,352},{32,384},{64,416},{96,448},{128,480},{161... | collective-permute-start | bytes 294920 | tf_op jit(solution)/shard_map/ppermute | solution.py:29
  44.5 13.1 %collective-permute-start.2 = (bf16[576,256]{1,0:T(8,128)(2,1)S(1)}, bf16[576,256]{1,0:T(8,128)(2,1)S(1)}, u32[]{:S(2)}, u32[]{:S(2)}) collective-permute-start(bf16[576,256]{1,0:T(8,128)(2,1)S(1)} %pad_maximum_fusion.refs_0_), channel_id=1, source_target_pairs={{0,32},{32,64},{64,96},{96,128},{128,160},{160,192},{192,224},{224... | collective-permute-start | bytes 884744 | tf_op jit(solution)/shard_map/ppermute | solution.py:29
  46.7 16.8 %collective-permute-start.3 = (bf16[576,256]{1,0:T(8,128)(2,1)S(1)}, bf16[576,256]{1,0:T(8,128)(2,1)S(1)}, u32[]{:S(2)}, u32[]{:S(2)}) collective-permute-start(bf16[576,256]{1,0:T(8,128)(2,1)S(1)} %pad_maximum_fusion.refs_0_), channel_id=1, source_target_pairs={{32,0},{160,128},{192,160},{224,192},{256,224},{288,256},{320,288}... | collective-permute-start | bytes 884744 | tf_op jit(solution)/shard_map/ppermute | solution.py:29
  57.6 14.3 %collective-permute-start.4 = (bf16[576,256]{1,0:T(8,128)(2,1)S(1)}, bf16[576,256]{1,0:T(8,128)(2,1)S(1)}, u32[]{:S(2)}, u32[]{:S(2)}) collective-permute-start(bf16[576,256]{1,0:T(8,128)(2,1)S(1)} %collective-permute-done.2.refs_1_), channel_id=1, source_target_pairs={{32,64},{64,96},{96,128},{128,160},{160,192},{192,224},{224,256},{... | collective-permute-start | bytes 884744 | tf_op jit(solution)/shard_map/ppermute | solution.py:29
  63.4 20.3 %collective-permute-start.5 = (bf16[576,256]{1,0:T(8,128)(2,1)S(1)}, bf16[576,256]{1,0:T(8,128)(2,1)S(1)}, u32[]{:S(2)}, u32[]{:S(2)}) collective-permute-start(bf16[576,256]{1,0:T(8,128)(2,1)S(1)} %collective-permute-done.3.refs_2_), channel_id=1, source_target_pairs={{128,96},{160,128},{192,160},{224,192},{256,224},{288,256},{320,28... | collective-permute-start | bytes 884744 | tf_op jit(solution)/shard_map/ppermute | solution.py:29
  71.9 11.8 %collective-permute-start.6 = (bf16[192,256]{1,0:T(8,128)(2,1)S(1)}, bf16[192,256]{1,0:T(8,128)(2,1)S(1)}, u32[]{:S(2)}, u32[]{:S(2)}) collective-permute-start(bf16[192,256]{1,0:T(8,128)(2,1)S(1)} %slice.101), channel_id=1, source_target_pairs={{224,256},{256,288},{288,320},{320,352},{352,384},{384,416},{416,4... | collective-permute-start | bytes 294920 | tf_op jit(solution)/shard_map/ppermute | solution.py:29
  94.7 11.0 %all-to-all-start = ((bf16[4,192,384]{2,1,0:T(8,128)(2,1)}), bf16[4,192,384]{2,1,0:T(8,128)(2,1)S(1)}, u32[]{:S(2)}, u32[]{:S(2)}) async-start(bf16[4,192,384]{2,1,0:T(8,128)(2,1)} %bitcast.3), calls=%async_computation | async-start | bytes 1179648 | tf_op jit(solution)/shard_map/all_to_all | solution.py:230
  106.5 1.1 copy-start.6
  108.1 18.3 %copy-start.1 = (bf16[24,2048]{1,0:T(8,128)(2,1)S(1)}, bf16[24,2048]{1,0:T(8,128)(2,1)}, u32[]{:S(2)}) copy-start(bf16[24,2048]{1,0:T(8,128)(2,1)} %param.13) | copy-start | bytes 294916
  108.1 18.5 %copy-start.4 = (f32[2048]{0:T(1024)S(1)}, f32[2048]{0:T(1024)}, u32[]{:S(2)}) copy-start(f32[2048]{0:T(1024)} %param.20) | copy-start | bytes 24580
  108.1 7.0 %collective-permute-start.7 = (bf16[4,24,2048]{2,1,0:T(8,128)(2,1)S(1)}, bf16[4,24,2048]{2,1,0:T(8,128)(2,1)S(1)}, u32[]{:S(2)}, u32[]{:S(2)}) collective-permute-start(bf16[4,24,2048]{2,1,0:T(8,128)(2,1)S(1)} %select_bitcast_fusion), channel_id=1, source_target_pairs={{0,1},{1,0},{2,3},{3,2},{4,5},{5,4},{6,7},{7,6},{8,9},{9,8},{10,11... | collective-permute-start | bytes 1179656 | tf_op jit(solution)/shard_map/ppermute | solution.py:174
  115.3 28.6 %copy-start.5 = (f32[704]{0:T(1024)S(1)}, f32[704]{0:T(1024)}, u32[]{:S(2)}) copy-start(f32[704]{0:T(1024)} %param.24) | copy-start | bytes 8452
  141.7 3.2 %collective-permute-start.8 = (bf16[8,2048]{1,0:T(8,128)(2,1)S(1)}, bf16[8,2048]{1,0:T(8,128)(2,1)S(1)}, u32[]{:S(2)}, u32[]{:S(2)}) collective-permute-start(bf16[8,2048]{1,0:T(8,128)(2,1)S(1)} %slice.112), channel_id=1, source_target_pairs={{0,8},{8,16},{16,24},{24,32},{32,40},{40,48},{48,56},{56,64},{64,7... | collective-permute-start | bytes 98312 | tf_op jit(solution)/shard_map/ppermute | solution.py:241
  158.1 4.5 %collective-permute-start.9 = (bf16[4,24,2048]{2,1,0:T(8,128)(2,1)S(1)}, bf16[4,24,2048]{2,1,0:T(8,128)(2,1)S(1)}, u32[]{:S(2)}, u32[]{:S(2)}) collective-permute-start(bf16[4,24,2048]{2,1,0:T(8,128)(2,1)S(1)} %fusion.2), channel_id=1, source_target_pairs={{0,1},{1,0},{2,3},{3,2},{4,5},{5,4},{6,7},{7,6},{8,9},{9,8},{10,11... | collective-permute-start | bytes 1179656 | tf_op jit(solution)/shard_map/ppermute | solution.py:174
Sparse Core Ops, SparseCore 0:
  21.6 130.6 all-gather.1

commit v10 on v9

--- a/solution.py
+++ b/solution.py
@@ -15,7 +15,7 @@
 NY = 4
 eps = 1e-05
 neg_fill = -1e30
-TILE = 128
+TILE = 384
 LANES = 128
 OFFSETS = (0, 5, 11, 1, 6, 12, 15, 4, 10, 2, 7, 13, 14, 3, 9, 8)
 CHUNK = 4
@@ -115,22 +115,52 @@
         )
 
 
-def ffn_kernel(rows_ref, rim_ref, w_ref, taps_ref, bias_ref, out_ref, x_ref, acc_ref, held_ref, sems):
-    rows = rows_ref.shape[0]
+def fold_kernel(rows_ref, out_ref, q_ref):
+    deep = rows_ref.shape[0]
+    blocks = out_ref.shape[0] // deep
+    for i in range(blocks):
+        out_ref[i * deep : (i + 1) * deep, :] = rows_ref[:, i * LANES : (i + 1) * LANES]
+    last = rows_ref[:, blocks * LANES : (blocks + 1) * LANES].astype(jnp.float32)
+    lane = lax.broadcasted_iota(jnp.int32, (deep // 2, LANES), 1)
+    low, high = last[: deep // 2], pltpu.roll(last[deep // 2 :], LANES // 2, 1)
+    out_ref[blocks * deep :, :] = jnp.where(lane < LANES // 2, low, high).astype(jnp.bfloat16)
+    q_ref[...] = rows_ref[:, (blocks + 1) * LANES :]
+
+
+def ffn_kernel(
+    rows_ref, rim_ref, w_ref, taps_ref, bias_ref, out_ref, x_ref, acc_ref, held_ref, tail_ref, sems
+):
+    rows, d = rows_ref.shape
     rim = rim_ref.shape[0]
     ff = bias_ref.shape[1]
-    edges = [*range(0, 2 * ff - 2 * LANES, 4 * LANES), 2 * ff, 3 * ff]
+    count, deep, _ = held_ref.shape
+    full = 3 * ff // LANES
     copies = []
-    for i, (start, end) in enumerate(zip(edges, edges[1:])):
-        part = pl.ds(start, end - start)
-        copies.append(pltpu.make_async_copy(w_ref.at[:, part], held_ref.at[:, part], sems.at[i]))
+    for i in range(full):
+        copies.append(
+            pltpu.make_async_copy(
+                w_ref.at[:, pl.ds(i * deep, deep), :],
+                held_ref.at[:, :, pl.ds(i * LANES, LANES)],
+                sems.at[i],
+            )
+        )
         copies[-1].start()
+    copies.append(
+        pltpu.make_async_copy(
+            w_ref.at[:, pl.ds(full * deep, deep // 2), :], tail_ref, sems.at[full]
+        )
+    )
+    copies[-1].start()
+    edges = [*range(0, 2 * ff - 2 * LANES, 4 * LANES), 2 * ff]
     x_ref[:rows, :] = rows_ref[...]
     x_ref[rows:, :] = rim_ref[...]
-    for i, (start, end) in enumerate(zip(edges[:-1], edges[1:-1])):
-        copies[i].wait()
+    for start, end in zip(edges, edges[1:]):
+        for i in range(start // LANES, end // LANES):
+            copies[i].wait()
         acc_ref[:, start:end] = jnp.dot(
-            x_ref[...], held_ref[:, start:end], preferred_element_type=jnp.float32
+            x_ref[...],
+            held_ref[:, :, start:end].reshape(d, end - start),
+            preferred_element_type=jnp.float32,
         ).astype(jnp.bfloat16)
     up = acc_ref[:, :ff].astype(jnp.float32)
     gate = acc_ref[:rows, ff : 2 * ff].astype(jnp.float32)
@@ -143,8 +173,15 @@
     two = jnp.where(at == 1, before[rim - 1 : rim], two)
     conv = bias_ref[...] + taps_ref[0:1] * two + taps_ref[1:2] * one + taps_ref[2:3] * up
     hidden = (conv / (1.0 + jnp.exp(-conv)) * gate).astype(jnp.bfloat16)
-    copies[-1].wait()
-    out_ref[...] = dot_nt(hidden, held_ref[:, 2 * ff :]).astype(jnp.bfloat16)
+    for copy in copies[2 * ff // LANES :]:
+        copy.wait()
+    tail = tail_ref[...].reshape(count * deep // 2, LANES).astype(jnp.float32)
+    pair = (tail, pltpu.roll(tail, LANES // 2, 1))
+    for i, half in enumerate(pair):
+        block = half.astype(jnp.bfloat16).reshape(count, deep // 2, LANES)
+        held_ref[:, i * deep // 2 : (i + 1) * deep // 2, full * LANES :] = block
+    down = held_ref[:, :, 2 * ff : 3 * ff].reshape(d, ff)
+    out_ref[...] = dot_nt(hidden, down).astype(jnp.bfloat16)
 
 
 def merged(got):
@@ -201,8 +238,19 @@
     cuts = [up_weight, gate_weight, down_weight.T, jnp.zeros((w_rows, tail), jnp.bfloat16)]
     cuts += [queries[i : i + w_rows] for i in range(0, rows, w_rows)]
     row_w = lax.all_gather(jnp.concatenate(cuts, axis=1), "y", axis=0, tiled=True)
-    all_w = lax.all_gather(row_w[:, :width], "z", axis=0, tiled=True)
-    q_rows = row_w[:, width + tail :]
+    deep = row_w.shape[0]
+    shard, q_rows = pl.pallas_call(
+        fold_kernel,
+        out_shape=[
+            jax.ShapeDtypeStruct((deep * width // LANES, LANES), jnp.bfloat16),
+            pltpu.VMEM((deep, row_w.shape[1] - width - tail), jnp.bfloat16),
+        ],
+        in_specs=[VMEM],
+        out_specs=[VMEM] * 2,
+        name="fold",
+    )(pltpu.with_memory_space_constraint(row_w, pltpu.VMEM))
+    all_w = lax.all_gather(shard, "z", axis=0, tiled=True)
+    all_w = all_w.reshape(-1, *shard.shape)
 
     kv = jnp.concatenate((key_pairs, values), axis=1)
     last = lax.axis_size("z")
@@ -251,8 +299,9 @@
         scratch_shapes=[
             pltpu.VMEM((rows + rim_rows.shape[0], d), jnp.bfloat16),
             pltpu.VMEM((rows + rim_rows.shape[0], 2 * ff), jnp.bfloat16),
-            pltpu.VMEM((d, width), jnp.bfloat16),
-            pltpu.SemaphoreType.DMA((4,)),
+            pltpu.VMEM((all_w.shape[0], deep, width + tail), jnp.bfloat16),
+            pltpu.VMEM((all_w.shape[0], deep // 2, LANES), jnp.bfloat16),
+            pltpu.SemaphoreType.DMA((width // LANES + 1,)),
         ],
         name="ffn",
     )(*in_vmem, all_w, conv_weight, conv_bias.reshape(1, ff))

time: 182 us -> 184 us (1.011)
  the two profiles are of different devices: /device:TPU:1 before, /device:TPU:384 now
where the time goes in v10:
time: 184 us
  waiting for transfers between devices  58.8 us (32%)
  blocking collectives  51 us (28%)
  starting transfers between devices  31.7 us (17%)
  Pallas kernels  21 us (11%)
  between operations  14.4 us (8%)
  other arithmetic  3.72 us (2%)
  local copies, waits for them, and re-layouts  2.66 us (1%)
    ppermute x7, waiting for transfers between devices, shifted(): return lax.ppermute(value, 'z', [((i - steps) % count, i) for i in targets])  41.8 us
    all_to_all x2, blocking collectives, summed_over_tp(): tiles = lax.all_to_all(both, 'x', 0, 0, tiled=True)  23.7 us
    ppermute x7, starting transfers between devices, shifted(): return lax.ppermute(value, 'z', [((i - steps) % count, i) for i in targets])  21.6 us
    pallas_call x1, Pallas kernels, local(): pl.pallas_call(attend_kernel, out_shape=pltpu.VMEM((NY * rows, 3 * VD), j...  14.2 us
    all_gather x1, blocking collectives, local(): lax.all_gather(jnp.concatenate(cuts, axis=1), 'y', axis=0, tiled=True)  13.9 us
    all_gather x1, blocking collectives, local(): lax.all_gather(normalize(mid, norm_gain), TP, axis=0, tiled=True)  13.4 us
    all_to_all x1, waiting for transfers between devices, local(): got = lax.all_to_all(parts.reshape(NY, rows, 3 * VD), 'y', 0, 0, tiled=True)  7.74 us
    ppermute x1, waiting for transfers between devices, local(): lax.ppermute(normed_all[rows - 8:], SP, [(i, i + 1) for i in range(count...  5.87 us
  transfers between devices with their start and end apart: 12, of which 11 were waited for; matrix products, arithmetic and copies ran while one was open for 2% of the time, Pallas kernels for 8%

profile of v10, /device:TPU:384, one launch (start us, length us, event | category | flops | bytes accessed | tf_op | source)
XLA Modules:
  0.0 183.7 jit_solution(12000799511150206553)
XLA Ops:
  6.5 0.0 copy-start
  6.5 0.0 all-gather.2.cloned.1.call-start
  6.5 0.8 fusion.20
  7.4 1.0 concatenate.9
  8.3 0.0 copy-start.3
  8.4 0.0 copy-start.4
  8.4 13.9 %all_gather.9.rows_ref = bf16[128,2944]{1,0:T(8,128)(2,1)S(1)} all-gather(bf16[32,2944]{1,0:T(8,128)(2,1)S(1)} %concatenate.9), channel_id=1, replica_groups=mesh['z'=16,'y'=4,'x'=4,'c'=2] {'y'}, dimensions={0}, use_global_device_ids=true | all-gather | bytes 942080 | tf_op jit(solution)/shard_map/all_gather | solution.py:240
  22.3 0.9 fold.1
  23.2 0.0 all-gather.2.cloned.1.call-update
  23.2 0.0 copy-done.3
  23.3 0.0 copy-done.4
  23.3 1.9 %collective-permute-start = (bf16[192,256]{1,0:T(8,128)(2,1)S(1)}, bf16[192,256]{1,0:T(8,128)(2,1)S(1)}, u32[]{:S(2)}, u32[]{:S(2)}) collective-permute-start(bf16[192,256]{1,0:T(8,128)(2,1)S(1)} %constant_dynamic-update-slice_fusion), channel_id=1, source_target_pairs={{352,0},{384,32},{0,160},{32,192},{64,224},{96,256},{128,288},{160... | collective-permute-start | bytes 294920 | tf_op jit(solution)/shard_map/ppermute | solution.py:29
  25.2 1.3 collective-permute-start.1
  26.5 11.8 %collective-permute-done = bf16[192,256]{1,0:T(8,128)(2,1)S(1)} collective-permute-done((bf16[192,256]{1,0:T(8,128)(2,1)S(1)}, bf16[192,256]{1,0:T(8,128)(2,1)S(1)}, u32[]{:S(2)}, u32[]{:S(2)}) %collective-permute-start) | collective-permute-done | bytes 98336 | tf_op jit(solution)/shard_map/ppermute | solution.py:29
  38.3 2.2 %collective-permute-done.1 = bf16[192,256]{1,0:T(8,128)(2,1)S(1)} collective-permute-done((bf16[192,256]{1,0:T(8,128)(2,1)S(1)}, bf16[192,256]{1,0:T(8,128)(2,1)S(1)}, u32[]{:S(2)}, u32[]{:S(2)}) %collective-permute-start.1) | collective-permute-done | bytes 98336 | tf_op jit(solution)/shard_map/ppermute | solution.py:29
  40.5 0.0 copy-done.1
  40.6 7.8 %collective-permute-start.2 = (bf16[576,256]{1,0:T(8,128)(2,1)S(1)}, bf16[576,256]{1,0:T(8,128)(2,1)S(1)}, u32[]{:S(2)}, u32[]{:S(2)}) collective-permute-start(bf16[576,256]{1,0:T(8,128)(2,1)S(1)} %pad_maximum_fusion.refs_0_), channel_id=1, source_target_pairs={{0,32},{32,64},{64,96},{96,128},{128,160},{160,192},{192,224},{224... | collective-permute-start | bytes 884744 | tf_op jit(solution)/shard_map/ppermute | solution.py:29
  48.4 1.9 %collective-permute-start.3 = (bf16[576,256]{1,0:T(8,128)(2,1)S(1)}, bf16[576,256]{1,0:T(8,128)(2,1)S(1)}, u32[]{:S(2)}, u32[]{:S(2)}) collective-permute-start(bf16[576,256]{1,0:T(8,128)(2,1)S(1)} %pad_maximum_fusion.refs_0_), channel_id=1, source_target_pairs={{32,0},{160,128},{192,160},{224,192},{256,224},{288,256},{320,288}... | collective-permute-start | bytes 884744 | tf_op jit(solution)/shard_map/ppermute | solution.py:29
  50.4 8.8 %collective-permute-done.2.refs_1_ = bf16[576,256]{1,0:T(8,128)(2,1)S(1)} collective-permute-done((bf16[576,256]{1,0:T(8,128)(2,1)S(1)}, bf16[576,256]{1,0:T(8,128)(2,1)S(1)}, u32[]{:S(2)}, u32[]{:S(2)}) %collective-permute-start.2) | collective-permute-done | bytes 294944 | tf_op jit(solution)/shard_map/ppermute | solution.py:29
  59.1 4.3 %collective-permute-start.4 = (bf16[576,256]{1,0:T(8,128)(2,1)S(1)}, bf16[576,256]{1,0:T(8,128)(2,1)S(1)}, u32[]{:S(2)}, u32[]{:S(2)}) collective-permute-start(bf16[576,256]{1,0:T(8,128)(2,1)S(1)} %collective-permute-done.2.refs_1_), channel_id=1, source_target_pairs={{32,64},{64,96},{96,128},{128,160},{160,192},{192,224},{224,256},{... | collective-permute-start | bytes 884744 | tf_op jit(solution)/shard_map/ppermute | solution.py:29
  63.4 1.3 collective-permute-done.3.refs_2_
  64.7 1.9 %collective-permute-start.5 = (bf16[576,256]{1,0:T(8,128)(2,1)S(1)}, bf16[576,256]{1,0:T(8,128)(2,1)S(1)}, u32[]{:S(2)}, u32[]{:S(2)}) collective-permute-start(bf16[576,256]{1,0:T(8,128)(2,1)S(1)} %collective-permute-done.3.refs_2_), channel_id=1, source_target_pairs={{128,96},{160,128},{192,160},{224,192},{256,224},{288,256},{320,28... | collective-permute-start | bytes 884744 | tf_op jit(solution)/shard_map/ppermute | solution.py:29
  66.6 10.8 %collective-permute-done.4.refs_3_ = bf16[576,256]{1,0:T(8,128)(2,1)S(1)} collective-permute-done((bf16[576,256]{1,0:T(8,128)(2,1)S(1)}, bf16[576,256]{1,0:T(8,128)(2,1)S(1)}, u32[]{:S(2)}, u32[]{:S(2)}) %collective-permute-start.4) | collective-permute-done | bytes 294944 | tf_op jit(solution)/shard_map/ppermute | solution.py:29
  77.4 2.4 %collective-permute-start.6 = (bf16[192,256]{1,0:T(8,128)(2,1)S(1)}, bf16[192,256]{1,0:T(8,128)(2,1)S(1)}, u32[]{:S(2)}, u32[]{:S(2)}) collective-permute-start(bf16[192,256]{1,0:T(8,128)(2,1)S(1)} %slice.92), channel_id=1, source_target_pairs={{224,256},{256,288},{288,320},{320,352},{352,384},{384,416},{416,4... | collective-permute-start | bytes 294920 | tf_op jit(solution)/shard_map/ppermute | solution.py:29
  79.8 0.6 pad_add_fusion.where_ref
  80.4 0.4 collective-permute-done.5.refs_4_
  80.9 6.5 %collective-permute-done.6.refs_5_ = bf16[192,256]{1,0:T(8,128)(2,1)S(1)} collective-permute-done((bf16[192,256]{1,0:T(8,128)(2,1)S(1)}, bf16[192,256]{1,0:T(8,128)(2,1)S(1)}, u32[]{:S(2)}, u32[]{:S(2)}) %collective-permute-start.6) | collective-permute-done | bytes 98336 | tf_op jit(solution)/shard_map/ppermute | solution.py:29
  87.4 14.2 %attend.1 = bf16[768,384]{1,0:T(8,128)(2,1)} custom-call(s32[2]{0:T(128)} %pad_add_fusion.where_ref, bf16[128,768]{1,0:T(8,128)(2,1)} %copy-done.1, bf16[576,256]{1,0:T(8,128)(2,1)S(1)} %pad_maximum_fusion.refs_0_, bf16[576,256]{1,0:T(8,128)(2,1)S(1)} %collective-permute-done.2.refs_1_, bf16[576,256]{1,0:T(8,128)(2,1)S(1)} %collective-permute-done.3.refs_2_, ...), custom_call_target="tpu_custom_call" | custom-call | tf_op jit(solution)/shard_map/attend/pallas_call | solution.py:267
  101.6 3.5 %all-to-all-start = ((bf16[4,192,384]{2,1,0:T(8,128)(2,1)}), bf16[4,192,384]{2,1,0:T(8,128)(2,1)S(1)}, u32[]{:S(2)}, u32[]{:S(2)}) async-start(bf16[4,192,384]{2,1,0:T(8,128)(2,1)} %bitcast.3), calls=%async_computation | async-start | bytes 1179648 | tf_op jit(solution)/shard_map/all_to_all | solution.py:278
  105.7 7.7 %all-to-all-done = bf16[4,192,384]{2,1,0:T(8,128)(2,1)S(1)} async-done(((bf16[4,192,384]{2,1,0:T(8,128)(2,1)}), bf16[4,192,384]{2,1,0:T(8,128)(2,1)S(1)}, u32[]{:S(2)}, u32[]{:S(2)}) %all-to-all-start) | async-done | bytes 589856 | tf_op jit(solution)/shard_map/all_to_all | solution.py:278
  113.4 0.1 convert_element_type.60
  113.5 0.7 fusion.18
  114.2 0.6 fusion.6
  114.8 0.3 fusion.4
  115.1 0.1 copy.35
  115.2 0.1 copy.36
  115.3 0.1 multiply_reduce_fusion
  115.4 0.0 copy-done
  115.4 0.0 copy-done.7
  115.4 0.5 convolution_convert_fusion
  115.9 0.0 copy-start.2
  115.9 0.0 copy-start.5
  115.9 2.1 %collective-permute-start.7 = (bf16[4,24,2048]{2,1,0:T(8,128)(2,1)S(1)}, bf16[4,24,2048]{2,1,0:T(8,128)(2,1)S(1)}, u32[]{:S(2)}, u32[]{:S(2)}) collective-permute-start(bf16[4,24,2048]{2,1,0:T(8,128)(2,1)S(1)} %select_bitcast_fusion), channel_id=1, source_target_pairs={{0,1},{1,0},{2,3},{3,2},{4,5},{5,4},{6,7},{7,6},{8,9},{9,8},{10,11... | collective-permute-start | bytes 1179656 | tf_op jit(solution)/shard_map/ppermute | solution.py:211
  118.0 1.7 collective-permute-done.7
  119.7 0.1 fusion.1
  119.8 0.0 copy-start.6
  119.8 12.7 %all_to_all.15 = bf16[4,24,2048]{2,1,0:T(8,128)(2,1)S(1)} all-to-all(bf16[4,24,2048]{2,1,0:T(8,128)(2,1)S(1)} %fusion.1), channel_id=1, replica_groups=mesh['z'=16,'y'=4,'x'=4,'c'=2] {'x'}, dimensions={0} | all-to-all | bytes 786432 | tf_op jit(solution)/shard_map/all_to_all | solution.py:213
  132.5 0.1 reduce_sum.83
  132.6 0.0 copy-done.2
  132.6 0.1 fusion.10
  132.7 0.0 copy-done.5
  132.7 0.1 fusion.12
  132.8 13.4 %all_gather.10.rows_ref = bf16[192,2048]{1,0:T(8,128)(2,1)S(1)} all-gather(bf16[24,2048]{1,0:T(8,128)(2,1)S(1)} %fusion.12), channel_id=1, replica_groups=mesh['z'=16,'y'=4,'x'=4,'c'=2] {'x','c'}, dimensions={0}, use_global_device_ids=true | all-gather | bytes 884736 | tf_op jit(solution)/shard_map/all_gather | solution.py:287
  146.2 2.6 %collective-permute-start.8 = (bf16[8,2048]{1,0:T(8,128)(2,1)S(1)}, bf16[8,2048]{1,0:T(8,128)(2,1)S(1)}, u32[]{:S(2)}, u32[]{:S(2)}) collective-permute-start(bf16[8,2048]{1,0:T(8,128)(2,1)S(1)} %slice.103), channel_id=1, source_target_pairs={{0,8},{8,16},{16,24},{24,32},{32,40},{40,48},{48,56},{56,64},{64,7... | collective-permute-start | bytes 98312 | tf_op jit(solution)/shard_map/ppermute | solution.py:289
  148.9 0.0 copy-done.6
  148.9 0.6 reshape.62.bias_ref
  149.5 5.9 %collective-permute-done.8.rim_ref = bf16[8,2048]{1,0:T(8,128)(2,1)S(1)} collective-permute-done((bf16[8,2048]{1,0:T(8,128)(2,1)S(1)}, bf16[8,2048]{1,0:T(8,128)(2,1)S(1)}, u32[]{:S(2)}, u32[]{:S(2)}) %collective-permute-start.8) | collective-permute-done | bytes 32800 | tf_op jit(solution)/shard_map/ppermute | solution.py:289
  155.3 5.8 %ffn.1 = bf16[192,2048]{1,0:T(8,128)(2,1)S(1)} custom-call(bf16[192,2048]{1,0:T(8,128)(2,1)S(1)} %all_gather.10.rows_ref, bf16[8,2048]{1,0:T(8,128)(2,1)S(1)} %collective-permute-done.8.rim_ref, bf16[16,2112,128]{2,1,0:T(8,128)(2,1)} %bitcast.50, f32[3,704]{1,0:T(4,128)} %taps_ref.1, f32[1,704]{1,0:T(1,128)} %reshape.62.bias_ref), custom_call_target="tpu_custom_call" | custom-call | tf_op jit(solution)/shard_map/ffn/pallas_call | solution.py:294
  161.3 1.9 %collective-permute-start.9 = (bf16[4,24,2048]{2,1,0:T(8,128)(2,1)S(1)}, bf16[4,24,2048]{2,1,0:T(8,128)(2,1)S(1)}, u32[]{:S(2)}, u32[]{:S(2)}) collective-permute-start(bf16[4,24,2048]{2,1,0:T(8,128)(2,1)S(1)} %fusion.2), channel_id=1, source_target_pairs={{0,1},{1,0},{2,3},{3,2},{4,5},{5,4},{6,7},{7,6},{8,9},{9,8},{10,11... | collective-permute-start | bytes 1179656 | tf_op jit(solution)/shard_map/ppermute | solution.py:211
  163.2 1.7 collective-permute-done.9
  164.9 0.1 fusion
  165.0 11.0 %all_to_all.16 = bf16[4,24,2048]{2,1,0:T(8,128)(2,1)S(1)} all-to-all(bf16[4,24,2048]{2,1,0:T(8,128)(2,1)S(1)} %fusion), channel_id=1, replica_groups=mesh['z'=16,'y'=4,'x'=4,'c'=2] {'x'}, dimensions={0} | all-to-all | bytes 786432 | tf_op jit(solution)/shard_map/all_to_all | solution.py:213
  176.1 0.1 reduce_sum.85
  176.1 0.7 fusion.13
  (13 shorter events, 0.2 us)
Async XLA Ops:
  6.5 108.8 %copy-start = (bf16[128,2048]{1,0:T(8,128)(2,1)S(1)}, bf16[128,2048]{1,0:T(8,128)(2,1)}, u32[]{:S(2)}) copy-start(bf16[128,2048]{1,0:T(8,128)(2,1)} %param.19) | copy-start | bytes 1572868
  6.5 148.8 %all-gather.2.cloned.1.call-start = ((), (), s32[]{:S(2)}) async-start(), calls=%async_computation.3 | async-start | bytes 9191424 | tf_op jit(solution)/shard_map/all_gather | solution.py:252
  8.3 14.9 %copy-start.3 = (bf16[192,128]{1,0:T(8,128)(2,1)S(1)}, bf16[192,128]{1,0:T(8,128)(2,1)}, u32[]{:S(2)}) copy-start(bf16[192,128]{1,0:T(8,128)(2,1)} %param.15) | copy-start | bytes 147460
  8.4 14.9 %copy-start.4 = (bf16[192,128]{1,0:T(8,128)(2,1)S(1)}, bf16[192,128]{1,0:T(8,128)(2,1)}, u32[]{:S(2)}) copy-start(bf16[192,128]{1,0:T(8,128)(2,1)} %param.16) | copy-start | bytes 147460
  23.2 17.3 %copy-start.1 = (bf16[128,768]{1,0:T(8,128)(2,1)}, bf16[128,768]{1,0:T(8,128)(2,1)S(1)}, u32[]{:S(2)}) copy-start(bf16[128,768]{1,0:T(8,128)(2,1)S(1)} %get-tuple-element.7.rows_ref) | copy-start | bytes 589828
  23.3 15.0 %collective-permute-start = (bf16[192,256]{1,0:T(8,128)(2,1)S(1)}, bf16[192,256]{1,0:T(8,128)(2,1)S(1)}, u32[]{:S(2)}, u32[]{:S(2)}) collective-permute-start(bf16[192,256]{1,0:T(8,128)(2,1)S(1)} %constant_dynamic-update-slice_fusion), channel_id=1, source_target_pairs={{352,0},{384,32},{0,160},{32,192},{64,224},{96,256},{128,288},{160... | collective-permute-start | bytes 294920 | tf_op jit(solution)/shard_map/ppermute | solution.py:29
  25.2 15.3 %collective-permute-start.1 = (bf16[192,256]{1,0:T(8,128)(2,1)S(1)}, bf16[192,256]{1,0:T(8,128)(2,1)S(1)}, u32[]{:S(2)}, u32[]{:S(2)}) collective-permute-start(bf16[192,256]{1,0:T(8,128)(2,1)S(1)} %constant_dynamic-update-slice_fusion), channel_id=1, source_target_pairs={{160,0},{192,32},{0,352},{32,384},{64,416},{96,448},{128,480},{161... | collective-permute-start | bytes 294920 | tf_op jit(solution)/shard_map/ppermute | solution.py:29
  40.6 18.5 %collective-permute-start.2 = (bf16[576,256]{1,0:T(8,128)(2,1)S(1)}, bf16[576,256]{1,0:T(8,128)(2,1)S(1)}, u32[]{:S(2)}, u32[]{:S(2)}) collective-permute-start(bf16[576,256]{1,0:T(8,128)(2,1)S(1)} %pad_maximum_fusion.refs_0_), channel_id=1, source_target_pairs={{0,32},{32,64},{64,96},{96,128},{128,160},{160,192},{192,224},{224... | collective-permute-start | bytes 884744 | tf_op jit(solution)/shard_map/ppermute | solution.py:29
  48.4 16.3 %collective-permute-start.3 = (bf16[576,256]{1,0:T(8,128)(2,1)S(1)}, bf16[576,256]{1,0:T(8,128)(2,1)S(1)}, u32[]{:S(2)}, u32[]{:S(2)}) collective-permute-start(bf16[576,256]{1,0:T(8,128)(2,1)S(1)} %pad_maximum_fusion.refs_0_), channel_id=1, source_target_pairs={{32,0},{160,128},{192,160},{224,192},{256,224},{288,256},{320,288}... | collective-permute-start | bytes 884744 | tf_op jit(solution)/shard_map/ppermute | solution.py:29
  59.1 18.3 %collective-permute-start.4 = (bf16[576,256]{1,0:T(8,128)(2,1)S(1)}, bf16[576,256]{1,0:T(8,128)(2,1)S(1)}, u32[]{:S(2)}, u32[]{:S(2)}) collective-permute-start(bf16[576,256]{1,0:T(8,128)(2,1)S(1)} %collective-permute-done.2.refs_1_), channel_id=1, source_target_pairs={{32,64},{64,96},{96,128},{128,160},{160,192},{192,224},{224,256},{... | collective-permute-start | bytes 884744 | tf_op jit(solution)/shard_map/ppermute | solution.py:29
  64.7 16.2 %collective-permute-start.5 = (bf16[576,256]{1,0:T(8,128)(2,1)S(1)}, bf16[576,256]{1,0:T(8,128)(2,1)S(1)}, u32[]{:S(2)}, u32[]{:S(2)}) collective-permute-start(bf16[576,256]{1,0:T(8,128)(2,1)S(1)} %collective-permute-done.3.refs_2_), channel_id=1, source_target_pairs={{128,96},{160,128},{192,160},{224,192},{256,224},{288,256},{320,28... | collective-permute-start | bytes 884744 | tf_op jit(solution)/shard_map/ppermute | solution.py:29
  77.4 10.0 %collective-permute-start.6 = (bf16[192,256]{1,0:T(8,128)(2,1)S(1)}, bf16[192,256]{1,0:T(8,128)(2,1)S(1)}, u32[]{:S(2)}, u32[]{:S(2)}) collective-permute-start(bf16[192,256]{1,0:T(8,128)(2,1)S(1)} %slice.92), channel_id=1, source_target_pairs={{224,256},{256,288},{288,320},{320,352},{352,384},{384,416},{416,4... | collective-permute-start | bytes 294920 | tf_op jit(solution)/shard_map/ppermute | solution.py:29
  101.6 11.9 %all-to-all-start = ((bf16[4,192,384]{2,1,0:T(8,128)(2,1)}), bf16[4,192,384]{2,1,0:T(8,128)(2,1)S(1)}, u32[]{:S(2)}, u32[]{:S(2)}) async-start(bf16[4,192,384]{2,1,0:T(8,128)(2,1)} %bitcast.3), calls=%async_computation | async-start | bytes 1179648 | tf_op jit(solution)/shard_map/all_to_all | solution.py:278
  114.2 1.1 copy-start.7
  115.9 16.7 %copy-start.2 = (bf16[24,2048]{1,0:T(8,128)(2,1)S(1)}, bf16[24,2048]{1,0:T(8,128)(2,1)}, u32[]{:S(2)}) copy-start(bf16[24,2048]{1,0:T(8,128)(2,1)} %param.13) | copy-start | bytes 294916
  115.9 16.8 %copy-start.5 = (f32[2048]{0:T(1024)S(1)}, f32[2048]{0:T(1024)}, u32[]{:S(2)}) copy-start(f32[2048]{0:T(1024)} %param.20) | copy-start | bytes 24580
  115.9 3.7 %collective-permute-start.7 = (bf16[4,24,2048]{2,1,0:T(8,128)(2,1)S(1)}, bf16[4,24,2048]{2,1,0:T(8,128)(2,1)S(1)}, u32[]{:S(2)}, u32[]{:S(2)}) collective-permute-start(bf16[4,24,2048]{2,1,0:T(8,128)(2,1)S(1)} %select_bitcast_fusion), channel_id=1, source_target_pairs={{0,1},{1,0},{2,3},{3,2},{4,5},{5,4},{6,7},{7,6},{8,9},{9,8},{10,11... | collective-permute-start | bytes 1179656 | tf_op jit(solution)/shard_map/ppermute | solution.py:211
  119.8 29.1 %copy-start.6 = (f32[704]{0:T(1024)S(1)}, f32[704]{0:T(1024)}, u32[]{:S(2)}) copy-start(f32[704]{0:T(1024)} %param.24) | copy-start | bytes 8452
  146.2 9.1 %collective-permute-start.8 = (bf16[8,2048]{1,0:T(8,128)(2,1)S(1)}, bf16[8,2048]{1,0:T(8,128)(2,1)S(1)}, u32[]{:S(2)}, u32[]{:S(2)}) collective-permute-start(bf16[8,2048]{1,0:T(8,128)(2,1)S(1)} %slice.103), channel_id=1, source_target_pairs={{0,8},{8,16},{16,24},{24,32},{32,40},{40,48},{48,56},{56,64},{64,7... | collective-permute-start | bytes 98312 | tf_op jit(solution)/shard_map/ppermute | solution.py:289
  161.3 3.6 %collective-permute-start.9 = (bf16[4,24,2048]{2,1,0:T(8,128)(2,1)S(1)}, bf16[4,24,2048]{2,1,0:T(8,128)(2,1)S(1)}, u32[]{:S(2)}, u32[]{:S(2)}) collective-permute-start(bf16[4,24,2048]{2,1,0:T(8,128)(2,1)S(1)} %fusion.2), channel_id=1, source_target_pairs={{0,1},{1,0},{2,3},{3,2},{4,5},{5,4},{6,7},{7,6},{8,9},{9,8},{10,11... | collective-permute-start | bytes 1179656 | tf_op jit(solution)/shard_map/ppermute | solution.py:211
Sparse Core Ops, SparseCore 0:
  23.3 121.9 all-gather.1

commit v11 on v10

--- a/solution.py
+++ b/solution.py
@@ -15,10 +15,10 @@
 NY = 4
 eps = 1e-05
 neg_fill = -1e30
-TILE = 384
+TILE = 128
 LANES = 128
 OFFSETS = (0, 5, 11, 1, 6, 12, 15, 4, 10, 2, 7, 13, 14, 3, 9, 8)
-CHUNK = 4
+CHUNK = 2
 
 VMEM = pl.BlockSpec(memory_space=pltpu.VMEM)
 SMEM = pl.BlockSpec(memory_space=pltpu.SMEM)
@@ -132,7 +132,7 @@
 ):
     rows, d = rows_ref.shape
     rim = rim_ref.shape[0]
-    ff = bias_ref.shape[1]
+    ff = bias_ref.shape[0]
     count, deep, _ = held_ref.shape
     full = 3 * ff // LANES
     copies = []
@@ -171,7 +171,7 @@
     two = pltpu.roll(up, 2, 0)
     two = jnp.where(at == 0, before[rim - 2 : rim - 1], two)
     two = jnp.where(at == 1, before[rim - 1 : rim], two)
-    conv = bias_ref[...] + taps_ref[0:1] * two + taps_ref[1:2] * one + taps_ref[2:3] * up
+    conv = bias_ref[...].reshape(1, ff) + taps_ref[0:1] * two + taps_ref[1:2] * one + taps_ref[2:3] * up
     hidden = (conv / (1.0 + jnp.exp(-conv)) * gate).astype(jnp.bfloat16)
     for copy in copies[2 * ff // LANES :]:
         copy.wait()
@@ -304,7 +304,7 @@
             pltpu.SemaphoreType.DMA((width // LANES + 1,)),
         ],
         name="ffn",
-    )(*in_vmem, all_w, conv_weight, conv_bias.reshape(1, ff))
+    )(*in_vmem, all_w, conv_weight, conv_bias)
     ffn_out = summed_over_tp(ffn)
     return (mid.astype(jnp.float32) + ffn_out.astype(jnp.float32)).astype(jnp.bfloat16)
 

time: 184 us -> 181 us (0.984)
  the two profiles are of different devices: /device:TPU:384 before, /device:TPU:1 now
where the time goes in v11:
time: 181 us; the launch traced here: 179 us
  blocking collectives  49.2 us (27%)
  starting transfers between devices  47.3 us (26%)
  waiting for transfers between devices  44.6 us (25%)
  Pallas kernels  17.3 us (10%)
  between operations  14.4 us (8%)
  other arithmetic  3.72 us (2%)
  local copies, waits for them, and re-layouts  2.07 us (1%)
    ppermute x7, starting transfers between devices, shifted(): return lax.ppermute(value, 'z', [((i - steps) % count, i) for i in targets])  32.8 us
    ppermute x7, waiting for transfers between devices, shifted(): return lax.ppermute(value, 'z', [((i - steps) % count, i) for i in targets])  28.6 us
    all_to_all x2, blocking collectives, summed_over_tp(): tiles = lax.all_to_all(both, 'x', 0, 0, tiled=True)  22 us
    all_gather x1, blocking collectives, local(): lax.all_gather(normalize(mid, norm_gain), TP, axis=0, tiled=True)  15 us
    all_gather x1, blocking collectives, local(): lax.all_gather(jnp.concatenate(cuts, axis=1), 'y', axis=0, tiled=True)  12.2 us
    pallas_call x1, Pallas kernels, local(): pl.pallas_call(attend_kernel, out_shape=pltpu.VMEM((NY * rows, 3 * VD), j...  10.5 us
    ppermute x2, starting transfers between devices, summed_over_tp(): from_peer = lax.ppermute(for_peer, 'c', [(0, 1), (1, 0)])  8.8 us
    all_to_all x1, waiting for transfers between devices, local(): got = lax.all_to_all(parts.reshape(NY, rows, 3 * VD), 'y', 0, 0, tiled=True)  6.82 us
  transfers between devices with their start and end apart: 12, of which 10 were waited for; matrix products, arithmetic and copies ran while one was open for 2% of the time, Pallas kernels for 6%

profile of v11, /device:TPU:1, one launch (start us, length us, event | category | flops | bytes accessed | tf_op | source)
XLA Modules:
  0.0 179.0 jit_solution(9933873115100061213)
XLA Ops:
  6.5 0.0 copy-start
  6.5 0.0 all-gather.2.cloned.1.call-start
  6.5 0.8 fusion.20
  7.4 1.0 concatenate.9
  8.3 0.0 copy-start.3
  8.4 0.0 copy-start.4
  8.4 12.2 %all_gather.9.rows_ref = bf16[128,2944]{1,0:T(8,128)(2,1)S(1)} all-gather(bf16[32,2944]{1,0:T(8,128)(2,1)S(1)} %concatenate.9), channel_id=1, replica_groups=mesh['z'=16,'y'=4,'x'=4,'c'=2] {'y'}, dimensions={0}, use_global_device_ids=true | all-gather | bytes 942080 | tf_op jit(solution)/shard_map/all_gather | solution.py:240
  20.6 0.9 fold.1
  21.5 0.0 copy-start.1
  21.5 0.0 all-gather.2.cloned.1.call-update
  21.6 0.0 copy-done.3
  21.6 0.0 copy-done.4
  21.6 11.2 %collective-permute-start = (bf16[192,256]{1,0:T(8,128)(2,1)S(1)}, bf16[192,256]{1,0:T(8,128)(2,1)S(1)}, u32[]{:S(2)}, u32[]{:S(2)}) collective-permute-start(bf16[192,256]{1,0:T(8,128)(2,1)S(1)} %constant_dynamic-update-slice_fusion), channel_id=1, source_target_pairs={{352,0},{384,32},{0,160},{32,192},{64,224},{96,256},{128,288},{160... | collective-permute-start | bytes 294920 | tf_op jit(solution)/shard_map/ppermute | solution.py:29
  32.8 5.9 %collective-permute-start.1 = (bf16[192,256]{1,0:T(8,128)(2,1)S(1)}, bf16[192,256]{1,0:T(8,128)(2,1)S(1)}, u32[]{:S(2)}, u32[]{:S(2)}) collective-permute-start(bf16[192,256]{1,0:T(8,128)(2,1)S(1)} %constant_dynamic-update-slice_fusion), channel_id=1, source_target_pairs={{160,0},{192,32},{0,352},{32,384},{64,416},{96,448},{128,480},{161... | collective-permute-start | bytes 294920 | tf_op jit(solution)/shard_map/ppermute | solution.py:29
  38.7 0.1 collective-permute-done
  38.8 5.8 %collective-permute-done.1 = bf16[192,256]{1,0:T(8,128)(2,1)S(1)} collective-permute-done((bf16[192,256]{1,0:T(8,128)(2,1)S(1)}, bf16[192,256]{1,0:T(8,128)(2,1)S(1)}, u32[]{:S(2)}, u32[]{:S(2)}) %collective-permute-start.1) | collective-permute-done | bytes 98336 | tf_op jit(solution)/shard_map/ppermute | solution.py:29
  44.6 0.0 copy-done.1
  44.6 2.1 %collective-permute-start.2 = (bf16[576,256]{1,0:T(8,128)(2,1)S(1)}, bf16[576,256]{1,0:T(8,128)(2,1)S(1)}, u32[]{:S(2)}, u32[]{:S(2)}) collective-permute-start(bf16[576,256]{1,0:T(8,128)(2,1)S(1)} %pad_maximum_fusion.refs_0_), channel_id=1, source_target_pairs={{0,32},{32,64},{64,96},{96,128},{128,160},{160,192},{192,224},{224... | collective-permute-start | bytes 884744 | tf_op jit(solution)/shard_map/ppermute | solution.py:29
  46.8 4.5 %collective-permute-start.3 = (bf16[576,256]{1,0:T(8,128)(2,1)S(1)}, bf16[576,256]{1,0:T(8,128)(2,1)S(1)}, u32[]{:S(2)}, u32[]{:S(2)}) collective-permute-start(bf16[576,256]{1,0:T(8,128)(2,1)S(1)} %pad_maximum_fusion.refs_0_), channel_id=1, source_target_pairs={{32,0},{160,128},{192,160},{224,192},{256,224},{288,256},{320,288}... | collective-permute-start | bytes 884744 | tf_op jit(solution)/shard_map/ppermute | solution.py:29
  51.3 6.2 %collective-permute-done.2.refs_1_ = bf16[576,256]{1,0:T(8,128)(2,1)S(1)} collective-permute-done((bf16[576,256]{1,0:T(8,128)(2,1)S(1)}, bf16[576,256]{1,0:T(8,128)(2,1)S(1)}, u32[]{:S(2)}, u32[]{:S(2)}) %collective-permute-start.2) | collective-permute-done | bytes 294944 | tf_op jit(solution)/shard_map/ppermute | solution.py:29
  57.5 0.7 collective-permute-start.4
  58.2 5.3 %collective-permute-done.3.refs_2_ = bf16[576,256]{1,0:T(8,128)(2,1)S(1)} collective-permute-done((bf16[576,256]{1,0:T(8,128)(2,1)S(1)}, bf16[576,256]{1,0:T(8,128)(2,1)S(1)}, u32[]{:S(2)}, u32[]{:S(2)}) %collective-permute-start.3) | collective-permute-done | bytes 294944 | tf_op jit(solution)/shard_map/ppermute | solution.py:29
  63.5 7.7 %collective-permute-start.5 = (bf16[576,256]{1,0:T(8,128)(2,1)S(1)}, bf16[576,256]{1,0:T(8,128)(2,1)S(1)}, u32[]{:S(2)}, u32[]{:S(2)}) collective-permute-start(bf16[576,256]{1,0:T(8,128)(2,1)S(1)} %collective-permute-done.3.refs_2_), channel_id=1, source_target_pairs={{128,96},{160,128},{192,160},{224,192},{256,224},{288,256},{320,28... | collective-permute-start | bytes 884744 | tf_op jit(solution)/shard_map/ppermute | solution.py:29
  71.3 0.0 collective-permute-done.4.refs_3_
  71.3 0.7 collective-permute-start.6
  72.0 0.6 pad_add_fusion.where_ref
  72.6 11.2 %collective-permute-done.5.refs_4_ = bf16[576,256]{1,0:T(8,128)(2,1)S(1)} collective-permute-done((bf16[576,256]{1,0:T(8,128)(2,1)S(1)}, bf16[576,256]{1,0:T(8,128)(2,1)S(1)}, u32[]{:S(2)}, u32[]{:S(2)}) %collective-permute-start.5) | collective-permute-done | bytes 294944 | tf_op jit(solution)/shard_map/ppermute | solution.py:29
  83.8 0.0 collective-permute-done.6.refs_5_
  83.8 10.5 %attend.1 = bf16[768,384]{1,0:T(8,128)(2,1)} custom-call(s32[2]{0:T(128)} %pad_add_fusion.where_ref, bf16[128,768]{1,0:T(8,128)(2,1)} %copy-done.1, bf16[576,256]{1,0:T(8,128)(2,1)S(1)} %pad_maximum_fusion.refs_0_, bf16[576,256]{1,0:T(8,128)(2,1)S(1)} %collective-permute-done.2.refs_1_, bf16[576,256]{1,0:T(8,128)(2,1)S(1)} %collective-permute-done.3.refs_2_, ...), custom_call_target="tpu_custom_call" | custom-call | tf_op jit(solution)/shard_map/attend/pallas_call | solution.py:267
  94.3 3.5 %all-to-all-start = ((bf16[4,192,384]{2,1,0:T(8,128)(2,1)}), bf16[4,192,384]{2,1,0:T(8,128)(2,1)S(1)}, u32[]{:S(2)}, u32[]{:S(2)}) async-start(bf16[4,192,384]{2,1,0:T(8,128)(2,1)} %bitcast.3), calls=%async_computation | async-start | bytes 1179648 | tf_op jit(solution)/shard_map/all_to_all | solution.py:278
  98.5 6.8 %all-to-all-done = bf16[4,192,384]{2,1,0:T(8,128)(2,1)S(1)} async-done(((bf16[4,192,384]{2,1,0:T(8,128)(2,1)}), bf16[4,192,384]{2,1,0:T(8,128)(2,1)S(1)}, u32[]{:S(2)}, u32[]{:S(2)}) %all-to-all-start) | async-done | bytes 589856 | tf_op jit(solution)/shard_map/all_to_all | solution.py:278
  105.3 0.1 convert_element_type.60
  105.4 0.7 fusion.18
  106.1 0.0 copy-start.6
  106.1 0.6 fusion.6
  106.7 0.3 fusion.4
  106.9 0.1 copy.35
  107.0 0.1 copy.36
  107.1 0.1 multiply_reduce_fusion
  107.2 0.0 copy-done
  107.2 0.0 copy-done.6
  107.2 0.5 convolution_convert_fusion
  107.8 0.0 copy-start.2
  107.8 0.0 copy-start.5
  107.8 5.7 %collective-permute-start.7 = (bf16[4,24,2048]{2,1,0:T(8,128)(2,1)S(1)}, bf16[4,24,2048]{2,1,0:T(8,128)(2,1)S(1)}, u32[]{:S(2)}, u32[]{:S(2)}) collective-permute-start(bf16[4,24,2048]{2,1,0:T(8,128)(2,1)S(1)} %select_bitcast_fusion), channel_id=1, source_target_pairs={{0,1},{1,0},{2,3},{3,2},{4,5},{5,4},{6,7},{7,6},{8,9},{9,8},{10,11... | collective-permute-start | bytes 1179656 | tf_op jit(solution)/shard_map/ppermute | solution.py:211
  113.5 1.3 collective-permute-done.7
  114.8 0.1 fusion.1
  114.9 11.0 %all_to_all.15 = bf16[4,24,2048]{2,1,0:T(8,128)(2,1)S(1)} all-to-all(bf16[4,24,2048]{2,1,0:T(8,128)(2,1)S(1)} %fusion.1), channel_id=1, replica_groups=mesh['z'=16,'y'=4,'x'=4,'c'=2] {'x'}, dimensions={0} | all-to-all | bytes 786432 | tf_op jit(solution)/shard_map/all_to_all | solution.py:213
  126.0 0.1 reduce_sum.83
  126.0 0.0 copy-done.2
  126.0 0.1 fusion.10
  126.2 0.0 copy-done.5
  126.2 0.1 fusion.12
  126.3 15.0 %all_gather.10.rows_ref = bf16[192,2048]{1,0:T(8,128)(2,1)S(1)} all-gather(bf16[24,2048]{1,0:T(8,128)(2,1)S(1)} %fusion.12), channel_id=1, replica_groups=mesh['z'=16,'y'=4,'x'=4,'c'=2] {'x','c'}, dimensions={0}, use_global_device_ids=true | all-gather | bytes 884736 | tf_op jit(solution)/shard_map/all_gather | solution.py:287
  141.3 2.2 %collective-permute-start.8 = (bf16[8,2048]{1,0:T(8,128)(2,1)S(1)}, bf16[8,2048]{1,0:T(8,128)(2,1)S(1)}, u32[]{:S(2)}, u32[]{:S(2)}) collective-permute-start(bf16[8,2048]{1,0:T(8,128)(2,1)S(1)} %slice.103), channel_id=1, source_target_pairs={{0,8},{8,16},{16,24},{24,32},{32,40},{40,48},{48,56},{56,64},{64,7... | collective-permute-start | bytes 98312 | tf_op jit(solution)/shard_map/ppermute | solution.py:289
  143.5 1.0 collective-permute-done.8.rim_ref
  144.5 5.5 %all-gather.2.cloned.1.call-done = bf16[33792,128]{1,0:T(8,128)(2,1)} async-done(((bf16[2112,128]{1,0:T(8,128)(2,1)}), bf16[33792,128]{1,0:T(8,128)(2,1)}) %all-gather.2.cloned.1.call-update) | async-done | bytes 8650768 | tf_op jit(solution)/shard_map/all_gather | solution.py:252
  149.9 5.8 %ffn.1 = bf16[192,2048]{1,0:T(8,128)(2,1)S(1)} custom-call(bf16[192,2048]{1,0:T(8,128)(2,1)S(1)} %all_gather.10.rows_ref, bf16[8,2048]{1,0:T(8,128)(2,1)S(1)} %collective-permute-done.8.rim_ref, bf16[16,2112,128]{2,1,0:T(8,128)(2,1)} %bitcast.50, f32[3,704]{1,0:T(4,128)} %taps_ref.1, f32[704]{0:T(1024)} %bias_ref.1), custom_call_target="tpu_custom_call" | custom-call | tf_op jit(solution)/shard_map/ffn/pallas_call | solution.py:294
  155.8 3.1 %collective-permute-start.9 = (bf16[4,24,2048]{2,1,0:T(8,128)(2,1)S(1)}, bf16[4,24,2048]{2,1,0:T(8,128)(2,1)S(1)}, u32[]{:S(2)}, u32[]{:S(2)}) collective-permute-start(bf16[4,24,2048]{2,1,0:T(8,128)(2,1)S(1)} %fusion.2), channel_id=1, source_target_pairs={{0,1},{1,0},{2,3},{3,2},{4,5},{5,4},{6,7},{7,6},{8,9},{9,8},{10,11... | collective-permute-start | bytes 1179656 | tf_op jit(solution)/shard_map/ppermute | solution.py:211
  159.0 1.3 collective-permute-done.9
  160.3 0.1 fusion
  160.5 11.0 %all_to_all.16 = bf16[4,24,2048]{2,1,0:T(8,128)(2,1)S(1)} all-to-all(bf16[4,24,2048]{2,1,0:T(8,128)(2,1)S(1)} %fusion), channel_id=1, replica_groups=mesh['z'=16,'y'=4,'x'=4,'c'=2] {'x'}, dimensions={0} | all-to-all | bytes 786432 | tf_op jit(solution)/shard_map/all_to_all | solution.py:213
  171.4 0.1 reduce_sum.85
  171.5 0.7 fusion.13
  (10 shorter events, 0.2 us)
Async XLA Ops:
  6.5 100.7 %copy-start = (bf16[128,2048]{1,0:T(8,128)(2,1)S(1)}, bf16[128,2048]{1,0:T(8,128)(2,1)}, u32[]{:S(2)}) copy-start(bf16[128,2048]{1,0:T(8,128)(2,1)} %param.19) | copy-start | bytes 1572868
  6.5 143.4 %all-gather.2.cloned.1.call-start = ((), (), s32[]{:S(2)}) async-start(), calls=%async_computation.3 | async-start | bytes 9191424 | tf_op jit(solution)/shard_map/all_gather | solution.py:252
  8.3 13.2 %copy-start.3 = (bf16[192,128]{1,0:T(8,128)(2,1)S(1)}, bf16[192,128]{1,0:T(8,128)(2,1)}, u32[]{:S(2)}) copy-start(bf16[192,128]{1,0:T(8,128)(2,1)} %param.15) | copy-start | bytes 147460
  8.4 13.2 %copy-start.4 = (bf16[192,128]{1,0:T(8,128)(2,1)S(1)}, bf16[192,128]{1,0:T(8,128)(2,1)}, u32[]{:S(2)}) copy-start(bf16[192,128]{1,0:T(8,128)(2,1)} %param.16) | copy-start | bytes 147460
  21.5 23.1 %copy-start.1 = (bf16[128,768]{1,0:T(8,128)(2,1)}, bf16[128,768]{1,0:T(8,128)(2,1)S(1)}, u32[]{:S(2)}) copy-start(bf16[128,768]{1,0:T(8,128)(2,1)S(1)} %get-tuple-element.7.rows_ref) | copy-start | bytes 589828
  21.6 17.2 %collective-permute-start = (bf16[192,256]{1,0:T(8,128)(2,1)S(1)}, bf16[192,256]{1,0:T(8,128)(2,1)S(1)}, u32[]{:S(2)}, u32[]{:S(2)}) collective-permute-start(bf16[192,256]{1,0:T(8,128)(2,1)S(1)} %constant_dynamic-update-slice_fusion), channel_id=1, source_target_pairs={{352,0},{384,32},{0,160},{32,192},{64,224},{96,256},{128,288},{160... | collective-permute-start | bytes 294920 | tf_op jit(solution)/shard_map/ppermute | solution.py:29
  32.8 11.8 %collective-permute-start.1 = (bf16[192,256]{1,0:T(8,128)(2,1)S(1)}, bf16[192,256]{1,0:T(8,128)(2,1)S(1)}, u32[]{:S(2)}, u32[]{:S(2)}) collective-permute-start(bf16[192,256]{1,0:T(8,128)(2,1)S(1)} %constant_dynamic-update-slice_fusion), channel_id=1, source_target_pairs={{160,0},{192,32},{0,352},{32,384},{64,416},{96,448},{128,480},{161... | collective-permute-start | bytes 294920 | tf_op jit(solution)/shard_map/ppermute | solution.py:29
  44.6 12.9 %collective-permute-start.2 = (bf16[576,256]{1,0:T(8,128)(2,1)S(1)}, bf16[576,256]{1,0:T(8,128)(2,1)S(1)}, u32[]{:S(2)}, u32[]{:S(2)}) collective-permute-start(bf16[576,256]{1,0:T(8,128)(2,1)S(1)} %pad_maximum_fusion.refs_0_), channel_id=1, source_target_pairs={{0,32},{32,64},{64,96},{96,128},{128,160},{160,192},{192,224},{224... | collective-permute-start | bytes 884744 | tf_op jit(solution)/shard_map/ppermute | solution.py:29
  46.8 16.7 %collective-permute-start.3 = (bf16[576,256]{1,0:T(8,128)(2,1)S(1)}, bf16[576,256]{1,0:T(8,128)(2,1)S(1)}, u32[]{:S(2)}, u32[]{:S(2)}) collective-permute-start(bf16[576,256]{1,0:T(8,128)(2,1)S(1)} %pad_maximum_fusion.refs_0_), channel_id=1, source_target_pairs={{32,0},{160,128},{192,160},{224,192},{256,224},{288,256},{320,288}... | collective-permute-start | bytes 884744 | tf_op jit(solution)/shard_map/ppermute | solution.py:29
  57.5 13.8 %collective-permute-start.4 = (bf16[576,256]{1,0:T(8,128)(2,1)S(1)}, bf16[576,256]{1,0:T(8,128)(2,1)S(1)}, u32[]{:S(2)}, u32[]{:S(2)}) collective-permute-start(bf16[576,256]{1,0:T(8,128)(2,1)S(1)} %collective-permute-done.2.refs_1_), channel_id=1, source_target_pairs={{32,64},{64,96},{96,128},{128,160},{160,192},{192,224},{224,256},{... | collective-permute-start | bytes 884744 | tf_op jit(solution)/shard_map/ppermute | solution.py:29
  63.5 20.3 %collective-permute-start.5 = (bf16[576,256]{1,0:T(8,128)(2,1)S(1)}, bf16[576,256]{1,0:T(8,128)(2,1)S(1)}, u32[]{:S(2)}, u32[]{:S(2)}) collective-permute-start(bf16[576,256]{1,0:T(8,128)(2,1)S(1)} %collective-permute-done.3.refs_2_), channel_id=1, source_target_pairs={{128,96},{160,128},{192,160},{224,192},{256,224},{288,256},{320,28... | collective-permute-start | bytes 884744 | tf_op jit(solution)/shard_map/ppermute | solution.py:29
  71.3 12.5 %collective-permute-start.6 = (bf16[192,256]{1,0:T(8,128)(2,1)S(1)}, bf16[192,256]{1,0:T(8,128)(2,1)S(1)}, u32[]{:S(2)}, u32[]{:S(2)}) collective-permute-start(bf16[192,256]{1,0:T(8,128)(2,1)S(1)} %slice.92), channel_id=1, source_target_pairs={{224,256},{256,288},{288,320},{320,352},{352,384},{384,416},{416,4... | collective-permute-start | bytes 294920 | tf_op jit(solution)/shard_map/ppermute | solution.py:29
  94.3 11.0 %all-to-all-start = ((bf16[4,192,384]{2,1,0:T(8,128)(2,1)}), bf16[4,192,384]{2,1,0:T(8,128)(2,1)S(1)}, u32[]{:S(2)}, u32[]{:S(2)}) async-start(bf16[4,192,384]{2,1,0:T(8,128)(2,1)} %bitcast.3), calls=%async_computation | async-start | bytes 1179648 | tf_op jit(solution)/shard_map/all_to_all | solution.py:278
  106.1 1.1 copy-start.6
  107.8 18.3 %copy-start.2 = (bf16[24,2048]{1,0:T(8,128)(2,1)S(1)}, bf16[24,2048]{1,0:T(8,128)(2,1)}, u32[]{:S(2)}) copy-start(bf16[24,2048]{1,0:T(8,128)(2,1)} %param.13) | copy-start | bytes 294916
  107.8 18.4 %copy-start.5 = (f32[2048]{0:T(1024)S(1)}, f32[2048]{0:T(1024)}, u32[]{:S(2)}) copy-start(f32[2048]{0:T(1024)} %param.20) | copy-start | bytes 24580
  107.8 7.0 %collective-permute-start.7 = (bf16[4,24,2048]{2,1,0:T(8,128)(2,1)S(1)}, bf16[4,24,2048]{2,1,0:T(8,128)(2,1)S(1)}, u32[]{:S(2)}, u32[]{:S(2)}) collective-permute-start(bf16[4,24,2048]{2,1,0:T(8,128)(2,1)S(1)} %select_bitcast_fusion), channel_id=1, source_target_pairs={{0,1},{1,0},{2,3},{3,2},{4,5},{5,4},{6,7},{7,6},{8,9},{9,8},{10,11... | collective-permute-start | bytes 1179656 | tf_op jit(solution)/shard_map/ppermute | solution.py:211
  141.3 3.2 %collective-permute-start.8 = (bf16[8,2048]{1,0:T(8,128)(2,1)S(1)}, bf16[8,2048]{1,0:T(8,128)(2,1)S(1)}, u32[]{:S(2)}, u32[]{:S(2)}) collective-permute-start(bf16[8,2048]{1,0:T(8,128)(2,1)S(1)} %slice.103), channel_id=1, source_target_pairs={{0,8},{8,16},{16,24},{24,32},{32,40},{40,48},{48,56},{56,64},{64,7... | collective-permute-start | bytes 98312 | tf_op jit(solution)/shard_map/ppermute | solution.py:289
  155.8 4.5 %collective-permute-start.9 = (bf16[4,24,2048]{2,1,0:T(8,128)(2,1)S(1)}, bf16[4,24,2048]{2,1,0:T(8,128)(2,1)S(1)}, u32[]{:S(2)}, u32[]{:S(2)}) collective-permute-start(bf16[4,24,2048]{2,1,0:T(8,128)(2,1)S(1)} %fusion.2), channel_id=1, source_target_pairs={{0,1},{1,0},{2,3},{3,2},{4,5},{5,4},{6,7},{7,6},{8,9},{9,8},{10,11... | collective-permute-start | bytes 1179656 | tf_op jit(solution)/shard_map/ppermute | solution.py:211
Sparse Core Ops, SparseCore 0:
  21.7 128.2 all-gather.1

commit v12 on v11

--- a/solution.py
+++ b/solution.py
@@ -59,17 +59,14 @@
     return block
 
 
-def attend_kernel(where_ref, rows_ref, *refs):
-    blocks, (out_ref, q_ref, kv_ref) = refs[:-3], refs[-3:]
+def attend_kernel(where_ref, *refs):
+    query_blocks, blocks, (out_ref, q_ref, kv_ref) = refs[:NY], refs[NY:-3], refs[-3:]
     z = where_ref[0]
     y = where_ref[1]
     rows = kv_ref.shape[0] // len(OFFSETS)
-    w_rows = rows_ref.shape[0] // NY
-    for i in range(NY * rows // w_rows):
-        y_at, lane_at = divmod(i, rows // w_rows)
-        q_ref[i * w_rows : (i + 1) * w_rows, :] = rows_ref[
-            y_at * w_rows : (y_at + 1) * w_rows, lane_at * 2 * HD : (lane_at + 1) * 2 * HD
-        ]
+    for behind, block in enumerate(query_blocks):
+        first = pl.multiple_of(((y - behind) & (NY - 1)) * rows, rows)
+        q_ref[pl.ds(first, rows), :] = block[...]
     filled = 0
     for block in blocks:
         kv_ref[filled : filled + block.shape[0], :] = block[...]
@@ -115,7 +112,7 @@
         )
 
 
-def fold_kernel(rows_ref, out_ref, q_ref):
+def fold_kernel(rows_ref, out_ref):
     deep = rows_ref.shape[0]
     blocks = out_ref.shape[0] // deep
     for i in range(blocks):
@@ -124,7 +121,6 @@
     lane = lax.broadcasted_iota(jnp.int32, (deep // 2, LANES), 1)
     low, high = last[: deep // 2], pltpu.roll(last[deep // 2 :], LANES // 2, 1)
     out_ref[blocks * deep :, :] = jnp.where(lane < LANES // 2, low, high).astype(jnp.bfloat16)
-    q_ref[...] = rows_ref[:, (blocks + 1) * LANES :]
 
 
 def ffn_kernel(
@@ -236,17 +232,13 @@
     width = 2 * ff + ff
     tail = -width % LANES
     cuts = [up_weight, gate_weight, down_weight.T, jnp.zeros((w_rows, tail), jnp.bfloat16)]
-    cuts += [queries[i : i + w_rows] for i in range(0, rows, w_rows)]
     row_w = lax.all_gather(jnp.concatenate(cuts, axis=1), "y", axis=0, tiled=True)
     deep = row_w.shape[0]
-    shard, q_rows = pl.pallas_call(
+    shard = pl.pallas_call(
         fold_kernel,
-        out_shape=[
-            jax.ShapeDtypeStruct((deep * width // LANES, LANES), jnp.bfloat16),
-            pltpu.VMEM((deep, row_w.shape[1] - width - tail), jnp.bfloat16),
-        ],
+        out_shape=jax.ShapeDtypeStruct((deep * width // LANES, LANES), jnp.bfloat16),
         in_specs=[VMEM],
-        out_specs=[VMEM] * 2,
+        out_specs=VMEM,
         name="fold",
     )(pltpu.with_memory_space_constraint(row_w, pltpu.VMEM))
     all_w = lax.all_gather(shard, "z", axis=0, tiled=True)
@@ -256,6 +248,10 @@
     last = lax.axis_size("z")
     f5 = shifted(kv, 5, [0, 1, *range(5, last)])
     f11 = shifted(kv, -5, [0, 1, *range(11, last)])
+    query_blocks = [queries]
+    for behind in range(1, NY):
+        pairs = [((i - behind) % NY, i) for i in range(NY)]
+        query_blocks.append(lax.ppermute(queries, "y", pairs))
     held = jnp.concatenate((kv, f5, f11), axis=0)
     n1 = shifted(held, 1, range(1, last))
     m1 = shifted(held, -1, [0, *range(4, last)])
@@ -263,18 +259,19 @@
     m2 = shifted(m1, -1, range(3, last))
     e8 = shifted(n2[rows : 2 * rows], 1, range(8, last))
     blocks = [held, n1, m1, n2, m2, e8]
+    blocks = query_blocks + blocks
     blocks = [pltpu.with_memory_space_constraint(b, pltpu.VMEM) for b in blocks]
     parts = pl.pallas_call(
         attend_kernel,
         out_shape=pltpu.VMEM((NY * rows, 3 * VD), jnp.bfloat16),
-        in_specs=[SMEM] + [VMEM] * (1 + len(blocks)),
+        in_specs=[SMEM] + [VMEM] * len(blocks),
         out_specs=VMEM,
         scratch_shapes=[
             pltpu.VMEM((NY * rows, 2 * HD), jnp.bfloat16),
             pltpu.VMEM((len(OFFSETS) * rows, 2 * HD + VD), jnp.bfloat16),
         ],
         name="attend",
-    )(where, q_rows, *blocks)
+    )(where, *blocks)
     got = lax.all_to_all(parts.reshape(NY, rows, 3 * VD), "y", 0, 0, tiled=True)
     means = merged(got)
     diff = means[0] - second_weight[0] * means[1]

time: 181 us -> 181 us (level)
  waiting for transfers between devices: 44.6 us -> 34.8 us
  starting transfers between devices: 47.3 us -> 56.7 us
    ppermute x7, waiting for transfers between devices: 28.6 us -> 19.2 us  [shifted(): return lax.ppermute(value, 'z', [((i - steps) % count, i) for i in targets])]
    ppermute x0 -> x3, starting transfers between devices: none -> 9.09 us  [local(): query_blocks.append(lax.ppermute(queries, 'y', pairs))]
    unnamed x17 -> x21, local copies, waits for them, and re-layouts: 0.24 us -> 2.34 us
  transfers between devices with their start and end apart: 12 -> 15, of which waited for: 10 -> 11; matrix products, arithmetic and copies ran while one was open for 2% -> 2% of each run, Pallas kernels for 6% -> 6%
where the time goes in v12:
time: 181 us; the launch traced here: 179 us
  starting transfers between devices  56.7 us (31%)
  blocking collectives  48.5 us (27%)
  waiting for transfers between devices  34.8 us (19%)
  Pallas kernels  17 us (9%)
  between operations  14.4 us (8%)
  other arithmetic  3.71 us (2%)
  local copies, waits for them, and re-layouts  3.38 us (2%)
    ppermute x7, starting transfers between devices, shifted(): return lax.ppermute(value, 'z', [((i - steps) % count, i) for i in targets])  33 us
    all_to_all x2, blocking collectives, summed_over_tp(): tiles = lax.all_to_all(both, 'x', 0, 0, tiled=True)  22.1 us
    ppermute x7, waiting for transfers between devices, shifted(): return lax.ppermute(value, 'z', [((i - steps) % count, i) for i in targets])  19.2 us
    all_gather x1, blocking collectives, local(): lax.all_gather(normalize(mid, norm_gain), TP, axis=0, tiled=True)  15 us
    all_gather x1, blocking collectives, local(): lax.all_gather(jnp.concatenate(cuts, axis=1), 'y', axis=0, tiled=True)  11.4 us
    pallas_call x1, Pallas kernels, local(): pl.pallas_call(attend_kernel, out_shape=pltpu.VMEM((NY * rows, 3 * VD), j...  10.3 us
    ppermute x3, starting transfers between devices, local(): query_blocks.append(lax.ppermute(queries, 'y', pairs))  9.09 us
    ppermute x2, starting transfers between devices, summed_over_tp(): from_peer = lax.ppermute(for_peer, 'c', [(0, 1), (1, 0)])  8.95 us
  transfers between devices with their start and end apart: 15, of which 11 were waited for; matrix products, arithmetic and copies ran while one was open for 2% of the time, Pallas kernels for 6%

profile of v12, /device:TPU:1, one launch (start us, length us, event | category | flops | bytes accessed | tf_op | source)
XLA Modules:
  0.0 178.8 jit_solution(13265626861882489003)
XLA Ops:
  6.5 0.0 copy-start
  6.5 0.0 all-gather.2.cloned.1.call-start
  6.5 1.0 concatenate.11
  7.6 0.0 copy-start.5
  7.6 0.0 copy-start.6
  7.6 11.4 %all_gather.10.rows_ref = bf16[128,2176]{1,0:T(8,128)(2,1)S(1)} all-gather(bf16[32,2176]{1,0:T(8,128)(2,1)S(1)} %concatenate.11), channel_id=1, replica_groups=mesh['z'=16,'y'=4,'x'=4,'c'=2] {'y'}, dimensions={0}, use_global_device_ids=true | all-gather | bytes 696320 | tf_op jit(solution)/shard_map/all_gather | solution.py:235
  19.0 0.9 fold.1
  19.9 0.0 all-gather.2.cloned.1.call-update
  19.9 0.0 copy-done.5
  20.0 0.0 copy-done.6
  20.0 11.5 %collective-permute-start.3 = (bf16[192,256]{1,0:T(8,128)(2,1)S(1)}, bf16[192,256]{1,0:T(8,128)(2,1)S(1)}, u32[]{:S(2)}, u32[]{:S(2)}) collective-permute-start(bf16[192,256]{1,0:T(8,128)(2,1)S(1)} %constant_dynamic-update-slice_fusion), channel_id=1, source_target_pairs={{352,0},{384,32},{0,160},{32,192},{64,224},{96,256},{128,288},{160... | collective-permute-start | bytes 294920 | tf_op jit(solution)/shard_map/ppermute | solution.py:29
  31.6 5.9 %collective-permute-start.4 = (bf16[192,256]{1,0:T(8,128)(2,1)S(1)}, bf16[192,256]{1,0:T(8,128)(2,1)S(1)}, u32[]{:S(2)}, u32[]{:S(2)}) collective-permute-start(bf16[192,256]{1,0:T(8,128)(2,1)S(1)} %constant_dynamic-update-slice_fusion), channel_id=1, source_target_pairs={{160,0},{192,32},{0,352},{32,384},{64,416},{96,448},{128,480},{161... | collective-permute-start | bytes 294920 | tf_op jit(solution)/shard_map/ppermute | solution.py:29
  37.4 0.1 collective-permute-done.3
  37.5 5.9 %collective-permute-done.4 = bf16[192,256]{1,0:T(8,128)(2,1)S(1)} collective-permute-done((bf16[192,256]{1,0:T(8,128)(2,1)S(1)}, bf16[192,256]{1,0:T(8,128)(2,1)S(1)}, u32[]{:S(2)}, u32[]{:S(2)}) %collective-permute-start.4) | collective-permute-done | bytes 98336 | tf_op jit(solution)/shard_map/ppermute | solution.py:29
  43.5 2.0 %collective-permute-start.5 = (bf16[576,256]{1,0:T(8,128)(2,1)S(1)}, bf16[576,256]{1,0:T(8,128)(2,1)S(1)}, u32[]{:S(2)}, u32[]{:S(2)}) collective-permute-start(bf16[576,256]{1,0:T(8,128)(2,1)S(1)} %pad_maximum_fusion.refs_4_), channel_id=1, source_target_pairs={{0,32},{32,64},{64,96},{96,128},{128,160},{160,192},{192,224},{224... | collective-permute-start | bytes 884744 | tf_op jit(solution)/shard_map/ppermute | solution.py:29
  45.5 4.6 %collective-permute-start.6 = (bf16[576,256]{1,0:T(8,128)(2,1)S(1)}, bf16[576,256]{1,0:T(8,128)(2,1)S(1)}, u32[]{:S(2)}, u32[]{:S(2)}) collective-permute-start(bf16[576,256]{1,0:T(8,128)(2,1)S(1)} %pad_maximum_fusion.refs_4_), channel_id=1, source_target_pairs={{32,0},{160,128},{192,160},{224,192},{256,224},{288,256},{320,288}... | collective-permute-start | bytes 884744 | tf_op jit(solution)/shard_map/ppermute | solution.py:29
  50.2 6.0 %collective-permute-done.5.refs_5_ = bf16[576,256]{1,0:T(8,128)(2,1)S(1)} collective-permute-done((bf16[576,256]{1,0:T(8,128)(2,1)S(1)}, bf16[576,256]{1,0:T(8,128)(2,1)S(1)}, u32[]{:S(2)}, u32[]{:S(2)}) %collective-permute-start.5) | collective-permute-done | bytes 294944 | tf_op jit(solution)/shard_map/ppermute | solution.py:29
  56.2 0.7 collective-permute-start.7
  56.8 5.5 %collective-permute-done.6.refs_6_ = bf16[576,256]{1,0:T(8,128)(2,1)S(1)} collective-permute-done((bf16[576,256]{1,0:T(8,128)(2,1)S(1)}, bf16[576,256]{1,0:T(8,128)(2,1)S(1)}, u32[]{:S(2)}, u32[]{:S(2)}) %collective-permute-start.6) | collective-permute-done | bytes 294944 | tf_op jit(solution)/shard_map/ppermute | solution.py:29
  62.4 7.6 %collective-permute-start.8 = (bf16[576,256]{1,0:T(8,128)(2,1)S(1)}, bf16[576,256]{1,0:T(8,128)(2,1)S(1)}, u32[]{:S(2)}, u32[]{:S(2)}) collective-permute-start(bf16[576,256]{1,0:T(8,128)(2,1)S(1)} %collective-permute-done.6.refs_6_), channel_id=1, source_target_pairs={{128,96},{160,128},{192,160},{224,192},{256,224},{288,256},{320,28... | collective-permute-start | bytes 884744 | tf_op jit(solution)/shard_map/ppermute | solution.py:29
  70.0 1.9 %collective-permute-start = (bf16[192,128]{1,0:T(8,128)(2,1)S(1)}, bf16[192,128]{1,0:T(8,128)(2,1)S(1)}, u32[]{:S(2)}, u32[]{:S(2)}) collective-permute-start(bf16[192,128]{1,0:T(8,128)(2,1)S(1)} %copy-done.3), channel_id=1, source_target_pairs={{24,0},{0,8},{8,16},{16,24},{25,1},{1,9},{9,17},{17,25},{26,2},{2,... | collective-permute-start | bytes 147464 | tf_op jit(solution)/shard_map/ppermute | solution.py:254
  71.9 3.2 %collective-permute-start.1 = (bf16[192,128]{1,0:T(8,128)(2,1)S(1)}, bf16[192,128]{1,0:T(8,128)(2,1)S(1)}, u32[]{:S(2)}, u32[]{:S(2)}) collective-permute-start(bf16[192,128]{1,0:T(8,128)(2,1)S(1)} %copy-done.3), channel_id=1, source_target_pairs={{16,0},{24,8},{0,16},{8,24},{17,1},{25,9},{1,17},{9,25},{18,2},{26... | collective-permute-start | bytes 147464 | tf_op jit(solution)/shard_map/ppermute | solution.py:254
  75.1 4.0 %collective-permute-start.2 = (bf16[192,128]{1,0:T(8,128)(2,1)S(1)}, bf16[192,128]{1,0:T(8,128)(2,1)S(1)}, u32[]{:S(2)}, u32[]{:S(2)}) collective-permute-start(bf16[192,128]{1,0:T(8,128)(2,1)S(1)} %copy-done.3), channel_id=1, source_target_pairs={{8,0},{16,8},{24,16},{0,24},{9,1},{17,9},{25,17},{1,25},{10,2},{18... | collective-permute-start | bytes 147464 | tf_op jit(solution)/shard_map/ppermute | solution.py:254
  79.1 0.0 collective-permute-done.7.refs_7_
  79.1 0.7 collective-permute-start.9
  79.8 0.6 pad_add_fusion.where_ref
  80.4 0.0 collective-permute-done.refs_1_
  80.4 0.0 collective-permute-done.1.refs_2_
  80.4 0.5 collective-permute-done.2.refs_3_
  80.8 1.6 collective-permute-done.8.refs_8_
  82.4 0.0 collective-permute-done.9.refs_9_
  82.4 10.3 %attend.1 = bf16[768,384]{1,0:T(8,128)(2,1)} custom-call(s32[2]{0:T(128)} %pad_add_fusion.where_ref, bf16[192,128]{1,0:T(8,128)(2,1)S(1)} %copy-done.3, bf16[192,128]{1,0:T(8,128)(2,1)S(1)} %collective-permute-done.refs_1_, bf16[192,128]{1,0:T(8,128)(2,1)S(1)} %collective-permute-done.1.refs_2_, bf16[192,128]{1,0:T(8,128)(2,1)S(1)} %collective-permute-done.2.refs_3_, ...), custom_call_target="tpu_custom_call" | custom-call | tf_op jit(solution)/shard_map/attend/pallas_call | solution.py:264
  92.7 3.5 %all-to-all-start = ((bf16[4,192,384]{2,1,0:T(8,128)(2,1)}), bf16[4,192,384]{2,1,0:T(8,128)(2,1)S(1)}, u32[]{:S(2)}, u32[]{:S(2)}) async-start(bf16[4,192,384]{2,1,0:T(8,128)(2,1)} %bitcast.2), calls=%async_computation | async-start | bytes 1179648 | tf_op jit(solution)/shard_map/all_to_all | solution.py:275
  96.8 6.7 %all-to-all-done = bf16[4,192,384]{2,1,0:T(8,128)(2,1)S(1)} async-done(((bf16[4,192,384]{2,1,0:T(8,128)(2,1)}), bf16[4,192,384]{2,1,0:T(8,128)(2,1)S(1)}, u32[]{:S(2)}, u32[]{:S(2)}) %all-to-all-start) | async-done | bytes 589856 | tf_op jit(solution)/shard_map/all_to_all | solution.py:275
  103.5 0.1 convert_element_type.60
  103.6 0.7 fusion.18
  104.3 0.6 fusion.6
  104.9 0.3 fusion.4
  105.2 0.1 copy.35
  105.3 0.1 copy.36
  105.4 0.1 multiply_reduce_fusion
  105.4 0.5 convolution_convert_fusion
  106.0 0.0 copy-start.4
  106.0 0.0 copy-start.7
  106.0 5.8 %collective-permute-start.10 = (bf16[4,24,2048]{2,1,0:T(8,128)(2,1)S(1)}, bf16[4,24,2048]{2,1,0:T(8,128)(2,1)S(1)}, u32[]{:S(2)}, u32[]{:S(2)}) collective-permute-start(bf16[4,24,2048]{2,1,0:T(8,128)(2,1)S(1)} %select_bitcast_fusion), channel_id=1, source_target_pairs={{0,1},{1,0},{2,3},{3,2},{4,5},{5,4},{6,7},{7,6},{8,9},{9,8},{10,11... | collective-permute-start | bytes 1179656 | tf_op jit(solution)/shard_map/ppermute | solution.py:207
  111.8 1.3 collective-permute-done.10
  113.1 0.1 fusion.1
  113.3 11.1 %all_to_all.15 = bf16[4,24,2048]{2,1,0:T(8,128)(2,1)S(1)} all-to-all(bf16[4,24,2048]{2,1,0:T(8,128)(2,1)S(1)} %fusion.1), channel_id=1, replica_groups=mesh['z'=16,'y'=4,'x'=4,'c'=2] {'x'}, dimensions={0} | all-to-all | bytes 786432 | tf_op jit(solution)/shard_map/all_to_all | solution.py:209
  124.4 0.1 reduce_sum.83
  124.4 0.1 fusion.10
  124.6 0.1 fusion.12
  124.7 15.0 %all_gather.9.rows_ref = bf16[192,2048]{1,0:T(8,128)(2,1)S(1)} all-gather(bf16[24,2048]{1,0:T(8,128)(2,1)S(1)} %fusion.12), channel_id=1, replica_groups=mesh['z'=16,'y'=4,'x'=4,'c'=2] {'x','c'}, dimensions={0}, use_global_device_ids=true | all-gather | bytes 884736 | tf_op jit(solution)/shard_map/all_gather | solution.py:284
  139.7 1.0 copy-done.1
  140.7 2.2 %collective-permute-start.11 = (bf16[8,2048]{1,0:T(8,128)(2,1)S(1)}, bf16[8,2048]{1,0:T(8,128)(2,1)S(1)}, u32[]{:S(2)}, u32[]{:S(2)}) collective-permute-start(bf16[8,2048]{1,0:T(8,128)(2,1)S(1)} %slice.79), channel_id=1, source_target_pairs={{0,8},{8,16},{16,24},{24,32},{32,40},{40,48},{48,56},{56,64},{64,7... | collective-permute-start | bytes 98312 | tf_op jit(solution)/shard_map/ppermute | solution.py:286
  142.8 1.0 collective-permute-done.11.rim_ref
  143.8 4.8 %all-gather.2.cloned.1.call-done = bf16[33792,128]{1,0:T(8,128)(2,1)} async-done(((bf16[2112,128]{1,0:T(8,128)(2,1)}), bf16[33792,128]{1,0:T(8,128)(2,1)}) %all-gather.2.cloned.1.call-update) | async-done | bytes 8650768 | tf_op jit(solution)/shard_map/all_gather | solution.py:244
  148.6 1.1 copy-done.2
  149.7 5.8 %ffn.1 = bf16[192,2048]{1,0:T(8,128)(2,1)S(1)} custom-call(bf16[192,2048]{1,0:T(8,128)(2,1)S(1)} %copy-done.2, bf16[8,2048]{1,0:T(8,128)(2,1)S(1)} %collective-permute-done.11.rim_ref, bf16[16,2112,128]{2,1,0:T(8,128)(2,1)} %bitcast.50, f32[3,704]{1,0:T(4,128)} %taps_ref.1, f32[704]{0:T(1024)} %bias_ref.1), custom_call_target="tpu_custom_call" | custom-call | tf_op jit(solution)/shard_map/ffn/pallas_call | solution.py:291
  155.6 3.1 %collective-permute-start.12 = (bf16[4,24,2048]{2,1,0:T(8,128)(2,1)S(1)}, bf16[4,24,2048]{2,1,0:T(8,128)(2,1)S(1)}, u32[]{:S(2)}, u32[]{:S(2)}) collective-permute-start(bf16[4,24,2048]{2,1,0:T(8,128)(2,1)S(1)} %fusion.2), channel_id=1, source_target_pairs={{0,1},{1,0},{2,3},{3,2},{4,5},{5,4},{6,7},{7,6},{8,9},{9,8},{10,11... | collective-permute-start | bytes 1179656 | tf_op jit(solution)/shard_map/ppermute | solution.py:207
  158.8 1.3 collective-permute-done.12
  160.1 0.1 fusion
  160.3 11.0 %all_to_all.16 = bf16[4,24,2048]{2,1,0:T(8,128)(2,1)S(1)} all-to-all(bf16[4,24,2048]{2,1,0:T(8,128)(2,1)S(1)} %fusion), channel_id=1, replica_groups=mesh['z'=16,'y'=4,'x'=4,'c'=2] {'x'}, dimensions={0} | all-to-all | bytes 786432 | tf_op jit(solution)/shard_map/all_to_all | solution.py:209
  171.3 0.1 reduce_sum.85
  171.3 0.7 fusion.13
  (19 shorter events, 0.2 us)
Async XLA Ops:
  6.5 98.9 %copy-start = (bf16[128,2048]{1,0:T(8,128)(2,1)S(1)}, bf16[128,2048]{1,0:T(8,128)(2,1)}, u32[]{:S(2)}) copy-start(bf16[128,2048]{1,0:T(8,128)(2,1)} %param.19) | copy-start | bytes 1572868
  6.5 142.1 %all-gather.2.cloned.1.call-start = ((), (), s32[]{:S(2)}) async-start(), calls=%async_computation.3 | async-start | bytes 9191424 | tf_op jit(solution)/shard_map/all_gather | solution.py:244
  7.6 12.4 %copy-start.5 = (bf16[192,128]{1,0:T(8,128)(2,1)S(1)}, bf16[192,128]{1,0:T(8,128)(2,1)}, u32[]{:S(2)}) copy-start(bf16[192,128]{1,0:T(8,128)(2,1)} %param.15) | copy-start | bytes 147460
  7.6 12.4 %copy-start.6 = (bf16[192,128]{1,0:T(8,128)(2,1)S(1)}, bf16[192,128]{1,0:T(8,128)(2,1)}, u32[]{:S(2)}) copy-start(bf16[192,128]{1,0:T(8,128)(2,1)} %param.16) | copy-start | bytes 147460
  19.0 51.0 %copy-start.3 = (bf16[192,128]{1,0:T(8,128)(2,1)S(1)}, bf16[192,128]{1,0:T(8,128)(2,1)}, u32[]{:S(2)}) copy-start(bf16[192,128]{1,0:T(8,128)(2,1)} %refs_0_.1) | copy-start | bytes 147460
  20.0 17.5 %collective-permute-start.3 = (bf16[192,256]{1,0:T(8,128)(2,1)S(1)}, bf16[192,256]{1,0:T(8,128)(2,1)S(1)}, u32[]{:S(2)}, u32[]{:S(2)}) collective-permute-start(bf16[192,256]{1,0:T(8,128)(2,1)S(1)} %constant_dynamic-update-slice_fusion), channel_id=1, source_target_pairs={{352,0},{384,32},{0,160},{32,192},{64,224},{96,256},{128,288},{160... | collective-permute-start | bytes 294920 | tf_op jit(solution)/shard_map/ppermute | solution.py:29
  31.6 11.9 %collective-permute-start.4 = (bf16[192,256]{1,0:T(8,128)(2,1)S(1)}, bf16[192,256]{1,0:T(8,128)(2,1)S(1)}, u32[]{:S(2)}, u32[]{:S(2)}) collective-permute-start(bf16[192,256]{1,0:T(8,128)(2,1)S(1)} %constant_dynamic-update-slice_fusion), channel_id=1, source_target_pairs={{160,0},{192,32},{0,352},{32,384},{64,416},{96,448},{128,480},{161... | collective-permute-start | bytes 294920 | tf_op jit(solution)/shard_map/ppermute | solution.py:29
  43.5 12.7 %collective-permute-start.5 = (bf16[576,256]{1,0:T(8,128)(2,1)S(1)}, bf16[576,256]{1,0:T(8,128)(2,1)S(1)}, u32[]{:S(2)}, u32[]{:S(2)}) collective-permute-start(bf16[576,256]{1,0:T(8,128)(2,1)S(1)} %pad_maximum_fusion.refs_4_), channel_id=1, source_target_pairs={{0,32},{32,64},{64,96},{96,128},{128,160},{160,192},{192,224},{224... | collective-permute-start | bytes 884744 | tf_op jit(solution)/shard_map/ppermute | solution.py:29
  45.5 16.9 %collective-permute-start.6 = (bf16[576,256]{1,0:T(8,128)(2,1)S(1)}, bf16[576,256]{1,0:T(8,128)(2,1)S(1)}, u32[]{:S(2)}, u32[]{:S(2)}) collective-permute-start(bf16[576,256]{1,0:T(8,128)(2,1)S(1)} %pad_maximum_fusion.refs_4_), channel_id=1, source_target_pairs={{32,0},{160,128},{192,160},{224,192},{256,224},{288,256},{320,288}... | collective-permute-start | bytes 884744 | tf_op jit(solution)/shard_map/ppermute | solution.py:29
  56.2 22.9 %collective-permute-start.7 = (bf16[576,256]{1,0:T(8,128)(2,1)S(1)}, bf16[576,256]{1,0:T(8,128)(2,1)S(1)}, u32[]{:S(2)}, u32[]{:S(2)}) collective-permute-start(bf16[576,256]{1,0:T(8,128)(2,1)S(1)} %collective-permute-done.5.refs_5_), channel_id=1, source_target_pairs={{32,64},{64,96},{96,128},{128,160},{160,192},{192,224},{224,256},{... | collective-permute-start | bytes 884744 | tf_op jit(solution)/shard_map/ppermute | solution.py:29
  62.4 20.0 %collective-permute-start.8 = (bf16[576,256]{1,0:T(8,128)(2,1)S(1)}, bf16[576,256]{1,0:T(8,128)(2,1)S(1)}, u32[]{:S(2)}, u32[]{:S(2)}) collective-permute-start(bf16[576,256]{1,0:T(8,128)(2,1)S(1)} %collective-permute-done.6.refs_6_), channel_id=1, source_target_pairs={{128,96},{160,128},{192,160},{224,192},{256,224},{288,256},{320,28... | collective-permute-start | bytes 884744 | tf_op jit(solution)/shard_map/ppermute | solution.py:29
  70.0 10.4 %collective-permute-start = (bf16[192,128]{1,0:T(8,128)(2,1)S(1)}, bf16[192,128]{1,0:T(8,128)(2,1)S(1)}, u32[]{:S(2)}, u32[]{:S(2)}) collective-permute-start(bf16[192,128]{1,0:T(8,128)(2,1)S(1)} %copy-done.3), channel_id=1, source_target_pairs={{24,0},{0,8},{8,16},{16,24},{25,1},{1,9},{9,17},{17,25},{26,2},{2,... | collective-permute-start | bytes 147464 | tf_op jit(solution)/shard_map/ppermute | solution.py:254
  71.9 8.5 %collective-permute-start.1 = (bf16[192,128]{1,0:T(8,128)(2,1)S(1)}, bf16[192,128]{1,0:T(8,128)(2,1)S(1)}, u32[]{:S(2)}, u32[]{:S(2)}) collective-permute-start(bf16[192,128]{1,0:T(8,128)(2,1)S(1)} %copy-done.3), channel_id=1, source_target_pairs={{16,0},{24,8},{0,16},{8,24},{17,1},{25,9},{1,17},{9,25},{18,2},{26... | collective-permute-start | bytes 147464 | tf_op jit(solution)/shard_map/ppermute | solution.py:254
  75.1 5.7 %collective-permute-start.2 = (bf16[192,128]{1,0:T(8,128)(2,1)S(1)}, bf16[192,128]{1,0:T(8,128)(2,1)S(1)}, u32[]{:S(2)}, u32[]{:S(2)}) collective-permute-start(bf16[192,128]{1,0:T(8,128)(2,1)S(1)} %copy-done.3), channel_id=1, source_target_pairs={{8,0},{16,8},{24,16},{0,24},{9,1},{17,9},{25,17},{1,25},{10,2},{18... | collective-permute-start | bytes 147464 | tf_op jit(solution)/shard_map/ppermute | solution.py:254
  79.1 3.3 %collective-permute-start.9 = (bf16[192,256]{1,0:T(8,128)(2,1)S(1)}, bf16[192,256]{1,0:T(8,128)(2,1)S(1)}, u32[]{:S(2)}, u32[]{:S(2)}) collective-permute-start(bf16[192,256]{1,0:T(8,128)(2,1)S(1)} %slice.68), channel_id=1, source_target_pairs={{224,256},{256,288},{288,320},{320,352},{352,384},{384,416},{416,4... | collective-permute-start | bytes 294920 | tf_op jit(solution)/shard_map/ppermute | solution.py:29
  92.7 10.8 %all-to-all-start = ((bf16[4,192,384]{2,1,0:T(8,128)(2,1)}), bf16[4,192,384]{2,1,0:T(8,128)(2,1)S(1)}, u32[]{:S(2)}, u32[]{:S(2)}) async-start(bf16[4,192,384]{2,1,0:T(8,128)(2,1)} %bitcast.2), calls=%async_computation | async-start | bytes 1179648 | tf_op jit(solution)/shard_map/all_to_all | solution.py:275
  104.3 1.1 copy-start.8
  106.0 18.5 %copy-start.4 = (bf16[24,2048]{1,0:T(8,128)(2,1)S(1)}, bf16[24,2048]{1,0:T(8,128)(2,1)}, u32[]{:S(2)}) copy-start(bf16[24,2048]{1,0:T(8,128)(2,1)} %param.13) | copy-start | bytes 294916
  106.0 18.6 %copy-start.7 = (f32[2048]{0:T(1024)S(1)}, f32[2048]{0:T(1024)}, u32[]{:S(2)}) copy-start(f32[2048]{0:T(1024)} %param.20) | copy-start | bytes 24580
  106.0 7.1 %collective-permute-start.10 = (bf16[4,24,2048]{2,1,0:T(8,128)(2,1)S(1)}, bf16[4,24,2048]{2,1,0:T(8,128)(2,1)S(1)}, u32[]{:S(2)}, u32[]{:S(2)}) collective-permute-start(bf16[4,24,2048]{2,1,0:T(8,128)(2,1)S(1)} %select_bitcast_fusion), channel_id=1, source_target_pairs={{0,1},{1,0},{2,3},{3,2},{4,5},{5,4},{6,7},{7,6},{8,9},{9,8},{10,11... | collective-permute-start | bytes 1179656 | tf_op jit(solution)/shard_map/ppermute | solution.py:207
  139.7 1.0 copy-start.1
  140.7 3.2 %collective-permute-start.11 = (bf16[8,2048]{1,0:T(8,128)(2,1)S(1)}, bf16[8,2048]{1,0:T(8,128)(2,1)S(1)}, u32[]{:S(2)}, u32[]{:S(2)}) collective-permute-start(bf16[8,2048]{1,0:T(8,128)(2,1)S(1)} %slice.79), channel_id=1, source_target_pairs={{0,8},{8,16},{16,24},{24,32},{32,40},{40,48},{48,56},{56,64},{64,7... | collective-permute-start | bytes 98312 | tf_op jit(solution)/shard_map/ppermute | solution.py:286
  148.6 1.1 copy-start.2
  155.6 4.5 %collective-permute-start.12 = (bf16[4,24,2048]{2,1,0:T(8,128)(2,1)S(1)}, bf16[4,24,2048]{2,1,0:T(8,128)(2,1)S(1)}, u32[]{:S(2)}, u32[]{:S(2)}) collective-permute-start(bf16[4,24,2048]{2,1,0:T(8,128)(2,1)S(1)} %fusion.2), channel_id=1, source_target_pairs={{0,1},{1,0},{2,3},{3,2},{4,5},{5,4},{6,7},{7,6},{8,9},{9,8},{10,11... | collective-permute-start | bytes 1179656 | tf_op jit(solution)/shard_map/ppermute | solution.py:207
Sparse Core Ops, SparseCore 0:
  20.1 128.4 all-gather.1

commit v13 on v12

--- a/solution.py
+++ b/solution.py
@@ -300,8 +300,9 @@
             pltpu.VMEM((all_w.shape[0], deep // 2, LANES), jnp.bfloat16),
             pltpu.SemaphoreType.DMA((width // LANES + 1,)),
         ],
+        compiler_params=pltpu.CompilerParams(vmem_limit_bytes=40 * 2**20),
         name="ffn",
-    )(*in_vmem, all_w, conv_weight, conv_bias)
+    )(*in_vmem, pltpu.with_memory_space_constraint(all_w, pltpu.HBM), conv_weight, conv_bias)
     ffn_out = summed_over_tp(ffn)
     return (mid.astype(jnp.float32) + ffn_out.astype(jnp.float32)).astype(jnp.bfloat16)
 

time: 181 us -> 179 us (0.989)
  local copies, waits for them, and re-layouts: 3.38 us -> 1.29 us
    unnamed x21, local copies, waits for them, and re-layouts: 2.34 us -> 0.25 us
where the time goes in v13:
time: 179 us; the launch traced here: 177 us
  starting transfers between devices  56.6 us (32%)
  blocking collectives  48.5 us (27%)
  waiting for transfers between devices  35.7 us (20%)
  Pallas kernels  16.3 us (9%)
  between operations  14.4 us (8%)
  other arithmetic  3.72 us (2%)
    ppermute x7, starting transfers between devices, shifted(): return lax.ppermute(value, 'z', [((i - steps) % count, i) for i in targets])  33 us
    all_to_all x2, blocking collectives, summed_over_tp(): tiles = lax.all_to_all(both, 'x', 0, 0, tiled=True)  22.1 us
    ppermute x7, waiting for transfers between devices, shifted(): return lax.ppermute(value, 'z', [((i - steps) % count, i) for i in targets])  19.2 us
    all_gather x1, blocking collectives, local(): lax.all_gather(normalize(mid, norm_gain), TP, axis=0, tiled=True)  15 us
    all_gather x1, blocking collectives, local(): lax.all_gather(jnp.concatenate(cuts, axis=1), 'y', axis=0, tiled=True)  11.4 us
    pallas_call x1, Pallas kernels, local(): pl.pallas_call(attend_kernel, out_shape=pltpu.VMEM((NY * rows, 3 * VD), j...  10.3 us
    ppermute x3, starting transfers between devices, local(): query_blocks.append(lax.ppermute(queries, 'y', pairs))  9.09 us
    ppermute x2, starting transfers between devices, summed_over_tp(): from_peer = lax.ppermute(for_peer, 'c', [(0, 1), (1, 0)])  8.92 us
  transfers between devices with their start and end apart: 15, of which 11 were waited for; matrix products, arithmetic and copies ran while one was open for 2% of the time, Pallas kernels for 6%

profile of v13, /device:TPU:1, one launch (start us, length us, event | category | flops | bytes accessed | tf_op | source)
XLA Modules:
  0.0 177.0 jit_solution(6217349067637838980)
XLA Ops:
  6.5 1.0 concatenate.11
  7.6 0.0 copy-start.5
  7.6 0.0 copy-start.6
  7.6 11.4 %all_gather.10.rows_ref = bf16[128,2176]{1,0:T(8,128)(2,1)S(1)} all-gather(bf16[32,2176]{1,0:T(8,128)(2,1)S(1)} %concatenate.11), channel_id=1, replica_groups=mesh['z'=16,'y'=4,'x'=4,'c'=2] {'y'}, dimensions={0}, use_global_device_ids=true | all-gather | bytes 696320 | tf_op jit(solution)/shard_map/all_gather | solution.py:235
  19.0 0.9 fold.1
  19.9 0.0 all-gather.2.cloned.1.call-update
  20.0 0.0 copy-done.5
  20.0 0.0 copy-done.6
  20.0 11.5 %collective-permute-start.3 = (bf16[192,256]{1,0:T(8,128)(2,1)S(1)}, bf16[192,256]{1,0:T(8,128)(2,1)S(1)}, u32[]{:S(2)}, u32[]{:S(2)}) collective-permute-start(bf16[192,256]{1,0:T(8,128)(2,1)S(1)} %constant_dynamic-update-slice_fusion), channel_id=1, source_target_pairs={{352,0},{384,32},{0,160},{32,192},{64,224},{96,256},{128,288},{160... | collective-permute-start | bytes 294920 | tf_op jit(solution)/shard_map/ppermute | solution.py:29
  31.6 5.9 %collective-permute-start.4 = (bf16[192,256]{1,0:T(8,128)(2,1)S(1)}, bf16[192,256]{1,0:T(8,128)(2,1)S(1)}, u32[]{:S(2)}, u32[]{:S(2)}) collective-permute-start(bf16[192,256]{1,0:T(8,128)(2,1)S(1)} %constant_dynamic-update-slice_fusion), channel_id=1, source_target_pairs={{160,0},{192,32},{0,352},{32,384},{64,416},{96,448},{128,480},{161... | collective-permute-start | bytes 294920 | tf_op jit(solution)/shard_map/ppermute | solution.py:29
  37.4 0.1 collective-permute-done.3
  37.5 5.9 %collective-permute-done.4 = bf16[192,256]{1,0:T(8,128)(2,1)S(1)} collective-permute-done((bf16[192,256]{1,0:T(8,128)(2,1)S(1)}, bf16[192,256]{1,0:T(8,128)(2,1)S(1)}, u32[]{:S(2)}, u32[]{:S(2)}) %collective-permute-start.4) | collective-permute-done | bytes 98336 | tf_op jit(solution)/shard_map/ppermute | solution.py:29
  43.5 2.0 %collective-permute-start.5 = (bf16[576,256]{1,0:T(8,128)(2,1)S(1)}, bf16[576,256]{1,0:T(8,128)(2,1)S(1)}, u32[]{:S(2)}, u32[]{:S(2)}) collective-permute-start(bf16[576,256]{1,0:T(8,128)(2,1)S(1)} %pad_maximum_fusion.refs_4_), channel_id=1, source_target_pairs={{0,32},{32,64},{64,96},{96,128},{128,160},{160,192},{192,224},{224... | collective-permute-start | bytes 884744 | tf_op jit(solution)/shard_map/ppermute | solution.py:29
  45.5 4.6 %collective-permute-start.6 = (bf16[576,256]{1,0:T(8,128)(2,1)S(1)}, bf16[576,256]{1,0:T(8,128)(2,1)S(1)}, u32[]{:S(2)}, u32[]{:S(2)}) collective-permute-start(bf16[576,256]{1,0:T(8,128)(2,1)S(1)} %pad_maximum_fusion.refs_4_), channel_id=1, source_target_pairs={{32,0},{160,128},{192,160},{224,192},{256,224},{288,256},{320,288}... | collective-permute-start | bytes 884744 | tf_op jit(solution)/shard_map/ppermute | solution.py:29
  50.2 6.0 %collective-permute-done.5.refs_5_ = bf16[576,256]{1,0:T(8,128)(2,1)S(1)} collective-permute-done((bf16[576,256]{1,0:T(8,128)(2,1)S(1)}, bf16[576,256]{1,0:T(8,128)(2,1)S(1)}, u32[]{:S(2)}, u32[]{:S(2)}) %collective-permute-start.5) | collective-permute-done | bytes 294944 | tf_op jit(solution)/shard_map/ppermute | solution.py:29
  56.2 0.7 collective-permute-start.7
  56.9 5.5 %collective-permute-done.6.refs_6_ = bf16[576,256]{1,0:T(8,128)(2,1)S(1)} collective-permute-done((bf16[576,256]{1,0:T(8,128)(2,1)S(1)}, bf16[576,256]{1,0:T(8,128)(2,1)S(1)}, u32[]{:S(2)}, u32[]{:S(2)}) %collective-permute-start.6) | collective-permute-done | bytes 294944 | tf_op jit(solution)/shard_map/ppermute | solution.py:29
  62.4 7.6 %collective-permute-start.8 = (bf16[576,256]{1,0:T(8,128)(2,1)S(1)}, bf16[576,256]{1,0:T(8,128)(2,1)S(1)}, u32[]{:S(2)}, u32[]{:S(2)}) collective-permute-start(bf16[576,256]{1,0:T(8,128)(2,1)S(1)} %collective-permute-done.6.refs_6_), channel_id=1, source_target_pairs={{128,96},{160,128},{192,160},{224,192},{256,224},{288,256},{320,28... | collective-permute-start | bytes 884744 | tf_op jit(solution)/shard_map/ppermute | solution.py:29
  70.0 1.9 %collective-permute-start = (bf16[192,128]{1,0:T(8,128)(2,1)S(1)}, bf16[192,128]{1,0:T(8,128)(2,1)S(1)}, u32[]{:S(2)}, u32[]{:S(2)}) collective-permute-start(bf16[192,128]{1,0:T(8,128)(2,1)S(1)} %copy-done.1), channel_id=1, source_target_pairs={{24,0},{0,8},{8,16},{16,24},{25,1},{1,9},{9,17},{17,25},{26,2},{2,... | collective-permute-start | bytes 147464 | tf_op jit(solution)/shard_map/ppermute | solution.py:254
  71.9 3.2 %collective-permute-start.1 = (bf16[192,128]{1,0:T(8,128)(2,1)S(1)}, bf16[192,128]{1,0:T(8,128)(2,1)S(1)}, u32[]{:S(2)}, u32[]{:S(2)}) collective-permute-start(bf16[192,128]{1,0:T(8,128)(2,1)S(1)} %copy-done.1), channel_id=1, source_target_pairs={{16,0},{24,8},{0,16},{8,24},{17,1},{25,9},{1,17},{9,25},{18,2},{26... | collective-permute-start | bytes 147464 | tf_op jit(solution)/shard_map/ppermute | solution.py:254
  75.1 4.0 %collective-permute-start.2 = (bf16[192,128]{1,0:T(8,128)(2,1)S(1)}, bf16[192,128]{1,0:T(8,128)(2,1)S(1)}, u32[]{:S(2)}, u32[]{:S(2)}) collective-permute-start(bf16[192,128]{1,0:T(8,128)(2,1)S(1)} %copy-done.1), channel_id=1, source_target_pairs={{8,0},{16,8},{24,16},{0,24},{9,1},{17,9},{25,17},{1,25},{10,2},{18... | collective-permute-start | bytes 147464 | tf_op jit(solution)/shard_map/ppermute | solution.py:254
  79.1 0.0 collective-permute-done.7.refs_7_
  79.1 0.7 collective-permute-start.9
  79.8 0.6 pad_add_fusion.where_ref
  80.4 0.0 collective-permute-done.refs_1_
  80.4 0.0 collective-permute-done.1.refs_2_
  80.4 0.4 collective-permute-done.2.refs_3_
  80.9 1.6 collective-permute-done.8.refs_8_
  82.5 0.0 collective-permute-done.9.refs_9_
  82.5 10.3 %attend.1 = bf16[768,384]{1,0:T(8,128)(2,1)} custom-call(s32[2]{0:T(128)} %pad_add_fusion.where_ref, bf16[192,128]{1,0:T(8,128)(2,1)S(1)} %copy-done.1, bf16[192,128]{1,0:T(8,128)(2,1)S(1)} %collective-permute-done.refs_1_, bf16[192,128]{1,0:T(8,128)(2,1)S(1)} %collective-permute-done.1.refs_2_, bf16[192,128]{1,0:T(8,128)(2,1)S(1)} %collective-permute-done.2.refs_3_, ...), custom_call_target="tpu_custom_call" | custom-call | tf_op jit(solution)/shard_map/attend/pallas_call | solution.py:264
  92.7 3.5 %all-to-all-start = ((bf16[4,192,384]{2,1,0:T(8,128)(2,1)}), bf16[4,192,384]{2,1,0:T(8,128)(2,1)S(1)}, u32[]{:S(2)}, u32[]{:S(2)}) async-start(bf16[4,192,384]{2,1,0:T(8,128)(2,1)} %bitcast.2), calls=%async_computation | async-start | bytes 1179648 | tf_op jit(solution)/shard_map/all_to_all | solution.py:275
  96.9 6.7 %all-to-all-done = bf16[4,192,384]{2,1,0:T(8,128)(2,1)S(1)} async-done(((bf16[4,192,384]{2,1,0:T(8,128)(2,1)}), bf16[4,192,384]{2,1,0:T(8,128)(2,1)S(1)}, u32[]{:S(2)}, u32[]{:S(2)}) %all-to-all-start) | async-done | bytes 589856 | tf_op jit(solution)/shard_map/all_to_all | solution.py:275
  103.5 0.1 convert_element_type.60
  103.6 0.7 fusion.18
  104.3 0.6 fusion.6
  104.9 0.3 fusion.4
  105.2 0.1 copy.35
  105.3 0.1 copy.36
  105.4 0.1 multiply_reduce_fusion
  105.5 0.5 convolution_convert_fusion
  106.0 0.0 copy-start.4
  106.0 0.0 copy-start.7
  106.0 5.8 %collective-permute-start.10 = (bf16[4,24,2048]{2,1,0:T(8,128)(2,1)S(1)}, bf16[4,24,2048]{2,1,0:T(8,128)(2,1)S(1)}, u32[]{:S(2)}, u32[]{:S(2)}) collective-permute-start(bf16[4,24,2048]{2,1,0:T(8,128)(2,1)S(1)} %select_bitcast_fusion), channel_id=1, source_target_pairs={{0,1},{1,0},{2,3},{3,2},{4,5},{5,4},{6,7},{7,6},{8,9},{9,8},{10,11... | collective-permute-start | bytes 1179656 | tf_op jit(solution)/shard_map/ppermute | solution.py:207
  111.8 1.3 collective-permute-done.10
  113.1 0.1 fusion.1
  113.3 0.0 copy-start.2
  113.3 0.0 copy-start.3
  113.3 11.1 %all_to_all.15 = bf16[4,24,2048]{2,1,0:T(8,128)(2,1)S(1)} all-to-all(bf16[4,24,2048]{2,1,0:T(8,128)(2,1)S(1)} %fusion.1), channel_id=1, replica_groups=mesh['z'=16,'y'=4,'x'=4,'c'=2] {'x'}, dimensions={0} | all-to-all | bytes 786432 | tf_op jit(solution)/shard_map/all_to_all | solution.py:209
  124.4 0.1 reduce_sum.83
  124.5 0.1 fusion.10
  124.6 0.0 copy-done.7
  124.6 0.1 fusion.12
  124.7 15.0 %all_gather.9.rows_ref = bf16[192,2048]{1,0:T(8,128)(2,1)S(1)} all-gather(bf16[24,2048]{1,0:T(8,128)(2,1)S(1)} %fusion.12), channel_id=1, replica_groups=mesh['z'=16,'y'=4,'x'=4,'c'=2] {'x','c'}, dimensions={0}, use_global_device_ids=true | all-gather | bytes 884736 | tf_op jit(solution)/shard_map/all_gather | solution.py:284
  139.7 2.2 %collective-permute-start.11 = (bf16[8,2048]{1,0:T(8,128)(2,1)S(1)}, bf16[8,2048]{1,0:T(8,128)(2,1)S(1)}, u32[]{:S(2)}, u32[]{:S(2)}) collective-permute-start(bf16[8,2048]{1,0:T(8,128)(2,1)S(1)} %slice.79), channel_id=1, source_target_pairs={{0,8},{8,16},{16,24},{24,32},{32,40},{40,48},{48,56},{56,64},{64,7... | collective-permute-start | bytes 98312 | tf_op jit(solution)/shard_map/ppermute | solution.py:286
  141.9 1.0 collective-permute-done.11.rim_ref
  142.9 5.7 %all-gather.2.cloned.1.call-done = bf16[33792,128]{1,0:T(8,128)(2,1)} async-done(((bf16[2112,128]{1,0:T(8,128)(2,1)}), bf16[33792,128]{1,0:T(8,128)(2,1)}) %all-gather.2.cloned.1.call-update) | async-done | bytes 8650768 | tf_op jit(solution)/shard_map/all_gather | solution.py:244
  148.6 0.0 copy-done.2
  148.6 5.1 %ffn.1 = bf16[192,2048]{1,0:T(8,128)(2,1)S(1)} custom-call(bf16[192,2048]{1,0:T(8,128)(2,1)S(1)} %all_gather.9.rows_ref, bf16[8,2048]{1,0:T(8,128)(2,1)S(1)} %collective-permute-done.11.rim_ref, bf16[16,2112,128]{2,1,0:T(8,128)(2,1)} %bitcast.50, f32[3,704]{1,0:T(4,128)S(1)} %copy-done.2, f32[704]{0:T(1024)S(1)} %copy-done.3), custom_call_target="tpu_custom_call" | custom-call | tf_op jit(solution)/shard_map/ffn/pallas_call | solution.py:291
  153.8 3.1 %collective-permute-start.12 = (bf16[4,24,2048]{2,1,0:T(8,128)(2,1)S(1)}, bf16[4,24,2048]{2,1,0:T(8,128)(2,1)S(1)}, u32[]{:S(2)}, u32[]{:S(2)}) collective-permute-start(bf16[4,24,2048]{2,1,0:T(8,128)(2,1)S(1)} %fusion.2), channel_id=1, source_target_pairs={{0,1},{1,0},{2,3},{3,2},{4,5},{5,4},{6,7},{7,6},{8,9},{9,8},{10,11... | collective-permute-start | bytes 1179656 | tf_op jit(solution)/shard_map/ppermute | solution.py:207
  157.0 1.3 collective-permute-done.12
  158.3 0.1 fusion
  158.4 11.0 %all_to_all.16 = bf16[4,24,2048]{2,1,0:T(8,128)(2,1)S(1)} all-to-all(bf16[4,24,2048]{2,1,0:T(8,128)(2,1)S(1)} %fusion), channel_id=1, replica_groups=mesh['z'=16,'y'=4,'x'=4,'c'=2] {'x'}, dimensions={0} | all-to-all | bytes 786432 | tf_op jit(solution)/shard_map/all_to_all | solution.py:209
  169.5 0.1 reduce_sum.85
  169.5 0.7 fusion.13
  (19 shorter events, 0.2 us)
Async XLA Ops:
  6.5 98.9 %copy-start = (bf16[128,2048]{1,0:T(8,128)(2,1)S(1)}, bf16[128,2048]{1,0:T(8,128)(2,1)}, u32[]{:S(2)}) copy-start(bf16[128,2048]{1,0:T(8,128)(2,1)} %param.19) | copy-start | bytes 1572868
  6.5 142.1 %all-gather.2.cloned.1.call-start = ((), (), s32[]{:S(2)}) async-start(), calls=%async_computation.3 | async-start | bytes 9191424 | tf_op jit(solution)/shard_map/all_gather | solution.py:244
  7.6 12.4 %copy-start.5 = (bf16[192,128]{1,0:T(8,128)(2,1)S(1)}, bf16[192,128]{1,0:T(8,128)(2,1)}, u32[]{:S(2)}) copy-start(bf16[192,128]{1,0:T(8,128)(2,1)} %param.15) | copy-start | bytes 147460
  7.6 12.4 %copy-start.6 = (bf16[192,128]{1,0:T(8,128)(2,1)S(1)}, bf16[192,128]{1,0:T(8,128)(2,1)}, u32[]{:S(2)}) copy-start(bf16[192,128]{1,0:T(8,128)(2,1)} %param.16) | copy-start | bytes 147460
  19.0 51.0 %copy-start.1 = (bf16[192,128]{1,0:T(8,128)(2,1)S(1)}, bf16[192,128]{1,0:T(8,128)(2,1)}, u32[]{:S(2)}) copy-start(bf16[192,128]{1,0:T(8,128)(2,1)} %refs_0_.1) | copy-start | bytes 147460
  20.0 17.5 %collective-permute-start.3 = (bf16[192,256]{1,0:T(8,128)(2,1)S(1)}, bf16[192,256]{1,0:T(8,128)(2,1)S(1)}, u32[]{:S(2)}, u32[]{:S(2)}) collective-permute-start(bf16[192,256]{1,0:T(8,128)(2,1)S(1)} %constant_dynamic-update-slice_fusion), channel_id=1, source_target_pairs={{352,0},{384,32},{0,160},{32,192},{64,224},{96,256},{128,288},{160... | collective-permute-start | bytes 294920 | tf_op jit(solution)/shard_map/ppermute | solution.py:29
  31.6 11.9 %collective-permute-start.4 = (bf16[192,256]{1,0:T(8,128)(2,1)S(1)}, bf16[192,256]{1,0:T(8,128)(2,1)S(1)}, u32[]{:S(2)}, u32[]{:S(2)}) collective-permute-start(bf16[192,256]{1,0:T(8,128)(2,1)S(1)} %constant_dynamic-update-slice_fusion), channel_id=1, source_target_pairs={{160,0},{192,32},{0,352},{32,384},{64,416},{96,448},{128,480},{161... | collective-permute-start | bytes 294920 | tf_op jit(solution)/shard_map/ppermute | solution.py:29
  43.5 12.7 %collective-permute-start.5 = (bf16[576,256]{1,0:T(8,128)(2,1)S(1)}, bf16[576,256]{1,0:T(8,128)(2,1)S(1)}, u32[]{:S(2)}, u32[]{:S(2)}) collective-permute-start(bf16[576,256]{1,0:T(8,128)(2,1)S(1)} %pad_maximum_fusion.refs_4_), channel_id=1, source_target_pairs={{0,32},{32,64},{64,96},{96,128},{128,160},{160,192},{192,224},{224... | collective-permute-start | bytes 884744 | tf_op jit(solution)/shard_map/ppermute | solution.py:29
  45.5 16.9 %collective-permute-start.6 = (bf16[576,256]{1,0:T(8,128)(2,1)S(1)}, bf16[576,256]{1,0:T(8,128)(2,1)S(1)}, u32[]{:S(2)}, u32[]{:S(2)}) collective-permute-start(bf16[576,256]{1,0:T(8,128)(2,1)S(1)} %pad_maximum_fusion.refs_4_), channel_id=1, source_target_pairs={{32,0},{160,128},{192,160},{224,192},{256,224},{288,256},{320,288}... | collective-permute-start | bytes 884744 | tf_op jit(solution)/shard_map/ppermute | solution.py:29
  56.2 22.9 %collective-permute-start.7 = (bf16[576,256]{1,0:T(8,128)(2,1)S(1)}, bf16[576,256]{1,0:T(8,128)(2,1)S(1)}, u32[]{:S(2)}, u32[]{:S(2)}) collective-permute-start(bf16[576,256]{1,0:T(8,128)(2,1)S(1)} %collective-permute-done.5.refs_5_), channel_id=1, source_target_pairs={{32,64},{64,96},{96,128},{128,160},{160,192},{192,224},{224,256},{... | collective-permute-start | bytes 884744 | tf_op jit(solution)/shard_map/ppermute | solution.py:29
  62.4 20.0 %collective-permute-start.8 = (bf16[576,256]{1,0:T(8,128)(2,1)S(1)}, bf16[576,256]{1,0:T(8,128)(2,1)S(1)}, u32[]{:S(2)}, u32[]{:S(2)}) collective-permute-start(bf16[576,256]{1,0:T(8,128)(2,1)S(1)} %collective-permute-done.6.refs_6_), channel_id=1, source_target_pairs={{128,96},{160,128},{192,160},{224,192},{256,224},{288,256},{320,28... | collective-permute-start | bytes 884744 | tf_op jit(solution)/shard_map/ppermute | solution.py:29
  70.0 10.4 %collective-permute-start = (bf16[192,128]{1,0:T(8,128)(2,1)S(1)}, bf16[192,128]{1,0:T(8,128)(2,1)S(1)}, u32[]{:S(2)}, u32[]{:S(2)}) collective-permute-start(bf16[192,128]{1,0:T(8,128)(2,1)S(1)} %copy-done.1), channel_id=1, source_target_pairs={{24,0},{0,8},{8,16},{16,24},{25,1},{1,9},{9,17},{17,25},{26,2},{2,... | collective-permute-start | bytes 147464 | tf_op jit(solution)/shard_map/ppermute | solution.py:254
  71.9 8.5 %collective-permute-start.1 = (bf16[192,128]{1,0:T(8,128)(2,1)S(1)}, bf16[192,128]{1,0:T(8,128)(2,1)S(1)}, u32[]{:S(2)}, u32[]{:S(2)}) collective-permute-start(bf16[192,128]{1,0:T(8,128)(2,1)S(1)} %copy-done.1), channel_id=1, source_target_pairs={{16,0},{24,8},{0,16},{8,24},{17,1},{25,9},{1,17},{9,25},{18,2},{26... | collective-permute-start | bytes 147464 | tf_op jit(solution)/shard_map/ppermute | solution.py:254
  75.1 5.7 %collective-permute-start.2 = (bf16[192,128]{1,0:T(8,128)(2,1)S(1)}, bf16[192,128]{1,0:T(8,128)(2,1)S(1)}, u32[]{:S(2)}, u32[]{:S(2)}) collective-permute-start(bf16[192,128]{1,0:T(8,128)(2,1)S(1)} %copy-done.1), channel_id=1, source_target_pairs={{8,0},{16,8},{24,16},{0,24},{9,1},{17,9},{25,17},{1,25},{10,2},{18... | collective-permute-start | bytes 147464 | tf_op jit(solution)/shard_map/ppermute | solution.py:254
  79.1 3.3 %collective-permute-start.9 = (bf16[192,256]{1,0:T(8,128)(2,1)S(1)}, bf16[192,256]{1,0:T(8,128)(2,1)S(1)}, u32[]{:S(2)}, u32[]{:S(2)}) collective-permute-start(bf16[192,256]{1,0:T(8,128)(2,1)S(1)} %slice.68), channel_id=1, source_target_pairs={{224,256},{256,288},{288,320},{320,352},{352,384},{384,416},{416,4... | collective-permute-start | bytes 294920 | tf_op jit(solution)/shard_map/ppermute | solution.py:29
  92.7 10.8 %all-to-all-start = ((bf16[4,192,384]{2,1,0:T(8,128)(2,1)}), bf16[4,192,384]{2,1,0:T(8,128)(2,1)S(1)}, u32[]{:S(2)}, u32[]{:S(2)}) async-start(bf16[4,192,384]{2,1,0:T(8,128)(2,1)} %bitcast.2), calls=%async_computation | async-start | bytes 1179648 | tf_op jit(solution)/shard_map/all_to_all | solution.py:275
  104.3 1.1 copy-start.8
  106.0 18.5 %copy-start.4 = (bf16[24,2048]{1,0:T(8,128)(2,1)S(1)}, bf16[24,2048]{1,0:T(8,128)(2,1)}, u32[]{:S(2)}) copy-start(bf16[24,2048]{1,0:T(8,128)(2,1)} %param.13) | copy-start | bytes 294916
  106.0 18.6 %copy-start.7 = (f32[2048]{0:T(1024)S(1)}, f32[2048]{0:T(1024)}, u32[]{:S(2)}) copy-start(f32[2048]{0:T(1024)} %param.20) | copy-start | bytes 24580
  106.0 7.1 %collective-permute-start.10 = (bf16[4,24,2048]{2,1,0:T(8,128)(2,1)S(1)}, bf16[4,24,2048]{2,1,0:T(8,128)(2,1)S(1)}, u32[]{:S(2)}, u32[]{:S(2)}) collective-permute-start(bf16[4,24,2048]{2,1,0:T(8,128)(2,1)S(1)} %select_bitcast_fusion), channel_id=1, source_target_pairs={{0,1},{1,0},{2,3},{3,2},{4,5},{5,4},{6,7},{7,6},{8,9},{9,8},{10,11... | collective-permute-start | bytes 1179656 | tf_op jit(solution)/shard_map/ppermute | solution.py:207
  113.3 35.3 %copy-start.2 = (f32[3,704]{1,0:T(4,128)S(1)}, f32[3,704]{1,0:T(4,128)}, u32[]{:S(2)}) copy-start(f32[3,704]{1,0:T(4,128)} %taps_ref.1) | copy-start | bytes 25348
  113.3 35.3 %copy-start.3 = (f32[704]{0:T(1024)S(1)}, f32[704]{0:T(1024)}, u32[]{:S(2)}) copy-start(f32[704]{0:T(1024)} %bias_ref.1) | copy-start | bytes 8452
  139.7 3.2 %collective-permute-start.11 = (bf16[8,2048]{1,0:T(8,128)(2,1)S(1)}, bf16[8,2048]{1,0:T(8,128)(2,1)S(1)}, u32[]{:S(2)}, u32[]{:S(2)}) collective-permute-start(bf16[8,2048]{1,0:T(8,128)(2,1)S(1)} %slice.79), channel_id=1, source_target_pairs={{0,8},{8,16},{16,24},{24,32},{32,40},{40,48},{48,56},{56,64},{64,7... | collective-permute-start | bytes 98312 | tf_op jit(solution)/shard_map/ppermute | solution.py:286
  153.8 4.5 %collective-permute-start.12 = (bf16[4,24,2048]{2,1,0:T(8,128)(2,1)S(1)}, bf16[4,24,2048]{2,1,0:T(8,128)(2,1)S(1)}, u32[]{:S(2)}, u32[]{:S(2)}) collective-permute-start(bf16[4,24,2048]{2,1,0:T(8,128)(2,1)S(1)} %fusion.2), channel_id=1, source_target_pairs={{0,1},{1,0},{2,3},{3,2},{4,5},{5,4},{6,7},{7,6},{8,9},{9,8},{10,11... | collective-permute-start | bytes 1179656 | tf_op jit(solution)/shard_map/ppermute | solution.py:207
Sparse Core Ops, SparseCore 0:
  20.1 128.4 all-gather.1

commit v14 on v13

--- a/solution.py
+++ b/solution.py
@@ -252,6 +252,7 @@
     for behind in range(1, NY):
         pairs = [((i - behind) % NY, i) for i in range(NY)]
         query_blocks.append(lax.ppermute(queries, "y", pairs))
+    f5, f11, query_blocks[1] = lax.optimization_barrier((f5, f11, query_blocks[1]))
     held = jnp.concatenate((kv, f5, f11), axis=0)
     n1 = shifted(held, 1, range(1, last))
     m1 = shifted(held, -1, [0, *range(4, last)])

time: 179 us -> 179 us (level)
  waiting for transfers between devices: 35.7 us -> 38.1 us
  starting transfers between devices: 56.6 us -> 54.3 us
    ppermute x3, waiting for transfers between devices: 0.45 us -> 6.41 us  [local(): query_blocks.append(lax.ppermute(queries, 'y', pairs))]
    ppermute x7, waiting for transfers between devices: 19.2 us -> 15.6 us  [shifted(): return lax.ppermute(value, 'z', [((i - steps) % count, i) for i in targets])]
    ppermute x3, starting transfers between devices: 9.09 us -> 7.05 us  [local(): query_blocks.append(lax.ppermute(queries, 'y', pairs))]
  transfers between devices with their start and end apart: 15 -> 15, of which waited for: 11 -> 10; matrix products, arithmetic and copies ran while one was open for 2% -> 2% of each run, Pallas kernels for 6% -> 6%
where the time goes in v14:
time: 179 us; the launch traced here: 177 us
  starting transfers between devices  54.3 us (30%)
  blocking collectives  48.5 us (27%)
  waiting for transfers between devices  38.1 us (21%)
  Pallas kernels  16.3 us (9%)
  between operations  14.4 us (8%)
  other arithmetic  3.72 us (2%)
    ppermute x7, starting transfers between devices, shifted(): return lax.ppermute(value, 'z', [((i - steps) % count, i) for i in targets])  32.6 us
    all_to_all x2, blocking collectives, summed_over_tp(): tiles = lax.all_to_all(both, 'x', 0, 0, tiled=True)  22.1 us
    ppermute x7, waiting for transfers between devices, shifted(): return lax.ppermute(value, 'z', [((i - steps) % count, i) for i in targets])  15.6 us
    all_gather x1, blocking collectives, local(): lax.all_gather(normalize(mid, norm_gain), TP, axis=0, tiled=True)  15 us
    all_gather x1, blocking collectives, local(): lax.all_gather(jnp.concatenate(cuts, axis=1), 'y', axis=0, tiled=True)  11.4 us
    pallas_call x1, Pallas kernels, local(): pl.pallas_call(attend_kernel, out_shape=pltpu.VMEM((NY * rows, 3 * VD), j...  10.2 us
    ppermute x2, starting transfers between devices, summed_over_tp(): from_peer = lax.ppermute(for_peer, 'c', [(0, 1), (1, 0)])  8.93 us
    ppermute x3, starting transfers between devices, local(): query_blocks.append(lax.ppermute(queries, 'y', pairs))  7.05 us
  transfers between devices with their start and end apart: 15, of which 10 were waited for; matrix products, arithmetic and copies ran while one was open for 2% of the time, Pallas kernels for 6%

profile of v14, /device:TPU:1, one launch (start us, length us, event | category | flops | bytes accessed | tf_op | source)
XLA Modules:
  0.0 177.1 jit_solution(15356960490129867573)
XLA Ops:
  6.5 1.0 concatenate.11
  7.6 0.0 copy-start.5
  7.6 0.0 copy-start.6
  7.6 0.0 copy-start.1
  7.6 11.4 %all_gather.10.rows_ref = bf16[128,2176]{1,0:T(8,128)(2,1)S(1)} all-gather(bf16[32,2176]{1,0:T(8,128)(2,1)S(1)} %concatenate.11), channel_id=1, replica_groups=mesh['z'=16,'y'=4,'x'=4,'c'=2] {'y'}, dimensions={0}, use_global_device_ids=true | all-gather | bytes 696320 | tf_op jit(solution)/shard_map/all_gather | solution.py:235
  19.0 0.9 fold.1
  19.9 0.0 all-gather.2.cloned.1.call-update
  20.0 0.0 copy-done.5
  20.0 0.0 copy-done.6
  20.0 11.5 %collective-permute-start = (bf16[192,256]{1,0:T(8,128)(2,1)S(1)}, bf16[192,256]{1,0:T(8,128)(2,1)S(1)}, u32[]{:S(2)}, u32[]{:S(2)}) collective-permute-start(bf16[192,256]{1,0:T(8,128)(2,1)S(1)} %constant_dynamic-update-slice_fusion), channel_id=1, source_target_pairs={{352,0},{384,32},{0,160},{32,192},{64,224},{96,256},{128,288},{160... | collective-permute-start | bytes 294920 | tf_op jit(solution)/shard_map/ppermute | solution.py:29
  31.6 5.9 %collective-permute-start.1 = (bf16[192,256]{1,0:T(8,128)(2,1)S(1)}, bf16[192,256]{1,0:T(8,128)(2,1)S(1)}, u32[]{:S(2)}, u32[]{:S(2)}) collective-permute-start(bf16[192,256]{1,0:T(8,128)(2,1)S(1)} %constant_dynamic-update-slice_fusion), channel_id=1, source_target_pairs={{160,0},{192,32},{0,352},{32,384},{64,416},{96,448},{128,480},{161... | collective-permute-start | bytes 294920 | tf_op jit(solution)/shard_map/ppermute | solution.py:29
  37.5 1.9 %collective-permute-start.2 = (bf16[192,128]{1,0:T(8,128)(2,1)S(1)}, bf16[192,128]{1,0:T(8,128)(2,1)S(1)}, u32[]{:S(2)}, u32[]{:S(2)}) collective-permute-start(bf16[192,128]{1,0:T(8,128)(2,1)S(1)} %copy-done.1), channel_id=1, source_target_pairs={{24,0},{0,8},{8,16},{16,24},{25,1},{1,9},{9,17},{17,25},{26,2},{2,... | collective-permute-start | bytes 147464 | tf_op jit(solution)/shard_map/ppermute | solution.py:254
  39.4 4.4 %collective-permute-done.2.refs_1_ = bf16[192,128]{1,0:T(8,128)(2,1)S(1)} collective-permute-done((bf16[192,128]{1,0:T(8,128)(2,1)S(1)}, bf16[192,128]{1,0:T(8,128)(2,1)S(1)}, u32[]{:S(2)}, u32[]{:S(2)}) %collective-permute-start.2) | collective-permute-done | bytes 49184 | tf_op jit(solution)/shard_map/ppermute | solution.py:254
  43.8 0.0 collective-permute-done
  43.8 0.0 collective-permute-done.1
  43.8 1.7 collective-permute-start.5
  45.5 4.6 %collective-permute-start.6 = (bf16[576,256]{1,0:T(8,128)(2,1)S(1)}, bf16[576,256]{1,0:T(8,128)(2,1)S(1)}, u32[]{:S(2)}, u32[]{:S(2)}) collective-permute-start(bf16[576,256]{1,0:T(8,128)(2,1)S(1)} %pad_maximum_fusion.refs_4_), channel_id=1, source_target_pairs={{32,0},{160,128},{192,160},{224,192},{256,224},{288,256},{320,288}... | collective-permute-start | bytes 884744 | tf_op jit(solution)/shard_map/ppermute | solution.py:29
  50.2 6.0 %collective-permute-done.5.refs_5_ = bf16[576,256]{1,0:T(8,128)(2,1)S(1)} collective-permute-done((bf16[576,256]{1,0:T(8,128)(2,1)S(1)}, bf16[576,256]{1,0:T(8,128)(2,1)S(1)}, u32[]{:S(2)}, u32[]{:S(2)}) %collective-permute-start.5) | collective-permute-done | bytes 294944 | tf_op jit(solution)/shard_map/ppermute | solution.py:29
  56.2 0.7 collective-permute-start.7
  56.9 5.5 %collective-permute-done.6.refs_6_ = bf16[576,256]{1,0:T(8,128)(2,1)S(1)} collective-permute-done((bf16[576,256]{1,0:T(8,128)(2,1)S(1)}, bf16[576,256]{1,0:T(8,128)(2,1)S(1)}, u32[]{:S(2)}, u32[]{:S(2)}) %collective-permute-start.6) | collective-permute-done | bytes 294944 | tf_op jit(solution)/shard_map/ppermute | solution.py:29
  62.4 7.6 %collective-permute-start.8 = (bf16[576,256]{1,0:T(8,128)(2,1)S(1)}, bf16[576,256]{1,0:T(8,128)(2,1)S(1)}, u32[]{:S(2)}, u32[]{:S(2)}) collective-permute-start(bf16[576,256]{1,0:T(8,128)(2,1)S(1)} %collective-permute-done.6.refs_6_), channel_id=1, source_target_pairs={{128,96},{160,128},{192,160},{224,192},{256,224},{288,256},{320,28... | collective-permute-start | bytes 884744 | tf_op jit(solution)/shard_map/ppermute | solution.py:29
  70.0 3.2 %collective-permute-start.3 = (bf16[192,128]{1,0:T(8,128)(2,1)S(1)}, bf16[192,128]{1,0:T(8,128)(2,1)S(1)}, u32[]{:S(2)}, u32[]{:S(2)}) collective-permute-start(bf16[192,128]{1,0:T(8,128)(2,1)S(1)} %copy-done.1), channel_id=1, source_target_pairs={{16,0},{24,8},{0,16},{8,24},{17,1},{25,9},{1,17},{9,25},{18,2},{26... | collective-permute-start | bytes 147464 | tf_op jit(solution)/shard_map/ppermute | solution.py:254
  73.2 1.9 %collective-permute-start.4 = (bf16[192,128]{1,0:T(8,128)(2,1)S(1)}, bf16[192,128]{1,0:T(8,128)(2,1)S(1)}, u32[]{:S(2)}, u32[]{:S(2)}) collective-permute-start(bf16[192,128]{1,0:T(8,128)(2,1)S(1)} %copy-done.1), channel_id=1, source_target_pairs={{8,0},{16,8},{24,16},{0,24},{9,1},{17,9},{25,17},{1,25},{10,2},{18... | collective-permute-start | bytes 147464 | tf_op jit(solution)/shard_map/ppermute | solution.py:254
  75.1 0.0 collective-permute-done.7.refs_7_
  75.2 0.7 collective-permute-start.9
  75.8 0.6 pad_add_fusion.where_ref
  76.4 0.0 collective-permute-done.3.refs_2_
  76.4 2.0 %collective-permute-done.4.refs_3_ = bf16[192,128]{1,0:T(8,128)(2,1)S(1)} collective-permute-done((bf16[192,128]{1,0:T(8,128)(2,1)S(1)}, bf16[192,128]{1,0:T(8,128)(2,1)S(1)}, u32[]{:S(2)}, u32[]{:S(2)}) %collective-permute-start.4) | collective-permute-done | bytes 49184 | tf_op jit(solution)/shard_map/ppermute | solution.py:254
  78.4 4.0 %collective-permute-done.8.refs_8_ = bf16[576,256]{1,0:T(8,128)(2,1)S(1)} collective-permute-done((bf16[576,256]{1,0:T(8,128)(2,1)S(1)}, bf16[576,256]{1,0:T(8,128)(2,1)S(1)}, u32[]{:S(2)}, u32[]{:S(2)}) %collective-permute-start.8) | collective-permute-done | bytes 294944 | tf_op jit(solution)/shard_map/ppermute | solution.py:29
  82.5 0.0 collective-permute-done.9.refs_9_
  82.5 10.2 %attend.1 = bf16[768,384]{1,0:T(8,128)(2,1)} custom-call(s32[2]{0:T(128)} %pad_add_fusion.where_ref, bf16[192,128]{1,0:T(8,128)(2,1)S(1)} %copy-done.1, bf16[192,128]{1,0:T(8,128)(2,1)S(1)} %collective-permute-done.2.refs_1_, bf16[192,128]{1,0:T(8,128)(2,1)S(1)} %collective-permute-done.3.refs_2_, bf16[192,128]{1,0:T(8,128)(2,1)S(1)} %collective-permute-done.4.refs_3_, ...), custom_call_target="tpu_custom_call" | custom-call | tf_op jit(solution)/shard_map/attend/pallas_call | solution.py:265
  92.7 3.5 %all-to-all-start = ((bf16[4,192,384]{2,1,0:T(8,128)(2,1)}), bf16[4,192,384]{2,1,0:T(8,128)(2,1)S(1)}, u32[]{:S(2)}, u32[]{:S(2)}) async-start(bf16[4,192,384]{2,1,0:T(8,128)(2,1)} %bitcast.2), calls=%async_computation | async-start | bytes 1179648 | tf_op jit(solution)/shard_map/all_to_all | solution.py:276
  96.8 6.7 %all-to-all-done = bf16[4,192,384]{2,1,0:T(8,128)(2,1)S(1)} async-done(((bf16[4,192,384]{2,1,0:T(8,128)(2,1)}), bf16[4,192,384]{2,1,0:T(8,128)(2,1)S(1)}, u32[]{:S(2)}, u32[]{:S(2)}) %all-to-all-start) | async-done | bytes 589856 | tf_op jit(solution)/shard_map/all_to_all | solution.py:276
  103.5 0.1 convert_element_type.60
  103.6 0.7 fusion.18
  104.3 0.6 fusion.6
  104.9 0.3 fusion.4
  105.2 0.1 copy.35
  105.3 0.1 copy.36
  105.4 0.1 multiply_reduce_fusion
  105.5 0.5 convolution_convert_fusion
  106.0 0.0 copy-start.4
  106.0 0.0 copy-start.7
  106.0 5.8 %collective-permute-start.10 = (bf16[4,24,2048]{2,1,0:T(8,128)(2,1)S(1)}, bf16[4,24,2048]{2,1,0:T(8,128)(2,1)S(1)}, u32[]{:S(2)}, u32[]{:S(2)}) collective-permute-start(bf16[4,24,2048]{2,1,0:T(8,128)(2,1)S(1)} %select_bitcast_fusion), channel_id=1, source_target_pairs={{0,1},{1,0},{2,3},{3,2},{4,5},{5,4},{6,7},{7,6},{8,9},{9,8},{10,11... | collective-permute-start | bytes 1179656 | tf_op jit(solution)/shard_map/ppermute | solution.py:207
  111.8 1.3 collective-permute-done.10
  113.1 0.1 fusion.1
  113.3 0.0 copy-start.2
  113.3 0.0 copy-start.3
  113.3 11.1 %all_to_all.15 = bf16[4,24,2048]{2,1,0:T(8,128)(2,1)S(1)} all-to-all(bf16[4,24,2048]{2,1,0:T(8,128)(2,1)S(1)} %fusion.1), channel_id=1, replica_groups=mesh['z'=16,'y'=4,'x'=4,'c'=2] {'x'}, dimensions={0} | all-to-all | bytes 786432 | tf_op jit(solution)/shard_map/all_to_all | solution.py:209
  124.4 0.1 reduce_sum.83
  124.5 0.0 copy-done.4
  124.5 0.1 fusion.10
  124.6 0.1 fusion.12
  124.7 15.0 %all_gather.9.rows_ref = bf16[192,2048]{1,0:T(8,128)(2,1)S(1)} all-gather(bf16[24,2048]{1,0:T(8,128)(2,1)S(1)} %fusion.12), channel_id=1, replica_groups=mesh['z'=16,'y'=4,'x'=4,'c'=2] {'x','c'}, dimensions={0}, use_global_device_ids=true | all-gather | bytes 884736 | tf_op jit(solution)/shard_map/all_gather | solution.py:285
  139.7 2.2 %collective-permute-start.11 = (bf16[8,2048]{1,0:T(8,128)(2,1)S(1)}, bf16[8,2048]{1,0:T(8,128)(2,1)S(1)}, u32[]{:S(2)}, u32[]{:S(2)}) collective-permute-start(bf16[8,2048]{1,0:T(8,128)(2,1)S(1)} %slice.79), channel_id=1, source_target_pairs={{0,8},{8,16},{16,24},{24,32},{32,40},{40,48},{48,56},{56,64},{64,7... | collective-permute-start | bytes 98312 | tf_op jit(solution)/shard_map/ppermute | solution.py:287
  141.9 1.0 collective-permute-done.11.rim_ref
  142.9 5.7 %all-gather.2.cloned.1.call-done = bf16[33792,128]{1,0:T(8,128)(2,1)} async-done(((bf16[2112,128]{1,0:T(8,128)(2,1)}), bf16[33792,128]{1,0:T(8,128)(2,1)}) %all-gather.2.cloned.1.call-update) | async-done | bytes 8650768 | tf_op jit(solution)/shard_map/all_gather | solution.py:244
  148.6 5.1 %ffn.1 = bf16[192,2048]{1,0:T(8,128)(2,1)S(1)} custom-call(bf16[192,2048]{1,0:T(8,128)(2,1)S(1)} %all_gather.9.rows_ref, bf16[8,2048]{1,0:T(8,128)(2,1)S(1)} %collective-permute-done.11.rim_ref, bf16[16,2112,128]{2,1,0:T(8,128)(2,1)} %bitcast.50, f32[3,704]{1,0:T(4,128)S(1)} %copy-done.2, f32[704]{0:T(1024)S(1)} %copy-done.3), custom_call_target="tpu_custom_call" | custom-call | tf_op jit(solution)/shard_map/ffn/pallas_call | solution.py:292
  153.8 3.1 %collective-permute-start.12 = (bf16[4,24,2048]{2,1,0:T(8,128)(2,1)S(1)}, bf16[4,24,2048]{2,1,0:T(8,128)(2,1)S(1)}, u32[]{:S(2)}, u32[]{:S(2)}) collective-permute-start(bf16[4,24,2048]{2,1,0:T(8,128)(2,1)S(1)} %fusion.2), channel_id=1, source_target_pairs={{0,1},{1,0},{2,3},{3,2},{4,5},{5,4},{6,7},{7,6},{8,9},{9,8},{10,11... | collective-permute-start | bytes 1179656 | tf_op jit(solution)/shard_map/ppermute | solution.py:207
  157.0 1.3 collective-permute-done.12
  158.3 0.1 fusion
  158.4 11.0 %all_to_all.16 = bf16[4,24,2048]{2,1,0:T(8,128)(2,1)S(1)} all-to-all(bf16[4,24,2048]{2,1,0:T(8,128)(2,1)S(1)} %fusion), channel_id=1, replica_groups=mesh['z'=16,'y'=4,'x'=4,'c'=2] {'x'}, dimensions={0} | all-to-all | bytes 786432 | tf_op jit(solution)/shard_map/all_to_all | solution.py:209
  169.5 0.1 reduce_sum.85
  169.5 0.7 fusion.13
  (19 shorter events, 0.2 us)
Async XLA Ops:
  6.5 98.9 %copy-start = (bf16[128,2048]{1,0:T(8,128)(2,1)S(1)}, bf16[128,2048]{1,0:T(8,128)(2,1)}, u32[]{:S(2)}) copy-start(bf16[128,2048]{1,0:T(8,128)(2,1)} %param.19) | copy-start | bytes 1572868
  6.5 142.1 %all-gather.2.cloned.1.call-start = ((), (), s32[]{:S(2)}) async-start(), calls=%async_computation.3 | async-start | bytes 9191424 | tf_op jit(solution)/shard_map/all_gather | solution.py:244
  7.6 12.4 %copy-start.5 = (bf16[192,128]{1,0:T(8,128)(2,1)S(1)}, bf16[192,128]{1,0:T(8,128)(2,1)}, u32[]{:S(2)}) copy-start(bf16[192,128]{1,0:T(8,128)(2,1)} %param.15) | copy-start | bytes 147460
  7.6 12.4 %copy-start.6 = (bf16[192,128]{1,0:T(8,128)(2,1)S(1)}, bf16[192,128]{1,0:T(8,128)(2,1)}, u32[]{:S(2)}) copy-start(bf16[192,128]{1,0:T(8,128)(2,1)} %param.16) | copy-start | bytes 147460
  7.6 29.9 %copy-start.1 = (bf16[192,128]{1,0:T(8,128)(2,1)S(1)}, bf16[192,128]{1,0:T(8,128)(2,1)}, u32[]{:S(2)}) copy-start(bf16[192,128]{1,0:T(8,128)(2,1)} %refs_0_.1) | copy-start | bytes 147460
  20.0 23.8 %collective-permute-start = (bf16[192,256]{1,0:T(8,128)(2,1)S(1)}, bf16[192,256]{1,0:T(8,128)(2,1)S(1)}, u32[]{:S(2)}, u32[]{:S(2)}) collective-permute-start(bf16[192,256]{1,0:T(8,128)(2,1)S(1)} %constant_dynamic-update-slice_fusion), channel_id=1, source_target_pairs={{352,0},{384,32},{0,160},{32,192},{64,224},{96,256},{128,288},{160... | collective-permute-start | bytes 294920 | tf_op jit(solution)/shard_map/ppermute | solution.py:29
  31.6 12.2 %collective-permute-start.1 = (bf16[192,256]{1,0:T(8,128)(2,1)S(1)}, bf16[192,256]{1,0:T(8,128)(2,1)S(1)}, u32[]{:S(2)}, u32[]{:S(2)}) collective-permute-start(bf16[192,256]{1,0:T(8,128)(2,1)S(1)} %constant_dynamic-update-slice_fusion), channel_id=1, source_target_pairs={{160,0},{192,32},{0,352},{32,384},{64,416},{96,448},{128,480},{161... | collective-permute-start | bytes 294920 | tf_op jit(solution)/shard_map/ppermute | solution.py:29
  37.5 6.3 %collective-permute-start.2 = (bf16[192,128]{1,0:T(8,128)(2,1)S(1)}, bf16[192,128]{1,0:T(8,128)(2,1)S(1)}, u32[]{:S(2)}, u32[]{:S(2)}) collective-permute-start(bf16[192,128]{1,0:T(8,128)(2,1)S(1)} %copy-done.1), channel_id=1, source_target_pairs={{24,0},{0,8},{8,16},{16,24},{25,1},{1,9},{9,17},{17,25},{26,2},{2,... | collective-permute-start | bytes 147464 | tf_op jit(solution)/shard_map/ppermute | solution.py:254
  43.8 12.4 %collective-permute-start.5 = (bf16[576,256]{1,0:T(8,128)(2,1)S(1)}, bf16[576,256]{1,0:T(8,128)(2,1)S(1)}, u32[]{:S(2)}, u32[]{:S(2)}) collective-permute-start(bf16[576,256]{1,0:T(8,128)(2,1)S(1)} %pad_maximum_fusion.refs_4_), channel_id=1, source_target_pairs={{0,32},{32,64},{64,96},{96,128},{128,160},{160,192},{192,224},{224... | collective-permute-start | bytes 884744 | tf_op jit(solution)/shard_map/ppermute | solution.py:29
  45.5 16.9 %collective-permute-start.6 = (bf16[576,256]{1,0:T(8,128)(2,1)S(1)}, bf16[576,256]{1,0:T(8,128)(2,1)S(1)}, u32[]{:S(2)}, u32[]{:S(2)}) collective-permute-start(bf16[576,256]{1,0:T(8,128)(2,1)S(1)} %pad_maximum_fusion.refs_4_), channel_id=1, source_target_pairs={{32,0},{160,128},{192,160},{224,192},{256,224},{288,256},{320,288}... | collective-permute-start | bytes 884744 | tf_op jit(solution)/shard_map/ppermute | solution.py:29
  56.2 18.9 %collective-permute-start.7 = (bf16[576,256]{1,0:T(8,128)(2,1)S(1)}, bf16[576,256]{1,0:T(8,128)(2,1)S(1)}, u32[]{:S(2)}, u32[]{:S(2)}) collective-permute-start(bf16[576,256]{1,0:T(8,128)(2,1)S(1)} %collective-permute-done.5.refs_5_), channel_id=1, source_target_pairs={{32,64},{64,96},{96,128},{128,160},{160,192},{192,224},{224,256},{... | collective-permute-start | bytes 884744 | tf_op jit(solution)/shard_map/ppermute | solution.py:29
  62.4 20.0 %collective-permute-start.8 = (bf16[576,256]{1,0:T(8,128)(2,1)S(1)}, bf16[576,256]{1,0:T(8,128)(2,1)S(1)}, u32[]{:S(2)}, u32[]{:S(2)}) collective-permute-start(bf16[576,256]{1,0:T(8,128)(2,1)S(1)} %collective-permute-done.6.refs_6_), channel_id=1, source_target_pairs={{128,96},{160,128},{192,160},{224,192},{256,224},{288,256},{320,28... | collective-permute-start | bytes 884744 | tf_op jit(solution)/shard_map/ppermute | solution.py:29
  70.0 6.4 %collective-permute-start.3 = (bf16[192,128]{1,0:T(8,128)(2,1)S(1)}, bf16[192,128]{1,0:T(8,128)(2,1)S(1)}, u32[]{:S(2)}, u32[]{:S(2)}) collective-permute-start(bf16[192,128]{1,0:T(8,128)(2,1)S(1)} %copy-done.1), channel_id=1, source_target_pairs={{16,0},{24,8},{0,16},{8,24},{17,1},{25,9},{1,17},{9,25},{18,2},{26... | collective-permute-start | bytes 147464 | tf_op jit(solution)/shard_map/ppermute | solution.py:254
  73.2 5.2 %collective-permute-start.4 = (bf16[192,128]{1,0:T(8,128)(2,1)S(1)}, bf16[192,128]{1,0:T(8,128)(2,1)S(1)}, u32[]{:S(2)}, u32[]{:S(2)}) collective-permute-start(bf16[192,128]{1,0:T(8,128)(2,1)S(1)} %copy-done.1), channel_id=1, source_target_pairs={{8,0},{16,8},{24,16},{0,24},{9,1},{17,9},{25,17},{1,25},{10,2},{18... | collective-permute-start | bytes 147464 | tf_op jit(solution)/shard_map/ppermute | solution.py:254
  75.2 7.3 %collective-permute-start.9 = (bf16[192,256]{1,0:T(8,128)(2,1)S(1)}, bf16[192,256]{1,0:T(8,128)(2,1)S(1)}, u32[]{:S(2)}, u32[]{:S(2)}) collective-permute-start(bf16[192,256]{1,0:T(8,128)(2,1)S(1)} %slice.68), channel_id=1, source_target_pairs={{224,256},{256,288},{288,320},{320,352},{352,384},{384,416},{416,4... | collective-permute-start | bytes 294920 | tf_op jit(solution)/shard_map/ppermute | solution.py:29
  92.7 10.8 %all-to-all-start = ((bf16[4,192,384]{2,1,0:T(8,128)(2,1)}), bf16[4,192,384]{2,1,0:T(8,128)(2,1)S(1)}, u32[]{:S(2)}, u32[]{:S(2)}) async-start(bf16[4,192,384]{2,1,0:T(8,128)(2,1)} %bitcast.2), calls=%async_computation | async-start | bytes 1179648 | tf_op jit(solution)/shard_map/all_to_all | solution.py:276
  104.3 1.1 copy-start.8
  106.0 18.5 %copy-start.4 = (bf16[24,2048]{1,0:T(8,128)(2,1)S(1)}, bf16[24,2048]{1,0:T(8,128)(2,1)}, u32[]{:S(2)}) copy-start(bf16[24,2048]{1,0:T(8,128)(2,1)} %param.13) | copy-start | bytes 294916
  106.0 18.6 %copy-start.7 = (f32[2048]{0:T(1024)S(1)}, f32[2048]{0:T(1024)}, u32[]{:S(2)}) copy-start(f32[2048]{0:T(1024)} %param.20) | copy-start | bytes 24580
  106.0 7.1 %collective-permute-start.10 = (bf16[4,24,2048]{2,1,0:T(8,128)(2,1)S(1)}, bf16[4,24,2048]{2,1,0:T(8,128)(2,1)S(1)}, u32[]{:S(2)}, u32[]{:S(2)}) collective-permute-start(bf16[4,24,2048]{2,1,0:T(8,128)(2,1)S(1)} %select_bitcast_fusion), channel_id=1, source_target_pairs={{0,1},{1,0},{2,3},{3,2},{4,5},{5,4},{6,7},{7,6},{8,9},{9,8},{10,11... | collective-permute-start | bytes 1179656 | tf_op jit(solution)/shard_map/ppermute | solution.py:207
  113.3 35.3 %copy-start.2 = (f32[3,704]{1,0:T(4,128)S(1)}, f32[3,704]{1,0:T(4,128)}, u32[]{:S(2)}) copy-start(f32[3,704]{1,0:T(4,128)} %taps_ref.1) | copy-start | bytes 25348
  113.3 35.3 %copy-start.3 = (f32[704]{0:T(1024)S(1)}, f32[704]{0:T(1024)}, u32[]{:S(2)}) copy-start(f32[704]{0:T(1024)} %bias_ref.1) | copy-start | bytes 8452
  139.7 3.2 %collective-permute-start.11 = (bf16[8,2048]{1,0:T(8,128)(2,1)S(1)}, bf16[8,2048]{1,0:T(8,128)(2,1)S(1)}, u32[]{:S(2)}, u32[]{:S(2)}) collective-permute-start(bf16[8,2048]{1,0:T(8,128)(2,1)S(1)} %slice.79), channel_id=1, source_target_pairs={{0,8},{8,16},{16,24},{24,32},{32,40},{40,48},{48,56},{56,64},{64,7... | collective-permute-start | bytes 98312 | tf_op jit(solution)/shard_map/ppermute | solution.py:287
  153.8 4.5 %collective-permute-start.12 = (bf16[4,24,2048]{2,1,0:T(8,128)(2,1)S(1)}, bf16[4,24,2048]{2,1,0:T(8,128)(2,1)S(1)}, u32[]{:S(2)}, u32[]{:S(2)}) collective-permute-start(bf16[4,24,2048]{2,1,0:T(8,128)(2,1)S(1)} %fusion.2), channel_id=1, source_target_pairs={{0,1},{1,0},{2,3},{3,2},{4,5},{5,4},{6,7},{7,6},{8,9},{9,8},{10,11... | collective-permute-start | bytes 1179656 | tf_op jit(solution)/shard_map/ppermute | solution.py:207
Sparse Core Ops, SparseCore 0:
  20.1 128.4 all-gather.1
